TPU v7x, 32 devices: a whole 2x2x4 slice. The times are simulated.
32 devices in a mesh: grp: 2 (over y), sp: 4 (over z), tp: 4 (over x, core).
Axes of the slice: x: 2, y: 2, z: 4, core: 2. Of those that a mesh axis runs over, the one named last changes fastest.
Arguments:
- tokens: bfloat16 [2048, 4096], P(('grp', 'sp')), parts along dimension 0, may hold values from -6 to 6
- norm_gain: bfloat16 [2, 4096], replicated, may hold values from 0.099609375 to 1.8984375
- w_query: bfloat16 [2, 4096, 2048], P(None, 'sp', 'tp'), may hold values from -0.09375 to 0.09375
- w_key: bfloat16 [2, 4096, 2048], P(None, 'sp', 'tp'), may hold values from -0.09375 to 0.09375
- w_value: bfloat16 [2, 4096, 2048], P(None, 'sp', 'tp'), may hold values from -0.09375 to 0.09375
- w_out: bfloat16 [2, 2048, 4096], P(None, 'tp', 'sp'), may hold values from -0.125 to 0.125
- offset_bias: float32 [2, 16, 15, 31], P(None, 'tp'), may hold values from -4 to 300
Outputs:
- mixed: bfloat16 [2048, 4096], P(('grp', 'sp')), parts along dimension 0
There are 2 independent parts, one for each index of `grp`. A program takes and returns all parts, laid end to end along the dimension named above; an argument that names none is the same for every part. Nothing has to cross between parts.
All inputs are finite; a program needn't handle non-finite values.
Results may differ from a plain program's by a relative error of at most 0.013.
Values may be sent and summed in bfloat16 or wider, within the bound.
No kernel may reach another device: no remote copies, remote signals or barrier semaphores. Data moves between devices by JAX's collectives and lax.ppermute only.
A program may use at most 128 MiB of HBM per device.

v0:
```python
import jax
import jax.numpy as jnp
from jax import lax
from jax.sharding import PartitionSpec as P

HD = 128
GRID_W = 64
KR = 8
KC = 16
LAYERS = 2


norm_eps = 1e-06


def with_halo(block, sides, width):
    for axis, dim in sides:
        count = lax.axis_size(axis)
        forward = [(i, i + 1) for i in range(count - 1)]
        backward = [(target, source) for source, target in forward]
        low = lax.ppermute(
            lax.slice_in_dim(block, block.shape[dim] - width, None, axis=dim), axis, forward
        )
        high = lax.ppermute(lax.slice_in_dim(block, 0, width, axis=dim), axis, backward)
        block = jnp.concatenate([low, block, high], axis=dim)
    return block


def rms_rows(values, gain):
    wide = values.astype(jnp.float32)
    scaled = wide * lax.rsqrt(jnp.mean(wide * wide, axis=-1, keepdims=True) + norm_eps)
    return (scaled * gain.astype(jnp.float32)).astype(jnp.bfloat16)


def on_device(tokens, norm_gain, w_query, w_key, w_value, w_out, offset_bias):
    sp_count = lax.axis_size("sp")
    sp_index = lax.axis_index("sp")
    tok_rows = tokens.shape[0]
    local_rows = tok_rows // GRID_W
    grid_rows = local_rows * sp_count
    heads_here = offset_bias.shape[1]
    head_width = heads_here * HD
    reach = KR // 2
    scale = HD ** (-0.5)
    columns = jnp.arange(GRID_W, dtype=jnp.int32)
    col_first = jnp.clip(columns - KC // 2, 0, GRID_W - KC)
    col_inside = (columns[None, :] >= col_first[:, None]) & (
        columns[None, :] < col_first[:, None] + KC
    )
    col_offset = jnp.clip(columns[None, :] - columns[:, None], 1 - KC, KC - 1) + KC - 1
    col_onehot = (
        jnp.arange(2 * KC - 1, dtype=jnp.int32)[:, None, None] == col_offset[None, :, :]
    ).astype(jnp.float32)
    first_row = sp_index * local_rows
    own_rows = first_row + jnp.arange(local_rows, dtype=jnp.int32)
    row_first = jnp.clip(own_rows - reach, 0, grid_rows - KR)
    band_start = row_first - first_row + reach
    row_offset = (
        row_first[:, None] + jnp.arange(KR, dtype=jnp.int32)[None, :] - own_rows[:, None] + KR - 1
    )
    row_onehot = (
        row_offset[:, :, None] == jnp.arange(2 * KR - 1, dtype=jnp.int32)[None, None, :]
    ).astype(jnp.float32)
    every_query, every_key, every_value, every_out = (
        lax.all_gather(w_query, "sp", axis=1, tiled=True),
        lax.all_gather(w_key, "sp", axis=1, tiled=True),
        lax.all_gather(w_value, "sp", axis=1, tiled=True),
        lax.all_gather(w_out, "sp", axis=2, tiled=True),
    )
    residual = tokens
    for layer_index in range(LAYERS):
        normed = rms_rows(residual, norm_gain[layer_index])
        queries = jnp.dot(normed, every_query[layer_index], preferred_element_type=jnp.float32)
        keys = jnp.dot(normed, every_key[layer_index], preferred_element_type=jnp.float32)
        values = jnp.dot(normed, every_value[layer_index], preferred_element_type=jnp.float32)
        out_weight = every_out[layer_index]
        queries = queries.astype(jnp.bfloat16).reshape(local_rows, GRID_W, heads_here, HD)
        key_values = jnp.concatenate(
            [keys.astype(jnp.bfloat16), values.astype(jnp.bfloat16)], axis=1
        )
        key_values = key_values.reshape(local_rows, GRID_W, 2 * head_width)
        padded = with_halo(key_values, (("sp", 0),), reach)
        bands = jax.vmap(lambda band_begin: lax.dynamic_slice_in_dim(padded, band_begin, KR, 0))(
            band_start
        )
        band_keys = bands[..., :head_width].reshape(local_rows, KR, GRID_W, heads_here, HD)
        band_values = bands[..., head_width:].reshape(local_rows, KR, GRID_W, heads_here, HD)
        col_bias = jnp.einsum(
            "hro,oqk->hrqk", offset_bias[layer_index], col_onehot, precision=lax.Precision.HIGHEST
        )
        full_bias = jnp.einsum(
            "ijr,hrqk->hiqjk", row_onehot, col_bias, precision=lax.Precision.HIGHEST
        )
        scores = jnp.einsum(
            "iqhd,ijkhd->hiqjk", queries, band_keys, preferred_element_type=jnp.float32
        )
        scores = scores * scale + full_bias
        scores = jnp.where(col_inside[None, None, :, None, :], scores, -jnp.inf)
        flattened = scores.reshape(heads_here, local_rows, GRID_W, KR * GRID_W)
        weights = jax.nn.softmax(flattened, axis=-1).astype(jnp.bfloat16)
        weights = weights.reshape(heads_here, local_rows, GRID_W, KR, GRID_W)
        attended = jnp.einsum(
            "hiqjk,ijkhd->iqhd", weights, band_values, preferred_element_type=jnp.float32
        )
        attended = attended.astype(jnp.bfloat16).reshape(tok_rows, head_width)
        branch = lax.psum(
            jnp.dot(attended, out_weight, preferred_element_type=jnp.float32).astype(jnp.bfloat16),
            "tp",
        ).astype(jnp.float32)
        residual = (residual.astype(jnp.float32) + branch).astype(jnp.bfloat16)
    return residual


def solution(mesh):
    return jax.shard_map(
        on_device,
        mesh=mesh,
        in_specs=(
            P(("grp", "sp"), None),
            P(),
            P(None, "sp", "tp"),
            P(None, "sp", "tp"),
            P(None, "sp", "tp"),
            P(None, "tp", "sp"),
            P(None, "tp", None, None),
        ),
        out_specs=P(("grp", "sp"), None),
        check_vma=False,
    )
```

profile of v0, /device:TPU:0, one launch (start us, length us, event | category | flops | bytes accessed | tf_op | source)
XLA Modules:
  0.0 783.5 jit_solution(1764364375646308337)
XLA Ops:
  10.7 3.8 fusion.30
  14.5 6.0 copy.16
  21.1 140.2 %all-gather.5.cloned.1.call-done = bf16[2,4096,512]{2,1,0:T(8,128)(2,1)} async-done(((bf16[2,1024,512]{2,1,0:T(8,128)(2,1)}), bf16[2,4096,512]{2,1,0:T(8,128)(2,1)}) %all-gather.5.cloned.1.call-update) | async-done | bytes 8388624 | tf_op jit(solution)/shard_map/all_gather | solution.py:66
  161.3 3.5 fusion.54
  164.7 145.9 %all-gather.7.cloned.1.call-done = bf16[2,4096,512]{2,1,0:T(8,128)(2,1)} async-done(((bf16[2,1024,512]{2,1,0:T(8,128)(2,1)}), bf16[2,4096,512]{2,1,0:T(8,128)(2,1)}) %all-gather.7.cloned.1.call-update) | async-done | bytes 8388624 | tf_op jit(solution)/shard_map/all_gather | solution.py:67
  310.7 3.5 fusion.55
  314.2 2.1 collective-permute-start
  316.3 1.5 collective-permute-start.1
  317.8 149.6 %all-gather.9.cloned.1.call-done = bf16[2,4096,512]{2,1,0:T(8,128)(2,1)} async-done(((bf16[2,1024,512]{2,1,0:T(8,128)(2,1)}), bf16[2,4096,512]{2,1,0:T(8,128)(2,1)}) %all-gather.9.cloned.1.call-update) | async-done | bytes 8388624 | tf_op jit(solution)/shard_map/all_gather | solution.py:65
  467.4 3.5 fusion.56
  471.0 2.5 pad_maximum_fusion
  473.5 4.4 gather_fusion
  477.9 3.5 slice_bitcast_fusion.19
  484.9 132.0 %all-gather.11.cloned.1.call-done = bf16[2,512,4096]{2,1,0:T(8,128)(2,1)} async-done(((bf16[2,512,1024]{2,1,0:T(8,128)(2,1)}), bf16[2,512,4096]{2,1,0:T(8,128)(2,1)}) %all-gather.11.cloned.1.call-update) | async-done | bytes 8388624 | tf_op jit(solution)/shard_map/all_gather | solution.py:68
  616.9 4.8 convolution_convert_fusion.1
  621.8 2.4 fusion.71
  624.2 47.2 %all-reduce.4.cloned.1.call-done = bf16[256,4096]{1,0:T(8,128)(2,1)} async-done(((bf16[256,4096]{1,0:T(8,128)(2,1)}), bf16[256,4096]{1,0:T(8,128)(2,1)}) %all-reduce.4.cloned.1.call-update) | async-done | bytes 2097168 | tf_op jit(solution)/shard_map/psum | solution.py:106
  671.5 2.5 fusion.4
  675.0 4.5 fusion.57
  679.5 1.2 fusion.58
  680.8 3.4 collective-permute-start.2
  684.3 1.5 collective-permute-start.3
  685.8 3.9 fusion.28
  689.7 5.8 copy.22
  695.4 4.8 fusion.59
  701.3 2.4 pad_maximum_fusion.1
  703.6 4.2 gather_fusion.1
  707.8 3.1 slice_bitcast_fusion.17
  714.5 1.5 slice-done.1
  715.9 2.6 convolution_convert_fusion
  718.6 53.4 %all-reduce.6.cloned.1.call-done = bf16[256,4096]{1,0:T(8,128)(2,1)} async-done(((bf16[256,4096]{1,0:T(8,128)(2,1)}), bf16[256,4096]{1,0:T(8,128)(2,1)}) %all-reduce.6.cloned.1.call-update) | async-done | bytes 2097168 | tf_op jit(solution)/shard_map/psum | solution.py:106
  771.9 4.7 fusion.7
  (67 shorter events, 13.9 us)
Async XLA Ops:
  6.5 2.9 copy-start.7
  6.5 154.7 %all-gather.5.cloned.1.call-start = ((), (), s32[]{:S(2)}) async-start(), calls=%async_computation | async-start | bytes 10485760 | tf_op jit(solution)/shard_map/all_gather | solution.py:66
  7.3 303.4 %all-gather.7.cloned.1.call-start = ((), (), s32[]{:S(2)}) async-start(), calls=%async_computation.1 | async-start | bytes 10485760 | tf_op jit(solution)/shard_map/all_gather | solution.py:67
  8.0 459.4 %all-gather.9.cloned.1.call-start = ((), (), s32[]{:S(2)}) async-start(), calls=%async_computation.2 | async-start | bytes 10485760 | tf_op jit(solution)/shard_map/all_gather | solution.py:65
  8.7 608.2 %all-gather.11.cloned.1.call-start = ((), (), s32[]{:S(2)}) async-start(), calls=%async_computation.3 | async-start | bytes 10485760 | tf_op jit(solution)/shard_map/all_gather | solution.py:68
  9.3 662.1 %all-reduce.4.cloned.1.call-start = ((), (), s32[]{:S(2)}) async-start(), calls=%async_computation.4 | async-start | bytes 4194304 | tf_op jit(solution)/shard_map/psum | solution.py:106
  14.5 6.0 copy-start
  14.5 6.6 copy-start.6
  314.2 156.7 %collective-permute-start = (bf16[4,64,1024]{2,1,0:T(8,128)(2,1)S(1)}, bf16[4,64,1024]{2,1,0:T(8,128)(2,1)}, u32[]{:S(2)}, u32[]{:S(2)}) collective-permute-start(bf16[4,64,1024]{2,1,0:T(8,128)(2,1)S(1)} %bitcast.150), channel_id=1, source_target_pairs={{0,4},{4,8},{8,12},{1,5},{5,9},{9,13},{2,6},{6,10},{10,14},{3,7},{... | collective-permute-start | bytes 1572872 | tf_op jit(solution)/shard_map/ppermute | solution.py:21
  316.3 154.6 %collective-permute-start.1 = (bf16[4,64,1024]{2,1,0:T(8,128)(2,1)S(1)}, bf16[4,64,1024]{2,1,0:T(8,128)(2,1)}, u32[]{:S(2)}, u32[]{:S(2)}) collective-permute-start(bf16[4,64,1024]{2,1,0:T(8,128)(2,1)S(1)} %bitcast.151), channel_id=1, source_target_pairs={{4,0},{8,4},{12,8},{5,1},{9,5},{13,9},{6,2},{10,6},{14,10},{7,3},{... | collective-permute-start | bytes 1572872 | tf_op jit(solution)/shard_map/ppermute | solution.py:24
  477.9 4.1 copy-start.2
  621.7 150.2 %all-reduce.6.cloned.1.call-start = ((), (), s32[]{:S(2)}) async-start(), calls=%async_computation.5 | async-start | bytes 4194304 | tf_op jit(solution)/shard_map/psum | solution.py:106
  671.5 2.5 copy-start.1
  674.0 5.5 slice-start.2
  674.9 4.5 copy-start.5
  675.0 4.6 slice-start.3
  679.5 6.3 copy-start.4
  680.8 20.4 %collective-permute-start.2 = (bf16[4,64,1024]{2,1,0:T(8,128)(2,1)S(1)}, bf16[4,64,1024]{2,1,0:T(8,128)(2,1)S(1)}, u32[]{:S(2)}, u32[]{:S(2)}) collective-permute-start(bf16[4,64,1024]{2,1,0:T(8,128)(2,1)S(1)} %bitcast.147), channel_id=1, source_target_pairs={{0,4},{4,8},{8,12},{1,5},{5,9},{9,13},{2,6},{6,10},{10,14},{3,7},{... | collective-permute-start | bytes 1572872 | tf_op jit(solution)/shard_map/ppermute | solution.py:21
  684.3 17.0 %collective-permute-start.3 = (bf16[4,64,1024]{2,1,0:T(8,128)(2,1)S(1)}, bf16[4,64,1024]{2,1,0:T(8,128)(2,1)}, u32[]{:S(2)}, u32[]{:S(2)}) collective-permute-start(bf16[4,64,1024]{2,1,0:T(8,128)(2,1)S(1)} %bitcast.148), channel_id=1, source_target_pairs={{4,0},{8,4},{12,8},{5,1},{9,5},{13,9},{6,2},{10,6},{14,10},{7,3},{... | collective-permute-start | bytes 1572872 | tf_op jit(solution)/shard_map/ppermute | solution.py:24
  707.8 3.4 copy-start.3
  712.3 2.2 slice-start
  713.0 2.9 slice-start.1
Sparse Core Ops, SparseCore 0:
  8.9 152.3 all-gather.4
  162.8 147.7 all-gather.6
  312.2 155.1 all-gather.8
  468.8 148.0 all-gather.10
  621.9 49.5 all-reduce.3
  718.7 53.1 all-reduce.5
where the time goes:
time: 784 us; the launch traced here: 783 us
  waiting for transfers between devices  671 us (86%)
  matrix products  43.4 us (6%)
  local copies, waits for them, and re-layouts  31.2 us (4%)
  other arithmetic  15.4 us (2%)
  between operations  13.8 us (2%)
  starting transfers between devices  8.71 us (1%)
    all_gather x1, waiting for transfers between devices, on_device(): lax.all_gather(w_query, 'sp', axis=1, tiled=True)  150 us
    all_gather x1, waiting for transfers between devices, on_device(): lax.all_gather(w_value, 'sp', axis=1, tiled=True)  146 us
    all_gather x1, waiting for transfers between devices, on_device(): lax.all_gather(w_key, 'sp', axis=1, tiled=True)  140 us
    all_gather x1, waiting for transfers between devices, on_device(): lax.all_gather(w_out, 'sp', axis=2, tiled=True)  132 us
    psum x2, waiting for transfers between devices, on_device(): lax.psum(jnp.dot(attended, out_weight, preferred_element_type=jnp.float32...  101 us
  transfers between devices with their start and end apart: 10, of which 6 were waited for; matrix products, arithmetic and copies ran while one was open for 7% of the time, Pallas kernels for 0%

commit v1 on v0

--- a/solution.py
+++ b/solution.py
@@ -1,6 +1,10 @@
+import functools
+
 import jax
 import jax.numpy as jnp
 from jax import lax
+from jax.experimental import pallas as pl
+from jax.experimental.pallas import tpu as pltpu
 from jax.sharding import PartitionSpec as P
 
 HD = 128
@@ -32,7 +36,7 @@
     return (scaled * gain.astype(jnp.float32)).astype(jnp.bfloat16)
 
 
-def on_device(tokens, norm_gain, w_query, w_key, w_value, w_out, offset_bias):
+def gathered_plan(tokens, norm_gain, w_query, w_key, w_value, w_out, offset_bias):
     sp_count = lax.axis_size("sp")
     sp_index = lax.axis_index("sp")
     tok_rows = tokens.shape[0]
@@ -111,6 +115,188 @@
     return residual
 
 
+def ring(count, shift):
+    return [(i, (i + shift) % count) for i in range(count)]
+
+
+def swapped(array, axis, distance):
+    count = lax.axis_size(axis)
+    return lax.ppermute(array, axis, [(i, i ^ distance) for i in range(count)])
+
+
+def ordered(mine, theirs, mine_is_low, axis):
+    low = jnp.where(mine_is_low, mine, theirs)
+    high = jnp.where(mine_is_low, theirs, mine)
+    return jnp.concatenate([low, high], axis=axis)
+
+
+def summed_over(vector, axis):
+    count = lax.axis_size(axis)
+    distance = 1
+    while distance < count:
+        vector = vector + swapped(vector, axis, distance)
+        distance *= 2
+    return vector
+
+
+def window_bias(table):
+    heads = table.shape[0]
+    columns = jnp.arange(GRID_W, dtype=jnp.int32)
+    first = jnp.clip(columns - KC // 2, 0, GRID_W - KC)
+    inside = (columns[None, :] >= first[:, None]) & (columns[None, :] < first[:, None] + KC)
+    offset = jnp.clip(columns[None, :] - columns[:, None], 1 - KC, KC - 1) + KC - 1
+    onehot = (
+        jnp.arange(2 * KC - 1, dtype=jnp.int32)[:, None, None] == offset[None, :, :]
+    ).astype(jnp.float32)
+    wide = jnp.einsum("hro,oqk->hqrk", table, onehot, precision=lax.Precision.HIGHEST)
+    wide = jnp.where(inside[None, :, None, :], wide, -jnp.inf)
+    return wide.reshape(heads, GRID_W, (2 * KR - 1) * GRID_W)
+
+
+def attend_kernel(heads, grid_rows, arrived_ref, own_ref, norm_ref, bias_ref, out_ref, qkv_ref):
+    total = arrived_ref[...].astype(jnp.float32) + own_ref[...].astype(jnp.float32)
+    qkv_ref[...] = (total * norm_ref[...]).astype(jnp.bfloat16)
+    width = heads * HD
+    for head in range(heads):
+        lanes = head * HD
+        for row in range(grid_rows):
+            first = min(max(row - KR // 2, 0), grid_rows - KR)
+            offset = first - row + KR - 1
+            queries = qkv_ref[pl.ds(row * GRID_W, GRID_W), pl.ds(lanes, HD)]
+            keys = qkv_ref[pl.ds(first * GRID_W, KR * GRID_W), pl.ds(width + lanes, HD)]
+            values = qkv_ref[pl.ds(first * GRID_W, KR * GRID_W), pl.ds(2 * width + lanes, HD)]
+            scores = lax.dot_general(
+                queries, keys, (((1,), (1,)), ((), ())), preferred_element_type=jnp.float32
+            )
+            bias = bias_ref[head, :, pl.ds(offset * GRID_W, KR * GRID_W)]
+            scores = scores * HD ** (-0.5) + bias
+            powers = jnp.exp(scores - jnp.max(scores, axis=-1, keepdims=True))
+            weights = powers / jnp.sum(powers, axis=-1, keepdims=True)
+            mixed = jnp.dot(
+                weights.astype(jnp.bfloat16), values, preferred_element_type=jnp.float32
+            )
+            out_ref[pl.ds(row * GRID_W, GRID_W), pl.ds(lanes, HD)] = mixed.astype(jnp.bfloat16)
+
+
+def attend(arrived, own, norm, bias):
+    tok, width = arrived.shape
+    heads = bias.shape[0]
+    grid_rows = tok // GRID_W
+    return pl.pallas_call(
+        functools.partial(attend_kernel, heads, grid_rows),
+        out_shape=jax.ShapeDtypeStruct((tok, width // 3), jnp.bfloat16),
+        in_specs=[pl.BlockSpec(memory_space=pltpu.VMEM)] * 4,
+        out_specs=pl.BlockSpec(memory_space=pltpu.VMEM),
+        scratch_shapes=[pltpu.VMEM((tok, width), jnp.bfloat16)],
+        compiler_params=pltpu.CompilerParams(vmem_limit_bytes=32 * 1024 * 1024),
+        cost_estimate=pl.CostEstimate(
+            flops=4 * heads * tok * KR * GRID_W * HD,
+            bytes_accessed=8 * tok * width,
+            transcendentals=heads * tok * KR * GRID_W,
+        ),
+        name="attend",
+    )(arrived, own, norm, bias)
+
+
+def stationary_plan(tokens, norm_gain, w_query, w_key, w_value, w_out, offset_bias):
+    sp_count, tp_count = lax.axis_size("sp"), lax.axis_size("tp")
+    sp_index, tp_index = lax.axis_index("sp"), lax.axis_index("tp")
+    core, far = tp_index % 2, tp_index // 2
+    tok_here = tokens.shape[0]
+    tok = tok_here * sp_count
+    feats = w_query.shape[1]
+    heads = offset_bias.shape[1] // sp_count
+    width = heads * HD
+    half, piece = feats // 2, feats // 4
+    slot = core * 2 + far
+    every_feat = feats * sp_count
+
+    def source(shift):
+        return (sp_index - shift) % sp_count
+
+    held = jnp.zeros((tok, piece), jnp.bfloat16)
+    for shift in range(sp_count):
+        target = (sp_index + shift) % sp_count
+        block = lax.dynamic_slice_in_dim(tokens, target * feats + slot * piece, piece, 1)
+        if shift:
+            block = lax.ppermute(block, "sp", ring(sp_count, shift))
+        held = lax.dynamic_update_slice_in_dim(held, block, source(shift) * tok_here, 0)
+    x_half = ordered(held, swapped(held, "tp", 2), far == 0, 1)
+    x = ordered(x_half, swapped(x_half, "tp", 1), core == 0, 1)
+
+    for layer in range(LAYERS):
+        gain = lax.dynamic_slice_in_dim(norm_gain[layer], sp_index * feats, feats, 0)
+        wide = x.astype(jnp.float32)
+        scaled = (wide * gain.astype(jnp.float32)).astype(jnp.bfloat16)
+        squares = summed_over(jnp.sum(wide * wide, axis=-1).reshape(tok // HD, HD), "sp")
+        norm = lax.rsqrt(squares.reshape(tok, 1) / every_feat + norm_eps)
+
+        def partial_of(chunk, layer=layer, scaled=scaled):
+            weights = jnp.concatenate(
+                [
+                    lax.dynamic_slice_in_dim(w[layer], chunk * width, width, 1)
+                    for w in (w_query, w_key, w_value)
+                ],
+                axis=1,
+            )
+            return jnp.dot(scaled, weights, preferred_element_type=jnp.float32)
+
+        travelling = partial_of(source(1)).astype(jnp.bfloat16)
+        for step in range(1, sp_count):
+            travelling = lax.ppermute(travelling, "sp", ring(sp_count, 1))
+            own = partial_of(source(step + 1))
+            if step < sp_count - 1:
+                travelling = (travelling.astype(jnp.float32) + own).astype(jnp.bfloat16)
+        table = lax.dynamic_slice_in_dim(offset_bias[layer], sp_index * heads, heads, 0)
+        attended = attend(travelling, own, norm, window_bias(table))
+
+        gathered = [attended] + [
+            lax.ppermute(attended, "sp", ring(sp_count, shift)) for shift in range(1, sp_count)
+        ]
+        out_rows = jnp.concatenate(
+            [
+                lax.dynamic_slice_in_dim(w_out[layer], source(shift) * width, width, 0)
+                for shift in range(sp_count)
+            ],
+            axis=0,
+        )
+        product = jnp.dot(
+            jnp.concatenate(gathered, axis=1), out_rows, preferred_element_type=jnp.float32
+        ).astype(jnp.bfloat16)
+        sent = lax.dynamic_slice_in_dim(product, (1 - core) * half, half, 1)
+        kept = lax.dynamic_slice_in_dim(product, core * half, half, 1)
+        pair = kept.astype(jnp.float32) + swapped(sent, "tp", 1).astype(jnp.float32)
+        pair = pair.astype(jnp.bfloat16)
+        if layer < LAYERS - 1:
+            branch = pair.astype(jnp.float32) + swapped(pair, "tp", 2).astype(jnp.float32)
+            x_half = (x_half.astype(jnp.float32) + branch).astype(jnp.bfloat16)
+            x = ordered(x_half, swapped(x_half, "tp", 1), core == 0, 1)
+
+    sent = lax.dynamic_slice_in_dim(pair, (1 - far) * piece, piece, 1)
+    kept = lax.dynamic_slice_in_dim(pair, far * piece, piece, 1)
+    branch = kept.astype(jnp.float32) + swapped(sent, "tp", 2).astype(jnp.float32)
+    residual = lax.dynamic_slice_in_dim(x_half, far * piece, piece, 1)
+    last = (residual.astype(jnp.float32) + branch).astype(jnp.bfloat16)
+    mixed = jnp.zeros((tok_here, sp_count, piece), jnp.bfloat16)
+    for shift in range(sp_count):
+        target = (sp_index + shift) % sp_count
+        block = lax.dynamic_slice_in_dim(last, target * tok_here, tok_here, 0)
+        if shift:
+            block = lax.ppermute(block, "sp", ring(sp_count, shift))
+        mixed = lax.dynamic_update_slice_in_dim(mixed, block[:, None], source(shift), 1)
+    mixed = ordered(mixed, swapped(mixed, "tp", 2), far == 0, 2)
+    mixed = ordered(mixed, swapped(mixed, "tp", 1), core == 0, 2)
+    return mixed.reshape(tok_here, every_feat)
+
+
+def on_device(tokens, norm_gain, w_query, w_key, w_value, w_out, offset_bias):
+    heads_here = offset_bias.shape[1]
+    plan = gathered_plan
+    if heads_here % lax.axis_size("sp") == 0 and lax.axis_size("tp") == 4:
+        plan = stationary_plan
+    return plan(tokens, norm_gain, w_query, w_key, w_value, w_out, offset_bias)
+
+
 def solution(mesh):
     return jax.shard_map(
         on_device,

time: 784 us -> 343 us (0.44)
  waiting for transfers between devices: 671 us -> 230 us
  starting transfers between devices: 8.71 us -> 28.3 us
  matrix products: 43.4 us -> 27 us
  between operations: 13.8 us -> 0.9 us
  Pallas kernels: 0 us -> 11.5 us
    all_gather x4 -> x0, waiting for transfers between devices: 568 us -> none  [the longest x1 150 us: on_device(): lax.all_gather(w_query, 'sp', axis=1, tiled=True)]
    ppermute x4 -> x31, waiting for transfers between devices: 0.01 us -> 230 us  [the longest x13 92.4 us: swapped(): return lax.ppermute(array, axis, [(i, i ^ distance) for i in range(count)])]
    psum x2 -> x0, waiting for transfers between devices: 101 us -> none  [on_device(): lax.psum(jnp.dot(attended, out_weight, preferred_element_type=jnp.float32...]
    ppermute x4 -> x31, starting transfers between devices: 8.51 us -> 28.3 us  [the longest x6 11.2 us: stationary_plan(): block = lax.ppermute(block, 'sp', ring(sp_count, shift))]
    dot_general x16 -> x12, matrix products: 43.4 us -> 27 us  [the longest x8 22.3 us: partial_of(): return jnp.dot(scaled, weights, preferred_element_type=jnp.float32)]
    dot_general x2 -> x0, local copies, waits for them, and re-layouts: 11.8 us -> none  [on_device(): jnp.einsum('ijr,hrqk->hiqjk', row_onehot, col_bias, precision=lax.Precisi...]
    pallas_call x0 -> x2, Pallas kernels: none -> 11.5 us  [attend(): pl.pallas_call(functools.partial(attend_kernel, heads, grid_rows), out_sh...]
    gather x2 -> x0, local copies, waits for them, and re-layouts: 8.6 us -> none  [on_device(): lax.dynamic_slice_in_dim(padded, band_begin, KR, 0)]
  transfers between devices with their start and end apart: 10 -> 31, of which waited for: 6 -> 23; matrix products, arithmetic and copies ran while one was open for 7% -> 7% of each run, Pallas kernels for 0% -> 0%
where the time goes in v1:
time: 343 us; the launch traced here: 341 us
  waiting for transfers between devices  230 us (67%)
  local copies, waits for them, and re-layouts  30.3 us (9%)
  starting transfers between devices  28.3 us (8%)
  matrix products  27 us (8%)
  other arithmetic  12.9 us (4%)
  Pallas kernels  11.5 us (3%)
    ppermute x13, waiting for transfers between devices, swapped(): return lax.ppermute(array, axis, [(i, i ^ distance) for i in range(count)])  92.4 us
    ppermute x6, waiting for transfers between devices, stationary_plan(): travelling = lax.ppermute(travelling, 'sp', ring(sp_count, 1))  84.1 us
    ppermute x6, waiting for transfers between devices, stationary_plan(): lax.ppermute(attended, 'sp', ring(sp_count, shift))  38.9 us
    dot_general x8, matrix products, partial_of(): return jnp.dot(scaled, weights, preferred_element_type=jnp.float32)  22.3 us
    ppermute x6, waiting for transfers between devices, stationary_plan(): block = lax.ppermute(block, 'sp', ring(sp_count, shift))  14.7 us
    pallas_call x2, Pallas kernels, attend(): pl.pallas_call(functools.partial(attend_kernel, heads, grid_rows), out_sh...  11.5 us
    ppermute x6, starting transfers between devices, stationary_plan(): block = lax.ppermute(block, 'sp', ring(sp_count, shift))  11.2 us
    unnamed x79, local copies, waits for them, and re-layouts  8.26 us
  transfers between devices with their start and end apart: 31, of which 23 were waited for; matrix products, arithmetic and copies ran while one was open for 7% of the time, Pallas kernels for 0%

profile of v1, /device:TPU:0, one launch (start us, length us, event | category | flops | bytes accessed | tf_op | source)
XLA Modules:
  0.0 341.1 jit_solution(18373506971367666570)
XLA Ops:
  1.3 3.1 collective-permute-start
  10.9 4.7 %collective-permute-done.1 = bf16[256,256]{0,1:T(8,128)(2,1)S(1)} collective-permute-done((bf16[256,256]{0,1:T(8,128)(2,1)S(1)}, bf16[256,256]{0,1:T(8,128)(2,1)S(1)}, u32[]{:S(2)}, u32[]{:S(2)}) %collective-permute-start.1) | collective-permute-done | bytes 131104 | tf_op jit(solution)/shard_map/ppermute | solution.py:222
  17.3 12.2 %collective-permute-done.3 = bf16[1024,256]{0,1:T(8,128)(2,1)S(1)} collective-permute-done((bf16[1024,256]{0,1:T(8,128)(2,1)S(1)}, bf16[1024,256]{0,1:T(8,128)(2,1)S(1)}, u32[]{:S(2)}, u32[]{:S(2)}) %collective-permute-start.3) | collective-permute-done | bytes 524320 | tf_op jit(solution)/shard_map/ppermute | solution.py:124
  41.3 3.3 collective-permute-start.5
  44.7 18.6 %collective-permute-done.5 = bf16[1024,384]{1,0:T(8,128)(2,1)} collective-permute-done((bf16[1024,384]{1,0:T(8,128)(2,1)}, bf16[1024,384]{1,0:T(8,128)(2,1)}, u32[]{:S(2)}, u32[]{:S(2)}) %collective-permute-start.5) | collective-permute-done | bytes 786464 | tf_op jit(solution)/shard_map/ppermute | solution.py:246
  63.3 3.4 %add_convert_fusion.6 = bf16[1024,384]{1,0:T(8,128)(2,1)} fusion(bf16[1024,384]{1,0:T(8,128)(2,1)} %collective-permute-done.5, bf16[1024,128]{1,0:T(8,128)(2,1)S(1)} %copy-done.30, bf16[1024,128]{1,0:T(8,128)(2,1)S(1)} %copy-done.31, bf16[1024,128]{1,0:T(8,128)(2,1)S(1)} %copy-done.21, f32[1024]{0:T(1024)S(1)} %bitcast.125, ...), kind=kOutput, calls=%fused_computation.19 | convolution fusion | flops 815136768 | bytes 4460544 | tf_op jit(solution)/shard_map/dot_general | solution.py:242
  69.9 18.1 %collective-permute-done.6 = bf16[1024,384]{1,0:T(8,128)(2,1)} collective-permute-done((bf16[1024,384]{1,0:T(8,128)(2,1)}, bf16[1024,384]{1,0:T(8,128)(2,1)}, u32[]{:S(2)}, u32[]{:S(2)}) %collective-permute-start.6) | collective-permute-done | bytes 786464 | tf_op jit(solution)/shard_map/ppermute | solution.py:246
  88.0 3.5 %add_convert_fusion.5 = bf16[1024,384]{1,0:T(8,128)(2,1)} fusion(bf16[1024,384]{1,0:T(8,128)(2,1)} %collective-permute-done.6, bf16[1024,128]{1,0:T(8,128)(2,1)S(1)} %copy-done.24, bf16[1024,128]{1,0:T(8,128)(2,1)S(1)} %copy-done.25, bf16[1024,128]{1,0:T(8,128)(2,1)S(1)} %copy-done.20, f32[1024]{0:T(1024)S(1)} %bitcast.126, ...), kind=kOutput, calls=%fused_computation.18 | convolution fusion | flops 815136768 | bytes 4460544 | tf_op jit(solution)/shard_map/dot_general | solution.py:242
  91.8 2.9 fusion.57.own_ref
  94.7 13.0 %collective-permute-done.9 = f32[8,128]{1,0:T(8,128)S(1)} collective-permute-done((f32[8,128]{1,0:T(8,128)S(1)}, f32[8,128]{1,0:T(8,128)S(1)}, u32[]{:S(2)}, u32[]{:S(2)}) %collective-permute-start.9) | collective-permute-done | bytes 4128 | tf_op jit(solution)/shard_map/ppermute | solution.py:124
  108.0 3.7 %collective-permute-done.7.arrived_ref = bf16[1024,384]{1,0:T(8,128)(2,1)S(1)} collective-permute-done((bf16[1024,384]{1,0:T(8,128)(2,1)}, bf16[1024,384]{1,0:T(8,128)(2,1)S(1)}, u32[]{:S(2)}, u32[]{:S(2)}) %collective-permute-start.7) | collective-permute-done | bytes 786464 | tf_op jit(solution)/shard_map/ppermute | solution.py:246
  111.6 5.8 %attend.2 = bf16[1024,128]{1,0:T(8,128)(2,1)S(1)} custom-call(bf16[1024,384]{1,0:T(8,128)(2,1)S(1)} %collective-permute-done.7.arrived_ref, f32[1024,384]{1,0:T(8,128)S(1)} %fusion.57.own_ref, f32[1024,1]{1,0:T(8,128)S(1)} %copy.29.norm_ref, f32[1,64,960]{2,1,0:T(8,128)S(1)} %reshape.177.bias_ref), custom_call_target="tpu_custom_call" | custom-call | flops 268435456 | bytes 3145728 | tf_op jit(solution)/shard_map/attend/pallas_call | solution.py:185
  121.1 3.3 collective-permute-done.12
  124.4 15.9 %collective-permute-done.11 = bf16[1024,128]{1,0:T(8,128)(2,1)S(1)} collective-permute-done((bf16[1024,128]{1,0:T(8,128)(2,1)S(1)}, bf16[1024,128]{1,0:T(8,128)(2,1)S(1)}, u32[]{:S(2)}, u32[]{:S(2)}) %collective-permute-start.11) | collective-permute-done | bytes 262176 | tf_op jit(solution)/shard_map/ppermute | solution.py:254
  144.6 3.0 collective-permute-done.13
  150.8 23.7 %collective-permute-done.14 = bf16[1024,512]{0,1:T(8,128)(2,1)S(1)} collective-permute-done((bf16[1024,512]{0,1:T(8,128)(2,1)S(1)}, bf16[1024,512]{0,1:T(8,128)(2,1)S(1)}, u32[]{:S(2)}, u32[]{:S(2)}) %collective-permute-start.14) | collective-permute-done | bytes 1048608 | tf_op jit(solution)/shard_map/ppermute | solution.py:124
  180.1 20.9 %collective-permute-done.16 = bf16[1024,384]{1,0:T(8,128)(2,1)S(1)} collective-permute-done((bf16[1024,384]{1,0:T(8,128)(2,1)S(1)}, bf16[1024,384]{1,0:T(8,128)(2,1)S(1)}, u32[]{:S(2)}, u32[]{:S(2)}) %collective-permute-start.16) | collective-permute-done | bytes 786464 | tf_op jit(solution)/shard_map/ppermute | solution.py:246
  204.6 19.2 %collective-permute-done.17 = bf16[1024,384]{1,0:T(8,128)(2,1)} collective-permute-done((bf16[1024,384]{1,0:T(8,128)(2,1)}, bf16[1024,384]{1,0:T(8,128)(2,1)}, u32[]{:S(2)}, u32[]{:S(2)}) %collective-permute-start.17) | collective-permute-done | bytes 786464 | tf_op jit(solution)/shard_map/ppermute | solution.py:246
  223.9 3.5 %add_convert_fusion.3 = bf16[1024,384]{1,0:T(8,128)(2,1)} fusion(bf16[1024,384]{1,0:T(8,128)(2,1)} %collective-permute-done.17, bf16[1024,128]{1,0:T(8,128)(2,1)S(1)} %copy-done.28, bf16[1024,128]{1,0:T(8,128)(2,1)S(1)} %copy-done.29, bf16[1024,128]{1,0:T(8,128)(2,1)S(1)} %get-tuple-element.26, f32[1024]{0:T(1024)S(1)} %bitcast.130, ...), kind=kOutput, calls=%fused_computation.16 | convolution fusion | flops 815136768 | bytes 4460544 | tf_op jit(solution)/shard_map/dot_general | solution.py:242
  227.5 2.9 fusion.84.own_ref
  230.4 12.5 %collective-permute-done.20 = f32[8,128]{1,0:T(8,128)S(1)} collective-permute-done((f32[8,128]{1,0:T(8,128)S(1)}, f32[8,128]{1,0:T(8,128)S(1)}, u32[]{:S(2)}, u32[]{:S(2)}) %collective-permute-start.20) | collective-permute-done | bytes 4128 | tf_op jit(solution)/shard_map/ppermute | solution.py:124
  243.2 3.7 %collective-permute-done.18.arrived_ref = bf16[1024,384]{1,0:T(8,128)(2,1)S(1)} collective-permute-done((bf16[1024,384]{1,0:T(8,128)(2,1)}, bf16[1024,384]{1,0:T(8,128)(2,1)S(1)}, u32[]{:S(2)}, u32[]{:S(2)}) %collective-permute-start.18) | collective-permute-done | bytes 786464 | tf_op jit(solution)/shard_map/ppermute | solution.py:246
  246.9 5.8 %attend.3 = bf16[1024,128]{1,0:T(8,128)(2,1)S(1)} custom-call(bf16[1024,384]{1,0:T(8,128)(2,1)S(1)} %collective-permute-done.18.arrived_ref, f32[1024,384]{1,0:T(8,128)S(1)} %fusion.84.own_ref, f32[1024,1]{1,0:T(8,128)S(1)} %copy.31.norm_ref, f32[1,64,960]{2,1,0:T(8,128)S(1)} %reshape.180.bias_ref), custom_call_target="tpu_custom_call" | custom-call | flops 268435456 | bytes 3145728 | tf_op jit(solution)/shard_map/attend/pallas_call | solution.py:185
  255.1 5.7 %collective-permute-done.23 = bf16[1024,128]{1,0:T(8,128)(2,1)S(1)} collective-permute-done((bf16[1024,128]{1,0:T(8,128)(2,1)S(1)}, bf16[1024,128]{1,0:T(8,128)(2,1)S(1)}, u32[]{:S(2)}, u32[]{:S(2)}) %collective-permute-start.23) | collective-permute-done | bytes 262176 | tf_op jit(solution)/shard_map/ppermute | solution.py:254
  260.8 14.0 %collective-permute-done.22 = bf16[1024,128]{1,0:T(8,128)(2,1)S(1)} collective-permute-done((bf16[1024,128]{1,0:T(8,128)(2,1)S(1)}, bf16[1024,128]{1,0:T(8,128)(2,1)S(1)}, u32[]{:S(2)}, u32[]{:S(2)}) %collective-permute-start.22) | collective-permute-done | bytes 262176 | tf_op jit(solution)/shard_map/ppermute | solution.py:254
  283.5 12.5 %collective-permute-done.25 = bf16[1024,256]{0,1:T(8,128)(2,1)S(1)} collective-permute-done((bf16[1024,256]{0,1:T(8,128)(2,1)S(1)}, bf16[1024,256]{0,1:T(8,128)(2,1)S(1)}, u32[]{:S(2)}, u32[]{:S(2)}) %collective-permute-start.25) | collective-permute-done | bytes 524320 | tf_op jit(solution)/shard_map/ppermute | solution.py:124
  297.6 2.8 collective-permute-start.28
  300.5 4.0 %collective-permute-done.26 = bf16[256,256]{0,1:T(8,128)(2,1)S(1)} collective-permute-done((bf16[256,256]{0,1:T(8,128)(2,1)S(1)}, bf16[256,256]{0,1:T(8,128)(2,1)S(1)}, u32[]{:S(2)}, u32[]{:S(2)}) %collective-permute-start.26) | collective-permute-done | bytes 131104 | tf_op jit(solution)/shard_map/ppermute | solution.py:285
  304.5 4.0 %collective-permute-done.27 = bf16[256,256]{0,1:T(8,128)(2,1)S(1)} collective-permute-done((bf16[256,256]{0,1:T(8,128)(2,1)S(1)}, bf16[256,256]{0,1:T(8,128)(2,1)S(1)}, u32[]{:S(2)}, u32[]{:S(2)}) %collective-permute-start.27) | collective-permute-done | bytes 131104 | tf_op jit(solution)/shard_map/ppermute | solution.py:285
  309.1 3.4 dynamic_update_slice.31
  314.3 10.1 %collective-permute-done.29 = bf16[256,4,256]{0,2,1:T(8,128)(2,1)S(1)} collective-permute-done((bf16[256,4,256]{0,2,1:T(8,128)(2,1)S(1)}, bf16[256,4,256]{0,2,1:T(8,128)(2,1)S(1)}, u32[]{:S(2)}, u32[]{:S(2)}) %collective-permute-start.29) | collective-permute-done | bytes 524320 | tf_op jit(solution)/shard_map/ppermute | solution.py:124
  333.8 2.9 broadcast_select_fusion
  (188 shorter events, 74.0 us)
Async XLA Ops:
  1.3 9.6 %collective-permute-start = (bf16[256,256]{0,1:T(8,128)(2,1)S(1)}, bf16[256,256]{0,1:T(8,128)(2,1)S(1)}, u32[]{:S(2)}, u32[]{:S(2)}) collective-permute-start(bf16[256,256]{0,1:T(8,128)(2,1)S(1)} %copy.45), channel_id=1, source_target_pairs={{0,4},{4,8},{8,12},{12,0},{1,5},{5,9},{9,13},{13,1},{2,6},{6,10},{... | collective-permute-start | bytes 393224 | tf_op jit(solution)/shard_map/ppermute | solution.py:222
  4.5 11.1 %collective-permute-start.1 = (bf16[256,256]{0,1:T(8,128)(2,1)S(1)}, bf16[256,256]{0,1:T(8,128)(2,1)S(1)}, u32[]{:S(2)}, u32[]{:S(2)}) collective-permute-start(bf16[256,256]{0,1:T(8,128)(2,1)S(1)} %copy.46), channel_id=1, source_target_pairs={{0,8},{4,12},{8,0},{12,4},{1,9},{5,13},{9,1},{13,5},{2,10},{6,14},... | collective-permute-start | bytes 393224 | tf_op jit(solution)/shard_map/ppermute | solution.py:222
  7.2 8.4 %collective-permute-start.2 = (bf16[256,256]{0,1:T(8,128)(2,1)S(1)}, bf16[256,256]{0,1:T(8,128)(2,1)S(1)}, u32[]{:S(2)}, u32[]{:S(2)}) collective-permute-start(bf16[256,256]{0,1:T(8,128)(2,1)S(1)} %copy.47), channel_id=1, source_target_pairs={{0,12},{4,0},{8,4},{12,8},{1,13},{5,1},{9,5},{13,9},{2,14},{6,2},{... | collective-permute-start | bytes 393224 | tf_op jit(solution)/shard_map/ppermute | solution.py:222
  15.6 13.8 %collective-permute-start.3 = (bf16[1024,256]{0,1:T(8,128)(2,1)S(1)}, bf16[1024,256]{0,1:T(8,128)(2,1)S(1)}, u32[]{:S(2)}, u32[]{:S(2)}) collective-permute-start(bf16[1024,256]{0,1:T(8,128)(2,1)S(1)} %constant_dynamic-update-slice_fusion), channel_id=1, source_target_pairs={{0,2},{1,3},{2,0},{3,1},{4,6},{5,7},{6,4},{7,5},{8,10},{9,11},{10,... | collective-permute-start | bytes 1572872 | tf_op jit(solution)/shard_map/ppermute | solution.py:124
  29.6 7.5 %collective-permute-start.4 = (bf16[1024,512]{0,1:T(8,128)(2,1)S(1)}, bf16[1024,512]{0,1:T(8,128)(2,1)}, u32[]{:S(2)}, u32[]{:S(2)}) collective-permute-start(bf16[1024,512]{0,1:T(8,128)(2,1)S(1)} %pad_maximum_fusion.3), channel_id=1, source_target_pairs={{0,1},{1,0},{2,3},{3,2},{4,5},{5,4},{6,7},{7,6},{8,9},{9,8},{10,11... | collective-permute-start | bytes 3145736 | tf_op jit(solution)/shard_map/ppermute | solution.py:124
  39.0 49.0 %copy-start.6 = (bf16[1024,512]{0,1:T(8,128)(2,1)}, bf16[1024,512]{0,1:T(8,128)(2,1)S(1)}, u32[]{:S(2)}) copy-start(bf16[1024,512]{0,1:T(8,128)(2,1)S(1)} %get-tuple-element.9) | copy-start | bytes 3145732
  41.3 22.0 %collective-permute-start.5 = (bf16[1024,384]{1,0:T(8,128)(2,1)}, bf16[1024,384]{1,0:T(8,128)(2,1)}, u32[]{:S(2)}, u32[]{:S(2)}) collective-permute-start(bf16[1024,384]{1,0:T(8,128)(2,1)} %convolution_convert_fusion.3), channel_id=1, source_target_pairs={{0,4},{4,8},{8,12},{12,0},{1,5},{5,9},{9,13},{13,1},{2,6},{6,10},{... | collective-permute-start | bytes 2359304 | tf_op jit(solution)/shard_map/ppermute | solution.py:246
  66.7 21.2 %collective-permute-start.6 = (bf16[1024,384]{1,0:T(8,128)(2,1)}, bf16[1024,384]{1,0:T(8,128)(2,1)}, u32[]{:S(2)}, u32[]{:S(2)}) collective-permute-start(bf16[1024,384]{1,0:T(8,128)(2,1)} %add_convert_fusion.6), channel_id=1, source_target_pairs={{0,4},{4,8},{8,12},{12,0},{1,5},{5,9},{9,13},{13,1},{2,6},{6,10},{... | collective-permute-start | bytes 2359304 | tf_op jit(solution)/shard_map/ppermute | solution.py:246
  69.5 21.9 %collective-permute-start.8 = (f32[8,128]{1,0:T(8,128)S(1)}, f32[8,128]{1,0:T(8,128)S(1)}, u32[]{:S(2)}, u32[]{:S(2)}) collective-permute-start(f32[8,128]{1,0:T(8,128)S(1)} %bitcast.120), channel_id=1, source_target_pairs={{0,4},{4,0},{8,12},{12,8},{1,5},{5,1},{9,13},{13,9},{2,6},{6,2},{1... | collective-permute-start | bytes 12296 | tf_op jit(solution)/shard_map/ppermute | solution.py:124
  91.5 20.2 %collective-permute-start.7 = (bf16[1024,384]{1,0:T(8,128)(2,1)}, bf16[1024,384]{1,0:T(8,128)(2,1)S(1)}, u32[]{:S(2)}, u32[]{:S(2)}) collective-permute-start(bf16[1024,384]{1,0:T(8,128)(2,1)} %add_convert_fusion.5), channel_id=1, source_target_pairs={{0,4},{4,8},{8,12},{12,0},{1,5},{5,9},{9,13},{13,1},{2,6},{6,10},{... | collective-permute-start | bytes 2359304 | tf_op jit(solution)/shard_map/ppermute | solution.py:246
  91.5 16.2 %collective-permute-start.9 = (f32[8,128]{1,0:T(8,128)S(1)}, f32[8,128]{1,0:T(8,128)S(1)}, u32[]{:S(2)}, u32[]{:S(2)}) collective-permute-start(f32[8,128]{1,0:T(8,128)S(1)} %bitcast_add_fusion.1), channel_id=1, source_target_pairs={{0,8},{4,12},{8,0},{12,4},{1,9},{5,13},{9,1},{13,5},{2,10},{6,14},... | collective-permute-start | bytes 12296 | tf_op jit(solution)/shard_map/ppermute | solution.py:124
  117.4 7.0 %collective-permute-start.12 = (bf16[1024,128]{1,0:T(8,128)(2,1)S(1)}, bf16[1024,128]{1,0:T(8,128)(2,1)S(1)}, u32[]{:S(2)}, u32[]{:S(2)}) collective-permute-start(bf16[1024,128]{1,0:T(8,128)(2,1)S(1)} %attend.2), channel_id=1, source_target_pairs={{0,12},{4,0},{8,4},{12,8},{1,13},{5,1},{9,5},{13,9},{2,14},{6,2},{... | collective-permute-start | bytes 786440 | tf_op jit(solution)/shard_map/ppermute | solution.py:254
  117.5 22.8 %collective-permute-start.11 = (bf16[1024,128]{1,0:T(8,128)(2,1)S(1)}, bf16[1024,128]{1,0:T(8,128)(2,1)S(1)}, u32[]{:S(2)}, u32[]{:S(2)}) collective-permute-start(bf16[1024,128]{1,0:T(8,128)(2,1)S(1)} %attend.2), channel_id=1, source_target_pairs={{0,8},{4,12},{8,0},{12,4},{1,9},{5,13},{9,1},{13,5},{2,10},{6,14},... | collective-permute-start | bytes 786440 | tf_op jit(solution)/shard_map/ppermute | solution.py:254
  119.8 20.5 %collective-permute-start.10 = (bf16[1024,128]{1,0:T(8,128)(2,1)S(1)}, bf16[1024,128]{1,0:T(8,128)(2,1)S(1)}, u32[]{:S(2)}, u32[]{:S(2)}) collective-permute-start(bf16[1024,128]{1,0:T(8,128)(2,1)S(1)} %attend.2), channel_id=1, source_target_pairs={{0,4},{4,8},{8,12},{12,0},{1,5},{5,9},{9,13},{13,1},{2,6},{6,10},{... | collective-permute-start | bytes 786440 | tf_op jit(solution)/shard_map/ppermute | solution.py:254
  144.6 3.0 collective-permute-start.13
  149.2 25.3 %collective-permute-start.14 = (bf16[1024,512]{0,1:T(8,128)(2,1)S(1)}, bf16[1024,512]{0,1:T(8,128)(2,1)S(1)}, u32[]{:S(2)}, u32[]{:S(2)}) collective-permute-start(bf16[1024,512]{0,1:T(8,128)(2,1)S(1)} %add_convert_fusion.2), channel_id=1, source_target_pairs={{0,2},{1,3},{2,0},{3,1},{4,6},{5,7},{6,4},{7,5},{8,10},{9,11},{10,... | collective-permute-start | bytes 3145736 | tf_op jit(solution)/shard_map/ppermute | solution.py:124
  175.2 3.2 collective-permute-start.15
  180.1 21.0 %collective-permute-start.16 = (bf16[1024,384]{1,0:T(8,128)(2,1)S(1)}, bf16[1024,384]{1,0:T(8,128)(2,1)S(1)}, u32[]{:S(2)}, u32[]{:S(2)}) collective-permute-start(bf16[1024,384]{1,0:T(8,128)(2,1)S(1)} %convolution_convert_fusion.2), channel_id=1, source_target_pairs={{0,4},{4,8},{8,12},{12,0},{1,5},{5,9},{9,13},{13,1},{2,6},{6,10},{... | collective-permute-start | bytes 2359304 | tf_op jit(solution)/shard_map/ppermute | solution.py:246
  203.4 20.4 %collective-permute-start.17 = (bf16[1024,384]{1,0:T(8,128)(2,1)}, bf16[1024,384]{1,0:T(8,128)(2,1)}, u32[]{:S(2)}, u32[]{:S(2)}) collective-permute-start(bf16[1024,384]{1,0:T(8,128)(2,1)} %add_convert_fusion.4), channel_id=1, source_target_pairs={{0,4},{4,8},{8,12},{12,0},{1,5},{5,9},{9,13},{13,1},{2,6},{6,10},{... | collective-permute-start | bytes 2359304 | tf_op jit(solution)/shard_map/ppermute | solution.py:246
  204.6 22.8 %collective-permute-start.19 = (f32[8,128]{1,0:T(8,128)S(1)}, f32[8,128]{1,0:T(8,128)S(1)}, u32[]{:S(2)}, u32[]{:S(2)}) collective-permute-start(f32[8,128]{1,0:T(8,128)S(1)} %bitcast.121), channel_id=1, source_target_pairs={{0,4},{4,0},{8,12},{12,8},{1,5},{5,1},{9,13},{13,9},{2,6},{6,2},{1... | collective-permute-start | bytes 12296 | tf_op jit(solution)/shard_map/ppermute | solution.py:124
  227.4 19.5 %collective-permute-start.18 = (bf16[1024,384]{1,0:T(8,128)(2,1)}, bf16[1024,384]{1,0:T(8,128)(2,1)S(1)}, u32[]{:S(2)}, u32[]{:S(2)}) collective-permute-start(bf16[1024,384]{1,0:T(8,128)(2,1)} %add_convert_fusion.3), channel_id=1, source_target_pairs={{0,4},{4,8},{8,12},{12,0},{1,5},{5,9},{9,13},{13,1},{2,6},{6,10},{... | collective-permute-start | bytes 2359304 | tf_op jit(solution)/shard_map/ppermute | solution.py:246
  227.4 15.5 %collective-permute-start.20 = (f32[8,128]{1,0:T(8,128)S(1)}, f32[8,128]{1,0:T(8,128)S(1)}, u32[]{:S(2)}, u32[]{:S(2)}) collective-permute-start(f32[8,128]{1,0:T(8,128)S(1)} %bitcast_add_fusion), channel_id=1, source_target_pairs={{0,8},{4,12},{8,0},{12,4},{1,9},{5,13},{9,1},{13,5},{2,10},{6,14},... | collective-permute-start | bytes 12296 | tf_op jit(solution)/shard_map/ppermute | solution.py:124
  252.6 8.2 %collective-permute-start.23 = (bf16[1024,128]{1,0:T(8,128)(2,1)S(1)}, bf16[1024,128]{1,0:T(8,128)(2,1)S(1)}, u32[]{:S(2)}, u32[]{:S(2)}) collective-permute-start(bf16[1024,128]{1,0:T(8,128)(2,1)S(1)} %attend.3), channel_id=1, source_target_pairs={{0,12},{4,0},{8,4},{12,8},{1,13},{5,1},{9,5},{13,9},{2,14},{6,2},{... | collective-permute-start | bytes 786440 | tf_op jit(solution)/shard_map/ppermute | solution.py:254
  252.7 22.1 %collective-permute-start.22 = (bf16[1024,128]{1,0:T(8,128)(2,1)S(1)}, bf16[1024,128]{1,0:T(8,128)(2,1)S(1)}, u32[]{:S(2)}, u32[]{:S(2)}) collective-permute-start(bf16[1024,128]{1,0:T(8,128)(2,1)S(1)} %attend.3), channel_id=1, source_target_pairs={{0,8},{4,12},{8,0},{12,4},{1,9},{5,13},{9,1},{13,5},{2,10},{6,14},... | collective-permute-start | bytes 786440 | tf_op jit(solution)/shard_map/ppermute | solution.py:254
  255.0 19.8 %collective-permute-start.21 = (bf16[1024,128]{1,0:T(8,128)(2,1)S(1)}, bf16[1024,128]{1,0:T(8,128)(2,1)S(1)}, u32[]{:S(2)}, u32[]{:S(2)}) collective-permute-start(bf16[1024,128]{1,0:T(8,128)(2,1)S(1)} %attend.3), channel_id=1, source_target_pairs={{0,4},{4,8},{8,12},{12,0},{1,5},{5,9},{9,13},{13,1},{2,6},{6,10},{... | collective-permute-start | bytes 786440 | tf_op jit(solution)/shard_map/ppermute | solution.py:254
  277.5 2.7 collective-permute-start.24
  281.9 14.0 %collective-permute-start.25 = (bf16[1024,256]{0,1:T(8,128)(2,1)S(1)}, bf16[1024,256]{0,1:T(8,128)(2,1)S(1)}, u32[]{:S(2)}, u32[]{:S(2)}) collective-permute-start(bf16[1024,256]{0,1:T(8,128)(2,1)S(1)} %constant_dynamic-slice_fusion.3), channel_id=1, source_target_pairs={{0,2},{1,3},{2,0},{3,1},{4,6},{5,7},{6,4},{7,5},{8,10},{9,11},{10,... | collective-permute-start | bytes 1572872 | tf_op jit(solution)/shard_map/ppermute | solution.py:124
  296.3 8.2 %collective-permute-start.26 = (bf16[256,256]{0,1:T(8,128)(2,1)S(1)}, bf16[256,256]{0,1:T(8,128)(2,1)S(1)}, u32[]{:S(2)}, u32[]{:S(2)}) collective-permute-start(bf16[256,256]{0,1:T(8,128)(2,1)S(1)} %get-tuple-element.57), channel_id=1, source_target_pairs={{0,4},{4,8},{8,12},{12,0},{1,5},{5,9},{9,13},{13,1},{2,6},{6,10},{... | collective-permute-start | bytes 393224 | tf_op jit(solution)/shard_map/ppermute | solution.py:285
  296.4 12.1 %collective-permute-start.27 = (bf16[256,256]{0,1:T(8,128)(2,1)S(1)}, bf16[256,256]{0,1:T(8,128)(2,1)S(1)}, u32[]{:S(2)}, u32[]{:S(2)}) collective-permute-start(bf16[256,256]{0,1:T(8,128)(2,1)S(1)} %get-tuple-element.56), channel_id=1, source_target_pairs={{0,8},{4,12},{8,0},{12,4},{1,9},{5,13},{9,1},{13,5},{2,10},{6,14},... | collective-permute-start | bytes 393224 | tf_op jit(solution)/shard_map/ppermute | solution.py:285
  297.6 11.3 %collective-permute-start.28 = (bf16[256,256]{0,1:T(8,128)(2,1)S(1)}, bf16[256,256]{0,1:T(8,128)(2,1)S(1)}, u32[]{:S(2)}, u32[]{:S(2)}) collective-permute-start(bf16[256,256]{0,1:T(8,128)(2,1)S(1)} %get-tuple-element.55), channel_id=1, source_target_pairs={{0,12},{4,0},{8,4},{12,8},{1,13},{5,1},{9,5},{13,9},{2,14},{6,2},{... | collective-permute-start | bytes 393224 | tf_op jit(solution)/shard_map/ppermute | solution.py:285
  312.8 11.7 %collective-permute-start.29 = (bf16[256,4,256]{0,2,1:T(8,128)(2,1)S(1)}, bf16[256,4,256]{0,2,1:T(8,128)(2,1)S(1)}, u32[]{:S(2)}, u32[]{:S(2)}) collective-permute-start(bf16[256,4,256]{0,2,1:T(8,128)(2,1)S(1)} %copy.35), channel_id=1, source_target_pairs={{0,2},{1,3},{2,0},{3,1},{4,6},{5,7},{6,4},{7,5},{8,10},{9,11},{10,... | collective-permute-start | bytes 1572872 | tf_op jit(solution)/shard_map/ppermute | solution.py:124
  328.3 2.9 collective-permute-start.30
  (36 other events, 534.8 us)

commit v2 on v0

--- a/solution.py
+++ b/solution.py
@@ -1,6 +1,10 @@
+import functools
+
 import jax
 import jax.numpy as jnp
 from jax import lax
+from jax.experimental import pallas as pl
+from jax.experimental.pallas import tpu as pltpu
 from jax.sharding import PartitionSpec as P
 
 HD = 128
@@ -32,7 +36,7 @@
     return (scaled * gain.astype(jnp.float32)).astype(jnp.bfloat16)
 
 
-def on_device(tokens, norm_gain, w_query, w_key, w_value, w_out, offset_bias):
+def gathered_plan(tokens, norm_gain, w_query, w_key, w_value, w_out, offset_bias):
     sp_count = lax.axis_size("sp")
     sp_index = lax.axis_index("sp")
     tok_rows = tokens.shape[0]
@@ -109,6 +113,440 @@
         ).astype(jnp.float32)
         residual = (residual.astype(jnp.float32) + branch).astype(jnp.bfloat16)
     return residual
+
+
+VMEM_BYTES = 40 * 1024 * 1024
+
+
+def ring(count, shift):
+    return [(i, (i + shift) % count) for i in range(count)]
+
+
+def swapped(array, axis, distance):
+    count = lax.axis_size(axis)
+    return lax.ppermute(array, axis, [(i, i ^ distance) for i in range(count)])
+
+
+def summed_over(vector, axis):
+    count = lax.axis_size(axis)
+    distance = 1
+    while distance < count:
+        vector = vector + swapped(vector, axis, distance)
+        distance *= 2
+    return vector
+
+
+def aligned(index, size):
+    return pl.ds(pl.multiple_of(index * size, size), size)
+
+
+def local_kernel(body, place, arrays, outs, name, scratch=(), hbm=(), flops=0):
+    vmem, smem = pl.BlockSpec(memory_space=pltpu.VMEM), pl.BlockSpec(memory_space=pltpu.SMEM)
+    moved = sum(a.size * a.dtype.itemsize for a in (*arrays, *outs))
+    return pl.pallas_call(
+        body,
+        out_shape=list(outs),
+        in_specs=[smem] + [vmem] * len(arrays) + [pl.BlockSpec(memory_space=pl.ANY)] * len(hbm),
+        out_specs=[vmem] * len(outs),
+        scratch_shapes=list(scratch),
+        compiler_params=pltpu.CompilerParams(vmem_limit_bytes=VMEM_BYTES),
+        cost_estimate=pl.CostEstimate(flops=flops, bytes_accessed=moved, transcendentals=0),
+        name=name,
+    )(place, *arrays, *hbm)
+
+
+def shaped(*shape, dtype=jnp.bfloat16):
+    return jax.ShapeDtypeStruct(shape, dtype)
+
+
+def window_bias(table):
+    heads = table.shape[0]
+    columns = jnp.arange(GRID_W, dtype=jnp.int32)
+    first = jnp.clip(columns - KC // 2, 0, GRID_W - KC)
+    inside = (columns[None, :] >= first[:, None]) & (columns[None, :] < first[:, None] + KC)
+    offset = jnp.clip(columns[None, :] - columns[:, None], 1 - KC, KC - 1) + KC - 1
+    onehot = (
+        jnp.arange(2 * KC - 1, dtype=jnp.int32)[:, None, None] == offset[None, :, :]
+    ).astype(jnp.float32)
+    wide = jnp.einsum("hro,oqk->hqrk", table, onehot, precision=lax.Precision.HIGHEST)
+    wide = jnp.where(inside[None, :, None, :], wide, -jnp.inf)
+    return wide.reshape(heads, GRID_W, (2 * KR - 1) * GRID_W)
+
+
+def scatter_tokens(tokens, place, sp_count, feats, piece):
+    tok_here = tokens.shape[0]
+    rows = tok_here // 2
+
+    def body(place_ref, tokens_ref, *rest):
+        out_refs, (buffer, sem) = rest[:-2], rest[-2:]
+        slot = place_ref[1] * 2 + place_ref[2]
+        copies = []
+        for shift in range(sp_count):
+            target = lax.rem(place_ref[0] + shift, sp_count)
+            column = pl.multiple_of(target * feats + slot * piece, piece)
+            copy = pltpu.make_async_copy(
+                tokens_ref.at[:, pl.ds(column, piece)], buffer.at[shift], sem.at[shift]
+            )
+            copy.start()
+            copies.append(copy)
+        for shift in range(sp_count):
+            copies[shift].wait()
+            for part in range(2):
+                out_refs[part * sp_count + shift][...] = buffer[shift, pl.ds(part * rows, rows), :]
+
+    blocks = local_kernel(
+        body,
+        place,
+        (),
+        [shaped(rows, piece)] * (2 * sp_count),
+        "scatter_tokens",
+        scratch=[
+            pltpu.VMEM((sp_count, tok_here, piece), jnp.bfloat16),
+            pltpu.SemaphoreType.DMA((sp_count,)),
+        ],
+        hbm=(tokens,),
+    )
+    return blocks[:sp_count], blocks[sp_count:]
+
+
+def stack_blocks(blocks, place):
+    count = len(blocks)
+    rows, width = blocks[0].shape
+
+    def body(place_ref, *refs):
+        out_ref = refs[-1]
+        for shift in range(count):
+            source = lax.rem(place_ref[0] + count - shift, count)
+            out_ref[aligned(source, rows), :] = refs[shift][...]
+
+    return local_kernel(body, place, blocks, [shaped(rows * count, width)], "stack_blocks")[0]
+
+
+def over_sp(blocks, count):
+    return [blocks[0]] + [
+        lax.ppermute(blocks[shift], "sp", ring(count, shift)) for shift in range(1, count)
+    ]
+
+
+def project(pieces, slots, gain, weights, layer, place, chunk_shift, width, arrived, last):
+    tok = pieces[0].shape[0]
+    feats = weights[0].shape[1]
+    sp_count = lax.axis_size("sp")
+    count = len(pieces)
+
+    def body(place_ref, *refs):
+        piece_refs, refs = refs[:count], refs[count:]
+        gain_ref, refs = refs[0], refs[1:]
+        arrived_ref = None
+        if arrived is not None:
+            arrived_ref, refs = refs[0], refs[1:]
+        weight_refs, (out_ref, held, sem) = refs[:3], refs[3:]
+        chunk = lax.rem(place_ref[0] + chunk_shift, sp_count)
+        copies = []
+        for index, weight_ref in enumerate(weight_refs):
+            copy = pltpu.make_async_copy(
+                weight_ref.at[layer, :, aligned(chunk, width)],
+                held.at[:, pl.ds(index * width, width)],
+                sem.at[index],
+            )
+            copy.start()
+            copies.append(copy)
+        for copy in copies:
+            copy.wait()
+        total = jnp.zeros((tok, 3 * width), jnp.float32)
+        if arrived is not None:
+            total = arrived_ref[...].astype(jnp.float32)
+        for piece_ref, slot in zip(piece_refs, slots):
+            span = aligned(slot(place_ref[1], place_ref[2]), piece_ref.shape[1])
+            scaled = piece_ref[...].astype(jnp.float32) * gain_ref[layer, :, span]
+            total += jnp.dot(
+                scaled.astype(jnp.bfloat16), held[span, :], preferred_element_type=jnp.float32
+            )
+        out_ref[...] = total.astype(out_ref.dtype)
+
+    arrays = (*pieces, gain) + (() if arrived is None else (arrived,))
+    return local_kernel(
+        body,
+        place,
+        arrays,
+        [shaped(tok, 3 * width, dtype=jnp.float32 if last else jnp.bfloat16)],
+        "project",
+        scratch=[
+            pltpu.VMEM((feats, 3 * width), jnp.bfloat16),
+            pltpu.SemaphoreType.DMA((3,)),
+        ],
+        hbm=weights,
+        flops=2 * tok * feats * 3 * width,
+    )[0]
+
+
+def attend(arrived, own, norms, bias, place, sp_count):
+    rows, total_width = arrived[0].shape
+    heads = bias.shape[0]
+    width = heads * HD
+    part_rows = rows // sp_count
+    grid_rows = 2 * rows // GRID_W
+    part_grid = part_rows // GRID_W
+
+    def body(place_ref, a0, a1, o0, o1, n0, n1, bias_ref, out0, out1, qkv_ref):
+        for part, (a_ref, o_ref, n_ref) in enumerate(((a0, o0, n0), (a1, o1, n1))):
+            for plane in range(sp_count):
+                span = pl.ds(plane * part_rows, part_rows)
+                total = a_ref[span, :].astype(jnp.float32) + o_ref[span, :]
+                qkv_ref[pl.ds((2 * plane + part) * part_rows, part_rows), :] = (
+                    total * n_ref[span, :]
+                ).astype(jnp.bfloat16)
+        for head in range(heads):
+            lanes = head * HD
+            for row in range(grid_rows):
+                first = min(max(row - KR // 2, 0), grid_rows - KR)
+                offset = first - row + KR - 1
+                queries = qkv_ref[pl.ds(row * GRID_W, GRID_W), pl.ds(lanes, HD)]
+                span = pl.ds(first * GRID_W, KR * GRID_W)
+                keys = qkv_ref[span, pl.ds(width + lanes, HD)]
+                values = qkv_ref[span, pl.ds(2 * width + lanes, HD)]
+                scores = lax.dot_general(
+                    queries, keys, (((1,), (1,)), ((), ())), preferred_element_type=jnp.float32
+                )
+                bias_here = bias_ref[head, :, pl.ds(offset * GRID_W, KR * GRID_W)]
+                scores = scores * HD ** (-0.5) + bias_here
+                powers = jnp.exp(scores - jnp.max(scores, axis=-1, keepdims=True))
+                weights = powers / jnp.sum(powers, axis=-1, keepdims=True)
+                mixed = jnp.dot(
+                    weights.astype(jnp.bfloat16), values, preferred_element_type=jnp.float32
+                )
+                block, inner = divmod(row, part_grid)
+                out_ref = (out0, out1)[block % 2]
+                at = (block // 2) * part_rows + inner * GRID_W
+                out_ref[pl.ds(at, GRID_W), pl.ds(lanes, HD)] = mixed.astype(jnp.bfloat16)
+
+    return local_kernel(
+        body,
+        place,
+        (*arrived, *own, *norms, bias),
+        [shaped(rows, width)] * 2,
+        "attend",
+        scratch=[pltpu.VMEM((2 * rows, total_width), jnp.bfloat16)],
+        flops=8 * heads * rows * KR * GRID_W * HD,
+    )
+
+
+def spread(attended, w_out, layer, place):
+    count = len(attended)
+    rows, width = attended[0].shape
+    inner, feats = w_out.shape[1:]
+    half = feats // 2
+
+    def body(place_ref, *refs):
+        piece_refs, (w_ref, sent_ref, kept_ref, gathered, held, sem) = refs[:count], refs[count:]
+        copy = pltpu.make_async_copy(w_ref.at[layer], held, sem.at[0])
+        copy.start()
+        for shift in range(count):
+            source = lax.rem(place_ref[0] + count - shift, count)
+            gathered[:, aligned(source, width)] = piece_refs[shift][...]
+        copy.wait()
+        core = place_ref[1]
+        for index, out_ref in ((1 - core, sent_ref), (core, kept_ref)):
+            out_ref[...] = jnp.dot(
+                gathered[...], held[:, aligned(index, half)], preferred_element_type=jnp.float32
+            ).astype(jnp.bfloat16)
+
+    return local_kernel(
+        body,
+        place,
+        attended,
+        [shaped(rows, half)] * 2,
+        "spread",
+        scratch=[
+            pltpu.VMEM((rows, inner), jnp.bfloat16),
+            pltpu.VMEM((inner, feats), jnp.bfloat16),
+            pltpu.SemaphoreType.DMA((1,)),
+        ],
+        hbm=(w_out,),
+        flops=2 * rows * inner * feats,
+    )
+
+
+def total_of(*refs):
+    total = refs[0][...].astype(jnp.float32)
+    for ref in refs[1:]:
+        total += ref[...].astype(jnp.float32)
+    return total
+
+
+def pair_up(kept, came, place):
+    def body(place_ref, kept_ref, came_ref, out_ref):
+        out_ref[...] = total_of(kept_ref, came_ref).astype(jnp.bfloat16)
+
+    return local_kernel(body, place, (kept, came), [shaped(*kept.shape)], "pair_up")[0]
+
+
+def pair_apart(kept, came, place):
+    rows, half = kept.shape
+    piece = half // 2
+
+    def body(place_ref, kept_ref, came_ref, sent_ref, stay_ref):
+        far = place_ref[2]
+        for index, out_ref in ((1 - far, sent_ref), (far, stay_ref)):
+            span = aligned(index, piece)
+            out_ref[...] = (
+                kept_ref[:, span].astype(jnp.float32) + came_ref[:, span].astype(jnp.float32)
+            ).astype(jnp.bfloat16)
+
+    return local_kernel(body, place, (kept, came), [shaped(rows, piece)] * 2, "pair_apart")
+
+
+def renew(residual, pair, came, place):
+    count = len(residual)
+
+    def body(place_ref, *refs):
+        piece_refs, (pair_ref, came_ref, out_ref) = refs[:count], refs[count:]
+        if count == 1:
+            branch = total_of(pair_ref, came_ref)
+            out_ref[...] = (piece_refs[0][...].astype(jnp.float32) + branch).astype(jnp.bfloat16)
+            return
+        far = place_ref[2]
+        for index, ref in ((far, piece_refs[0]), (1 - far, piece_refs[1])):
+            span = aligned(index, ref.shape[1])
+            branch = pair_ref[:, span].astype(jnp.float32) + came_ref[:, span].astype(jnp.float32)
+            out_ref[:, span] = (ref[...].astype(jnp.float32) + branch).astype(jnp.bfloat16)
+
+    return local_kernel(body, place, (*residual, pair, came), [shaped(*pair.shape)], "renew")[0]
+
+
+def finish(residual, stay, came, place, sp_count):
+    rows, piece = stay.shape
+    part = rows // sp_count
+
+    def body(place_ref, x_ref, stay_ref, came_ref, *out_refs):
+        for shift in range(sp_count):
+            target = lax.rem(place_ref[0] + shift, sp_count)
+            span = aligned(target, part)
+            branch = stay_ref[span, :].astype(jnp.float32) + came_ref[span, :].astype(jnp.float32)
+            x_here = x_ref[span, aligned(place_ref[2], piece)].astype(jnp.float32)
+            out_refs[shift][...] = (x_here + branch).astype(jnp.bfloat16)
+
+    return local_kernel(
+        body, place, (residual, stay, came), [shaped(part, piece)] * sp_count, "finish"
+    )
+
+
+SLOTS = (
+    lambda core, far: core * 2 + far,
+    lambda core, far: core * 2 + 1 - far,
+    lambda core, far: (1 - core) * 2 + far,
+    lambda core, far: (1 - core) * 2 + 1 - far,
+)
+
+
+def assemble(parts, place, sp_count):
+    rows, piece = parts[0][0].shape
+    part = rows // sp_count
+    count = len(parts[0])
+
+    def body(place_ref, *refs):
+        out_ref = refs[-1]
+        for index in range(len(parts)):
+            for which in range(count):
+                slot = SLOTS[which](place_ref[1], place_ref[2])
+                for plane in range(sp_count):
+                    out_ref[pl.ds(index * part, part), aligned(plane * count + slot, piece)] = refs[
+                        index * count + which
+                    ][pl.ds(plane * part, part), :]
+
+    flat = [array for pieces in parts for array in pieces]
+    return local_kernel(
+        body, place, flat, [shaped(part * len(parts), piece * count * sp_count)], "assemble"
+    )[0]
+
+
+def exchanged(held):
+    far = swapped(held, "tp", 2)
+    return [held, far, swapped(held, "tp", 1), swapped(far, "tp", 1)]
+
+
+def stationary_plan(tokens, norm_gain, w_query, w_key, w_value, w_out, offset_bias):
+    sp_count = lax.axis_size("sp")
+    sp_index, tp_index = lax.axis_index("sp"), lax.axis_index("tp")
+    place = jnp.stack([sp_index, tp_index % 2, tp_index // 2]).astype(jnp.int32)
+    feats = w_query.shape[1]
+    heads = offset_bias.shape[1] // sp_count
+    width = heads * HD
+    piece = feats // 4
+    every_feat = feats * sp_count
+    weights = (w_query, w_key, w_value)
+    tables = lax.dynamic_slice_in_dim(offset_bias, sp_index * heads, heads, 1)
+    gain = lax.dynamic_slice_in_dim(norm_gain, sp_index * feats, feats, 1)[:, None, :]
+
+    halves = []
+    for blocks in scatter_tokens(tokens, place, sp_count, feats, piece):
+        halves.append(exchanged(stack_blocks(over_sp(blocks, sp_count), place)))
+    slots = SLOTS
+    shifts = (1, -1)
+
+    for layer in range(LAYERS):
+        squares = jnp.concatenate(
+            [
+                sum(jnp.sum(jnp.square(p.astype(jnp.float32)), axis=-1) for p in pieces)
+                for pieces in halves
+            ]
+        )
+        squares = summed_over(squares.reshape(-1, HD), "sp").reshape(2, -1, 1)
+        norms = lax.rsqrt(squares / every_feat + norm_eps)
+        bias = window_bias(tables[layer])
+
+        arrived, own = [], []
+        travelling = [None, None]
+        for step in range(sp_count):
+            for part in range(2):
+                chunk_shift = (-shifts[part] * (step + 1)) % sp_count
+                final = step == sp_count - 1
+                made = project(
+                    halves[part],
+                    slots,
+                    gain,
+                    weights,
+                    layer,
+                    place,
+                    chunk_shift,
+                    width,
+                    None if final else travelling[part],
+                    final,
+                )
+                if final:
+                    arrived.append(travelling[part])
+                    own.append(made)
+                else:
+                    travelling[part] = lax.ppermute(made, "sp", ring(sp_count, shifts[part]))
+        attended = attend(arrived, own, (norms[0], norms[1]), bias, place, sp_count)
+
+        residuals = [pieces[:2] if layer == 0 else pieces[:1] for pieces in halves]
+        halves = []
+        for part in range(2):
+            gathered = over_sp([attended[part]] * sp_count, sp_count)
+            sent, kept = spread(gathered, w_out, layer, place)
+            came = swapped(sent, "tp", 1)
+            if layer < LAYERS - 1:
+                pair = pair_up(kept, came, place)
+                mine = renew(residuals[part], pair, swapped(pair, "tp", 2), place)
+                halves.append([mine, swapped(mine, "tp", 1)])
+            else:
+                sent, stay = pair_apart(kept, came, place)
+                blocks = finish(
+                    residuals[part][0], stay, swapped(sent, "tp", 2), place, sp_count
+                )
+                halves.append(exchanged(stack_blocks(over_sp(blocks, sp_count), place)))
+        slots = (lambda core, far: core, lambda core, far: 1 - core)
+    return assemble(halves, place, sp_count)
+
+
+def on_device(tokens, norm_gain, w_query, w_key, w_value, w_out, offset_bias):
+    heads_here, sp_count = offset_bias.shape[1], lax.axis_size("sp")
+    part_rows = tokens.shape[0] // 2
+    plan = gathered_plan
+    if heads_here % sp_count == 0 and lax.axis_size("tp") == 4 and part_rows % GRID_W == 0:
+        plan = stationary_plan
+    return plan(tokens, norm_gain, w_query, w_key, w_value, w_out, offset_bias)
 
 
 def solution(mesh):

time: 784 us -> 309 us (0.39)
  waiting for transfers between devices: 671 us -> 153 us
  Pallas kernels: 0 us -> 60.7 us
  starting transfers between devices: 8.71 us -> 66.8 us
  matrix products: 43.4 us -> 2.56 us
  between operations: 13.8 us -> 0.71 us
  other arithmetic: 15.4 us -> 4.22 us
  local copies, waits for them, and re-layouts: 31.2 us -> 20.3 us
    all_gather x4 -> x0, waiting for transfers between devices: 568 us -> none  [the longest x1 150 us: on_device(): lax.all_gather(w_query, 'sp', axis=1, tiled=True)]
    ppermute x4 -> x62, waiting for transfers between devices: 0.01 us -> 153 us  [the longest x26 62.5 us: swapped(): return lax.ppermute(array, axis, [(i, i ^ distance) for i in range(count)])]
    psum x2 -> x0, waiting for transfers between devices: 101 us -> none  [on_device(): lax.psum(jnp.dot(attended, out_weight, preferred_element_type=jnp.float32...]
    pallas_call x0 -> x36, Pallas kernels: none -> 60.7 us  [local_kernel(): pl.pallas_call(body, out_shape=list(outs), in_specs=[smem] + [vmem] * len...]
    ppermute x4 -> x62, starting transfers between devices: 8.51 us -> 66.8 us  [the longest x24 32.1 us: over_sp(): lax.ppermute(blocks[shift], 'sp', ring(count, shift))]
    dot_general x16 -> x2, matrix products: 43.4 us -> 2.56 us  [window_bias(): jnp.einsum('hro,oqk->hqrk', table, onehot, precision=lax.Precision.HIGHEST)]
    dot_general x2 -> x0, local copies, waits for them, and re-layouts: 11.8 us -> none  [on_device(): jnp.einsum('ijr,hrqk->hiqjk', row_onehot, col_bias, precision=lax.Precisi...]
    gather x2 -> x0, local copies, waits for them, and re-layouts: 8.6 us -> none  [on_device(): lax.dynamic_slice_in_dim(padded, band_begin, KR, 0)]
  transfers between devices with their start and end apart: 10 -> 62, of which waited for: 6 -> 30; matrix products, arithmetic and copies ran while one was open for 7% -> 4% of each run, Pallas kernels for 0% -> 14%
where the time goes in v2:
time: 309 us; the launch traced here: 308 us
  waiting for transfers between devices  153 us (50%)
  starting transfers between devices  66.8 us (22%)
  Pallas kernels  60.7 us (20%)
  local copies, waits for them, and re-layouts  20.3 us (7%)
  other arithmetic  4.22 us (1%)
    ppermute x26, waiting for transfers between devices, swapped(): return lax.ppermute(array, axis, [(i, i ^ distance) for i in range(count)])  62.5 us
    pallas_call x36, Pallas kernels, local_kernel(): pl.pallas_call(body, out_shape=list(outs), in_specs=[smem] + [vmem] * len...  60.7 us
    ppermute x12, waiting for transfers between devices, stationary_plan(): travelling[part] = lax.ppermute(made, 'sp', ring(sp_count, shifts[part]))  53.1 us
    ppermute x24, waiting for transfers between devices, over_sp(): lax.ppermute(blocks[shift], 'sp', ring(count, shift))  37.1 us
    ppermute x24, starting transfers between devices, over_sp(): lax.ppermute(blocks[shift], 'sp', ring(count, shift))  32.1 us
    ppermute x12, starting transfers between devices, stationary_plan(): travelling[part] = lax.ppermute(made, 'sp', ring(sp_count, shifts[part]))  22 us
    unnamed x48, local copies, waits for them, and re-layouts  14.4 us
    ppermute x26, starting transfers between devices, swapped(): return lax.ppermute(array, axis, [(i, i ^ distance) for i in range(count)])  12.8 us
  transfers between devices with their start and end apart: 62, of which 30 were waited for; matrix products, arithmetic and copies ran while one was open for 4% of the time, Pallas kernels for 14%

profile of v2, /device:TPU:0, one launch (start us, length us, event | category | flops | bytes accessed | tf_op | source)
XLA Modules:
  0.0 308.0 jit_solution(4822803483746712724)
XLA Ops:
  2.4 3.1 %collective-permute-start = (bf16[128,256]{1,0:T(8,128)(2,1)S(1)}, bf16[128,256]{1,0:T(8,128)(2,1)S(1)}, u32[]{:S(2)}, u32[]{:S(2)}) collective-permute-start(bf16[128,256]{1,0:T(8,128)(2,1)S(1)} %get-tuple-element.38), channel_id=1, source_target_pairs={{0,4},{4,8},{8,12},{12,0},{1,5},{5,9},{9,13},{13,1},{2,6},{6,10},{... | collective-permute-start | bytes 196616 | tf_op jit(solution)/shard_map/ppermute | solution.py:227
  22.9 3.8 %collective-permute-done.12.refs_1_ = bf16[512,256]{1,0:T(8,128)(2,1)S(1)} collective-permute-done((bf16[512,256]{1,0:T(8,128)(2,1)S(1)}, bf16[512,256]{1,0:T(8,128)(2,1)S(1)}, u32[]{:S(2)}, u32[]{:S(2)}) %collective-permute-start.12) | collective-permute-done | bytes 262176 | tf_op jit(solution)/shard_map/ppermute | solution.py:127
  26.8 4.3 %collective-permute-done.3.refs_1_ = bf16[512,256]{1,0:T(8,128)(2,1)S(1)} collective-permute-done((bf16[512,256]{1,0:T(8,128)(2,1)S(1)}, bf16[512,256]{1,0:T(8,128)(2,1)S(1)}, u32[]{:S(2)}, u32[]{:S(2)}) %collective-permute-start.3) | collective-permute-done | bytes 262176 | tf_op jit(solution)/shard_map/ppermute | solution.py:127
  43.0 8.2 %collective-permute-done.6.refs_5_ = bf16[512,384]{1,0:T(8,128)(2,1)S(1)} collective-permute-done((bf16[512,384]{1,0:T(8,128)(2,1)S(1)}, bf16[512,384]{1,0:T(8,128)(2,1)S(1)}, u32[]{:S(2)}, u32[]{:S(2)}) %collective-permute-start.6) | collective-permute-done | bytes 393248 | tf_op jit(solution)/shard_map/ppermute | solution.py:520
  52.8 6.7 %collective-permute-done.15.refs_5_ = bf16[512,384]{1,0:T(8,128)(2,1)S(1)} collective-permute-done((bf16[512,384]{1,0:T(8,128)(2,1)S(1)}, bf16[512,384]{1,0:T(8,128)(2,1)S(1)}, u32[]{:S(2)}, u32[]{:S(2)}) %collective-permute-start.15) | collective-permute-done | bytes 393248 | tf_op jit(solution)/shard_map/ppermute | solution.py:520
  66.0 9.7 %collective-permute-done.18 = f32[8,128]{1,0:T(8,128)S(1)} collective-permute-done((f32[8,128]{1,0:T(8,128)S(1)}, f32[8,128]{1,0:T(8,128)S(1)}, u32[]{:S(2)}, u32[]{:S(2)}) %collective-permute-start.18) | collective-permute-done | bytes 4128 | tf_op jit(solution)/shard_map/ppermute | solution.py:127
  80.9 4.0 %collective-permute-start.17 = (bf16[512,384]{1,0:T(8,128)(2,1)}, bf16[512,384]{1,0:T(8,128)(2,1)}, u32[]{:S(2)}, u32[]{:S(2)}) collective-permute-start(bf16[512,384]{1,0:T(8,128)(2,1)} %project.21), channel_id=1, source_target_pairs={{0,12},{4,0},{8,4},{12,8},{1,13},{5,1},{9,5},{13,9},{2,14},{6,2},{... | collective-permute-start | bytes 1179656 | tf_op jit(solution)/shard_map/ppermute | solution.py:520
  85.3 7.5 %collective-permute-done.8.a0 = bf16[512,384]{1,0:T(8,128)(2,1)} collective-permute-done((bf16[512,384]{1,0:T(8,128)(2,1)}, bf16[512,384]{1,0:T(8,128)(2,1)}, u32[]{:S(2)}, u32[]{:S(2)}) %collective-permute-start.8) | collective-permute-done | bytes 393248 | tf_op jit(solution)/shard_map/ppermute | solution.py:520
  92.8 6.9 %collective-permute-done.17.a1 = bf16[512,384]{1,0:T(8,128)(2,1)} collective-permute-done((bf16[512,384]{1,0:T(8,128)(2,1)}, bf16[512,384]{1,0:T(8,128)(2,1)}, u32[]{:S(2)}, u32[]{:S(2)}) %collective-permute-start.17) | collective-permute-done | bytes 393248 | tf_op jit(solution)/shard_map/ppermute | solution.py:520
  101.9 6.9 %attend.2 = (bf16[512,128]{1,0:T(8,128)(2,1)S(1)}, bf16[512,128]{1,0:T(8,128)(2,1)S(1)}) custom-call(s32[3]{0:T(128)S(1)} %pad_add_fusion.place_ref, bf16[512,384]{1,0:T(8,128)(2,1)} %collective-permute-done.8.a0, bf16[512,384]{1,0:T(8,128)(2,1)} %collective-permute-done.17.a1, f32[512,384]{1,0:T(8,128)S(1)} %copy-done.13, f32[512,384]{1,0:T(8,128)S(1)} %copy-done.15, ...), custom_call_target="tpu_custom_call" | custom-call | flops 268435456 | bytes 2871296 | tf_op jit(solution)/shard_map/attend/pallas_call | solution.py:146
  110.0 2.7 collective-permute-start.22
  117.7 5.1 %collective-permute-done.21.refs_2_ = bf16[512,128]{1,0:T(8,128)(2,1)S(1)} collective-permute-done((bf16[512,128]{1,0:T(8,128)(2,1)S(1)}, bf16[512,128]{1,0:T(8,128)(2,1)S(1)}, u32[]{:S(2)}, u32[]{:S(2)}) %collective-permute-start.21) | collective-permute-done | bytes 131104 | tf_op jit(solution)/shard_map/ppermute | solution.py:227
  125.6 7.4 %collective-permute-done.30.refs_2_ = bf16[512,128]{1,0:T(8,128)(2,1)S(1)} collective-permute-done((bf16[512,128]{1,0:T(8,128)(2,1)S(1)}, bf16[512,128]{1,0:T(8,128)(2,1)S(1)}, u32[]{:S(2)}, u32[]{:S(2)}) %collective-permute-start.30) | collective-permute-done | bytes 131104 | tf_op jit(solution)/shard_map/ppermute | solution.py:227
  138.6 11.6 %collective-permute-done.24.refs_3_ = bf16[512,512]{1,0:T(8,128)(2,1)S(1)} collective-permute-done((bf16[512,512]{1,0:T(8,128)(2,1)S(1)}, bf16[512,512]{1,0:T(8,128)(2,1)S(1)}, u32[]{:S(2)}, u32[]{:S(2)}) %collective-permute-start.24) | collective-permute-done | bytes 524320 | tf_op jit(solution)/shard_map/ppermute | solution.py:127
  151.0 9.9 %collective-permute-done.33.refs_3_ = bf16[512,512]{1,0:T(8,128)(2,1)S(1)} collective-permute-done((bf16[512,512]{1,0:T(8,128)(2,1)S(1)}, bf16[512,512]{1,0:T(8,128)(2,1)S(1)}, u32[]{:S(2)}, u32[]{:S(2)}) %collective-permute-start.33) | collective-permute-done | bytes 524320 | tf_op jit(solution)/shard_map/ppermute | solution.py:127
  169.7 2.7 collective-permute-start.26
  178.1 5.5 %collective-permute-done.26.refs_3_ = bf16[512,384]{1,0:T(8,128)(2,1)S(1)} collective-permute-done((bf16[512,384]{1,0:T(8,128)(2,1)S(1)}, bf16[512,384]{1,0:T(8,128)(2,1)S(1)}, u32[]{:S(2)}, u32[]{:S(2)}) %collective-permute-start.26) | collective-permute-done | bytes 393248 | tf_op jit(solution)/shard_map/ppermute | solution.py:520
  186.5 5.6 %collective-permute-done.35.refs_3_ = bf16[512,384]{1,0:T(8,128)(2,1)S(1)} collective-permute-done((bf16[512,384]{1,0:T(8,128)(2,1)S(1)}, bf16[512,384]{1,0:T(8,128)(2,1)S(1)}, u32[]{:S(2)}, u32[]{:S(2)}) %collective-permute-start.35) | collective-permute-done | bytes 393248 | tf_op jit(solution)/shard_map/ppermute | solution.py:520
  194.0 3.0 collective-permute-start.36
  201.2 7.3 %collective-permute-done.38 = f32[8,128]{1,0:T(8,128)S(1)} collective-permute-done((f32[8,128]{1,0:T(8,128)S(1)}, f32[8,128]{1,0:T(8,128)S(1)}, u32[]{:S(2)}, u32[]{:S(2)}) %collective-permute-start.38) | collective-permute-done | bytes 4128 | tf_op jit(solution)/shard_map/ppermute | solution.py:127
  209.2 2.7 project.26
  212.3 2.7 project.29
  215.0 3.6 %collective-permute-start.37 = (bf16[512,384]{1,0:T(8,128)(2,1)}, bf16[512,384]{1,0:T(8,128)(2,1)}, u32[]{:S(2)}, u32[]{:S(2)}) collective-permute-start(bf16[512,384]{1,0:T(8,128)(2,1)} %project.29), channel_id=1, source_target_pairs={{0,12},{4,0},{8,4},{12,8},{1,13},{5,1},{9,5},{13,9},{2,14},{6,2},{... | collective-permute-start | bytes 1179656 | tf_op jit(solution)/shard_map/ppermute | solution.py:520
  220.3 5.8 %collective-permute-done.28.a0 = bf16[512,384]{1,0:T(8,128)(2,1)} collective-permute-done((bf16[512,384]{1,0:T(8,128)(2,1)}, bf16[512,384]{1,0:T(8,128)(2,1)}, u32[]{:S(2)}, u32[]{:S(2)}) %collective-permute-start.28) | collective-permute-done | bytes 393248 | tf_op jit(solution)/shard_map/ppermute | solution.py:520
  226.1 6.8 %collective-permute-done.37.a1 = bf16[512,384]{1,0:T(8,128)(2,1)} collective-permute-done((bf16[512,384]{1,0:T(8,128)(2,1)}, bf16[512,384]{1,0:T(8,128)(2,1)}, u32[]{:S(2)}, u32[]{:S(2)}) %collective-permute-start.37) | collective-permute-done | bytes 393248 | tf_op jit(solution)/shard_map/ppermute | solution.py:520
  237.1 6.9 %attend.3 = (bf16[512,128]{1,0:T(8,128)(2,1)S(1)}, bf16[512,128]{1,0:T(8,128)(2,1)S(1)}) custom-call(s32[3]{0:T(128)S(1)} %pad_add_fusion.place_ref, bf16[512,384]{1,0:T(8,128)(2,1)} %collective-permute-done.28.a0, bf16[512,384]{1,0:T(8,128)(2,1)} %collective-permute-done.37.a1, f32[512,384]{1,0:T(8,128)S(1)} %copy-done.17, f32[512,384]{1,0:T(8,128)S(1)} %copy-done.19, ...), custom_call_target="tpu_custom_call" | custom-call | flops 268435456 | bytes 2871296 | tf_op jit(solution)/shard_map/attend/pallas_call | solution.py:146
  252.9 5.1 %collective-permute-done.41.refs_2_ = bf16[512,128]{1,0:T(8,128)(2,1)S(1)} collective-permute-done((bf16[512,128]{1,0:T(8,128)(2,1)S(1)}, bf16[512,128]{1,0:T(8,128)(2,1)S(1)}, u32[]{:S(2)}, u32[]{:S(2)}) %collective-permute-start.41) | collective-permute-done | bytes 131104 | tf_op jit(solution)/shard_map/ppermute | solution.py:227
  260.9 7.4 %collective-permute-done.52.refs_2_ = bf16[512,128]{1,0:T(8,128)(2,1)S(1)} collective-permute-done((bf16[512,128]{1,0:T(8,128)(2,1)S(1)}, bf16[512,128]{1,0:T(8,128)(2,1)S(1)}, u32[]{:S(2)}, u32[]{:S(2)}) %collective-permute-start.52) | collective-permute-done | bytes 131104 | tf_op jit(solution)/shard_map/ppermute | solution.py:227
  273.8 6.0 %collective-permute-done.44.came_ref = bf16[512,256]{1,0:T(8,128)(2,1)S(1)} collective-permute-done((bf16[512,256]{1,0:T(8,128)(2,1)S(1)}, bf16[512,256]{1,0:T(8,128)(2,1)S(1)}, u32[]{:S(2)}, u32[]{:S(2)}) %collective-permute-start.44) | collective-permute-done | bytes 262176 | tf_op jit(solution)/shard_map/ppermute | solution.py:127
  280.5 2.7 collective-permute-start.45
  297.1 2.7 collective-permute-done.48.refs_1_
  299.8 4.5 %collective-permute-done.59.refs_5_ = bf16[512,256]{1,0:T(8,128)(2,1)S(1)} collective-permute-done((bf16[512,256]{1,0:T(8,128)(2,1)S(1)}, bf16[512,256]{1,0:T(8,128)(2,1)S(1)}, u32[]{:S(2)}, u32[]{:S(2)}) %collective-permute-start.59) | collective-permute-done | bytes 262176 | tf_op jit(solution)/shard_map/ppermute | solution.py:127
  (215 shorter events, 128.2 us)
Async XLA Ops:
  2.4 18.7 %collective-permute-start = (bf16[128,256]{1,0:T(8,128)(2,1)S(1)}, bf16[128,256]{1,0:T(8,128)(2,1)S(1)}, u32[]{:S(2)}, u32[]{:S(2)}) collective-permute-start(bf16[128,256]{1,0:T(8,128)(2,1)S(1)} %get-tuple-element.38), channel_id=1, source_target_pairs={{0,4},{4,8},{8,12},{12,0},{1,5},{5,9},{9,13},{13,1},{2,6},{6,10},{... | collective-permute-start | bytes 196616 | tf_op jit(solution)/shard_map/ppermute | solution.py:227
  5.5 15.6 %collective-permute-start.1 = (bf16[128,256]{1,0:T(8,128)(2,1)S(1)}, bf16[128,256]{1,0:T(8,128)(2,1)S(1)}, u32[]{:S(2)}, u32[]{:S(2)}) collective-permute-start(bf16[128,256]{1,0:T(8,128)(2,1)S(1)} %get-tuple-element.39), channel_id=1, source_target_pairs={{0,8},{4,12},{8,0},{12,4},{1,9},{5,13},{9,1},{13,5},{2,10},{6,14},... | collective-permute-start | bytes 196616 | tf_op jit(solution)/shard_map/ppermute | solution.py:227
  26.6 12.7 %collective-permute-start.14 = (bf16[512,256]{1,0:T(8,128)(2,1)S(1)}, bf16[512,256]{1,0:T(8,128)(2,1)S(1)}, u32[]{:S(2)}, u32[]{:S(2)}) collective-permute-start(bf16[512,256]{1,0:T(8,128)(2,1)S(1)} %collective-permute-done.12.refs_1_), channel_id=1, source_target_pairs={{0,1},{1,0},{2,3},{3,2},{4,5},{5,4},{6,7},{7,6},{8,9},{9,8},{10,11... | collective-permute-start | bytes 786440 | tf_op jit(solution)/shard_map/ppermute | solution.py:127
  37.3 13.9 %collective-permute-start.6 = (bf16[512,384]{1,0:T(8,128)(2,1)S(1)}, bf16[512,384]{1,0:T(8,128)(2,1)S(1)}, u32[]{:S(2)}, u32[]{:S(2)}) collective-permute-start(bf16[512,384]{1,0:T(8,128)(2,1)S(1)} %project.16), channel_id=1, source_target_pairs={{0,4},{4,8},{8,12},{12,0},{1,5},{5,9},{9,13},{13,1},{2,6},{6,10},{... | collective-permute-start | bytes 1179656 | tf_op jit(solution)/shard_map/ppermute | solution.py:520
  40.7 18.8 %collective-permute-start.15 = (bf16[512,384]{1,0:T(8,128)(2,1)S(1)}, bf16[512,384]{1,0:T(8,128)(2,1)S(1)}, u32[]{:S(2)}, u32[]{:S(2)}) collective-permute-start(bf16[512,384]{1,0:T(8,128)(2,1)S(1)} %project.19), channel_id=1, source_target_pairs={{0,12},{4,0},{8,4},{12,8},{1,13},{5,1},{9,5},{13,9},{2,14},{6,2},{... | collective-permute-start | bytes 1179656 | tf_op jit(solution)/shard_map/ppermute | solution.py:520
  52.6 23.8 %collective-permute-start.7 = (bf16[512,384]{1,0:T(8,128)(2,1)S(1)}, bf16[512,384]{1,0:T(8,128)(2,1)S(1)}, u32[]{:S(2)}, u32[]{:S(2)}) collective-permute-start(bf16[512,384]{1,0:T(8,128)(2,1)S(1)} %project.17), channel_id=1, source_target_pairs={{0,4},{4,8},{8,12},{12,0},{1,5},{5,9},{9,13},{13,1},{2,6},{6,10},{... | collective-permute-start | bytes 1179656 | tf_op jit(solution)/shard_map/ppermute | solution.py:520
  60.9 17.7 %collective-permute-start.16 = (bf16[512,384]{1,0:T(8,128)(2,1)S(1)}, bf16[512,384]{1,0:T(8,128)(2,1)S(1)}, u32[]{:S(2)}, u32[]{:S(2)}) collective-permute-start(bf16[512,384]{1,0:T(8,128)(2,1)S(1)} %project.20), channel_id=1, source_target_pairs={{0,12},{4,0},{8,4},{12,8},{1,13},{5,1},{9,5},{13,9},{2,14},{6,2},{... | collective-permute-start | bytes 1179656 | tf_op jit(solution)/shard_map/ppermute | solution.py:520
  63.0 12.6 %collective-permute-start.18 = (f32[8,128]{1,0:T(8,128)S(1)}, f32[8,128]{1,0:T(8,128)S(1)}, u32[]{:S(2)}, u32[]{:S(2)}) collective-permute-start(f32[8,128]{1,0:T(8,128)S(1)} %pad_maximum_fusion), channel_id=1, source_target_pairs={{0,4},{4,0},{8,12},{12,8},{1,5},{5,1},{9,13},{13,9},{2,6},{6,2},{1... | collective-permute-start | bytes 12296 | tf_op jit(solution)/shard_map/ppermute | solution.py:127
  78.6 14.2 %collective-permute-start.8 = (bf16[512,384]{1,0:T(8,128)(2,1)}, bf16[512,384]{1,0:T(8,128)(2,1)}, u32[]{:S(2)}, u32[]{:S(2)}) collective-permute-start(bf16[512,384]{1,0:T(8,128)(2,1)} %project.18), channel_id=1, source_target_pairs={{0,4},{4,8},{8,12},{12,0},{1,5},{5,9},{9,13},{13,1},{2,6},{6,10},{... | collective-permute-start | bytes 1179656 | tf_op jit(solution)/shard_map/ppermute | solution.py:520
  80.9 18.8 %collective-permute-start.17 = (bf16[512,384]{1,0:T(8,128)(2,1)}, bf16[512,384]{1,0:T(8,128)(2,1)}, u32[]{:S(2)}, u32[]{:S(2)}) collective-permute-start(bf16[512,384]{1,0:T(8,128)(2,1)} %project.21), channel_id=1, source_target_pairs={{0,12},{4,0},{8,4},{12,8},{1,13},{5,1},{9,5},{13,9},{2,14},{6,2},{... | collective-permute-start | bytes 1179656 | tf_op jit(solution)/shard_map/ppermute | solution.py:520
  109.4 13.3 %collective-permute-start.21 = (bf16[512,128]{1,0:T(8,128)(2,1)S(1)}, bf16[512,128]{1,0:T(8,128)(2,1)S(1)}, u32[]{:S(2)}, u32[]{:S(2)}) collective-permute-start(bf16[512,128]{1,0:T(8,128)(2,1)S(1)} %get-tuple-element.45.refs_0_), channel_id=1, source_target_pairs={{0,8},{4,12},{8,0},{12,4},{1,9},{5,13},{9,1},{13,5},{2,10},{6,14},... | collective-permute-start | bytes 393224 | tf_op jit(solution)/shard_map/ppermute | solution.py:227
  110.0 12.8 %collective-permute-start.22 = (bf16[512,128]{1,0:T(8,128)(2,1)S(1)}, bf16[512,128]{1,0:T(8,128)(2,1)S(1)}, u32[]{:S(2)}, u32[]{:S(2)}) collective-permute-start(bf16[512,128]{1,0:T(8,128)(2,1)S(1)} %get-tuple-element.45.refs_0_), channel_id=1, source_target_pairs={{0,12},{4,0},{8,4},{12,8},{1,13},{5,1},{9,5},{13,9},{2,14},{6,2},{... | collective-permute-start | bytes 393224 | tf_op jit(solution)/shard_map/ppermute | solution.py:227
  112.7 12.9 %collective-permute-start.29 = (bf16[512,128]{1,0:T(8,128)(2,1)S(1)}, bf16[512,128]{1,0:T(8,128)(2,1)S(1)}, u32[]{:S(2)}, u32[]{:S(2)}) collective-permute-start(bf16[512,128]{1,0:T(8,128)(2,1)S(1)} %get-tuple-element.48.refs_0_), channel_id=1, source_target_pairs={{0,4},{4,8},{8,12},{12,0},{1,5},{5,9},{9,13},{13,1},{2,6},{6,10},{... | collective-permute-start | bytes 393224 | tf_op jit(solution)/shard_map/ppermute | solution.py:227
  113.3 19.8 %collective-permute-start.30 = (bf16[512,128]{1,0:T(8,128)(2,1)S(1)}, bf16[512,128]{1,0:T(8,128)(2,1)S(1)}, u32[]{:S(2)}, u32[]{:S(2)}) collective-permute-start(bf16[512,128]{1,0:T(8,128)(2,1)S(1)} %get-tuple-element.48.refs_0_), channel_id=1, source_target_pairs={{0,8},{4,12},{8,0},{12,4},{1,9},{5,13},{9,1},{13,5},{2,10},{6,14},... | collective-permute-start | bytes 393224 | tf_op jit(solution)/shard_map/ppermute | solution.py:227
  117.2 15.9 %collective-permute-start.31 = (bf16[512,128]{1,0:T(8,128)(2,1)S(1)}, bf16[512,128]{1,0:T(8,128)(2,1)S(1)}, u32[]{:S(2)}, u32[]{:S(2)}) collective-permute-start(bf16[512,128]{1,0:T(8,128)(2,1)S(1)} %get-tuple-element.48.refs_0_), channel_id=1, source_target_pairs={{0,12},{4,0},{8,4},{12,8},{1,13},{5,1},{9,5},{13,9},{2,14},{6,2},{... | collective-permute-start | bytes 393224 | tf_op jit(solution)/shard_map/ppermute | solution.py:227
  135.3 14.9 %collective-permute-start.24 = (bf16[512,512]{1,0:T(8,128)(2,1)S(1)}, bf16[512,512]{1,0:T(8,128)(2,1)S(1)}, u32[]{:S(2)}, u32[]{:S(2)}) collective-permute-start(bf16[512,512]{1,0:T(8,128)(2,1)S(1)} %pair_up.2.refs_2_), channel_id=1, source_target_pairs={{0,2},{1,3},{2,0},{3,1},{4,6},{5,7},{6,4},{7,5},{8,10},{9,11},{10,... | collective-permute-start | bytes 1572872 | tf_op jit(solution)/shard_map/ppermute | solution.py:127
  137.4 23.6 %collective-permute-start.33 = (bf16[512,512]{1,0:T(8,128)(2,1)S(1)}, bf16[512,512]{1,0:T(8,128)(2,1)S(1)}, u32[]{:S(2)}, u32[]{:S(2)}) collective-permute-start(bf16[512,512]{1,0:T(8,128)(2,1)S(1)} %pair_up.3.refs_2_), channel_id=1, source_target_pairs={{0,2},{1,3},{2,0},{3,1},{4,6},{5,7},{6,4},{7,5},{8,10},{9,11},{10,... | collective-permute-start | bytes 1572872 | tf_op jit(solution)/shard_map/ppermute | solution.py:127
  151.0 13.6 %collective-permute-start.25 = (bf16[512,512]{1,0:T(8,128)(2,1)S(1)}, bf16[512,512]{1,0:T(8,128)(2,1)}, u32[]{:S(2)}, u32[]{:S(2)}) collective-permute-start(bf16[512,512]{1,0:T(8,128)(2,1)S(1)} %renew.2.refs_0_.x_ref), channel_id=1, source_target_pairs={{0,1},{1,0},{2,3},{3,2},{4,5},{5,4},{6,7},{7,6},{8,9},{9,8},{10,11... | collective-permute-start | bytes 1572872 | tf_op jit(solution)/shard_map/ppermute | solution.py:127
  161.7 10.8 %collective-permute-start.34 = (bf16[512,512]{1,0:T(8,128)(2,1)S(1)}, bf16[512,512]{1,0:T(8,128)(2,1)}, u32[]{:S(2)}, u32[]{:S(2)}) collective-permute-start(bf16[512,512]{1,0:T(8,128)(2,1)S(1)} %renew.3.refs_0_.x_ref), channel_id=1, source_target_pairs={{0,1},{1,0},{2,3},{3,2},{4,5},{5,4},{6,7},{7,6},{8,9},{9,8},{10,11... | collective-permute-start | bytes 1572872 | tf_op jit(solution)/shard_map/ppermute | solution.py:127
  169.7 13.9 %collective-permute-start.26 = (bf16[512,384]{1,0:T(8,128)(2,1)S(1)}, bf16[512,384]{1,0:T(8,128)(2,1)S(1)}, u32[]{:S(2)}, u32[]{:S(2)}) collective-permute-start(bf16[512,384]{1,0:T(8,128)(2,1)S(1)} %project.24), channel_id=1, source_target_pairs={{0,4},{4,8},{8,12},{12,0},{1,5},{5,9},{9,13},{13,1},{2,6},{6,10},{... | collective-permute-start | bytes 1179656 | tf_op jit(solution)/shard_map/ppermute | solution.py:520
  174.4 17.6 %collective-permute-start.35 = (bf16[512,384]{1,0:T(8,128)(2,1)S(1)}, bf16[512,384]{1,0:T(8,128)(2,1)S(1)}, u32[]{:S(2)}, u32[]{:S(2)}) collective-permute-start(bf16[512,384]{1,0:T(8,128)(2,1)S(1)} %project.27), channel_id=1, source_target_pairs={{0,12},{4,0},{8,4},{12,8},{1,13},{5,1},{9,5},{13,9},{2,14},{6,2},{... | collective-permute-start | bytes 1179656 | tf_op jit(solution)/shard_map/ppermute | solution.py:520
  185.6 23.6 %collective-permute-start.27 = (bf16[512,384]{1,0:T(8,128)(2,1)S(1)}, bf16[512,384]{1,0:T(8,128)(2,1)S(1)}, u32[]{:S(2)}, u32[]{:S(2)}) collective-permute-start(bf16[512,384]{1,0:T(8,128)(2,1)S(1)} %project.25), channel_id=1, source_target_pairs={{0,4},{4,8},{8,12},{12,0},{1,5},{5,9},{9,13},{13,1},{2,6},{6,10},{... | collective-permute-start | bytes 1179656 | tf_op jit(solution)/shard_map/ppermute | solution.py:520
  194.0 18.3 %collective-permute-start.36 = (bf16[512,384]{1,0:T(8,128)(2,1)S(1)}, bf16[512,384]{1,0:T(8,128)(2,1)S(1)}, u32[]{:S(2)}, u32[]{:S(2)}) collective-permute-start(bf16[512,384]{1,0:T(8,128)(2,1)S(1)} %project.28), channel_id=1, source_target_pairs={{0,12},{4,0},{8,4},{12,8},{1,13},{5,1},{9,5},{13,9},{2,14},{6,2},{... | collective-permute-start | bytes 1179656 | tf_op jit(solution)/shard_map/ppermute | solution.py:520
  196.9 11.6 %collective-permute-start.38 = (f32[8,128]{1,0:T(8,128)S(1)}, f32[8,128]{1,0:T(8,128)S(1)}, u32[]{:S(2)}, u32[]{:S(2)}) collective-permute-start(f32[8,128]{1,0:T(8,128)S(1)} %pad_maximum_fusion.1), channel_id=1, source_target_pairs={{0,4},{4,0},{8,12},{12,8},{1,5},{5,1},{9,13},{13,9},{2,6},{6,2},{1... | collective-permute-start | bytes 12296 | tf_op jit(solution)/shard_map/ppermute | solution.py:127
  211.9 14.2 %collective-permute-start.28 = (bf16[512,384]{1,0:T(8,128)(2,1)}, bf16[512,384]{1,0:T(8,128)(2,1)}, u32[]{:S(2)}, u32[]{:S(2)}) collective-permute-start(bf16[512,384]{1,0:T(8,128)(2,1)} %project.26), channel_id=1, source_target_pairs={{0,4},{4,8},{8,12},{12,0},{1,5},{5,9},{9,13},{13,1},{2,6},{6,10},{... | collective-permute-start | bytes 1179656 | tf_op jit(solution)/shard_map/ppermute | solution.py:520
  215.0 18.0 %collective-permute-start.37 = (bf16[512,384]{1,0:T(8,128)(2,1)}, bf16[512,384]{1,0:T(8,128)(2,1)}, u32[]{:S(2)}, u32[]{:S(2)}) collective-permute-start(bf16[512,384]{1,0:T(8,128)(2,1)} %project.29), channel_id=1, source_target_pairs={{0,12},{4,0},{8,4},{12,8},{1,13},{5,1},{9,5},{13,9},{2,14},{6,2},{... | collective-permute-start | bytes 1179656 | tf_op jit(solution)/shard_map/ppermute | solution.py:520
  244.7 13.3 %collective-permute-start.41 = (bf16[512,128]{1,0:T(8,128)(2,1)S(1)}, bf16[512,128]{1,0:T(8,128)(2,1)S(1)}, u32[]{:S(2)}, u32[]{:S(2)}) collective-permute-start(bf16[512,128]{1,0:T(8,128)(2,1)S(1)} %get-tuple-element.51.refs_0_), channel_id=1, source_target_pairs={{0,8},{4,12},{8,0},{12,4},{1,9},{5,13},{9,1},{13,5},{2,10},{6,14},... | collective-permute-start | bytes 393224 | tf_op jit(solution)/shard_map/ppermute | solution.py:227
  245.4 12.6 %collective-permute-start.42 = (bf16[512,128]{1,0:T(8,128)(2,1)S(1)}, bf16[512,128]{1,0:T(8,128)(2,1)S(1)}, u32[]{:S(2)}, u32[]{:S(2)}) collective-permute-start(bf16[512,128]{1,0:T(8,128)(2,1)S(1)} %get-tuple-element.51.refs_0_), channel_id=1, source_target_pairs={{0,12},{4,0},{8,4},{12,8},{1,13},{5,1},{9,5},{13,9},{2,14},{6,2},{... | collective-permute-start | bytes 393224 | tf_op jit(solution)/shard_map/ppermute | solution.py:227
  247.9 12.9 %collective-permute-start.51 = (bf16[512,128]{1,0:T(8,128)(2,1)S(1)}, bf16[512,128]{1,0:T(8,128)(2,1)S(1)}, u32[]{:S(2)}, u32[]{:S(2)}) collective-permute-start(bf16[512,128]{1,0:T(8,128)(2,1)S(1)} %get-tuple-element.60.refs_0_), channel_id=1, source_target_pairs={{0,4},{4,8},{8,12},{12,0},{1,5},{5,9},{9,13},{13,1},{2,6},{6,10},{... | collective-permute-start | bytes 393224 | tf_op jit(solution)/shard_map/ppermute | solution.py:227
  248.5 19.8 %collective-permute-start.52 = (bf16[512,128]{1,0:T(8,128)(2,1)S(1)}, bf16[512,128]{1,0:T(8,128)(2,1)S(1)}, u32[]{:S(2)}, u32[]{:S(2)}) collective-permute-start(bf16[512,128]{1,0:T(8,128)(2,1)S(1)} %get-tuple-element.60.refs_0_), channel_id=1, source_target_pairs={{0,8},{4,12},{8,0},{12,4},{1,9},{5,13},{9,1},{13,5},{2,10},{6,14},... | collective-permute-start | bytes 393224 | tf_op jit(solution)/shard_map/ppermute | solution.py:227
  252.4 15.9 %collective-permute-start.53 = (bf16[512,128]{1,0:T(8,128)(2,1)S(1)}, bf16[512,128]{1,0:T(8,128)(2,1)S(1)}, u32[]{:S(2)}, u32[]{:S(2)}) collective-permute-start(bf16[512,128]{1,0:T(8,128)(2,1)S(1)} %get-tuple-element.60.refs_0_), channel_id=1, source_target_pairs={{0,12},{4,0},{8,4},{12,8},{1,13},{5,1},{9,5},{13,9},{2,14},{6,2},{... | collective-permute-start | bytes 393224 | tf_op jit(solution)/shard_map/ppermute | solution.py:227
  272.6 13.0 %collective-permute-start.55 = (bf16[512,256]{1,0:T(8,128)(2,1)S(1)}, bf16[512,256]{1,0:T(8,128)(2,1)S(1)}, u32[]{:S(2)}, u32[]{:S(2)}) collective-permute-start(bf16[512,256]{1,0:T(8,128)(2,1)S(1)} %get-tuple-element.64), channel_id=1, source_target_pairs={{0,2},{1,3},{2,0},{3,1},{4,6},{5,7},{6,4},{7,5},{8,10},{9,11},{10,... | collective-permute-start | bytes 786440 | tf_op jit(solution)/shard_map/ppermute | solution.py:127
  (54 other events, 549.2 us)

commit v3 on v2

--- a/solution.py
+++ b/solution.py
@@ -115,7 +115,7 @@
     return residual
 
 
-VMEM_BYTES = 40 * 1024 * 1024
+VMEM_BYTES = 24 * 1024 * 1024
 
 
 def ring(count, shift):
@@ -140,19 +140,27 @@
     return pl.ds(pl.multiple_of(index * size, size), size)
 
 
-def local_kernel(body, place, arrays, outs, name, scratch=(), hbm=(), flops=0):
+def local_kernel(body, place, arrays, outs, name, scratch=(), hbm=(), flops=0, after=()):
     vmem, smem = pl.BlockSpec(memory_space=pltpu.VMEM), pl.BlockSpec(memory_space=pltpu.SMEM)
     moved = sum(a.size * a.dtype.itemsize for a in (*arrays, *outs))
+    inputs = 1 + len(arrays) + len(hbm)
+
+    def ordered(*refs):
+        body(*refs[:inputs], *refs[inputs + len(after) :])
+
     return pl.pallas_call(
-        body,
+        ordered,
         out_shape=list(outs),
-        in_specs=[smem] + [vmem] * len(arrays) + [pl.BlockSpec(memory_space=pl.ANY)] * len(hbm),
+        in_specs=[smem]
+        + [vmem] * len(arrays)
+        + [pl.BlockSpec(memory_space=pltpu.HBM)] * len(hbm)
+        + [pl.BlockSpec(memory_space=pl.ANY)] * len(after),
         out_specs=[vmem] * len(outs),
         scratch_shapes=list(scratch),
         compiler_params=pltpu.CompilerParams(vmem_limit_bytes=VMEM_BYTES),
         cost_estimate=pl.CostEstimate(flops=flops, bytes_accessed=moved, transcendentals=0),
         name=name,
-    )(place, *arrays, *hbm)
+    )(place, *arrays, *(pltpu.with_memory_space_constraint(a, pltpu.HBM) for a in hbm), *after)
 
 
 def shaped(*shape, dtype=jnp.bfloat16):
@@ -175,51 +183,49 @@
 
 def scatter_tokens(tokens, place, sp_count, feats, piece):
     tok_here = tokens.shape[0]
-    rows = tok_here // 2
 
     def body(place_ref, tokens_ref, *rest):
-        out_refs, (buffer, sem) = rest[:-2], rest[-2:]
+        out_refs, sem = rest[:-1], rest[-1]
         slot = place_ref[1] * 2 + place_ref[2]
         copies = []
         for shift in range(sp_count):
             target = lax.rem(place_ref[0] + shift, sp_count)
             column = pl.multiple_of(target * feats + slot * piece, piece)
             copy = pltpu.make_async_copy(
-                tokens_ref.at[:, pl.ds(column, piece)], buffer.at[shift], sem.at[shift]
+                tokens_ref.at[:, pl.ds(column, piece)], out_refs[shift], sem.at[shift]
             )
             copy.start()
             copies.append(copy)
-        for shift in range(sp_count):
-            copies[shift].wait()
-            for part in range(2):
-                out_refs[part * sp_count + shift][...] = buffer[shift, pl.ds(part * rows, rows), :]
-
-    blocks = local_kernel(
+        for copy in copies:
+            copy.wait()
+
+    return local_kernel(
         body,
         place,
         (),
-        [shaped(rows, piece)] * (2 * sp_count),
+        [shaped(tok_here, piece)] * sp_count,
         "scatter_tokens",
-        scratch=[
-            pltpu.VMEM((sp_count, tok_here, piece), jnp.bfloat16),
-            pltpu.SemaphoreType.DMA((sp_count,)),
-        ],
+        scratch=[pltpu.SemaphoreType.DMA((sp_count,))],
         hbm=(tokens,),
     )
-    return blocks[:sp_count], blocks[sp_count:]
-
-
-def stack_blocks(blocks, place):
+
+
+def stack_blocks(blocks, place, parts=1):
     count = len(blocks)
     rows, width = blocks[0].shape
+    rows = rows // parts
 
     def body(place_ref, *refs):
-        out_ref = refs[-1]
-        for shift in range(count):
-            source = lax.rem(place_ref[0] + count - shift, count)
-            out_ref[aligned(source, rows), :] = refs[shift][...]
-
-    return local_kernel(body, place, blocks, [shaped(rows * count, width)], "stack_blocks")[0]
+        for part in range(parts):
+            for shift in range(count):
+                source = lax.rem(place_ref[0] + count - shift, count)
+                refs[count + part][aligned(source, rows), :] = refs[shift][
+                    pl.ds(part * rows, rows), :
+                ]
+
+    return local_kernel(
+        body, place, blocks, [shaped(rows * count, width)] * parts, "stack_blocks"
+    )
 
 
 def over_sp(blocks, count):
@@ -280,15 +286,42 @@
     )[0]
 
 
+def attend_rows(qkv_ref, bias_ref, out_ref, part, sp_count, heads):
+    grid_rows = qkv_ref.shape[0] // GRID_W
+    width = heads * HD
+    part_grid = grid_rows // sp_count // 2
+    for head in range(heads):
+        lanes = head * HD
+        for index in range(sp_count * part_grid):
+            plane, inner = divmod(index, part_grid)
+            row = (2 * plane + part) * part_grid + inner
+            first = min(max(row - KR // 2, 0), grid_rows - KR)
+            offset = first - row + KR - 1
+            queries = qkv_ref[pl.ds(row * GRID_W, GRID_W), pl.ds(lanes, HD)]
+            span = pl.ds(first * GRID_W, KR * GRID_W)
+            keys = qkv_ref[span, pl.ds(width + lanes, HD)]
+            values = qkv_ref[span, pl.ds(2 * width + lanes, HD)]
+            scores = lax.dot_general(
+                queries, keys, (((1,), (1,)), ((), ())), preferred_element_type=jnp.float32
+            )
+            bias_here = bias_ref[head, :, pl.ds(offset * GRID_W, KR * GRID_W)]
+            scores = scores * HD ** (-0.5) + bias_here
+            powers = jnp.exp(scores - jnp.max(scores, axis=-1, keepdims=True))
+            weights = powers * (1.0 / jnp.sum(powers, axis=-1, keepdims=True))
+            mixed = jnp.dot(
+                weights.astype(jnp.bfloat16), values, preferred_element_type=jnp.float32
+            )
+            out_ref[pl.ds(index * GRID_W, GRID_W), pl.ds(lanes, HD)] = mixed.astype(jnp.bfloat16)
+
+
 def attend(arrived, own, norms, bias, place, sp_count):
     rows, total_width = arrived[0].shape
     heads = bias.shape[0]
     width = heads * HD
     part_rows = rows // sp_count
-    grid_rows = 2 * rows // GRID_W
-    part_grid = part_rows // GRID_W
-
-    def body(place_ref, a0, a1, o0, o1, n0, n1, bias_ref, out0, out1, qkv_ref):
+    flops = 4 * heads * rows * KR * GRID_W * HD
+
+    def low(place_ref, a0, a1, o0, o1, n0, n1, bias_ref, out_ref, qkv_ref):
         for part, (a_ref, o_ref, n_ref) in enumerate(((a0, o0, n0), (a1, o1, n1))):
             for plane in range(sp_count):
                 span = pl.ds(plane * part_rows, part_rows)
@@ -296,42 +329,24 @@
                 qkv_ref[pl.ds((2 * plane + part) * part_rows, part_rows), :] = (
                     total * n_ref[span, :]
                 ).astype(jnp.bfloat16)
-        for head in range(heads):
-            lanes = head * HD
-            for row in range(grid_rows):
-                first = min(max(row - KR // 2, 0), grid_rows - KR)
-                offset = first - row + KR - 1
-                queries = qkv_ref[pl.ds(row * GRID_W, GRID_W), pl.ds(lanes, HD)]
-                span = pl.ds(first * GRID_W, KR * GRID_W)
-                keys = qkv_ref[span, pl.ds(width + lanes, HD)]
-                values = qkv_ref[span, pl.ds(2 * width + lanes, HD)]
-                scores = lax.dot_general(
-                    queries, keys, (((1,), (1,)), ((), ())), preferred_element_type=jnp.float32
-                )
-                bias_here = bias_ref[head, :, pl.ds(offset * GRID_W, KR * GRID_W)]
-                scores = scores * HD ** (-0.5) + bias_here
-                powers = jnp.exp(scores - jnp.max(scores, axis=-1, keepdims=True))
-                weights = powers / jnp.sum(powers, axis=-1, keepdims=True)
-                mixed = jnp.dot(
-                    weights.astype(jnp.bfloat16), values, preferred_element_type=jnp.float32
-                )
-                block, inner = divmod(row, part_grid)
-                out_ref = (out0, out1)[block % 2]
-                at = (block // 2) * part_rows + inner * GRID_W
-                out_ref[pl.ds(at, GRID_W), pl.ds(lanes, HD)] = mixed.astype(jnp.bfloat16)
-
-    return local_kernel(
-        body,
+        attend_rows(qkv_ref, bias_ref, out_ref, 0, sp_count, heads)
+
+    def high(place_ref, qkv_ref, bias_ref, out_ref):
+        attend_rows(qkv_ref, bias_ref, out_ref, 1, sp_count, heads)
+
+    out0, qkv = local_kernel(
+        low,
         place,
         (*arrived, *own, *norms, bias),
-        [shaped(rows, width)] * 2,
-        "attend",
-        scratch=[pltpu.VMEM((2 * rows, total_width), jnp.bfloat16)],
-        flops=8 * heads * rows * KR * GRID_W * HD,
-    )
-
-
-def spread(attended, w_out, layer, place):
+        [shaped(rows, width), shaped(2 * rows, total_width)],
+        "attend_low",
+        flops=flops,
+    )
+    out1 = local_kernel(high, place, (qkv, bias), [shaped(rows, width)], "attend_high", flops=flops)
+    return out0, out1[0]
+
+
+def spread(attended, w_out, layer, place, after):
     count = len(attended)
     rows, width = attended[0].shape
     inner, feats = w_out.shape[1:]
@@ -364,6 +379,7 @@
         ],
         hbm=(w_out,),
         flops=2 * rows * inner * feats,
+        after=after,
     )
 
 
@@ -378,7 +394,7 @@
     def body(place_ref, kept_ref, came_ref, out_ref):
         out_ref[...] = total_of(kept_ref, came_ref).astype(jnp.bfloat16)
 
-    return local_kernel(body, place, (kept, came), [shaped(*kept.shape)], "pair_up")[0]
+    return local_kernel(body, place, (kept, came), [shaped(*kept.shape)], "pair_up")
 
 
 def pair_apart(kept, came, place):
@@ -396,7 +412,7 @@
     return local_kernel(body, place, (kept, came), [shaped(rows, piece)] * 2, "pair_apart")
 
 
-def renew(residual, pair, came, place):
+def renew(residual, pair, came, place, after):
     count = len(residual)
 
     def body(place_ref, *refs):
@@ -411,7 +427,9 @@
             branch = pair_ref[:, span].astype(jnp.float32) + came_ref[:, span].astype(jnp.float32)
             out_ref[:, span] = (ref[...].astype(jnp.float32) + branch).astype(jnp.bfloat16)
 
-    return local_kernel(body, place, (*residual, pair, came), [shaped(*pair.shape)], "renew")[0]
+    return local_kernel(
+        body, place, (*residual, pair, came), [shaped(*pair.shape)], "renew", after=after
+    )[0]
 
 
 def finish(residual, stay, came, place, sp_count):
@@ -437,6 +455,9 @@
     lambda core, far: (1 - core) * 2 + far,
     lambda core, far: (1 - core) * 2 + 1 - far,
 )
+
+
+HALF_SLOTS = (lambda core, far: core, lambda core, far: 1 - core)
 
 
 def assemble(parts, place, sp_count):
@@ -476,67 +497,75 @@
     every_feat = feats * sp_count
     weights = (w_query, w_key, w_value)
     tables = lax.dynamic_slice_in_dim(offset_bias, sp_index * heads, heads, 1)
+    biases = window_bias(tables.reshape(LAYERS * heads, *tables.shape[2:]))
     gain = lax.dynamic_slice_in_dim(norm_gain, sp_index * feats, feats, 1)[:, None, :]
-
-    halves = []
-    for blocks in scatter_tokens(tokens, place, sp_count, feats, piece):
-        halves.append(exchanged(stack_blocks(over_sp(blocks, sp_count), place)))
-    slots = SLOTS
     shifts = (1, -1)
+    halves = [None, None]
+    travelling = [None, None]
+
+    def shared(part, step, layer, arrived=None):
+        slots = SLOTS if layer == 0 else HALF_SLOTS
+        final = step == sp_count - 1
+        chunk = (-shifts[part] * (step + 1)) % sp_count
+        return project(
+            halves[part], slots, gain, weights, layer, place, chunk, width, arrived, final
+        )
+
+    def sent_on(made, part):
+        return lax.ppermute(made, "sp", ring(sp_count, shifts[part]))
+
+    blocks = over_sp(scatter_tokens(tokens, place, sp_count, feats, piece), sp_count)
+    held = stack_blocks(blocks, place, 2)
+    far = [swapped(h, "tp", 2) for h in held]
+    near = [swapped(h, "tp", 1) for h in held]
+    halves[0] = [held[0], far[0], near[0], swapped(far[0], "tp", 1)]
+    made = [shared(0, 0, 0), None]
+    far[1] = lax.optimization_barrier((far[1], made[0]))[0]
+    halves[1] = [held[1], far[1], near[1], swapped(far[1], "tp", 1)]
+    made[1] = shared(1, 0, 0)
 
     for layer in range(LAYERS):
+        summed = lax.optimization_barrier((halves, made))[0]
+        travelling = [sent_on(made[part], part) for part in range(2)]
         squares = jnp.concatenate(
             [
                 sum(jnp.sum(jnp.square(p.astype(jnp.float32)), axis=-1) for p in pieces)
-                for pieces in halves
+                for pieces in summed
             ]
         )
         squares = summed_over(squares.reshape(-1, HD), "sp").reshape(2, -1, 1)
         norms = lax.rsqrt(squares / every_feat + norm_eps)
-        bias = window_bias(tables[layer])
-
-        arrived, own = [], []
-        travelling = [None, None]
-        for step in range(sp_count):
+        for step in range(1, sp_count - 1):
             for part in range(2):
-                chunk_shift = (-shifts[part] * (step + 1)) % sp_count
-                final = step == sp_count - 1
-                made = project(
-                    halves[part],
-                    slots,
-                    gain,
-                    weights,
-                    layer,
-                    place,
-                    chunk_shift,
-                    width,
-                    None if final else travelling[part],
-                    final,
-                )
-                if final:
-                    arrived.append(travelling[part])
-                    own.append(made)
-                else:
-                    travelling[part] = lax.ppermute(made, "sp", ring(sp_count, shifts[part]))
-        attended = attend(arrived, own, (norms[0], norms[1]), bias, place, sp_count)
+                travelling[part] = sent_on(shared(part, step, layer, travelling[part]), part)
+        own = [shared(part, sp_count - 1, layer) for part in range(2)]
+        bias = biases[layer * heads : (layer + 1) * heads]
+        attended = attend(travelling, own, (norms[0], norms[1]), bias, place, sp_count)
 
         residuals = [pieces[:2] if layer == 0 else pieces[:1] for pieces in halves]
-        halves = []
+        pairs, after = [], (attended[1],)
         for part in range(2):
             gathered = over_sp([attended[part]] * sp_count, sp_count)
-            sent, kept = spread(gathered, w_out, layer, place)
+            sent, kept = spread(gathered, w_out, layer, place, after)
             came = swapped(sent, "tp", 1)
+            pair = (pair_up if layer < LAYERS - 1 else pair_apart)(kept, came, place)
+            pairs.append(pair)
+            after = (pair[0],)
+        after = ()
+        for part in range(2):
             if layer < LAYERS - 1:
-                pair = pair_up(kept, came, place)
-                mine = renew(residuals[part], pair, swapped(pair, "tp", 2), place)
-                halves.append([mine, swapped(mine, "tp", 1)])
+                pair = pairs[part][0]
+                mine = renew(residuals[part], pair, swapped(pair, "tp", 2), place, after)
+                halves[part] = [mine, swapped(mine, "tp", 1)]
+                made[part] = shared(part, 0, layer + 1)
+                after = (made[part],)
             else:
-                sent, stay = pair_apart(kept, came, place)
+                sent, stay = pairs[part]
                 blocks = finish(
                     residuals[part][0], stay, swapped(sent, "tp", 2), place, sp_count
                 )
-                halves.append(exchanged(stack_blocks(over_sp(blocks, sp_count), place)))
-        slots = (lambda core, far: core, lambda core, far: 1 - core)
+                stacked = stack_blocks(over_sp(blocks, sp_count), place)[0]
+                halves[part] = exchanged(stacked)
     return assemble(halves, place, sp_count)
 
 

time: 309 us -> 308 us (level)
  Pallas kernels: 60.7 us -> 78.7 us
  local copies, waits for them, and re-layouts: 20.3 us -> 8.45 us
    pallas_call x36 -> x37, Pallas kernels: 60.7 us -> 78.7 us  [local_kernel(): pl.pallas_call(ordered, out_shape=list(outs), in_specs=[smem] + [vmem] *...]
    ppermute x26, waiting for transfers between devices: 62.5 us -> 48.4 us  [swapped(): return lax.ppermute(array, axis, [(i, i ^ distance) for i in range(count)])]
    unnamed x48 -> x14, local copies, waits for them, and re-layouts: 14.4 us -> 4.91 us
    ppermute x12, waiting for transfers between devices: 53.1 us -> 59.5 us  [sent_on(): return lax.ppermute(made, 'sp', ring(sp_count, shifts[part]))]
    ppermute x24 -> x21, waiting for transfers between devices: 37.1 us -> 41.8 us  [over_sp(): lax.ppermute(blocks[shift], 'sp', ring(count, shift))]
    ppermute x26, starting transfers between devices: 12.8 us -> 16.3 us  [swapped(): return lax.ppermute(array, axis, [(i, i ^ distance) for i in range(count)])]
    ppermute x24 -> x21, starting transfers between devices: 32.1 us -> 28.8 us  [over_sp(): lax.ppermute(blocks[shift], 'sp', ring(count, shift))]
  transfers between devices with their start and end apart: 62 -> 59, of which waited for: 30 -> 28; matrix products, arithmetic and copies ran while one was open for 4% -> 2% of each run, Pallas kernels for 14% -> 19%
where the time goes in v3:
time: 308 us; the launch traced here: 307 us
  waiting for transfers between devices  150 us (49%)
  Pallas kernels  78.7 us (26%)
  starting transfers between devices  66.7 us (22%)
  local copies, waits for them, and re-layouts  8.45 us (3%)
    pallas_call x37, Pallas kernels, local_kernel(): pl.pallas_call(ordered, out_shape=list(outs), in_specs=[smem] + [vmem] *...  78.7 us
    ppermute x12, waiting for transfers between devices, sent_on(): return lax.ppermute(made, 'sp', ring(sp_count, shifts[part]))  59.5 us
    ppermute x26, waiting for transfers between devices, swapped(): return lax.ppermute(array, axis, [(i, i ^ distance) for i in range(count)])  48.4 us
    ppermute x21, waiting for transfers between devices, over_sp(): lax.ppermute(blocks[shift], 'sp', ring(count, shift))  41.8 us
    ppermute x21, starting transfers between devices, over_sp(): lax.ppermute(blocks[shift], 'sp', ring(count, shift))  28.8 us
    ppermute x12, starting transfers between devices, sent_on(): return lax.ppermute(made, 'sp', ring(sp_count, shifts[part]))  21.6 us
    ppermute x26, starting transfers between devices, swapped(): return lax.ppermute(array, axis, [(i, i ^ distance) for i in range(count)])  16.3 us
  transfers between devices with their start and end apart: 59, of which 28 were waited for; matrix products, arithmetic and copies ran while one was open for 2% of the time, Pallas kernels for 19%

profile of v3, /device:TPU:0, one launch (start us, length us, event | category | flops | bytes accessed | tf_op | source)
XLA Modules:
  0.0 306.5 jit_solution(13050671650414851524)
XLA Ops:
  11.3 4.8 %collective-permute-done.1.refs_3_ = bf16[256,256]{1,0:T(8,128)(2,1)S(1)} collective-permute-done((bf16[256,256]{1,0:T(8,128)(2,1)S(1)}, bf16[256,256]{1,0:T(8,128)(2,1)S(1)}, u32[]{:S(2)}, u32[]{:S(2)}) %collective-permute-start.1) | collective-permute-done | bytes 131104 | tf_op jit(solution)/shard_map/ppermute | solution.py:233
  18.4 6.5 %collective-permute-done.3.refs_2_ = bf16[512,256]{1,0:T(8,128)(2,1)S(1)} collective-permute-done((bf16[512,256]{1,0:T(8,128)(2,1)S(1)}, bf16[512,256]{1,0:T(8,128)(2,1)S(1)}, u32[]{:S(2)}, u32[]{:S(2)}) %collective-permute-start.3) | collective-permute-done | bytes 262176 | tf_op jit(solution)/shard_map/ppermute | solution.py:127
  28.1 3.2 %project.16 = bf16[512,384]{1,0:T(8,128)(2,1)} custom-call(s32[3]{0:T(128)S(1)} %pad_add_fusion.refs_0_, bf16[512,256]{1,0:T(8,128)(2,1)S(1)} %get-tuple-element.55.refs_1_, bf16[512,256]{1,0:T(8,128)(2,1)S(1)} %collective-permute-done.3.refs_2_, bf16[512,256]{1,0:T(8,128)(2,1)S(1)} %collective-permute-done.4.refs_3_, ...), custom_call_target="tpu_custom_call" | custom-call | flops 402653184 | bytes 1445888 | tf_op jit(solution)/shard_map/project/pallas_call | solution.py:151
  35.5 3.4 %collective-permute-start.6 = (bf16[512,384]{1,0:T(8,128)(2,1)}, bf16[512,384]{1,0:T(8,128)(2,1)S(1)}, u32[]{:S(2)}, u32[]{:S(2)}) collective-permute-start(bf16[512,384]{1,0:T(8,128)(2,1)} %project.16), channel_id=1, source_target_pairs={{0,4},{4,8},{8,12},{12,0},{1,5},{5,9},{9,13},{13,1},{2,6},{6,10},{... | collective-permute-start | bytes 1179656 | tf_op jit(solution)/shard_map/ppermute | solution.py:515
  45.2 4.4 %collective-permute-done.6.refs_6_ = bf16[512,384]{1,0:T(8,128)(2,1)S(1)} collective-permute-done((bf16[512,384]{1,0:T(8,128)(2,1)}, bf16[512,384]{1,0:T(8,128)(2,1)S(1)}, u32[]{:S(2)}, u32[]{:S(2)}) %collective-permute-start.6) | collective-permute-done | bytes 393248 | tf_op jit(solution)/shard_map/ppermute | solution.py:515
  53.5 4.4 %collective-permute-done.12.refs_6_ = bf16[512,384]{1,0:T(8,128)(2,1)S(1)} collective-permute-done((bf16[512,384]{1,0:T(8,128)(2,1)S(1)}, bf16[512,384]{1,0:T(8,128)(2,1)S(1)}, u32[]{:S(2)}, u32[]{:S(2)}) %collective-permute-start.12) | collective-permute-done | bytes 393248 | tf_op jit(solution)/shard_map/ppermute | solution.py:515
  60.3 3.5 %collective-permute-start.13 = (bf16[512,384]{1,0:T(8,128)(2,1)S(1)}, bf16[512,384]{1,0:T(8,128)(2,1)S(1)}, u32[]{:S(2)}, u32[]{:S(2)}) collective-permute-start(bf16[512,384]{1,0:T(8,128)(2,1)S(1)} %project.20), channel_id=1, source_target_pairs={{0,12},{4,0},{8,4},{12,8},{1,13},{5,1},{9,5},{13,9},{2,14},{6,2},{... | collective-permute-start | bytes 1179656 | tf_op jit(solution)/shard_map/ppermute | solution.py:515
  67.1 7.3 %collective-permute-done.15 = f32[8,128]{1,0:T(8,128)S(1)} collective-permute-done((f32[8,128]{1,0:T(8,128)S(1)}, f32[8,128]{1,0:T(8,128)S(1)}, u32[]{:S(2)}, u32[]{:S(2)}) %collective-permute-start.15) | collective-permute-done | bytes 4128 | tf_op jit(solution)/shard_map/ppermute | solution.py:127
  75.1 3.2 %project.18 = bf16[512,384]{1,0:T(8,128)(2,1)} custom-call(s32[3]{0:T(128)S(1)} %pad_add_fusion.refs_0_, bf16[512,256]{1,0:T(8,128)(2,1)S(1)} %get-tuple-element.55.refs_1_, bf16[512,256]{1,0:T(8,128)(2,1)S(1)} %collective-permute-done.3.refs_2_, bf16[512,256]{1,0:T(8,128)(2,1)S(1)} %collective-permute-done.4.refs_3_, ...), custom_call_target="tpu_custom_call" | custom-call | flops 402653184 | bytes 1839104 | tf_op jit(solution)/shard_map/project/pallas_call | solution.py:151
  79.4 3.2 %project.21 = bf16[512,384]{1,0:T(8,128)(2,1)} custom-call(s32[3]{0:T(128)S(1)} %pad_add_fusion.refs_0_, bf16[512,256]{1,0:T(8,128)(2,1)S(1)} %get-tuple-element.59.refs_1_, bf16[512,256]{1,0:T(8,128)(2,1)S(1)} %collective-permute-done.9.refs_2_, bf16[512,256]{1,0:T(8,128)(2,1)S(1)} %collective-permute-done.10.refs_3_, ...), custom_call_target="tpu_custom_call" | custom-call | flops 402653184 | bytes 1839104 | tf_op jit(solution)/shard_map/project/pallas_call | solution.py:151
  85.8 6.7 %collective-permute-done.8.refs_1_ = bf16[512,384]{1,0:T(8,128)(2,1)} collective-permute-done((bf16[512,384]{1,0:T(8,128)(2,1)}, bf16[512,384]{1,0:T(8,128)(2,1)}, u32[]{:S(2)}, u32[]{:S(2)}) %collective-permute-start.8) | collective-permute-done | bytes 393248 | tf_op jit(solution)/shard_map/ppermute | solution.py:515
  92.5 6.7 %collective-permute-done.14.refs_2_ = bf16[512,384]{1,0:T(8,128)(2,1)S(1)} collective-permute-done((bf16[512,384]{1,0:T(8,128)(2,1)}, bf16[512,384]{1,0:T(8,128)(2,1)S(1)}, u32[]{:S(2)}, u32[]{:S(2)}) %collective-permute-start.14) | collective-permute-done | bytes 393248 | tf_op jit(solution)/shard_map/ppermute | solution.py:515
  100.4 4.0 %attend_low.2 = (bf16[512,128]{1,0:T(8,128)(2,1)S(1)}, bf16[1024,384]{1,0:T(8,128)(2,1)S(1)}) custom-call(s32[3]{0:T(128)S(1)} %pad_add_fusion.refs_0_, bf16[512,384]{1,0:T(8,128)(2,1)} %collective-permute-done.8.refs_1_, bf16[512,384]{1,0:T(8,128)(2,1)S(1)} %collective-permute-done.14.refs_2_, f32[512,384]{1,0:T(8,128)S(1)} %project.22.refs_3_, ...), custom_call_target="tpu_custom_call" | custom-call | flops 134217728 | bytes 3526656 | tf_op jit(solution)/shard_map/attend_low/pallas_call | solution.py:151
  107.4 3.3 %attend_high.2.refs_6_.refs_1_ = bf16[512,128]{1,0:T(8,128)(2,1)S(1)} custom-call(s32[3]{0:T(128)S(1)} %pad_add_fusion.refs_0_, bf16[1024,384]{1,0:T(8,128)(2,1)S(1)} %get-tuple-element.64.refs_1_, f32[1,64,960]{2,1,0:T(8,128)S(1)} %slice.31.refs_7_.refs_2_), custom_call_target="tpu_custom_call" | custom-call | flops 134217728 | bytes 1163264 | tf_op jit(solution)/shard_map/attend_high/pallas_call | solution.py:151
  110.8 7.5 %collective-permute-done.18.refs_3_ = bf16[512,128]{1,0:T(8,128)(2,1)S(1)} collective-permute-done((bf16[512,128]{1,0:T(8,128)(2,1)S(1)}, bf16[512,128]{1,0:T(8,128)(2,1)S(1)}, u32[]{:S(2)}, u32[]{:S(2)}) %collective-permute-start.18) | collective-permute-done | bytes 131104 | tf_op jit(solution)/shard_map/ppermute | solution.py:233
  128.0 6.8 %collective-permute-done.27.refs_3_ = bf16[512,128]{1,0:T(8,128)(2,1)S(1)} collective-permute-done((bf16[512,128]{1,0:T(8,128)(2,1)S(1)}, bf16[512,128]{1,0:T(8,128)(2,1)S(1)}, u32[]{:S(2)}, u32[]{:S(2)}) %collective-permute-start.27) | collective-permute-done | bytes 131104 | tf_op jit(solution)/shard_map/ppermute | solution.py:233
  141.5 3.2 %project.24.refs_5_ = bf16[512,384]{1,0:T(8,128)(2,1)} custom-call(s32[3]{0:T(128)S(1)} %pad_add_fusion.refs_0_, bf16[512,512]{1,0:T(8,128)(2,1)S(1)} %renew.2.refs_1_, bf16[512,512]{1,0:T(8,128)(2,1)S(1)} %collective-permute-done.22.refs_2_, bf16[2,1,1024]{2,1,0:T(2,128)(2,1)S(1)} %copy.10.refs_5_.refs_3_, bf16[2,1024,512]{2,1,0:T(8,128)(2,1)} %refs_4_.7, ...), custom_call_target="tpu_custom_call" | custom-call | flops 402653184 | bytes 1445888 | tf_op jit(solution)/shard_map/project/pallas_call | solution.py:151
  144.6 9.7 %collective-permute-done.30.refs_4_ = bf16[512,512]{1,0:T(8,128)(2,1)S(1)} collective-permute-done((bf16[512,512]{1,0:T(8,128)(2,1)S(1)}, bf16[512,512]{1,0:T(8,128)(2,1)S(1)}, u32[]{:S(2)}, u32[]{:S(2)}) %collective-permute-start.30) | collective-permute-done | bytes 524320 | tf_op jit(solution)/shard_map/ppermute | solution.py:127
  159.3 9.5 %collective-permute-done.23.refs_4_ = bf16[512,384]{1,0:T(8,128)(2,1)} collective-permute-done((bf16[512,384]{1,0:T(8,128)(2,1)}, bf16[512,384]{1,0:T(8,128)(2,1)}, u32[]{:S(2)}, u32[]{:S(2)}) %collective-permute-start.23) | collective-permute-done | bytes 393248 | tf_op jit(solution)/shard_map/ppermute | solution.py:515
  174.2 3.9 %collective-permute-start.32 = (bf16[512,384]{1,0:T(8,128)(2,1)S(1)}, bf16[512,384]{1,0:T(8,128)(2,1)S(1)}, u32[]{:S(2)}, u32[]{:S(2)}) collective-permute-start(bf16[512,384]{1,0:T(8,128)(2,1)S(1)} %project.27), channel_id=1, source_target_pairs={{0,12},{4,0},{8,4},{12,8},{1,13},{5,1},{9,5},{13,9},{2,14},{6,2},{... | collective-permute-start | bytes 1179656 | tf_op jit(solution)/shard_map/ppermute | solution.py:515
  178.7 13.8 %collective-permute-done.32.refs_4_ = bf16[512,384]{1,0:T(8,128)(2,1)S(1)} collective-permute-done((bf16[512,384]{1,0:T(8,128)(2,1)S(1)}, bf16[512,384]{1,0:T(8,128)(2,1)S(1)}, u32[]{:S(2)}, u32[]{:S(2)}) %collective-permute-start.32) | collective-permute-done | bytes 393248 | tf_op jit(solution)/shard_map/ppermute | solution.py:515
  199.5 6.7 %collective-permute-done.35 = f32[8,128]{1,0:T(8,128)S(1)} collective-permute-done((f32[8,128]{1,0:T(8,128)S(1)}, f32[8,128]{1,0:T(8,128)S(1)}, u32[]{:S(2)}, u32[]{:S(2)}) %collective-permute-start.35) | collective-permute-done | bytes 4128 | tf_op jit(solution)/shard_map/ppermute | solution.py:127
  206.3 3.2 %project.26 = bf16[512,384]{1,0:T(8,128)(2,1)} custom-call(s32[3]{0:T(128)S(1)} %pad_add_fusion.refs_0_, bf16[512,512]{1,0:T(8,128)(2,1)S(1)} %renew.2.refs_1_, bf16[512,512]{1,0:T(8,128)(2,1)S(1)} %collective-permute-done.22.refs_2_, bf16[2,1,1024]{2,1,0:T(2,128)(2,1)S(1)} %copy.10.refs_5_.refs_3_, bf16[512,384]{1,0:T(8,128)(2,1)S(1)} %collective-permute-done.24.refs_4_, ...), custom_call_target="tpu_custom_call" | custom-call | flops 402653184 | bytes 1839104 | tf_op jit(solution)/shard_map/project/pallas_call | solution.py:151
  212.2 3.6 %collective-permute-start.34 = (bf16[512,384]{1,0:T(8,128)(2,1)S(1)}, bf16[512,384]{1,0:T(8,128)(2,1)S(1)}, u32[]{:S(2)}, u32[]{:S(2)}) collective-permute-start(bf16[512,384]{1,0:T(8,128)(2,1)S(1)} %project.29), channel_id=1, source_target_pairs={{0,12},{4,0},{8,4},{12,8},{1,13},{5,1},{9,5},{13,9},{2,14},{6,2},{... | collective-permute-start | bytes 1179656 | tf_op jit(solution)/shard_map/ppermute | solution.py:515
  216.2 7.5 %collective-permute-done.25.refs_1_ = bf16[512,384]{1,0:T(8,128)(2,1)} collective-permute-done((bf16[512,384]{1,0:T(8,128)(2,1)}, bf16[512,384]{1,0:T(8,128)(2,1)}, u32[]{:S(2)}, u32[]{:S(2)}) %collective-permute-start.25) | collective-permute-done | bytes 393248 | tf_op jit(solution)/shard_map/ppermute | solution.py:515
  223.7 6.5 %collective-permute-done.34.refs_2_ = bf16[512,384]{1,0:T(8,128)(2,1)S(1)} collective-permute-done((bf16[512,384]{1,0:T(8,128)(2,1)S(1)}, bf16[512,384]{1,0:T(8,128)(2,1)S(1)}, u32[]{:S(2)}, u32[]{:S(2)}) %collective-permute-start.34) | collective-permute-done | bytes 393248 | tf_op jit(solution)/shard_map/ppermute | solution.py:515
  233.0 4.0 %attend_low.3 = (bf16[512,128]{1,0:T(8,128)(2,1)S(1)}, bf16[1024,384]{1,0:T(8,128)(2,1)S(1)}) custom-call(s32[3]{0:T(128)S(1)} %pad_add_fusion.refs_0_, bf16[512,384]{1,0:T(8,128)(2,1)} %collective-permute-done.25.refs_1_, bf16[512,384]{1,0:T(8,128)(2,1)S(1)} %copy-done.6, f32[512,384]{1,0:T(8,128)S(1)} %project.30.refs_3_, f32[512,384]{1,0:T(8,128)S(1)} %copy-done.4, ...), custom_call_target="tpu_custom_call" | custom-call | flops 134217728 | bytes 3526656 | tf_op jit(solution)/shard_map/attend_low/pallas_call | solution.py:151
  240.1 3.3 %attend_high.3.refs_6_.refs_1_ = bf16[512,128]{1,0:T(8,128)(2,1)S(1)} custom-call(s32[3]{0:T(128)S(1)} %pad_add_fusion.refs_0_, bf16[1024,384]{1,0:T(8,128)(2,1)S(1)} %get-tuple-element.74.refs_1_, f32[1,64,960]{2,1,0:T(8,128)S(1)} %slice.35.refs_7_.refs_2_), custom_call_target="tpu_custom_call" | custom-call | flops 134217728 | bytes 1163264 | tf_op jit(solution)/shard_map/attend_high/pallas_call | solution.py:151
  243.4 7.5 %collective-permute-done.38.refs_3_ = bf16[512,128]{1,0:T(8,128)(2,1)S(1)} collective-permute-done((bf16[512,128]{1,0:T(8,128)(2,1)S(1)}, bf16[512,128]{1,0:T(8,128)(2,1)S(1)}, u32[]{:S(2)}, u32[]{:S(2)}) %collective-permute-start.38) | collective-permute-done | bytes 131104 | tf_op jit(solution)/shard_map/ppermute | solution.py:233
  260.6 6.7 %collective-permute-done.49.refs_3_ = bf16[512,128]{1,0:T(8,128)(2,1)S(1)} collective-permute-done((bf16[512,128]{1,0:T(8,128)(2,1)S(1)}, bf16[512,128]{1,0:T(8,128)(2,1)S(1)}, u32[]{:S(2)}, u32[]{:S(2)}) %collective-permute-start.49) | collective-permute-done | bytes 131104 | tf_op jit(solution)/shard_map/ppermute | solution.py:233
  274.1 5.1 %collective-permute-done.41.refs_3_ = bf16[512,256]{1,0:T(8,128)(2,1)S(1)} collective-permute-done((bf16[512,256]{1,0:T(8,128)(2,1)S(1)}, bf16[512,256]{1,0:T(8,128)(2,1)S(1)}, u32[]{:S(2)}, u32[]{:S(2)}) %collective-permute-start.41) | collective-permute-done | bytes 262176 | tf_op jit(solution)/shard_map/ppermute | solution.py:127
  295.3 4.2 %collective-permute-done.45.refs_2_ = bf16[512,256]{1,0:T(8,128)(2,1)S(1)} collective-permute-done((bf16[512,256]{1,0:T(8,128)(2,1)S(1)}, bf16[512,256]{1,0:T(8,128)(2,1)S(1)}, u32[]{:S(2)}, u32[]{:S(2)}) %collective-permute-start.45) | collective-permute-done | bytes 262176 | tf_op jit(solution)/shard_map/ppermute | solution.py:127
  (173 shorter events, 128.8 us)
Async XLA Ops:
  4.9 11.2 %collective-permute-start.1 = (bf16[256,256]{1,0:T(8,128)(2,1)S(1)}, bf16[256,256]{1,0:T(8,128)(2,1)S(1)}, u32[]{:S(2)}, u32[]{:S(2)}) collective-permute-start(bf16[256,256]{1,0:T(8,128)(2,1)S(1)} %get-tuple-element.50), channel_id=1, source_target_pairs={{0,8},{4,12},{8,0},{12,4},{1,9},{5,13},{9,1},{13,5},{2,10},{6,14},... | collective-permute-start | bytes 393224 | tf_op jit(solution)/shard_map/ppermute | solution.py:233
  18.4 9.7 %collective-permute-start.4 = (bf16[512,256]{1,0:T(8,128)(2,1)S(1)}, bf16[512,256]{1,0:T(8,128)(2,1)S(1)}, u32[]{:S(2)}, u32[]{:S(2)}) collective-permute-start(bf16[512,256]{1,0:T(8,128)(2,1)S(1)} %get-tuple-element.55.refs_1_), channel_id=1, source_target_pairs={{0,1},{1,0},{2,3},{3,2},{4,5},{5,4},{6,7},{7,6},{8,9},{9,8},{10,11... | collective-permute-start | bytes 786440 | tf_op jit(solution)/shard_map/ppermute | solution.py:127
  27.8 13.5 %collective-permute-start.10 = (bf16[512,256]{1,0:T(8,128)(2,1)S(1)}, bf16[512,256]{1,0:T(8,128)(2,1)S(1)}, u32[]{:S(2)}, u32[]{:S(2)}) collective-permute-start(bf16[512,256]{1,0:T(8,128)(2,1)S(1)} %get-tuple-element.59.refs_1_), channel_id=1, source_target_pairs={{0,1},{1,0},{2,3},{3,2},{4,5},{5,4},{6,7},{7,6},{8,9},{9,8},{10,11... | collective-permute-start | bytes 786440 | tf_op jit(solution)/shard_map/ppermute | solution.py:127
  35.5 14.1 %collective-permute-start.6 = (bf16[512,384]{1,0:T(8,128)(2,1)}, bf16[512,384]{1,0:T(8,128)(2,1)S(1)}, u32[]{:S(2)}, u32[]{:S(2)}) collective-permute-start(bf16[512,384]{1,0:T(8,128)(2,1)} %project.16), channel_id=1, source_target_pairs={{0,4},{4,8},{8,12},{12,0},{1,5},{5,9},{9,13},{13,1},{2,6},{6,10},{... | collective-permute-start | bytes 1179656 | tf_op jit(solution)/shard_map/ppermute | solution.py:515
  43.8 14.2 %collective-permute-start.12 = (bf16[512,384]{1,0:T(8,128)(2,1)S(1)}, bf16[512,384]{1,0:T(8,128)(2,1)S(1)}, u32[]{:S(2)}, u32[]{:S(2)}) collective-permute-start(bf16[512,384]{1,0:T(8,128)(2,1)S(1)} %project.19), channel_id=1, source_target_pairs={{0,12},{4,0},{8,4},{12,8},{1,13},{5,1},{9,5},{13,9},{2,14},{6,2},{... | collective-permute-start | bytes 1179656 | tf_op jit(solution)/shard_map/ppermute | solution.py:515
  52.0 23.2 %collective-permute-start.7 = (bf16[512,384]{1,0:T(8,128)(2,1)S(1)}, bf16[512,384]{1,0:T(8,128)(2,1)S(1)}, u32[]{:S(2)}, u32[]{:S(2)}) collective-permute-start(bf16[512,384]{1,0:T(8,128)(2,1)S(1)} %project.17), channel_id=1, source_target_pairs={{0,4},{4,8},{8,12},{12,0},{1,5},{5,9},{9,13},{13,1},{2,6},{6,10},{... | collective-permute-start | bytes 1179656 | tf_op jit(solution)/shard_map/ppermute | solution.py:515
  60.3 19.0 %collective-permute-start.13 = (bf16[512,384]{1,0:T(8,128)(2,1)S(1)}, bf16[512,384]{1,0:T(8,128)(2,1)S(1)}, u32[]{:S(2)}, u32[]{:S(2)}) collective-permute-start(bf16[512,384]{1,0:T(8,128)(2,1)S(1)} %project.20), channel_id=1, source_target_pairs={{0,12},{4,0},{8,4},{12,8},{1,13},{5,1},{9,5},{13,9},{2,14},{6,2},{... | collective-permute-start | bytes 1179656 | tf_op jit(solution)/shard_map/ppermute | solution.py:515
  63.8 10.6 %collective-permute-start.15 = (f32[8,128]{1,0:T(8,128)S(1)}, f32[8,128]{1,0:T(8,128)S(1)}, u32[]{:S(2)}, u32[]{:S(2)}) collective-permute-start(f32[8,128]{1,0:T(8,128)S(1)} %pad_maximum_fusion), channel_id=1, source_target_pairs={{0,4},{4,0},{8,12},{12,8},{1,5},{5,1},{9,13},{13,9},{2,6},{6,2},{1... | collective-permute-start | bytes 12296 | tf_op jit(solution)/shard_map/ppermute | solution.py:127
  74.5 11.0 %collective-permute-start.16 = (f32[8,128]{1,0:T(8,128)S(1)}, f32[8,128]{1,0:T(8,128)S(1)}, u32[]{:S(2)}, u32[]{:S(2)}) collective-permute-start(f32[8,128]{1,0:T(8,128)S(1)} %fusion.8), channel_id=1, source_target_pairs={{0,8},{4,12},{8,0},{12,4},{1,9},{5,13},{9,1},{13,5},{2,10},{6,14},... | collective-permute-start | bytes 12296 | tf_op jit(solution)/shard_map/ppermute | solution.py:127
  78.3 14.2 %collective-permute-start.8 = (bf16[512,384]{1,0:T(8,128)(2,1)}, bf16[512,384]{1,0:T(8,128)(2,1)}, u32[]{:S(2)}, u32[]{:S(2)}) collective-permute-start(bf16[512,384]{1,0:T(8,128)(2,1)} %project.18), channel_id=1, source_target_pairs={{0,4},{4,8},{8,12},{12,0},{1,5},{5,9},{9,13},{13,1},{2,6},{6,10},{... | collective-permute-start | bytes 1179656 | tf_op jit(solution)/shard_map/ppermute | solution.py:515
  82.5 16.7 %collective-permute-start.14 = (bf16[512,384]{1,0:T(8,128)(2,1)}, bf16[512,384]{1,0:T(8,128)(2,1)S(1)}, u32[]{:S(2)}, u32[]{:S(2)}) collective-permute-start(bf16[512,384]{1,0:T(8,128)(2,1)} %project.21), channel_id=1, source_target_pairs={{0,12},{4,0},{8,4},{12,8},{1,13},{5,1},{9,5},{13,9},{2,14},{6,2},{... | collective-permute-start | bytes 1179656 | tf_op jit(solution)/shard_map/ppermute | solution.py:515
  105.7 12.6 %collective-permute-start.18 = (bf16[512,128]{1,0:T(8,128)(2,1)S(1)}, bf16[512,128]{1,0:T(8,128)(2,1)S(1)}, u32[]{:S(2)}, u32[]{:S(2)}) collective-permute-start(bf16[512,128]{1,0:T(8,128)(2,1)S(1)} %get-tuple-element.63.refs_1_), channel_id=1, source_target_pairs={{0,8},{4,12},{8,0},{12,4},{1,9},{5,13},{9,1},{13,5},{2,10},{6,14},... | collective-permute-start | bytes 393224 | tf_op jit(solution)/shard_map/ppermute | solution.py:233
  106.5 11.8 %collective-permute-start.17 = (bf16[512,128]{1,0:T(8,128)(2,1)S(1)}, bf16[512,128]{1,0:T(8,128)(2,1)S(1)}, u32[]{:S(2)}, u32[]{:S(2)}) collective-permute-start(bf16[512,128]{1,0:T(8,128)(2,1)S(1)} %get-tuple-element.63.refs_1_), channel_id=1, source_target_pairs={{0,4},{4,8},{8,12},{12,0},{1,5},{5,9},{9,13},{13,1},{2,6},{6,10},{... | collective-permute-start | bytes 393224 | tf_op jit(solution)/shard_map/ppermute | solution.py:233
  121.0 13.8 %collective-permute-start.27 = (bf16[512,128]{1,0:T(8,128)(2,1)S(1)}, bf16[512,128]{1,0:T(8,128)(2,1)S(1)}, u32[]{:S(2)}, u32[]{:S(2)}) collective-permute-start(bf16[512,128]{1,0:T(8,128)(2,1)S(1)} %attend_high.2.refs_6_.refs_1_), channel_id=1, source_target_pairs={{0,8},{4,12},{8,0},{12,4},{1,9},{5,13},{9,1},{13,5},{2,10},{6,14},... | collective-permute-start | bytes 393224 | tf_op jit(solution)/shard_map/ppermute | solution.py:233
  122.3 12.5 %collective-permute-start.26 = (bf16[512,128]{1,0:T(8,128)(2,1)S(1)}, bf16[512,128]{1,0:T(8,128)(2,1)S(1)}, u32[]{:S(2)}, u32[]{:S(2)}) collective-permute-start(bf16[512,128]{1,0:T(8,128)(2,1)S(1)} %attend_high.2.refs_6_.refs_1_), channel_id=1, source_target_pairs={{0,4},{4,8},{8,12},{12,0},{1,5},{5,9},{9,13},{13,1},{2,6},{6,10},{... | collective-permute-start | bytes 393224 | tf_op jit(solution)/shard_map/ppermute | solution.py:233
  124.9 13.5 %collective-permute-start.21 = (bf16[512,512]{1,0:T(8,128)(2,1)S(1)}, bf16[512,512]{1,0:T(8,128)(2,1)S(1)}, u32[]{:S(2)}, u32[]{:S(2)}) collective-permute-start(bf16[512,512]{1,0:T(8,128)(2,1)S(1)} %pair_up.2.refs_3_.refs_6_), channel_id=1, source_target_pairs={{0,2},{1,3},{2,0},{3,1},{4,6},{5,7},{6,4},{7,5},{8,10},{9,11},{10,... | collective-permute-start | bytes 1572872 | tf_op jit(solution)/shard_map/ppermute | solution.py:127
  139.9 14.4 %collective-permute-start.30 = (bf16[512,512]{1,0:T(8,128)(2,1)S(1)}, bf16[512,512]{1,0:T(8,128)(2,1)S(1)}, u32[]{:S(2)}, u32[]{:S(2)}) collective-permute-start(bf16[512,512]{1,0:T(8,128)(2,1)S(1)} %pair_up.3.refs_3_), channel_id=1, source_target_pairs={{0,2},{1,3},{2,0},{3,1},{4,6},{5,7},{6,4},{7,5},{8,10},{9,11},{10,... | collective-permute-start | bytes 1572872 | tf_op jit(solution)/shard_map/ppermute | solution.py:127
  155.1 16.7 %collective-permute-start.31 = (bf16[512,512]{1,0:T(8,128)(2,1)S(1)}, bf16[512,512]{1,0:T(8,128)(2,1)S(1)}, u32[]{:S(2)}, u32[]{:S(2)}) collective-permute-start(bf16[512,512]{1,0:T(8,128)(2,1)S(1)} %renew.3.refs_1_), channel_id=1, source_target_pairs={{0,1},{1,0},{2,3},{3,2},{4,5},{5,4},{6,7},{7,6},{8,9},{9,8},{10,11... | collective-permute-start | bytes 1572872 | tf_op jit(solution)/shard_map/ppermute | solution.py:127
  155.1 13.6 %collective-permute-start.23 = (bf16[512,384]{1,0:T(8,128)(2,1)}, bf16[512,384]{1,0:T(8,128)(2,1)}, u32[]{:S(2)}, u32[]{:S(2)}) collective-permute-start(bf16[512,384]{1,0:T(8,128)(2,1)} %project.24.refs_5_), channel_id=1, source_target_pairs={{0,4},{4,8},{8,12},{12,0},{1,5},{5,9},{9,13},{13,1},{2,6},{6,10},{... | collective-permute-start | bytes 1179656 | tf_op jit(solution)/shard_map/ppermute | solution.py:515
  171.7 34.6 %collective-permute-start.24 = (bf16[512,384]{1,0:T(8,128)(2,1)S(1)}, bf16[512,384]{1,0:T(8,128)(2,1)S(1)}, u32[]{:S(2)}, u32[]{:S(2)}) collective-permute-start(bf16[512,384]{1,0:T(8,128)(2,1)S(1)} %project.25), channel_id=1, source_target_pairs={{0,4},{4,8},{8,12},{12,0},{1,5},{5,9},{9,13},{13,1},{2,6},{6,10},{... | collective-permute-start | bytes 1179656 | tf_op jit(solution)/shard_map/ppermute | solution.py:515
  174.2 18.4 %collective-permute-start.32 = (bf16[512,384]{1,0:T(8,128)(2,1)S(1)}, bf16[512,384]{1,0:T(8,128)(2,1)S(1)}, u32[]{:S(2)}, u32[]{:S(2)}) collective-permute-start(bf16[512,384]{1,0:T(8,128)(2,1)S(1)} %project.27), channel_id=1, source_target_pairs={{0,12},{4,0},{8,4},{12,8},{1,13},{5,1},{9,5},{13,9},{2,14},{6,2},{... | collective-permute-start | bytes 1179656 | tf_op jit(solution)/shard_map/ppermute | solution.py:515
  195.0 14.8 %collective-permute-start.33 = (bf16[512,384]{1,0:T(8,128)(2,1)S(1)}, bf16[512,384]{1,0:T(8,128)(2,1)S(1)}, u32[]{:S(2)}, u32[]{:S(2)}) collective-permute-start(bf16[512,384]{1,0:T(8,128)(2,1)S(1)} %project.28), channel_id=1, source_target_pairs={{0,12},{4,0},{8,4},{12,8},{1,13},{5,1},{9,5},{13,9},{2,14},{6,2},{... | collective-permute-start | bytes 1179656 | tf_op jit(solution)/shard_map/ppermute | solution.py:515
  195.3 10.9 %collective-permute-start.35 = (f32[8,128]{1,0:T(8,128)S(1)}, f32[8,128]{1,0:T(8,128)S(1)}, u32[]{:S(2)}, u32[]{:S(2)}) collective-permute-start(f32[8,128]{1,0:T(8,128)S(1)} %pad_maximum_fusion.1), channel_id=1, source_target_pairs={{0,4},{4,0},{8,12},{12,8},{1,5},{5,1},{9,13},{13,9},{2,6},{6,2},{1... | collective-permute-start | bytes 12296 | tf_op jit(solution)/shard_map/ppermute | solution.py:127
  206.2 9.7 %collective-permute-start.36 = (f32[8,128]{1,0:T(8,128)S(1)}, f32[8,128]{1,0:T(8,128)S(1)}, u32[]{:S(2)}, u32[]{:S(2)}) collective-permute-start(f32[8,128]{1,0:T(8,128)S(1)} %fusion.7), channel_id=1, source_target_pairs={{0,8},{4,12},{8,0},{12,4},{1,9},{5,13},{9,1},{13,5},{2,10},{6,14},... | collective-permute-start | bytes 12296 | tf_op jit(solution)/shard_map/ppermute | solution.py:127
  209.5 14.2 %collective-permute-start.25 = (bf16[512,384]{1,0:T(8,128)(2,1)}, bf16[512,384]{1,0:T(8,128)(2,1)}, u32[]{:S(2)}, u32[]{:S(2)}) collective-permute-start(bf16[512,384]{1,0:T(8,128)(2,1)} %project.26), channel_id=1, source_target_pairs={{0,4},{4,8},{8,12},{12,0},{1,5},{5,9},{9,13},{13,1},{2,6},{6,10},{... | collective-permute-start | bytes 1179656 | tf_op jit(solution)/shard_map/ppermute | solution.py:515
  212.2 17.9 %collective-permute-start.34 = (bf16[512,384]{1,0:T(8,128)(2,1)S(1)}, bf16[512,384]{1,0:T(8,128)(2,1)S(1)}, u32[]{:S(2)}, u32[]{:S(2)}) collective-permute-start(bf16[512,384]{1,0:T(8,128)(2,1)S(1)} %project.29), channel_id=1, source_target_pairs={{0,12},{4,0},{8,4},{12,8},{1,13},{5,1},{9,5},{13,9},{2,14},{6,2},{... | collective-permute-start | bytes 1179656 | tf_op jit(solution)/shard_map/ppermute | solution.py:515
  237.8 13.1 %collective-permute-start.38 = (bf16[512,128]{1,0:T(8,128)(2,1)S(1)}, bf16[512,128]{1,0:T(8,128)(2,1)S(1)}, u32[]{:S(2)}, u32[]{:S(2)}) collective-permute-start(bf16[512,128]{1,0:T(8,128)(2,1)S(1)} %get-tuple-element.73.refs_1_), channel_id=1, source_target_pairs={{0,8},{4,12},{8,0},{12,4},{1,9},{5,13},{9,1},{13,5},{2,10},{6,14},... | collective-permute-start | bytes 393224 | tf_op jit(solution)/shard_map/ppermute | solution.py:233
  239.2 11.8 %collective-permute-start.37 = (bf16[512,128]{1,0:T(8,128)(2,1)S(1)}, bf16[512,128]{1,0:T(8,128)(2,1)S(1)}, u32[]{:S(2)}, u32[]{:S(2)}) collective-permute-start(bf16[512,128]{1,0:T(8,128)(2,1)S(1)} %get-tuple-element.73.refs_1_), channel_id=1, source_target_pairs={{0,4},{4,8},{8,12},{12,0},{1,5},{5,9},{9,13},{13,1},{2,6},{6,10},{... | collective-permute-start | bytes 393224 | tf_op jit(solution)/shard_map/ppermute | solution.py:233
  253.6 13.7 %collective-permute-start.49 = (bf16[512,128]{1,0:T(8,128)(2,1)S(1)}, bf16[512,128]{1,0:T(8,128)(2,1)S(1)}, u32[]{:S(2)}, u32[]{:S(2)}) collective-permute-start(bf16[512,128]{1,0:T(8,128)(2,1)S(1)} %attend_high.3.refs_6_.refs_1_), channel_id=1, source_target_pairs={{0,8},{4,12},{8,0},{12,4},{1,9},{5,13},{9,1},{13,5},{2,10},{6,14},... | collective-permute-start | bytes 393224 | tf_op jit(solution)/shard_map/ppermute | solution.py:233
  254.9 12.5 %collective-permute-start.48 = (bf16[512,128]{1,0:T(8,128)(2,1)S(1)}, bf16[512,128]{1,0:T(8,128)(2,1)S(1)}, u32[]{:S(2)}, u32[]{:S(2)}) collective-permute-start(bf16[512,128]{1,0:T(8,128)(2,1)S(1)} %attend_high.3.refs_6_.refs_1_), channel_id=1, source_target_pairs={{0,4},{4,8},{8,12},{12,0},{1,5},{5,9},{9,13},{13,1},{2,6},{6,10},{... | collective-permute-start | bytes 393224 | tf_op jit(solution)/shard_map/ppermute | solution.py:233
  272.6 12.0 %collective-permute-start.52 = (bf16[512,256]{1,0:T(8,128)(2,1)S(1)}, bf16[512,256]{1,0:T(8,128)(2,1)S(1)}, u32[]{:S(2)}, u32[]{:S(2)}) collective-permute-start(bf16[512,256]{1,0:T(8,128)(2,1)S(1)} %get-tuple-element.86), channel_id=1, source_target_pairs={{0,2},{1,3},{2,0},{3,1},{4,6},{5,7},{6,4},{7,5},{8,10},{9,11},{10,... | collective-permute-start | bytes 786440 | tf_op jit(solution)/shard_map/ppermute | solution.py:127
  280.0 9.7 %collective-permute-start.43 = (bf16[128,256]{1,0:T(8,128)(2,1)S(1)}, bf16[128,256]{1,0:T(8,128)(2,1)S(1)}, u32[]{:S(2)}, u32[]{:S(2)}) collective-permute-start(bf16[128,256]{1,0:T(8,128)(2,1)S(1)} %get-tuple-element.81), channel_id=1, source_target_pairs={{0,8},{4,12},{8,0},{12,4},{1,9},{5,13},{9,1},{13,5},{2,10},{6,14},... | collective-permute-start | bytes 196616 | tf_op jit(solution)/shard_map/ppermute | solution.py:233
  (34 other events, 188.1 us)

commit v4 on v3

--- a/solution.py
+++ b/solution.py
@@ -1,11 +1,10 @@
-import functools
-
 import jax
 import jax.numpy as jnp
 from jax import lax
 from jax.experimental import pallas as pl
 from jax.experimental.pallas import tpu as pltpu
 from jax.sharding import PartitionSpec as P
+
 
 HD = 128
 GRID_W = 64
@@ -127,20 +126,11 @@
     return lax.ppermute(array, axis, [(i, i ^ distance) for i in range(count)])
 
 
-def summed_over(vector, axis):
-    count = lax.axis_size(axis)
-    distance = 1
-    while distance < count:
-        vector = vector + swapped(vector, axis, distance)
-        distance *= 2
-    return vector
-
-
 def aligned(index, size):
     return pl.ds(pl.multiple_of(index * size, size), size)
 
 
-def local_kernel(body, place, arrays, outs, name, scratch=(), hbm=(), flops=0, after=()):
+def local_kernel(body, place, arrays, outs, scratch=(), hbm=(), flops=0, after=()):
     vmem, smem = pl.BlockSpec(memory_space=pltpu.VMEM), pl.BlockSpec(memory_space=pltpu.SMEM)
     moved = sum(a.size * a.dtype.itemsize for a in (*arrays, *outs))
     inputs = 1 + len(arrays) + len(hbm)
@@ -159,7 +149,6 @@
         scratch_shapes=list(scratch),
         compiler_params=pltpu.CompilerParams(vmem_limit_bytes=VMEM_BYTES),
         cost_estimate=pl.CostEstimate(flops=flops, bytes_accessed=moved, transcendentals=0),
-        name=name,
     )(place, *arrays, *(pltpu.with_memory_space_constraint(a, pltpu.HBM) for a in hbm), *after)
 
 
@@ -167,18 +156,62 @@
     return jax.ShapeDtypeStruct(shape, dtype)
 
 
-def window_bias(table):
-    heads = table.shape[0]
-    columns = jnp.arange(GRID_W, dtype=jnp.int32)
-    first = jnp.clip(columns - KC // 2, 0, GRID_W - KC)
-    inside = (columns[None, :] >= first[:, None]) & (columns[None, :] < first[:, None] + KC)
-    offset = jnp.clip(columns[None, :] - columns[:, None], 1 - KC, KC - 1) + KC - 1
-    onehot = (
-        jnp.arange(2 * KC - 1, dtype=jnp.int32)[:, None, None] == offset[None, :, :]
-    ).astype(jnp.float32)
-    wide = jnp.einsum("hro,oqk->hqrk", table, onehot, precision=lax.Precision.HIGHEST)
-    wide = jnp.where(inside[None, :, None, :], wide, -jnp.inf)
-    return wide.reshape(heads, GRID_W, (2 * KR - 1) * GRID_W)
+def window_bias(offset_bias, place, heads):
+    layers, _, offsets, reach = offset_bias.shape
+    pairs = -(-offsets // 2)
+    lanes = 2 * GRID_W
+
+    def body(place_ref, table_ref, out_ref, padded):
+        padded[...] = jnp.zeros_like(padded)
+        lane = lax.broadcasted_iota(jnp.int32, (GRID_W, lanes), 1)
+        query = lax.broadcasted_iota(jnp.int32, (GRID_W, lanes), 0)
+        column = jnp.where(lane < GRID_W, lane, lane - GRID_W)
+        first = jnp.clip(query - KC // 2, 0, GRID_W - KC)
+        inside = (column >= first) & (column < first + KC)
+        for layer in range(layers):
+            for head in range(heads):
+                padded[pl.ds(0, offsets), pl.ds(0, reach)] = table_ref[
+                    layer, place_ref[0] * heads + head
+                ]
+                for pair in range(pairs):
+                    sides = []
+                    for side in range(2):
+                        row = jnp.broadcast_to(
+                            padded[pl.ds(2 * pair + side, 1), :], (GRID_W, lanes)
+                        )
+                        start = (side * GRID_W - (KC - 1)) % lanes
+                        sides.append(pltpu.roll(row, start, 1, stride=1, stride_axis=0))
+                    both = jnp.where(lane < GRID_W, sides[0], sides[1])
+                    out_ref[layer * heads + head, :, pl.ds(pair * lanes, lanes)] = jnp.where(
+                        inside, both, -jnp.inf
+                    )
+
+    return local_kernel(
+        body,
+        place,
+        (offset_bias,),
+        [shaped(layers * heads, GRID_W, pairs * lanes, dtype=jnp.float32)],
+        scratch=[pltpu.VMEM((2 * pairs, lanes), jnp.float32)],
+    )[0]
+
+
+def squares_of(halves, place):
+    flat = [piece for pieces in halves for piece in pieces]
+    count = len(halves[0])
+    runs = halves[0][0].shape[0] // HD
+
+    def body(place_ref, *refs):
+        out_ref = refs[-1]
+        for index in range(len(halves)):
+            for run in range(runs):
+                total = jnp.zeros((HD, HD), jnp.float32)
+                for ref in refs[index * count : (index + 1) * count]:
+                    for lane in range(ref.shape[1] // HD):
+                        part = ref[pl.ds(run * HD, HD), pl.ds(lane * HD, HD)].astype(jnp.float32)
+                        total += part * part
+                out_ref[pl.ds(index * runs + run, 1), :] = jnp.sum(total.T, axis=0, keepdims=True)
+
+    return local_kernel(body, place, flat, [shaped(len(halves) * runs, HD, dtype=jnp.float32)])[0]
 
 
 def scatter_tokens(tokens, place, sp_count, feats, piece):
@@ -204,13 +237,12 @@
         place,
         (),
         [shaped(tok_here, piece)] * sp_count,
-        "scatter_tokens",
         scratch=[pltpu.SemaphoreType.DMA((sp_count,))],
         hbm=(tokens,),
     )
 
 
-def stack_blocks(blocks, place, parts=1):
+def stack_blocks(blocks, place, parts=1, after=()):
     count = len(blocks)
     rows, width = blocks[0].shape
     rows = rows // parts
@@ -223,9 +255,7 @@
                     pl.ds(part * rows, rows), :
                 ]
 
-    return local_kernel(
-        body, place, blocks, [shaped(rows * count, width)] * parts, "stack_blocks"
-    )
+    return local_kernel(body, place, blocks, [shaped(rows * count, width)] * parts, after=after)
 
 
 def over_sp(blocks, count):
@@ -234,19 +264,30 @@
     ]
 
 
-def project(pieces, slots, gain, weights, layer, place, chunk_shift, width, arrived, last):
-    tok = pieces[0].shape[0]
+def scaled_by(slots, layer, feats, place_ref, piece_refs, gain_ref, out_ref):
+    for piece_ref, slot in zip(piece_refs, slots):
+        span = aligned(slot(place_ref[1], place_ref[2]), piece_ref.shape[1])
+        start = pl.multiple_of(
+            place_ref[0] * feats + slot(place_ref[1], place_ref[2]) * piece_ref.shape[1],
+            piece_ref.shape[1],
+        )
+        factor = gain_ref[pl.ds(layer, 1), pl.ds(start, piece_ref.shape[1])].astype(jnp.float32)
+        out_ref[:, span] = (piece_ref[...].astype(jnp.float32) * factor).astype(jnp.bfloat16)
+
+
+def project(source, weights, layer, place, chunk_shift, width, arrived=None, last=False):
+    fresh = isinstance(source, tuple)
     feats = weights[0].shape[1]
     sp_count = lax.axis_size("sp")
-    count = len(pieces)
+    arrays = (*source[0], source[2]) if fresh else (source,)
+    tok = arrays[0].shape[0]
+    if arrived is not None:
+        arrays += (arrived,)
+    count = len(arrays)
 
     def body(place_ref, *refs):
-        piece_refs, refs = refs[:count], refs[count:]
-        gain_ref, refs = refs[0], refs[1:]
-        arrived_ref = None
-        if arrived is not None:
-            arrived_ref, refs = refs[0], refs[1:]
-        weight_refs, (out_ref, held, sem) = refs[:3], refs[3:]
+        array_refs, weight_refs, refs = refs[:count], refs[count : count + 3], refs[count + 3 :]
+        out_ref, held, sem = refs[0], refs[-2], refs[-1]
         chunk = lax.rem(place_ref[0] + chunk_shift, sp_count)
         copies = []
         for index, weight_ref in enumerate(weight_refs):
@@ -257,36 +298,37 @@
             )
             copy.start()
             copies.append(copy)
+        scaled_ref = array_refs[0]
+        if fresh:
+            scaled_ref = refs[1]
+            pieces, slots, _ = source
+            scaled_by(
+                slots, layer, feats, place_ref,
+                array_refs[: len(pieces)], array_refs[len(pieces)], scaled_ref,
+            )
         for copy in copies:
             copy.wait()
-        total = jnp.zeros((tok, 3 * width), jnp.float32)
+        total = jnp.dot(scaled_ref[...], held[...], preferred_element_type=jnp.float32)
         if arrived is not None:
-            total = arrived_ref[...].astype(jnp.float32)
-        for piece_ref, slot in zip(piece_refs, slots):
-            span = aligned(slot(place_ref[1], place_ref[2]), piece_ref.shape[1])
-            scaled = piece_ref[...].astype(jnp.float32) * gain_ref[layer, :, span]
-            total += jnp.dot(
-                scaled.astype(jnp.bfloat16), held[span, :], preferred_element_type=jnp.float32
-            )
+            total += array_refs[-1][...].astype(jnp.float32)
         out_ref[...] = total.astype(out_ref.dtype)
 
-    arrays = (*pieces, gain) + (() if arrived is None else (arrived,))
+    outs = [shaped(tok, 3 * width, dtype=jnp.float32 if last else jnp.bfloat16)]
     return local_kernel(
         body,
         place,
         arrays,
-        [shaped(tok, 3 * width, dtype=jnp.float32 if last else jnp.bfloat16)],
-        "project",
+        outs + [shaped(tok, feats)] * fresh,
         scratch=[
             pltpu.VMEM((feats, 3 * width), jnp.bfloat16),
             pltpu.SemaphoreType.DMA((3,)),
         ],
         hbm=weights,
         flops=2 * tok * feats * 3 * width,
-    )[0]
-
-
-def attend_rows(qkv_ref, bias_ref, out_ref, part, sp_count, heads):
+    )
+
+
+def attend_rows(qkv_ref, bias_ref, out_ref, part, sp_count, heads, layer):
     grid_rows = qkv_ref.shape[0] // GRID_W
     width = heads * HD
     part_grid = grid_rows // sp_count // 2
@@ -304,7 +346,7 @@
             scores = lax.dot_general(
                 queries, keys, (((1,), (1,)), ((), ())), preferred_element_type=jnp.float32
             )
-            bias_here = bias_ref[head, :, pl.ds(offset * GRID_W, KR * GRID_W)]
+            bias_here = bias_ref[layer * heads + head, :, pl.ds(offset * GRID_W, KR * GRID_W)]
             scores = scores * HD ** (-0.5) + bias_here
             powers = jnp.exp(scores - jnp.max(scores, axis=-1, keepdims=True))
             weights = powers * (1.0 / jnp.sum(powers, axis=-1, keepdims=True))
@@ -314,35 +356,40 @@
             out_ref[pl.ds(index * GRID_W, GRID_W), pl.ds(lanes, HD)] = mixed.astype(jnp.bfloat16)
 
 
-def attend(arrived, own, norms, bias, place, sp_count):
+def attend(arrived, own, squares, bias, place, sp_count, heads, layer, every_feat):
     rows, total_width = arrived[0].shape
-    heads = bias.shape[0]
     width = heads * HD
     part_rows = rows // sp_count
+    runs = rows // HD
     flops = 4 * heads * rows * KR * GRID_W * HD
 
-    def low(place_ref, a0, a1, o0, o1, n0, n1, bias_ref, out_ref, qkv_ref):
-        for part, (a_ref, o_ref, n_ref) in enumerate(((a0, o0, n0), (a1, o1, n1))):
-            for plane in range(sp_count):
-                span = pl.ds(plane * part_rows, part_rows)
-                total = a_ref[span, :].astype(jnp.float32) + o_ref[span, :]
-                qkv_ref[pl.ds((2 * plane + part) * part_rows, part_rows), :] = (
-                    total * n_ref[span, :]
-                ).astype(jnp.bfloat16)
-        attend_rows(qkv_ref, bias_ref, out_ref, 0, sp_count, heads)
+    def low(place_ref, a0, a1, o0, o1, *refs):
+        square_refs, (bias_ref, out_ref, qkv_ref) = refs[:-3], refs[-3:]
+        norm = lax.rsqrt(total_of(*square_refs) / every_feat + norm_eps)
+        for part, (a_ref, o_ref) in enumerate(((a0, o0), (a1, o1))):
+            for run in range(runs):
+                row = part * runs + run
+                factor = jnp.broadcast_to(norm[row : row + 1, :], (HD, HD)).T
+                plane, inner = divmod(run * HD, part_rows)
+                to = pl.ds((2 * plane + part) * part_rows + inner, HD)
+                span = pl.ds(run * HD, HD)
+                for lane in range(total_width // HD):
+                    lanes = pl.ds(lane * HD, HD)
+                    total = a_ref[span, lanes].astype(jnp.float32) + o_ref[span, lanes]
+                    qkv_ref[to, lanes] = (total * factor).astype(jnp.bfloat16)
+        attend_rows(qkv_ref, bias_ref, out_ref, 0, sp_count, heads, layer)
 
     def high(place_ref, qkv_ref, bias_ref, out_ref):
-        attend_rows(qkv_ref, bias_ref, out_ref, 1, sp_count, heads)
+        attend_rows(qkv_ref, bias_ref, out_ref, 1, sp_count, heads, layer)
 
     out0, qkv = local_kernel(
         low,
         place,
-        (*arrived, *own, *norms, bias),
+        (*arrived, *own, *squares, bias),
         [shaped(rows, width), shaped(2 * rows, total_width)],
-        "attend_low",
         flops=flops,
     )
-    out1 = local_kernel(high, place, (qkv, bias), [shaped(rows, width)], "attend_high", flops=flops)
+    out1 = local_kernel(high, place, (qkv, bias), [shaped(rows, width)], flops=flops)
     return out0, out1[0]
 
 
@@ -371,7 +418,6 @@
         place,
         attended,
         [shaped(rows, half)] * 2,
-        "spread",
         scratch=[
             pltpu.VMEM((rows, inner), jnp.bfloat16),
             pltpu.VMEM((inner, feats), jnp.bfloat16),
@@ -394,7 +440,7 @@
     def body(place_ref, kept_ref, came_ref, out_ref):
         out_ref[...] = total_of(kept_ref, came_ref).astype(jnp.bfloat16)
 
-    return local_kernel(body, place, (kept, came), [shaped(*kept.shape)], "pair_up")
+    return local_kernel(body, place, (kept, came), [shaped(*kept.shape)])
 
 
 def pair_apart(kept, came, place):
@@ -409,7 +455,7 @@
                 kept_ref[:, span].astype(jnp.float32) + came_ref[:, span].astype(jnp.float32)
             ).astype(jnp.bfloat16)
 
-    return local_kernel(body, place, (kept, came), [shaped(rows, piece)] * 2, "pair_apart")
+    return local_kernel(body, place, (kept, came), [shaped(rows, piece)] * 2)
 
 
 def renew(residual, pair, came, place, after):
@@ -427,9 +473,7 @@
             branch = pair_ref[:, span].astype(jnp.float32) + came_ref[:, span].astype(jnp.float32)
             out_ref[:, span] = (ref[...].astype(jnp.float32) + branch).astype(jnp.bfloat16)
 
-    return local_kernel(
-        body, place, (*residual, pair, came), [shaped(*pair.shape)], "renew", after=after
-    )[0]
+    return local_kernel(body, place, (*residual, pair, came), [shaped(*pair.shape)], after=after)[0]
 
 
 def finish(residual, stay, came, place, sp_count):
@@ -444,9 +488,7 @@
             x_here = x_ref[span, aligned(place_ref[2], piece)].astype(jnp.float32)
             out_refs[shift][...] = (x_here + branch).astype(jnp.bfloat16)
 
-    return local_kernel(
-        body, place, (residual, stay, came), [shaped(part, piece)] * sp_count, "finish"
-    )
+    return local_kernel(body, place, (residual, stay, came), [shaped(part, piece)] * sp_count)
 
 
 SLOTS = (
@@ -476,9 +518,7 @@
                     ][pl.ds(plane * part, part), :]
 
     flat = [array for pieces in parts for array in pieces]
-    return local_kernel(
-        body, place, flat, [shaped(part * len(parts), piece * count * sp_count)], "assemble"
-    )[0]
+    return local_kernel(body, place, flat, [shaped(part * len(parts), piece * count * sp_count)])[0]
 
 
 def exchanged(held):
@@ -496,51 +536,48 @@
     piece = feats // 4
     every_feat = feats * sp_count
     weights = (w_query, w_key, w_value)
-    tables = lax.dynamic_slice_in_dim(offset_bias, sp_index * heads, heads, 1)
-    biases = window_bias(tables.reshape(LAYERS * heads, *tables.shape[2:]))
-    gain = lax.dynamic_slice_in_dim(norm_gain, sp_index * feats, feats, 1)[:, None, :]
     shifts = (1, -1)
-    halves = [None, None]
-    travelling = [None, None]
-
-    def shared(part, step, layer, arrived=None):
+    halves, scaled, made = [None, None], [None, None], [None, None]
+
+    def chunk_of(part, step):
+        return (-shifts[part] * (step + 1)) % sp_count
+
+    def first_share(part, layer):
         slots = SLOTS if layer == 0 else HALF_SLOTS
-        final = step == sp_count - 1
-        chunk = (-shifts[part] * (step + 1)) % sp_count
+        made[part], scaled[part] = project(
+            (halves[part], slots, norm_gain), weights, layer, place, chunk_of(part, 0), width
+        )
+
+    def share(part, step, layer, arrived=None):
+        last = step == sp_count - 1
         return project(
-            halves[part], slots, gain, weights, layer, place, chunk, width, arrived, final
-        )
-
-    def sent_on(made, part):
-        return lax.ppermute(made, "sp", ring(sp_count, shifts[part]))
-
+            scaled[part], weights, layer, place, chunk_of(part, step), width, arrived, last
+        )[0]
+
+    def sent_on(block, part):
+        return lax.ppermute(block, "sp", ring(sp_count, shifts[part]))
+
+    bias = window_bias(offset_bias, place, heads)
     blocks = over_sp(scatter_tokens(tokens, place, sp_count, feats, piece), sp_count)
-    held = stack_blocks(blocks, place, 2)
+    held = stack_blocks(blocks, place, 2, (bias,))
     far = [swapped(h, "tp", 2) for h in held]
     near = [swapped(h, "tp", 1) for h in held]
     halves[0] = [held[0], far[0], near[0], swapped(far[0], "tp", 1)]
-    made = [shared(0, 0, 0), None]
+    first_share(0, 0)
     far[1] = lax.optimization_barrier((far[1], made[0]))[0]
-    halves[1] = [held[1], far[1], near[1], swapped(far[1], "tp", 1)]
-    made[1] = shared(1, 0, 0)
+    near_far = swapped(far[1], "tp", 1)
+    halves[1] = [held[1], far[1], near[1], near_far]
+    first_share(1, 0)
 
     for layer in range(LAYERS):
+        travelling = [sent_on(made[part], part) for part in range(2)]
         summed = lax.optimization_barrier((halves, made))[0]
-        travelling = [sent_on(made[part], part) for part in range(2)]
-        squares = jnp.concatenate(
-            [
-                sum(jnp.sum(jnp.square(p.astype(jnp.float32)), axis=-1) for p in pieces)
-                for pieces in summed
-            ]
-        )
-        squares = summed_over(squares.reshape(-1, HD), "sp").reshape(2, -1, 1)
-        norms = lax.rsqrt(squares / every_feat + norm_eps)
+        squares = over_sp([squares_of(summed, place)] * sp_count, sp_count)
         for step in range(1, sp_count - 1):
             for part in range(2):
-                travelling[part] = sent_on(shared(part, step, layer, travelling[part]), part)
-        own = [shared(part, sp_count - 1, layer) for part in range(2)]
-        bias = biases[layer * heads : (layer + 1) * heads]
-        attended = attend(travelling, own, (norms[0], norms[1]), bias, place, sp_count)
+                travelling[part] = sent_on(share(part, step, layer, travelling[part]), part)
+        own = [share(part, sp_count - 1, layer) for part in range(2)]
+        attended = attend(travelling, own, squares, bias, place, sp_count, heads, layer, every_feat)
 
         residuals = [pieces[:2] if layer == 0 else pieces[:1] for pieces in halves]
         pairs, after = [], (attended[1],)
@@ -549,21 +586,18 @@
             sent, kept = spread(gathered, w_out, layer, place, after)
             came = swapped(sent, "tp", 1)
             pair = (pair_up if layer < LAYERS - 1 else pair_apart)(kept, came, place)
-            pairs.append(pair)
+            pairs.append((pair, swapped(pair[0], "tp", 2)))
             after = (pair[0],)
         after = ()
         for part in range(2):
+            pair, came = pairs[part]
             if layer < LAYERS - 1:
-                pair = pairs[part][0]
-                mine = renew(residuals[part], pair, swapped(pair, "tp", 2), place, after)
+                mine = renew(residuals[part], pair[0], came, place, after)
                 halves[part] = [mine, swapped(mine, "tp", 1)]
-                made[part] = shared(part, 0, layer + 1)
+                first_share(part, layer + 1)
                 after = (made[part],)
             else:
-                sent, stay = pairs[part]
-                blocks = finish(
-                    residuals[part][0], stay, swapped(sent, "tp", 2), place, sp_count
-                )
+                blocks = finish(residuals[part][0], pair[1], came, place, sp_count)
                 stacked = stack_blocks(over_sp(blocks, sp_count), place)[0]
                 halves[part] = exchanged(stacked)
     return assemble(halves, place, sp_count)
@@ -572,10 +606,10 @@
 def on_device(tokens, norm_gain, w_query, w_key, w_value, w_out, offset_bias):
     heads_here, sp_count = offset_bias.shape[1], lax.axis_size("sp")
     part_rows = tokens.shape[0] // 2
-    plan = gathered_plan
-    if heads_here % sp_count == 0 and lax.axis_size("tp") == 4 and part_rows % GRID_W == 0:
-        plan = stationary_plan
-    return plan(tokens, norm_gain, w_query, w_key, w_value, w_out, offset_bias)
+    arrays = (tokens, norm_gain, w_query, w_key, w_value, w_out, offset_bias)
+    if heads_here % sp_count == 0 and lax.axis_size("tp") == 4 and part_rows % HD == 0:
+        return stationary_plan(*arrays)
+    return gathered_plan(*arrays)
 
 
 def solution(mesh):

time: 308 us -> 275 us (0.89)
  waiting for transfers between devices: 150 us -> 118 us
  starting transfers between devices: 66.7 us -> 78.9 us
  local copies, waits for them, and re-layouts: 8.45 us -> 0.01 us
    ppermute x12, waiting for transfers between devices: 59.5 us -> 42.2 us  [sent_on(): return lax.ppermute(block, 'sp', ring(sp_count, shifts[part]))]
    ppermute x21 -> x27, starting transfers between devices: 28.8 us -> 45.5 us  [over_sp(): lax.ppermute(blocks[shift], 'sp', ring(count, shift))]
    ppermute x26 -> x22, waiting for transfers between devices: 48.4 us -> 40 us  [swapped(): return lax.ppermute(array, axis, [(i, i ^ distance) for i in range(count)])]
    ppermute x21 -> x27, waiting for transfers between devices: 41.8 us -> 36.1 us  [over_sp(): lax.ppermute(blocks[shift], 'sp', ring(count, shift))]
    unnamed x14 -> x5, local copies, waits for them, and re-layouts: 4.91 us -> 0.01 us
    ppermute x26 -> x22, starting transfers between devices: 16.3 us -> 13.6 us  [swapped(): return lax.ppermute(array, axis, [(i, i ^ distance) for i in range(count)])]
    pallas_call x37 -> x40, Pallas kernels: 78.7 us -> 76.5 us  [local_kernel(): pl.pallas_call(ordered, out_shape=list(outs), in_specs=[smem] + [vmem] *...]
  transfers between devices with their start and end apart: 59 -> 61, of which waited for: 28 -> 31; matrix products, arithmetic and copies ran while one was open for 2% -> 0% of each run, Pallas kernels for 19% -> 21%
where the time goes in v4:
time: 275 us; the launch traced here: 274 us
  waiting for transfers between devices  118 us (43%)
  starting transfers between devices  78.9 us (29%)
  Pallas kernels  76.5 us (28%)
    pallas_call x40, Pallas kernels, local_kernel(): pl.pallas_call(ordered, out_shape=list(outs), in_specs=[smem] + [vmem] *...  76.5 us
    ppermute x27, starting transfers between devices, over_sp(): lax.ppermute(blocks[shift], 'sp', ring(count, shift))  45.5 us
    ppermute x12, waiting for transfers between devices, sent_on(): return lax.ppermute(block, 'sp', ring(sp_count, shifts[part]))  42.2 us
    ppermute x22, waiting for transfers between devices, swapped(): return lax.ppermute(array, axis, [(i, i ^ distance) for i in range(count)])  40 us
    ppermute x27, waiting for transfers between devices, over_sp(): lax.ppermute(blocks[shift], 'sp', ring(count, shift))  36.1 us
    ppermute x12, starting transfers between devices, sent_on(): return lax.ppermute(block, 'sp', ring(sp_count, shifts[part]))  19.8 us
    ppermute x22, starting transfers between devices, swapped(): return lax.ppermute(array, axis, [(i, i ^ distance) for i in range(count)])  13.6 us
  transfers between devices with their start and end apart: 61, of which 31 were waited for; matrix products, arithmetic and copies ran while one was open for 0% of the time, Pallas kernels for 21%

profile of v4, /device:TPU:0, one launch (start us, length us, event | category | flops | bytes accessed | tf_op | source)
XLA Modules:
  0.0 274.2 jit_solution(15455836495846456381)
XLA Ops:
  1.8 3.1 %collective-permute-start = (bf16[256,256]{1,0:T(8,128)(2,1)S(1)}, bf16[256,256]{1,0:T(8,128)(2,1)S(1)}, u32[]{:S(2)}, u32[]{:S(2)}) collective-permute-start(bf16[256,256]{1,0:T(8,128)(2,1)S(1)} %get-tuple-element.57), channel_id=1, source_target_pairs={{0,4},{4,8},{8,12},{12,0},{1,5},{5,9},{9,13},{13,1},{2,6},{6,10},{... | collective-permute-start | bytes 393224 | tf_op jit(solution)/shard_map/ppermute | solution.py:263
  11.4 4.8 %collective-permute-done.1.refs_3_ = bf16[256,256]{1,0:T(8,128)(2,1)S(1)} collective-permute-done((bf16[256,256]{1,0:T(8,128)(2,1)S(1)}, bf16[256,256]{1,0:T(8,128)(2,1)S(1)}, u32[]{:S(2)}, u32[]{:S(2)}) %collective-permute-start.1) | collective-permute-done | bytes 131104 | tf_op jit(solution)/shard_map/ppermute | solution.py:263
  18.3 6.6 %collective-permute-done.3.refs_2_ = bf16[512,256]{1,0:T(8,128)(2,1)S(1)} collective-permute-done((bf16[512,256]{1,0:T(8,128)(2,1)S(1)}, bf16[512,256]{1,0:T(8,128)(2,1)S(1)}, u32[]{:S(2)}, u32[]{:S(2)}) %collective-permute-start.3) | collective-permute-done | bytes 262176 | tf_op jit(solution)/shard_map/ppermute | solution.py:126
  29.1 4.6 %collective-permute-done.9.refs_2_.refs_6_ = bf16[512,256]{1,0:T(8,128)(2,1)S(1)} collective-permute-done((bf16[512,256]{1,0:T(8,128)(2,1)S(1)}, bf16[512,256]{1,0:T(8,128)(2,1)S(1)}, u32[]{:S(2)}, u32[]{:S(2)}) %collective-permute-start.9) | collective-permute-done | bytes 262176 | tf_op jit(solution)/shard_map/ppermute | solution.py:126
  33.6 3.4 %collective-permute-start.6 = (bf16[512,384]{1,0:T(8,128)(2,1)S(1)}, bf16[512,384]{1,0:T(8,128)(2,1)S(1)}, u32[]{:S(2)}, u32[]{:S(2)}) collective-permute-start(bf16[512,384]{1,0:T(8,128)(2,1)S(1)} %get-tuple-element.62), channel_id=1, source_target_pairs={{0,4},{4,8},{8,12},{12,0},{1,5},{5,9},{9,13},{13,1},{2,6},{6,10},{... | collective-permute-start | bytes 1179656 | tf_op jit(solution)/shard_map/ppermute | solution.py:558
  41.0 6.4 %collective-permute-done.6.refs_2_ = bf16[512,384]{1,0:T(8,128)(2,1)S(1)} collective-permute-done((bf16[512,384]{1,0:T(8,128)(2,1)S(1)}, bf16[512,384]{1,0:T(8,128)(2,1)S(1)}, u32[]{:S(2)}, u32[]{:S(2)}) %collective-permute-start.6) | collective-permute-done | bytes 393248 | tf_op jit(solution)/shard_map/ppermute | solution.py:558
  51.5 4.3 %collective-permute-done.12.refs_2_ = bf16[512,384]{1,0:T(8,128)(2,1)S(1)} collective-permute-done((bf16[512,384]{1,0:T(8,128)(2,1)S(1)}, bf16[512,384]{1,0:T(8,128)(2,1)S(1)}, u32[]{:S(2)}, u32[]{:S(2)}) %collective-permute-start.12) | collective-permute-done | bytes 393248 | tf_op jit(solution)/shard_map/ppermute | solution.py:558
  58.2 3.5 %collective-permute-start.13 = (bf16[512,384]{1,0:T(8,128)(2,1)S(1)}, bf16[512,384]{1,0:T(8,128)(2,1)S(1)}, u32[]{:S(2)}, u32[]{:S(2)}) collective-permute-start(bf16[512,384]{1,0:T(8,128)(2,1)S(1)} %shard_map.80), channel_id=1, source_target_pairs={{0,12},{4,0},{8,4},{12,8},{1,13},{5,1},{9,5},{13,9},{2,14},{6,2},{... | collective-permute-start | bytes 1179656 | tf_op jit(solution)/shard_map/ppermute | solution.py:558
  68.4 4.3 %collective-permute-done.13.refs_2_ = bf16[512,384]{1,0:T(8,128)(2,1)S(1)} collective-permute-done((bf16[512,384]{1,0:T(8,128)(2,1)S(1)}, bf16[512,384]{1,0:T(8,128)(2,1)S(1)}, u32[]{:S(2)}, u32[]{:S(2)}) %collective-permute-start.13) | collective-permute-done | bytes 393248 | tf_op jit(solution)/shard_map/ppermute | solution.py:558
  75.1 3.5 %collective-permute-start.14 = (bf16[512,384]{1,0:T(8,128)(2,1)S(1)}, bf16[512,384]{1,0:T(8,128)(2,1)S(1)}, u32[]{:S(2)}, u32[]{:S(2)}) collective-permute-start(bf16[512,384]{1,0:T(8,128)(2,1)S(1)} %shard_map.81), channel_id=1, source_target_pairs={{0,12},{4,0},{8,4},{12,8},{1,13},{5,1},{9,5},{13,9},{2,14},{6,2},{... | collective-permute-start | bytes 1179656 | tf_op jit(solution)/shard_map/ppermute | solution.py:558
  82.7 3.2 %collective-permute-start.17 = (f32[8,128]{1,0:T(8,128)S(1)}, f32[8,128]{1,0:T(8,128)S(1)}, u32[]{:S(2)}, u32[]{:S(2)}) collective-permute-start(f32[8,128]{1,0:T(8,128)S(1)} %shard_map.84.refs_5_), channel_id=1, source_target_pairs={{0,12},{4,0},{8,4},{12,8},{1,13},{5,1},{9,5},{13,9},{2,14},{6,2},{... | collective-permute-start | bytes 12296 | tf_op jit(solution)/shard_map/ppermute | solution.py:263
  89.5 3.6 %shard_map.85 = (bf16[512,128]{1,0:T(8,128)(2,1)S(1)}, bf16[1024,384]{1,0:T(8,128)(2,1)S(1)}) custom-call(s32[3]{0:T(128)S(1)} %pad_add_fusion.refs_0_, bf16[512,384]{1,0:T(8,128)(2,1)S(1)} %collective-permute-done.8.refs_1_, bf16[512,384]{1,0:T(8,128)(2,1)S(1)} %collective-permute-done.14.refs_2_, f32[512,384]{1,0:T(8,128)S(1)} %shard_map.82.refs_3_, ...), custom_call_target="tpu_custom_call" | custom-call | flops 134217728 | bytes 3817472 | tf_op jit(solution)/shard_map/pallas_call | solution.py:141
  98.5 3.3 %shard_map.86.refs_6_.refs_1_ = bf16[512,128]{1,0:T(8,128)(2,1)S(1)} custom-call(s32[3]{0:T(128)S(1)} %pad_add_fusion.refs_0_, bf16[1024,384]{1,0:T(8,128)(2,1)S(1)} %get-tuple-element.76.refs_1_, f32[2,64,1024]{2,1,0:T(8,128)S(1)} %shard_map.74.refs_5_.refs_9_.refs_2_), custom_call_target="tpu_custom_call" | custom-call | flops 134217728 | bytes 1441792 | tf_op jit(solution)/shard_map/pallas_call | solution.py:141
  101.9 4.1 %collective-permute-done.19.refs_3_ = bf16[512,128]{1,0:T(8,128)(2,1)S(1)} collective-permute-done((bf16[512,128]{1,0:T(8,128)(2,1)S(1)}, bf16[512,128]{1,0:T(8,128)(2,1)S(1)}, u32[]{:S(2)}, u32[]{:S(2)}) %collective-permute-start.19) | collective-permute-done | bytes 131104 | tf_op jit(solution)/shard_map/ppermute | solution.py:263
  108.6 3.2 %collective-permute-start.27 = (bf16[512,128]{1,0:T(8,128)(2,1)S(1)}, bf16[512,128]{1,0:T(8,128)(2,1)S(1)}, u32[]{:S(2)}, u32[]{:S(2)}) collective-permute-start(bf16[512,128]{1,0:T(8,128)(2,1)S(1)} %shard_map.86.refs_6_.refs_1_), channel_id=1, source_target_pairs={{0,4},{4,8},{8,12},{12,0},{1,5},{5,9},{9,13},{13,1},{2,6},{6,10},{... | collective-permute-start | bytes 393224 | tf_op jit(solution)/shard_map/ppermute | solution.py:263
  117.0 5.3 %collective-permute-done.28.refs_3_ = bf16[512,128]{1,0:T(8,128)(2,1)S(1)} collective-permute-done((bf16[512,128]{1,0:T(8,128)(2,1)S(1)}, bf16[512,128]{1,0:T(8,128)(2,1)S(1)}, u32[]{:S(2)}, u32[]{:S(2)}) %collective-permute-start.28) | collective-permute-done | bytes 131104 | tf_op jit(solution)/shard_map/ppermute | solution.py:263
  125.0 3.6 %collective-permute-done.22.refs_4_ = bf16[512,512]{1,0:T(8,128)(2,1)S(1)} collective-permute-done((bf16[512,512]{1,0:T(8,128)(2,1)S(1)}, bf16[512,512]{1,0:T(8,128)(2,1)S(1)}, u32[]{:S(2)}, u32[]{:S(2)}) %collective-permute-start.22) | collective-permute-done | bytes 524320 | tf_op jit(solution)/shard_map/ppermute | solution.py:126
  134.1 10.4 %collective-permute-done.31.refs_4_ = bf16[512,512]{1,0:T(8,128)(2,1)S(1)} collective-permute-done((bf16[512,512]{1,0:T(8,128)(2,1)S(1)}, bf16[512,512]{1,0:T(8,128)(2,1)S(1)}, u32[]{:S(2)}, u32[]{:S(2)}) %collective-permute-start.31) | collective-permute-done | bytes 524320 | tf_op jit(solution)/shard_map/ppermute | solution.py:126
  151.7 7.5 %collective-permute-done.24.refs_2_ = bf16[512,384]{1,0:T(8,128)(2,1)S(1)} collective-permute-done((bf16[512,384]{1,0:T(8,128)(2,1)S(1)}, bf16[512,384]{1,0:T(8,128)(2,1)S(1)}, u32[]{:S(2)}, u32[]{:S(2)}) %collective-permute-start.24) | collective-permute-done | bytes 393248 | tf_op jit(solution)/shard_map/ppermute | solution.py:558
  161.7 5.9 %collective-permute-done.33.refs_2_ = bf16[512,384]{1,0:T(8,128)(2,1)S(1)} collective-permute-done((bf16[512,384]{1,0:T(8,128)(2,1)S(1)}, bf16[512,384]{1,0:T(8,128)(2,1)S(1)}, u32[]{:S(2)}, u32[]{:S(2)}) %collective-permute-start.33) | collective-permute-done | bytes 393248 | tf_op jit(solution)/shard_map/ppermute | solution.py:558
  170.8 5.3 %collective-permute-done.25.refs_2_ = bf16[512,384]{1,0:T(8,128)(2,1)S(1)} collective-permute-done((bf16[512,384]{1,0:T(8,128)(2,1)S(1)}, bf16[512,384]{1,0:T(8,128)(2,1)S(1)}, u32[]{:S(2)}, u32[]{:S(2)}) %collective-permute-start.25) | collective-permute-done | bytes 393248 | tf_op jit(solution)/shard_map/ppermute | solution.py:558
  178.6 5.9 %collective-permute-done.34.refs_2_ = bf16[512,384]{1,0:T(8,128)(2,1)S(1)} collective-permute-done((bf16[512,384]{1,0:T(8,128)(2,1)S(1)}, bf16[512,384]{1,0:T(8,128)(2,1)S(1)}, u32[]{:S(2)}, u32[]{:S(2)}) %collective-permute-start.34) | collective-permute-done | bytes 393248 | tf_op jit(solution)/shard_map/ppermute | solution.py:558
  197.7 3.4 %collective-permute-done.36.refs_6_ = f32[8,128]{1,0:T(8,128)S(1)} collective-permute-done((f32[8,128]{1,0:T(8,128)S(1)}, f32[8,128]{1,0:T(8,128)S(1)}, u32[]{:S(2)}, u32[]{:S(2)}) %collective-permute-start.36) | collective-permute-done | bytes 4128 | tf_op jit(solution)/shard_map/ppermute | solution.py:263
  201.2 3.6 %shard_map.102 = (bf16[512,128]{1,0:T(8,128)(2,1)S(1)}, bf16[1024,384]{1,0:T(8,128)(2,1)S(1)}) custom-call(s32[3]{0:T(128)S(1)} %pad_add_fusion.refs_0_, bf16[512,384]{1,0:T(8,128)(2,1)S(1)} %collective-permute-done.26.refs_1_, bf16[512,384]{1,0:T(8,128)(2,1)S(1)} %collective-permute-done.35.refs_2_, f32[512,384]{1,0:T(8,128)S(1)} %shard_map.99.refs_3_, ...), custom_call_target="tpu_custom_call" | custom-call | flops 134217728 | bytes 3817472 | tf_op jit(solution)/shard_map/pallas_call | solution.py:141
  208.7 3.3 %shard_map.103.refs_6_.refs_1_ = bf16[512,128]{1,0:T(8,128)(2,1)S(1)} custom-call(s32[3]{0:T(128)S(1)} %pad_add_fusion.refs_0_, bf16[1024,384]{1,0:T(8,128)(2,1)S(1)} %get-tuple-element.90.refs_1_, f32[2,64,1024]{2,1,0:T(8,128)S(1)} %shard_map.74.refs_5_.refs_9_.refs_2_), custom_call_target="tpu_custom_call" | custom-call | flops 134217728 | bytes 1441792 | tf_op jit(solution)/shard_map/pallas_call | solution.py:141
  213.1 4.6 %collective-permute-done.40.refs_3_ = bf16[512,128]{1,0:T(8,128)(2,1)S(1)} collective-permute-done((bf16[512,128]{1,0:T(8,128)(2,1)S(1)}, bf16[512,128]{1,0:T(8,128)(2,1)S(1)}, u32[]{:S(2)}, u32[]{:S(2)}) %collective-permute-start.40) | collective-permute-done | bytes 131104 | tf_op jit(solution)/shard_map/ppermute | solution.py:263
  220.3 2.8 %collective-permute-start.50 = (bf16[512,128]{1,0:T(8,128)(2,1)S(1)}, bf16[512,128]{1,0:T(8,128)(2,1)S(1)}, u32[]{:S(2)}, u32[]{:S(2)}) collective-permute-start(bf16[512,128]{1,0:T(8,128)(2,1)S(1)} %shard_map.103.refs_6_.refs_1_), channel_id=1, source_target_pairs={{0,4},{4,8},{8,12},{12,0},{1,5},{5,9},{9,13},{13,1},{2,6},{6,10},{... | collective-permute-start | bytes 393224 | tf_op jit(solution)/shard_map/ppermute | solution.py:263
  228.6 5.1 %collective-permute-done.51.refs_3_ = bf16[512,128]{1,0:T(8,128)(2,1)S(1)} collective-permute-done((bf16[512,128]{1,0:T(8,128)(2,1)S(1)}, bf16[512,128]{1,0:T(8,128)(2,1)S(1)}, u32[]{:S(2)}, u32[]{:S(2)}) %collective-permute-start.51) | collective-permute-done | bytes 131104 | tf_op jit(solution)/shard_map/ppermute | solution.py:263
  240.4 5.1 %collective-permute-done.43.refs_3_ = bf16[512,256]{1,0:T(8,128)(2,1)S(1)} collective-permute-done((bf16[512,256]{1,0:T(8,128)(2,1)S(1)}, bf16[512,256]{1,0:T(8,128)(2,1)S(1)}, u32[]{:S(2)}, u32[]{:S(2)}) %collective-permute-start.43) | collective-permute-done | bytes 262176 | tf_op jit(solution)/shard_map/ppermute | solution.py:126
  246.2 3.3 %collective-permute-start.44 = (bf16[128,256]{1,0:T(8,128)(2,1)S(1)}, bf16[128,256]{1,0:T(8,128)(2,1)S(1)}, u32[]{:S(2)}, u32[]{:S(2)}) collective-permute-start(bf16[128,256]{1,0:T(8,128)(2,1)S(1)} %get-tuple-element.96), channel_id=1, source_target_pairs={{0,4},{4,8},{8,12},{12,0},{1,5},{5,9},{9,13},{13,1},{2,6},{6,10},{... | collective-permute-start | bytes 196616 | tf_op jit(solution)/shard_map/ppermute | solution.py:263
  263.4 2.7 collective-permute-done.47.refs_2_
  266.6 3.9 %collective-permute-done.58.refs_6_ = bf16[512,256]{1,0:T(8,128)(2,1)S(1)} collective-permute-done((bf16[512,256]{1,0:T(8,128)(2,1)S(1)}, bf16[512,256]{1,0:T(8,128)(2,1)S(1)}, u32[]{:S(2)}, u32[]{:S(2)}) %collective-permute-start.58) | collective-permute-done | bytes 262176 | tf_op jit(solution)/shard_map/ppermute | solution.py:126
  (136 shorter events, 130.0 us)
Async XLA Ops:
  1.8 9.6 %collective-permute-start = (bf16[256,256]{1,0:T(8,128)(2,1)S(1)}, bf16[256,256]{1,0:T(8,128)(2,1)S(1)}, u32[]{:S(2)}, u32[]{:S(2)}) collective-permute-start(bf16[256,256]{1,0:T(8,128)(2,1)S(1)} %get-tuple-element.57), channel_id=1, source_target_pairs={{0,4},{4,8},{8,12},{12,0},{1,5},{5,9},{9,13},{13,1},{2,6},{6,10},{... | collective-permute-start | bytes 393224 | tf_op jit(solution)/shard_map/ppermute | solution.py:263
  4.9 11.2 %collective-permute-start.1 = (bf16[256,256]{1,0:T(8,128)(2,1)S(1)}, bf16[256,256]{1,0:T(8,128)(2,1)S(1)}, u32[]{:S(2)}, u32[]{:S(2)}) collective-permute-start(bf16[256,256]{1,0:T(8,128)(2,1)S(1)} %get-tuple-element.58), channel_id=1, source_target_pairs={{0,8},{4,12},{8,0},{12,4},{1,9},{5,13},{9,1},{13,5},{2,10},{6,14},... | collective-permute-start | bytes 393224 | tf_op jit(solution)/shard_map/ppermute | solution.py:263
  24.9 8.7 %collective-permute-start.9 = (bf16[512,256]{1,0:T(8,128)(2,1)S(1)}, bf16[512,256]{1,0:T(8,128)(2,1)S(1)}, u32[]{:S(2)}, u32[]{:S(2)}) collective-permute-start(bf16[512,256]{1,0:T(8,128)(2,1)S(1)} %get-tuple-element.71.refs_1_.refs_5_), channel_id=1, source_target_pairs={{0,2},{1,3},{2,0},{3,1},{4,6},{5,7},{6,4},{7,5},{8,10},{9,11},{10,... | collective-permute-start | bytes 786440 | tf_op jit(solution)/shard_map/ppermute | solution.py:126
  26.4 10.6 %collective-permute-start.10 = (bf16[512,256]{1,0:T(8,128)(2,1)S(1)}, bf16[512,256]{1,0:T(8,128)(2,1)S(1)}, u32[]{:S(2)}, u32[]{:S(2)}) collective-permute-start(bf16[512,256]{1,0:T(8,128)(2,1)S(1)} %get-tuple-element.71.refs_1_.refs_5_), channel_id=1, source_target_pairs={{0,1},{1,0},{2,3},{3,2},{4,5},{5,4},{6,7},{7,6},{8,9},{9,8},{10,11... | collective-permute-start | bytes 786440 | tf_op jit(solution)/shard_map/ppermute | solution.py:126
  33.6 13.8 %collective-permute-start.6 = (bf16[512,384]{1,0:T(8,128)(2,1)S(1)}, bf16[512,384]{1,0:T(8,128)(2,1)S(1)}, u32[]{:S(2)}, u32[]{:S(2)}) collective-permute-start(bf16[512,384]{1,0:T(8,128)(2,1)S(1)} %get-tuple-element.62), channel_id=1, source_target_pairs={{0,4},{4,8},{8,12},{12,0},{1,5},{5,9},{9,13},{13,1},{2,6},{6,10},{... | collective-permute-start | bytes 1179656 | tf_op jit(solution)/shard_map/ppermute | solution.py:558
  39.4 16.4 %collective-permute-start.12 = (bf16[512,384]{1,0:T(8,128)(2,1)S(1)}, bf16[512,384]{1,0:T(8,128)(2,1)S(1)}, u32[]{:S(2)}, u32[]{:S(2)}) collective-permute-start(bf16[512,384]{1,0:T(8,128)(2,1)S(1)} %get-tuple-element.66), channel_id=1, source_target_pairs={{0,12},{4,0},{8,4},{12,8},{1,13},{5,1},{9,5},{13,9},{2,14},{6,2},{... | collective-permute-start | bytes 1179656 | tf_op jit(solution)/shard_map/ppermute | solution.py:558
  49.9 14.5 %collective-permute-start.7 = (bf16[512,384]{1,0:T(8,128)(2,1)S(1)}, bf16[512,384]{1,0:T(8,128)(2,1)S(1)}, u32[]{:S(2)}, u32[]{:S(2)}) collective-permute-start(bf16[512,384]{1,0:T(8,128)(2,1)S(1)} %shard_map.77), channel_id=1, source_target_pairs={{0,4},{4,8},{8,12},{12,0},{1,5},{5,9},{9,13},{13,1},{2,6},{6,10},{... | collective-permute-start | bytes 1179656 | tf_op jit(solution)/shard_map/ppermute | solution.py:558
  58.2 14.5 %collective-permute-start.13 = (bf16[512,384]{1,0:T(8,128)(2,1)S(1)}, bf16[512,384]{1,0:T(8,128)(2,1)S(1)}, u32[]{:S(2)}, u32[]{:S(2)}) collective-permute-start(bf16[512,384]{1,0:T(8,128)(2,1)S(1)} %shard_map.80), channel_id=1, source_target_pairs={{0,12},{4,0},{8,4},{12,8},{1,13},{5,1},{9,5},{13,9},{2,14},{6,2},{... | collective-permute-start | bytes 1179656 | tf_op jit(solution)/shard_map/ppermute | solution.py:558
  66.8 22.7 %collective-permute-start.8 = (bf16[512,384]{1,0:T(8,128)(2,1)S(1)}, bf16[512,384]{1,0:T(8,128)(2,1)S(1)}, u32[]{:S(2)}, u32[]{:S(2)}) collective-permute-start(bf16[512,384]{1,0:T(8,128)(2,1)S(1)} %shard_map.78), channel_id=1, source_target_pairs={{0,4},{4,8},{8,12},{12,0},{1,5},{5,9},{9,13},{13,1},{2,6},{6,10},{... | collective-permute-start | bytes 1179656 | tf_op jit(solution)/shard_map/ppermute | solution.py:558
  75.1 14.3 %collective-permute-start.14 = (bf16[512,384]{1,0:T(8,128)(2,1)S(1)}, bf16[512,384]{1,0:T(8,128)(2,1)S(1)}, u32[]{:S(2)}, u32[]{:S(2)}) collective-permute-start(bf16[512,384]{1,0:T(8,128)(2,1)S(1)} %shard_map.81), channel_id=1, source_target_pairs={{0,12},{4,0},{8,4},{12,8},{1,13},{5,1},{9,5},{13,9},{2,14},{6,2},{... | collective-permute-start | bytes 1179656 | tf_op jit(solution)/shard_map/ppermute | solution.py:558
  93.1 8.8 %collective-permute-start.18 = (bf16[512,128]{1,0:T(8,128)(2,1)S(1)}, bf16[512,128]{1,0:T(8,128)(2,1)S(1)}, u32[]{:S(2)}, u32[]{:S(2)}) collective-permute-start(bf16[512,128]{1,0:T(8,128)(2,1)S(1)} %get-tuple-element.75.refs_1_), channel_id=1, source_target_pairs={{0,4},{4,8},{8,12},{12,0},{1,5},{5,9},{9,13},{13,1},{2,6},{6,10},{... | collective-permute-start | bytes 393224 | tf_op jit(solution)/shard_map/ppermute | solution.py:263
  94.7 11.3 %collective-permute-start.19 = (bf16[512,128]{1,0:T(8,128)(2,1)S(1)}, bf16[512,128]{1,0:T(8,128)(2,1)S(1)}, u32[]{:S(2)}, u32[]{:S(2)}) collective-permute-start(bf16[512,128]{1,0:T(8,128)(2,1)S(1)} %get-tuple-element.75.refs_1_), channel_id=1, source_target_pairs={{0,8},{4,12},{8,0},{12,4},{1,9},{5,13},{9,1},{13,5},{2,10},{6,14},... | collective-permute-start | bytes 393224 | tf_op jit(solution)/shard_map/ppermute | solution.py:263
  97.1 8.9 %collective-permute-start.20 = (bf16[512,128]{1,0:T(8,128)(2,1)S(1)}, bf16[512,128]{1,0:T(8,128)(2,1)S(1)}, u32[]{:S(2)}, u32[]{:S(2)}) collective-permute-start(bf16[512,128]{1,0:T(8,128)(2,1)S(1)} %get-tuple-element.75.refs_1_), channel_id=1, source_target_pairs={{0,12},{4,0},{8,4},{12,8},{1,13},{5,1},{9,5},{13,9},{2,14},{6,2},{... | collective-permute-start | bytes 393224 | tf_op jit(solution)/shard_map/ppermute | solution.py:263
  111.8 10.6 %collective-permute-start.28 = (bf16[512,128]{1,0:T(8,128)(2,1)S(1)}, bf16[512,128]{1,0:T(8,128)(2,1)S(1)}, u32[]{:S(2)}, u32[]{:S(2)}) collective-permute-start(bf16[512,128]{1,0:T(8,128)(2,1)S(1)} %shard_map.86.refs_6_.refs_1_), channel_id=1, source_target_pairs={{0,8},{4,12},{8,0},{12,4},{1,9},{5,13},{9,1},{13,5},{2,10},{6,14},... | collective-permute-start | bytes 393224 | tf_op jit(solution)/shard_map/ppermute | solution.py:263
  113.1 9.2 %collective-permute-start.29 = (bf16[512,128]{1,0:T(8,128)(2,1)S(1)}, bf16[512,128]{1,0:T(8,128)(2,1)S(1)}, u32[]{:S(2)}, u32[]{:S(2)}) collective-permute-start(bf16[512,128]{1,0:T(8,128)(2,1)S(1)} %shard_map.86.refs_6_.refs_1_), channel_id=1, source_target_pairs={{0,12},{4,0},{8,4},{12,8},{1,13},{5,1},{9,5},{13,9},{2,14},{6,2},{... | collective-permute-start | bytes 393224 | tf_op jit(solution)/shard_map/ppermute | solution.py:263
  114.9 13.7 %collective-permute-start.22 = (bf16[512,512]{1,0:T(8,128)(2,1)S(1)}, bf16[512,512]{1,0:T(8,128)(2,1)S(1)}, u32[]{:S(2)}, u32[]{:S(2)}) collective-permute-start(bf16[512,512]{1,0:T(8,128)(2,1)S(1)} %shard_map.88.refs_3_.refs_6_), channel_id=1, source_target_pairs={{0,2},{1,3},{2,0},{3,1},{4,6},{5,7},{6,4},{7,5},{8,10},{9,11},{10,... | collective-permute-start | bytes 1572872 | tf_op jit(solution)/shard_map/ppermute | solution.py:126
  130.1 14.4 %collective-permute-start.31 = (bf16[512,512]{1,0:T(8,128)(2,1)S(1)}, bf16[512,512]{1,0:T(8,128)(2,1)S(1)}, u32[]{:S(2)}, u32[]{:S(2)}) collective-permute-start(bf16[512,512]{1,0:T(8,128)(2,1)S(1)} %shard_map.94.refs_3_), channel_id=1, source_target_pairs={{0,2},{1,3},{2,0},{3,1},{4,6},{5,7},{6,4},{7,5},{8,10},{9,11},{10,... | collective-permute-start | bytes 1572872 | tf_op jit(solution)/shard_map/ppermute | solution.py:126
  145.3 13.9 %collective-permute-start.24 = (bf16[512,384]{1,0:T(8,128)(2,1)S(1)}, bf16[512,384]{1,0:T(8,128)(2,1)S(1)}, u32[]{:S(2)}, u32[]{:S(2)}) collective-permute-start(bf16[512,384]{1,0:T(8,128)(2,1)S(1)} %get-tuple-element.80.refs_5_), channel_id=1, source_target_pairs={{0,4},{4,8},{8,12},{12,0},{1,5},{5,9},{9,13},{13,1},{2,6},{6,10},{... | collective-permute-start | bytes 1179656 | tf_op jit(solution)/shard_map/ppermute | solution.py:558
  149.6 17.9 %collective-permute-start.33 = (bf16[512,384]{1,0:T(8,128)(2,1)S(1)}, bf16[512,384]{1,0:T(8,128)(2,1)S(1)}, u32[]{:S(2)}, u32[]{:S(2)}) collective-permute-start(bf16[512,384]{1,0:T(8,128)(2,1)S(1)} %get-tuple-element.84), channel_id=1, source_target_pairs={{0,12},{4,0},{8,4},{12,8},{1,13},{5,1},{9,5},{13,9},{2,14},{6,2},{... | collective-permute-start | bytes 1179656 | tf_op jit(solution)/shard_map/ppermute | solution.py:558
  161.6 14.5 %collective-permute-start.25 = (bf16[512,384]{1,0:T(8,128)(2,1)S(1)}, bf16[512,384]{1,0:T(8,128)(2,1)S(1)}, u32[]{:S(2)}, u32[]{:S(2)}) collective-permute-start(bf16[512,384]{1,0:T(8,128)(2,1)S(1)} %shard_map.91), channel_id=1, source_target_pairs={{0,4},{4,8},{8,12},{12,0},{1,5},{5,9},{9,13},{13,1},{2,6},{6,10},{... | collective-permute-start | bytes 1179656 | tf_op jit(solution)/shard_map/ppermute | solution.py:558
  169.9 14.5 %collective-permute-start.34 = (bf16[512,384]{1,0:T(8,128)(2,1)S(1)}, bf16[512,384]{1,0:T(8,128)(2,1)S(1)}, u32[]{:S(2)}, u32[]{:S(2)}) collective-permute-start(bf16[512,384]{1,0:T(8,128)(2,1)S(1)} %shard_map.97), channel_id=1, source_target_pairs={{0,12},{4,0},{8,4},{12,8},{1,13},{5,1},{9,5},{13,9},{2,14},{6,2},{... | collective-permute-start | bytes 1179656 | tf_op jit(solution)/shard_map/ppermute | solution.py:558
  178.5 22.7 %collective-permute-start.26 = (bf16[512,384]{1,0:T(8,128)(2,1)S(1)}, bf16[512,384]{1,0:T(8,128)(2,1)S(1)}, u32[]{:S(2)}, u32[]{:S(2)}) collective-permute-start(bf16[512,384]{1,0:T(8,128)(2,1)S(1)} %shard_map.92), channel_id=1, source_target_pairs={{0,4},{4,8},{8,12},{12,0},{1,5},{5,9},{9,13},{13,1},{2,6},{6,10},{... | collective-permute-start | bytes 1179656 | tf_op jit(solution)/shard_map/ppermute | solution.py:558
  186.8 14.3 %collective-permute-start.35 = (bf16[512,384]{1,0:T(8,128)(2,1)S(1)}, bf16[512,384]{1,0:T(8,128)(2,1)S(1)}, u32[]{:S(2)}, u32[]{:S(2)}) collective-permute-start(bf16[512,384]{1,0:T(8,128)(2,1)S(1)} %shard_map.98), channel_id=1, source_target_pairs={{0,12},{4,0},{8,4},{12,8},{1,13},{5,1},{9,5},{13,9},{2,14},{6,2},{... | collective-permute-start | bytes 1179656 | tf_op jit(solution)/shard_map/ppermute | solution.py:558
  191.1 10.0 %collective-permute-start.36 = (f32[8,128]{1,0:T(8,128)S(1)}, f32[8,128]{1,0:T(8,128)S(1)}, u32[]{:S(2)}, u32[]{:S(2)}) collective-permute-start(f32[8,128]{1,0:T(8,128)S(1)} %shard_map.101.refs_5_), channel_id=1, source_target_pairs={{0,4},{4,8},{8,12},{12,0},{1,5},{5,9},{9,13},{13,1},{2,6},{6,10},{... | collective-permute-start | bytes 12296 | tf_op jit(solution)/shard_map/ppermute | solution.py:263
  192.4 8.7 %collective-permute-start.37 = (f32[8,128]{1,0:T(8,128)S(1)}, f32[8,128]{1,0:T(8,128)S(1)}, u32[]{:S(2)}, u32[]{:S(2)}) collective-permute-start(f32[8,128]{1,0:T(8,128)S(1)} %shard_map.101.refs_5_), channel_id=1, source_target_pairs={{0,8},{4,12},{8,0},{12,4},{1,9},{5,13},{9,1},{13,5},{2,10},{6,14},... | collective-permute-start | bytes 12296 | tf_op jit(solution)/shard_map/ppermute | solution.py:263
  205.4 12.2 %collective-permute-start.40 = (bf16[512,128]{1,0:T(8,128)(2,1)S(1)}, bf16[512,128]{1,0:T(8,128)(2,1)S(1)}, u32[]{:S(2)}, u32[]{:S(2)}) collective-permute-start(bf16[512,128]{1,0:T(8,128)(2,1)S(1)} %get-tuple-element.89.refs_1_), channel_id=1, source_target_pairs={{0,8},{4,12},{8,0},{12,4},{1,9},{5,13},{9,1},{13,5},{2,10},{6,14},... | collective-permute-start | bytes 393224 | tf_op jit(solution)/shard_map/ppermute | solution.py:263
  206.2 11.5 %collective-permute-start.41 = (bf16[512,128]{1,0:T(8,128)(2,1)S(1)}, bf16[512,128]{1,0:T(8,128)(2,1)S(1)}, u32[]{:S(2)}, u32[]{:S(2)}) collective-permute-start(bf16[512,128]{1,0:T(8,128)(2,1)S(1)} %get-tuple-element.89.refs_1_), channel_id=1, source_target_pairs={{0,12},{4,0},{8,4},{12,8},{1,13},{5,1},{9,5},{13,9},{2,14},{6,2},{... | collective-permute-start | bytes 393224 | tf_op jit(solution)/shard_map/ppermute | solution.py:263
  223.1 10.6 %collective-permute-start.51 = (bf16[512,128]{1,0:T(8,128)(2,1)S(1)}, bf16[512,128]{1,0:T(8,128)(2,1)S(1)}, u32[]{:S(2)}, u32[]{:S(2)}) collective-permute-start(bf16[512,128]{1,0:T(8,128)(2,1)S(1)} %shard_map.103.refs_6_.refs_1_), channel_id=1, source_target_pairs={{0,8},{4,12},{8,0},{12,4},{1,9},{5,13},{9,1},{13,5},{2,10},{6,14},... | collective-permute-start | bytes 393224 | tf_op jit(solution)/shard_map/ppermute | solution.py:263
  223.3 10.4 %collective-permute-start.52 = (bf16[512,128]{1,0:T(8,128)(2,1)S(1)}, bf16[512,128]{1,0:T(8,128)(2,1)S(1)}, u32[]{:S(2)}, u32[]{:S(2)}) collective-permute-start(bf16[512,128]{1,0:T(8,128)(2,1)S(1)} %shard_map.103.refs_6_.refs_1_), channel_id=1, source_target_pairs={{0,12},{4,0},{8,4},{12,8},{1,13},{5,1},{9,5},{13,9},{2,14},{6,2},{... | collective-permute-start | bytes 393224 | tf_op jit(solution)/shard_map/ppermute | solution.py:263
  236.3 9.2 %collective-permute-start.43 = (bf16[512,256]{1,0:T(8,128)(2,1)S(1)}, bf16[512,256]{1,0:T(8,128)(2,1)S(1)}, u32[]{:S(2)}, u32[]{:S(2)}) collective-permute-start(bf16[512,256]{1,0:T(8,128)(2,1)S(1)} %get-tuple-element.94.refs_6_), channel_id=1, source_target_pairs={{0,2},{1,3},{2,0},{3,1},{4,6},{5,7},{6,4},{7,5},{8,10},{9,11},{10,... | collective-permute-start | bytes 786440 | tf_op jit(solution)/shard_map/ppermute | solution.py:126
  238.9 13.1 %collective-permute-start.54 = (bf16[512,256]{1,0:T(8,128)(2,1)S(1)}, bf16[512,256]{1,0:T(8,128)(2,1)S(1)}, u32[]{:S(2)}, u32[]{:S(2)}) collective-permute-start(bf16[512,256]{1,0:T(8,128)(2,1)S(1)} %get-tuple-element.102), channel_id=1, source_target_pairs={{0,2},{1,3},{2,0},{3,1},{4,6},{5,7},{6,4},{7,5},{8,10},{9,11},{10,... | collective-permute-start | bytes 786440 | tf_op jit(solution)/shard_map/ppermute | solution.py:126
  246.2 10.0 %collective-permute-start.44 = (bf16[128,256]{1,0:T(8,128)(2,1)S(1)}, bf16[128,256]{1,0:T(8,128)(2,1)S(1)}, u32[]{:S(2)}, u32[]{:S(2)}) collective-permute-start(bf16[128,256]{1,0:T(8,128)(2,1)S(1)} %get-tuple-element.96), channel_id=1, source_target_pairs={{0,4},{4,8},{8,12},{12,0},{1,5},{5,9},{9,13},{13,1},{2,6},{6,10},{... | collective-permute-start | bytes 196616 | tf_op jit(solution)/shard_map/ppermute | solution.py:263
  (31 other events, 208.6 us)

commit v5 on v4

--- a/solution.py
+++ b/solution.py
@@ -195,25 +195,6 @@
     )[0]
 
 
-def squares_of(halves, place):
-    flat = [piece for pieces in halves for piece in pieces]
-    count = len(halves[0])
-    runs = halves[0][0].shape[0] // HD
-
-    def body(place_ref, *refs):
-        out_ref = refs[-1]
-        for index in range(len(halves)):
-            for run in range(runs):
-                total = jnp.zeros((HD, HD), jnp.float32)
-                for ref in refs[index * count : (index + 1) * count]:
-                    for lane in range(ref.shape[1] // HD):
-                        part = ref[pl.ds(run * HD, HD), pl.ds(lane * HD, HD)].astype(jnp.float32)
-                        total += part * part
-                out_ref[pl.ds(index * runs + run, 1), :] = jnp.sum(total.T, axis=0, keepdims=True)
-
-    return local_kernel(body, place, flat, [shaped(len(halves) * runs, HD, dtype=jnp.float32)])[0]
-
-
 def scatter_tokens(tokens, place, sp_count, feats, piece):
     tok_here = tokens.shape[0]
 
@@ -275,57 +256,123 @@
         out_ref[:, span] = (piece_ref[...].astype(jnp.float32) * factor).astype(jnp.bfloat16)
 
 
-def project(source, weights, layer, place, chunk_shift, width, arrived=None, last=False):
-    fresh = isinstance(source, tuple)
-    feats = weights[0].shape[1]
-    sp_count = lax.axis_size("sp")
-    arrays = (*source[0], source[2]) if fresh else (source,)
-    tok = arrays[0].shape[0]
-    if arrived is not None:
-        arrays += (arrived,)
-    count = len(arrays)
+def stage_weights(weights, layer, place, sp_count):
+    feats, every_width = weights[0].shape[1:]
+    width = every_width // sp_count
+    count = len(weights)
 
     def body(place_ref, *refs):
-        array_refs, weight_refs, refs = refs[:count], refs[count : count + 3], refs[count + 3 :]
-        out_ref, held, sem = refs[0], refs[-2], refs[-1]
-        chunk = lax.rem(place_ref[0] + chunk_shift, sp_count)
+        weight_refs, (out_ref, sem) = refs[:count], refs[count:]
         copies = []
-        for index, weight_ref in enumerate(weight_refs):
-            copy = pltpu.make_async_copy(
-                weight_ref.at[layer, :, aligned(chunk, width)],
-                held.at[:, pl.ds(index * width, width)],
-                sem.at[index],
-            )
-            copy.start()
-            copies.append(copy)
-        scaled_ref = array_refs[0]
-        if fresh:
-            scaled_ref = refs[1]
-            pieces, slots, _ = source
-            scaled_by(
-                slots, layer, feats, place_ref,
-                array_refs[: len(pieces)], array_refs[len(pieces)], scaled_ref,
-            )
+        for chunk in range(sp_count):
+            for index, weight_ref in enumerate(weight_refs):
+                copy = pltpu.make_async_copy(
+                    weight_ref.at[layer, :, pl.ds(chunk * width, width)],
+                    out_ref.at[chunk, :, pl.ds(index * width, width)],
+                    sem.at[chunk, index],
+                )
+                copy.start()
+                copies.append(copy)
         for copy in copies:
             copy.wait()
-        total = jnp.dot(scaled_ref[...], held[...], preferred_element_type=jnp.float32)
-        if arrived is not None:
-            total += array_refs[-1][...].astype(jnp.float32)
-        out_ref[...] = total.astype(out_ref.dtype)
-
-    outs = [shaped(tok, 3 * width, dtype=jnp.float32 if last else jnp.bfloat16)]
+
     return local_kernel(
         body,
         place,
-        arrays,
-        outs + [shaped(tok, feats)] * fresh,
-        scratch=[
-            pltpu.VMEM((feats, 3 * width), jnp.bfloat16),
-            pltpu.SemaphoreType.DMA((3,)),
-        ],
+        (),
+        [shaped(sp_count, feats, count * width)],
+        scratch=[pltpu.SemaphoreType.DMA((sp_count, count))],
         hbm=weights,
-        flops=2 * tok * feats * 3 * width,
-    )
+    )[0]
+
+
+EXTRA = 16
+
+
+def put_squares(out_ref, squares, tok):
+    for term in range(3):
+        part = squares.astype(jnp.bfloat16)
+        out_ref[pl.ds(tok, EXTRA), pl.ds(term * HD, HD)] = part
+        squares = squares - part.astype(jnp.float32)
+
+
+def get_squares(ref, tok):
+    terms = [ref[pl.ds(tok, EXTRA), pl.ds(term * HD, HD)].astype(jnp.float32) for term in range(3)]
+    return terms[0] + (terms[1] + terms[2])
+
+
+def share(source, staged, layer, place, link, message, arrived=None):
+    fresh = len(source) == 3
+    sp_count, feats, total_width = staged.shape
+    arrays = (*source[0], source[2]) if fresh else source
+    tok = arrays[0].shape[0]
+    count = len(arrays)
+    inputs = (*arrays, staged) + (() if arrived is None else (arrived,))
+
+    def body(place_ref, *refs):
+        array_refs, staged_ref = refs[:count], refs[count]
+        out_ref = refs[len(inputs)]
+        if fresh:
+            scaled_ref, squares_ref = refs[len(inputs) + 1 :]
+            pieces, slots, _ = source
+            scaled_by(
+                slots,
+                layer,
+                feats,
+                place_ref,
+                array_refs[: len(pieces)],
+                array_refs[len(pieces)],
+                scaled_ref,
+            )
+            squares_ref[...] = jnp.zeros_like(squares_ref)
+            for run in range(tok // HD):
+                total = jnp.zeros((HD, HD), jnp.float32)
+                for ref in array_refs[: len(pieces)]:
+                    for lane in range(ref.shape[1] // HD):
+                        part = ref[pl.ds(run * HD, HD), pl.ds(lane * HD, HD)].astype(jnp.float32)
+                        total += part * part
+                squares_ref[pl.ds(run, 1), :] = jnp.sum(total.T, axis=0, keepdims=True)
+        else:
+            scaled_ref, squares_ref = array_refs
+        forward = place_ref[0] == link
+        backward = place_ref[0] == sp_count - 1 - link
+
+        @pl.when(forward | backward)
+        def _():
+            chunk = jnp.where(forward, sp_count - 1 - message, message)
+            total = jnp.dot(
+                scaled_ref[...], staged_ref[chunk], preferred_element_type=jnp.float32
+            )
+            squares = squares_ref[...]
+            if arrived is not None:
+                arrived_ref = refs[count + 1]
+                total += arrived_ref[pl.ds(0, tok), :].astype(jnp.float32)
+                squares += get_squares(arrived_ref, tok)
+            out_ref[pl.ds(0, tok), :] = total.astype(jnp.bfloat16)
+            put_squares(out_ref, squares, tok)
+
+    outs = [shaped(tok + EXTRA, total_width)]
+    if fresh:
+        outs += [shaped(tok, feats), shaped(EXTRA, HD, dtype=jnp.float32)]
+    return local_kernel(body, place, inputs, outs, flops=2 * tok * feats * total_width)
+
+
+def own_share(scaled, staged, place):
+    tok = scaled.shape[0]
+    total_width = staged.shape[2]
+
+    def body(place_ref, scaled_ref, staged_ref, out_ref):
+        out_ref[...] = jnp.dot(
+            scaled_ref[...], staged_ref[place_ref[0]], preferred_element_type=jnp.float32
+        )
+
+    return local_kernel(
+        body,
+        place,
+        (scaled, staged),
+        [shaped(tok, total_width, dtype=jnp.float32)],
+        flops=2 * tok * scaled.shape[1] * total_width,
+    )[0]
 
 
 def attend_rows(qkv_ref, bias_ref, out_ref, part, sp_count, heads, layer):
@@ -356,26 +403,32 @@
             out_ref[pl.ds(index * GRID_W, GRID_W), pl.ds(lanes, HD)] = mixed.astype(jnp.bfloat16)
 
 
-def attend(arrived, own, squares, bias, place, sp_count, heads, layer, every_feat):
-    rows, total_width = arrived[0].shape
+def attend(arrived, own, squares, bias, place, sp_count, heads, layer, every_feat, after):
+    rows, total_width = own[0].shape
     width = heads * HD
     part_rows = rows // sp_count
     runs = rows // HD
     flops = 4 * heads * rows * KR * GRID_W * HD
-
-    def low(place_ref, a0, a1, o0, o1, *refs):
-        square_refs, (bias_ref, out_ref, qkv_ref) = refs[:-3], refs[-3:]
-        norm = lax.rsqrt(total_of(*square_refs) / every_feat + norm_eps)
-        for part, (a_ref, o_ref) in enumerate(((a0, o0), (a1, o1))):
+    count = len(arrived[0])
+
+    def low(place_ref, *refs):
+        arrived_refs, refs = (refs[:count], refs[count : 2 * count]), refs[2 * count :]
+        own_refs, square_refs, (bias_ref, out_ref, qkv_ref) = refs[:2], refs[2:4], refs[4:]
+        for part in range(2):
+            total_squares = square_refs[part][...]
+            for ref in arrived_refs[part]:
+                total_squares += get_squares(ref, rows)
+            norm = lax.rsqrt(total_squares / every_feat + norm_eps)
             for run in range(runs):
-                row = part * runs + run
-                factor = jnp.broadcast_to(norm[row : row + 1, :], (HD, HD)).T
+                factor = jnp.broadcast_to(norm[run : run + 1, :], (HD, HD)).T
                 plane, inner = divmod(run * HD, part_rows)
                 to = pl.ds((2 * plane + part) * part_rows + inner, HD)
                 span = pl.ds(run * HD, HD)
                 for lane in range(total_width // HD):
                     lanes = pl.ds(lane * HD, HD)
-                    total = a_ref[span, lanes].astype(jnp.float32) + o_ref[span, lanes]
+                    total = own_refs[part][span, lanes]
+                    for ref in arrived_refs[part]:
+                        total += ref[span, lanes].astype(jnp.float32)
                     qkv_ref[to, lanes] = (total * factor).astype(jnp.bfloat16)
         attend_rows(qkv_ref, bias_ref, out_ref, 0, sp_count, heads, layer)
 
@@ -385,45 +438,67 @@
     out0, qkv = local_kernel(
         low,
         place,
-        (*arrived, *own, *squares, bias),
+        (*arrived[0], *arrived[1], *own, *squares, bias),
         [shaped(rows, width), shaped(2 * rows, total_width)],
         flops=flops,
+        after=after,
     )
     out1 = local_kernel(high, place, (qkv, bias), [shaped(rows, width)], flops=flops)
     return out0, out1[0]
 
 
+def gathered_on_line(block):
+    count = lax.axis_size("sp")
+    up = [(i, i + 1) for i in range(count - 1)]
+    across = lax.ppermute(block, "sp", ring(count, 2))
+    below = lax.ppermute(block, "sp", up)
+    above = lax.ppermute(block, "sp", [(target, source) for source, target in up])
+    relayed = lax.ppermute(across, "sp", [(count - 2, count - 1), (1, 0)])
+    return block, below, above, across, relayed
+
+
 def spread(attended, w_out, layer, place, after):
-    count = len(attended)
+    sp_count = lax.axis_size("sp")
     rows, width = attended[0].shape
     inner, feats = w_out.shape[1:]
     half = feats // 2
 
-    def body(place_ref, *refs):
-        piece_refs, (w_ref, sent_ref, kept_ref, gathered, held, sem) = refs[:count], refs[count:]
-        copy = pltpu.make_async_copy(w_ref.at[layer], held, sem.at[0])
-        copy.start()
-        for shift in range(count):
-            source = lax.rem(place_ref[0] + count - shift, count)
-            gathered[:, aligned(source, width)] = piece_refs[shift][...]
-        copy.wait()
+    def body(place_ref, own_ref, below_ref, above_ref, across_ref, relayed_ref, w_ref, *rest):
+        sent_ref, kept_ref, gathered = rest
+        here = place_ref[0]
+
+        def put(ref, index):
+            gathered[:, aligned(lax.rem(index + sp_count, sp_count), width)] = ref[...]
+
+        put(own_ref, here)
+        put(across_ref, here + 2)
+
+        @pl.when(here > 0)
+        def _():
+            put(below_ref, here - 1)
+
+        @pl.when(here < sp_count - 1)
+        def _():
+            put(above_ref, here + 1)
+
+        @pl.when((here == 0) | (here == sp_count - 1))
+        def _():
+            put(relayed_ref, sp_count - 1 - here)
+
         core = place_ref[1]
         for index, out_ref in ((1 - core, sent_ref), (core, kept_ref)):
             out_ref[...] = jnp.dot(
-                gathered[...], held[:, aligned(index, half)], preferred_element_type=jnp.float32
+                gathered[...],
+                w_ref[layer, :, aligned(index, half)],
+                preferred_element_type=jnp.float32,
             ).astype(jnp.bfloat16)
 
     return local_kernel(
         body,
         place,
-        attended,
+        (*attended, w_out),
         [shaped(rows, half)] * 2,
-        scratch=[
-            pltpu.VMEM((rows, inner), jnp.bfloat16),
-            pltpu.VMEM((inner, feats), jnp.bfloat16),
-            pltpu.SemaphoreType.DMA((1,)),
-        ],
-        hbm=(w_out,),
+        scratch=[pltpu.VMEM((rows, inner), jnp.bfloat16)],
         flops=2 * rows * inner * feats,
         after=after,
     )
@@ -532,72 +607,89 @@
     place = jnp.stack([sp_index, tp_index % 2, tp_index // 2]).astype(jnp.int32)
     feats = w_query.shape[1]
     heads = offset_bias.shape[1] // sp_count
-    width = heads * HD
     piece = feats // 4
     every_feat = feats * sp_count
     weights = (w_query, w_key, w_value)
-    shifts = (1, -1)
-    halves, scaled, made = [None, None], [None, None], [None, None]
-
-    def chunk_of(part, step):
-        return (-shifts[part] * (step + 1)) % sp_count
-
-    def first_share(part, layer):
-        slots = SLOTS if layer == 0 else HALF_SLOTS
-        made[part], scaled[part] = project(
-            (halves[part], slots, norm_gain), weights, layer, place, chunk_of(part, 0), width
-        )
-
-    def share(part, step, layer, arrived=None):
-        last = step == sp_count - 1
-        return project(
-            scaled[part], weights, layer, place, chunk_of(part, step), width, arrived, last
-        )[0]
-
-    def sent_on(block, part):
-        return lax.ppermute(block, "sp", ring(sp_count, shifts[part]))
+    halves = [None, None]
+    sources = [None, None]
+    links = sp_count - 1
+
+    def line(block, link):
+        pairs = [(link, link + 1), (sp_count - 1 - link, sp_count - 2 - link)]
+        return lax.ppermute(block, "sp", pairs)
+
+    def made(layer, link, message, part, arrived=None):
+        return share(sources[part], staged[layer], layer, place, link, message, arrived)
+
+    def first_made(layer, part):
+        sources[part] = (halves[part], SLOTS if layer == 0 else HALF_SLOTS, norm_gain)
+        block, scaled, squares = made(layer, 0, 0, part)
+        sources[part] = (scaled, squares)
+        return block
 
     bias = window_bias(offset_bias, place, heads)
+    staged = []
+    for layer in range(LAYERS):
+        staged.append(stage_weights(weights, layer, place, sp_count))
     blocks = over_sp(scatter_tokens(tokens, place, sp_count, feats, piece), sp_count)
-    held = stack_blocks(blocks, place, 2, (bias,))
+    held = stack_blocks(blocks, place, 2, (bias, staged[0]))
     far = [swapped(h, "tp", 2) for h in held]
     near = [swapped(h, "tp", 1) for h in held]
     halves[0] = [held[0], far[0], near[0], swapped(far[0], "tp", 1)]
-    first_share(0, 0)
-    far[1] = lax.optimization_barrier((far[1], made[0]))[0]
+    first = [first_made(0, 0), None]
+    far[1] = lax.optimization_barrier((far[1], first[0]))[0]
     near_far = swapped(far[1], "tp", 1)
     halves[1] = [held[1], far[1], near[1], near_far]
-    first_share(1, 0)
+    first[1] = first_made(0, 1)
 
     for layer in range(LAYERS):
-        travelling = [sent_on(made[part], part) for part in range(2)]
-        summed = lax.optimization_barrier((halves, made))[0]
-        squares = over_sp([squares_of(summed, place)] * sp_count, sp_count)
-        for step in range(1, sp_count - 1):
-            for part in range(2):
-                travelling[part] = sent_on(share(part, step, layer, travelling[part]), part)
-        own = [share(part, sp_count - 1, layer) for part in range(2)]
-        attended = attend(travelling, own, squares, bias, place, sp_count, heads, layer, every_feat)
+        came = [{}, {}]
+        for link in range(links):
+            for message in range(links - link):
+                for part in range(2):
+                    if link == 0 and message == 0:
+                        block = first[part]
+                    else:
+                        arrived = came[part].get((link - 1, message))
+                        block = made(layer, link, message, part, arrived)[0]
+                    came[part][link, message] = line(block, link)
+        arrived = [[came[part][link, links - 1 - link] for link in range(links)] for part in range(2)]
+        own = []
+        for part in range(2):
+            own.append(own_share(sources[part][0], staged[layer], place))
+        squares = [source[1] for source in sources]
+        attended = attend(
+            arrived,
+            own,
+            squares,
+            bias,
+            place,
+            sp_count,
+            heads,
+            layer,
+            every_feat,
+            staged[layer + 1 : layer + 2],
+        )
 
         residuals = [pieces[:2] if layer == 0 else pieces[:1] for pieces in halves]
         pairs, after = [], (attended[1],)
         for part in range(2):
-            gathered = over_sp([attended[part]] * sp_count, sp_count)
+            gathered = gathered_on_line(attended[part])
             sent, kept = spread(gathered, w_out, layer, place, after)
-            came = swapped(sent, "tp", 1)
-            pair = (pair_up if layer < LAYERS - 1 else pair_apart)(kept, came, place)
+            other = swapped(sent, "tp", 1)
+            pair = (pair_up if layer < LAYERS - 1 else pair_apart)(kept, other, place)
             pairs.append((pair, swapped(pair[0], "tp", 2)))
             after = (pair[0],)
         after = ()
         for part in range(2):
-            pair, came = pairs[part]
+            pair, other = pairs[part]
             if layer < LAYERS - 1:
-                mine = renew(residuals[part], pair[0], came, place, after)
+                mine = renew(residuals[part], pair[0], other, place, after)
                 halves[part] = [mine, swapped(mine, "tp", 1)]
-                first_share(part, layer + 1)
-                after = (made[part],)
+                first[part] = first_made(layer + 1, part)
+                after = (first[part],)
             else:
-                blocks = finish(residuals[part][0], pair[1], came, place, sp_count)
+                blocks = finish(residuals[part][0], pair[1], other, place, sp_count)
                 stacked = stack_blocks(over_sp(blocks, sp_count), place)[0]
                 halves[part] = exchanged(stacked)
     return assemble(halves, place, sp_count)
@@ -607,7 +699,7 @@
     heads_here, sp_count = offset_bias.shape[1], lax.axis_size("sp")
     part_rows = tokens.shape[0] // 2
     arrays = (tokens, norm_gain, w_query, w_key, w_value, w_out, offset_bias)
-    if heads_here % sp_count == 0 and lax.axis_size("tp") == 4 and part_rows % HD == 0:
+    if heads_here == sp_count == 4 and lax.axis_size("tp") == 4 and part_rows % HD == 0:
         return stationary_plan(*arrays)
     return gathered_plan(*arrays)
 

time: 275 us -> 302 us (1.098)
  starting transfers between devices: 78.9 us -> 115 us
  Pallas kernels: 76.5 us -> 65.6 us
    ppermute x12 -> x40, starting transfers between devices: 19.8 us -> 86.5 us  [the longest x24 57.1 us: line(): return lax.ppermute(block, 'sp', pairs)]
    ppermute x27 -> x9, waiting for transfers between devices: 36.1 us -> 5.63 us  [over_sp(): lax.ppermute(blocks[shift], 'sp', ring(count, shift))]
    ppermute x27 -> x9, starting transfers between devices: 45.5 us -> 15.5 us  [over_sp(): lax.ppermute(blocks[shift], 'sp', ring(count, shift))]
    ppermute x12 -> x40, waiting for transfers between devices: 42.2 us -> 69.1 us  [the longest x24 48.1 us: line(): return lax.ppermute(block, 'sp', pairs)]
    pallas_call x40 -> x52, Pallas kernels: 76.5 us -> 65.6 us  [local_kernel(): pl.pallas_call(ordered, out_shape=list(outs), in_specs=[smem] + [vmem] *...]
    ppermute x22, waiting for transfers between devices: 40 us -> 43.8 us  [swapped(): return lax.ppermute(array, axis, [(i, i ^ distance) for i in range(count)])]
  transfers between devices with their start and end apart: 61 -> 71, of which waited for: 31 -> 35; matrix products, arithmetic and copies ran while one was open for 0% -> 0% of each run, Pallas kernels for 21% -> 16%
where the time goes in v5:
time: 302 us; the launch traced here: 301 us
  waiting for transfers between devices  118 us (39%)
  starting transfers between devices  115 us (38%)
  Pallas kernels  65.6 us (22%)
    pallas_call x52, Pallas kernels, local_kernel(): pl.pallas_call(ordered, out_shape=list(outs), in_specs=[smem] + [vmem] *...  65.6 us
    ppermute x24, starting transfers between devices, line(): return lax.ppermute(block, 'sp', pairs)  57.1 us
    ppermute x24, waiting for transfers between devices, line(): return lax.ppermute(block, 'sp', pairs)  48.1 us
    ppermute x22, waiting for transfers between devices, swapped(): return lax.ppermute(array, axis, [(i, i ^ distance) for i in range(count)])  43.8 us
    ppermute x9, starting transfers between devices, over_sp(): lax.ppermute(blocks[shift], 'sp', ring(count, shift))  15.5 us
    ppermute x4, starting transfers between devices, gathered_on_line(): below = lax.ppermute(block, 'sp', up)  14.3 us
    ppermute x22, starting transfers between devices, swapped(): return lax.ppermute(array, axis, [(i, i ^ distance) for i in range(count)])  13.5 us
    ppermute x4, waiting for transfers between devices, gathered_on_line(): relayed = lax.ppermute(across, 'sp', [(count - 2, count - 1), (1, 0)])  11.1 us
  transfers between devices with their start and end apart: 71, of which 35 were waited for; matrix products, arithmetic and copies ran while one was open for 0% of the time, Pallas kernels for 16%

profile of v5, /device:TPU:0, one launch (start us, length us, event | category | flops | bytes accessed | tf_op | source)
XLA Modules:
  0.0 300.6 jit_solution(12080696540499477287)
XLA Ops:
  12.3 3.8 %collective-permute-done.1.refs_3_ = bf16[256,256]{1,0:T(8,128)(2,1)S(1)} collective-permute-done((bf16[256,256]{1,0:T(8,128)(2,1)S(1)}, bf16[256,256]{1,0:T(8,128)(2,1)S(1)}, u32[]{:S(2)}, u32[]{:S(2)}) %collective-permute-start.1) | collective-permute-done | bytes 131104 | tf_op jit(solution)/shard_map/ppermute | solution.py:244
  18.3 6.6 %collective-permute-done.3.refs_2_ = bf16[512,256]{1,0:T(8,128)(2,1)S(1)} collective-permute-done((bf16[512,256]{1,0:T(8,128)(2,1)S(1)}, bf16[512,256]{1,0:T(8,128)(2,1)S(1)}, u32[]{:S(2)}, u32[]{:S(2)}) %collective-permute-start.3) | collective-permute-done | bytes 262176 | tf_op jit(solution)/shard_map/ppermute | solution.py:126
  28.5 5.2 %collective-permute-done.12.refs_2_ = bf16[512,256]{1,0:T(8,128)(2,1)S(1)} collective-permute-done((bf16[512,256]{1,0:T(8,128)(2,1)S(1)}, bf16[512,256]{1,0:T(8,128)(2,1)S(1)}, u32[]{:S(2)}, u32[]{:S(2)}) %collective-permute-start.12) | collective-permute-done | bytes 262176 | tf_op jit(solution)/shard_map/ppermute | solution.py:126
  33.6 5.3 %collective-permute-start.9 = (bf16[528,384]{1,0:T(8,128)(2,1)S(1)}, bf16[528,384]{1,0:T(8,128)(2,1)S(1)}, u32[]{:S(2)}, u32[]{:S(2)}) collective-permute-start(bf16[528,384]{1,0:T(8,128)(2,1)S(1)} %get-tuple-element.55), channel_id=1, source_target_pairs={{0,4},{12,8},{1,5},{13,9},{2,6},{14,10},{3,7},{15,11},{16,20},{28,... | collective-permute-start | bytes 1216520 | tf_op jit(solution)/shard_map/ppermute | solution.py:619
  49.9 7.4 %collective-permute-done.18.refs_4_ = bf16[528,384]{1,0:T(8,128)(2,1)S(1)} collective-permute-done((bf16[528,384]{1,0:T(8,128)(2,1)S(1)}, bf16[528,384]{1,0:T(8,128)(2,1)S(1)}, u32[]{:S(2)}, u32[]{:S(2)}) %collective-permute-start.18) | collective-permute-done | bytes 405536 | tf_op jit(solution)/shard_map/ppermute | solution.py:619
  59.9 5.6 %collective-permute-start.6 = (bf16[528,384]{1,0:T(8,128)(2,1)S(1)}, bf16[528,384]{1,0:T(8,128)(2,1)S(1)}, u32[]{:S(2)}, u32[]{:S(2)}) collective-permute-start(bf16[528,384]{1,0:T(8,128)(2,1)S(1)} %shard_map.78), channel_id=1, source_target_pairs={{0,4},{12,8},{1,5},{13,9},{2,6},{14,10},{3,7},{15,11},{16,20},{28,... | collective-permute-start | bytes 1216520 | tf_op jit(solution)/shard_map/ppermute | solution.py:619
  66.8 3.6 %collective-permute-start.15 = (bf16[528,384]{1,0:T(8,128)(2,1)S(1)}, bf16[528,384]{1,0:T(8,128)(2,1)S(1)}, u32[]{:S(2)}, u32[]{:S(2)}) collective-permute-start(bf16[528,384]{1,0:T(8,128)(2,1)S(1)} %shard_map.84), channel_id=1, source_target_pairs={{0,4},{12,8},{1,5},{13,9},{2,6},{14,10},{3,7},{15,11},{16,20},{28,... | collective-permute-start | bytes 1216520 | tf_op jit(solution)/shard_map/ppermute | solution.py:619
  71.0 3.7 %collective-permute-done.16.refs_4_ = bf16[528,384]{1,0:T(8,128)(2,1)S(1)} collective-permute-done((bf16[528,384]{1,0:T(8,128)(2,1)S(1)}, bf16[528,384]{1,0:T(8,128)(2,1)S(1)}, u32[]{:S(2)}, u32[]{:S(2)}) %collective-permute-start.16) | collective-permute-done | bytes 405536 | tf_op jit(solution)/shard_map/ppermute | solution.py:619
  79.1 4.3 %collective-permute-done.6.refs_1_ = bf16[528,384]{1,0:T(8,128)(2,1)S(1)} collective-permute-done((bf16[528,384]{1,0:T(8,128)(2,1)S(1)}, bf16[528,384]{1,0:T(8,128)(2,1)S(1)}, u32[]{:S(2)}, u32[]{:S(2)}) %collective-permute-start.6) | collective-permute-done | bytes 405536 | tf_op jit(solution)/shard_map/ppermute | solution.py:619
  91.6 5.5 %collective-permute-done.11.refs_3_ = bf16[528,384]{1,0:T(8,128)(2,1)S(1)} collective-permute-done((bf16[528,384]{1,0:T(8,128)(2,1)S(1)}, bf16[528,384]{1,0:T(8,128)(2,1)S(1)}, u32[]{:S(2)}, u32[]{:S(2)}) %collective-permute-start.11) | collective-permute-done | bytes 405536 | tf_op jit(solution)/shard_map/ppermute | solution.py:619
  97.1 6.6 %collective-permute-done.20.refs_6_ = bf16[528,384]{1,0:T(8,128)(2,1)S(1)} collective-permute-done((bf16[528,384]{1,0:T(8,128)(2,1)S(1)}, bf16[528,384]{1,0:T(8,128)(2,1)S(1)}, u32[]{:S(2)}, u32[]{:S(2)}) %collective-permute-start.20) | collective-permute-done | bytes 405536 | tf_op jit(solution)/shard_map/ppermute | solution.py:619
  103.8 3.7 %shard_map.92 = (bf16[512,128]{1,0:T(8,128)(2,1)S(1)}, bf16[1024,384]{1,0:T(8,128)(2,1)S(1)}) custom-call(s32[3]{0:T(128)S(1)} %pad_add_fusion.refs_0_, bf16[528,384]{1,0:T(8,128)(2,1)S(1)} %collective-permute-done.6.refs_1_, bf16[528,384]{1,0:T(8,128)(2,1)S(1)} %collective-permute-done.8.refs_2_, bf16[528,384]{1,0:T(8,128)(2,1)S(1)} %collective-permute-done.11.refs_3_, ...), custom_call_target="tpu_custom_call" | custom-call | flops 134217728 | bytes 5464064 | tf_op jit(solution)/shard_map/pallas_call | solution.py:141
  107.6 3.6 %collective-permute-start.21 = (bf16[512,128]{1,0:T(8,128)(2,1)S(1)}, bf16[512,128]{1,0:T(8,128)(2,1)S(1)}, u32[]{:S(2)}, u32[]{:S(2)}) collective-permute-start(bf16[512,128]{1,0:T(8,128)(2,1)S(1)} %get-tuple-element.61.refs_1_), channel_id=1, source_target_pairs={{0,4},{4,8},{8,12},{1,5},{5,9},{9,13},{2,6},{6,10},{10,14},{3,7},{... | collective-permute-start | bytes 393224 | tf_op jit(solution)/shard_map/ppermute | solution.py:454
  115.3 3.4 %shard_map.93.refs_7_.refs_1_ = bf16[512,128]{1,0:T(8,128)(2,1)S(1)} custom-call(s32[3]{0:T(128)S(1)} %pad_add_fusion.refs_0_, bf16[1024,384]{1,0:T(8,128)(2,1)S(1)} %get-tuple-element.62.refs_1_, f32[2,64,1024]{2,1,0:T(8,128)S(1)} %shard_map.74.refs_5_.refs_11_.refs_2_), custom_call_target="tpu_custom_call" | custom-call | flops 134217728 | bytes 1441792 | tf_op jit(solution)/shard_map/pallas_call | solution.py:141
  135.3 3.3 %collective-permute-done.37.refs_5_ = bf16[512,128]{1,0:T(8,128)(2,1)S(1)} collective-permute-done((bf16[512,128]{1,0:T(8,128)(2,1)S(1)}, bf16[512,128]{1,0:T(8,128)(2,1)S(1)}, u32[]{:S(2)}, u32[]{:S(2)}) %collective-permute-start.37) | collective-permute-done | bytes 131104 | tf_op jit(solution)/shard_map/ppermute | solution.py:456
  140.1 7.1 %collective-permute-done.26.refs_4_ = bf16[512,512]{1,0:T(8,128)(2,1)S(1)} collective-permute-done((bf16[512,512]{1,0:T(8,128)(2,1)S(1)}, bf16[512,512]{1,0:T(8,128)(2,1)S(1)}, u32[]{:S(2)}, u32[]{:S(2)}) %collective-permute-start.26) | collective-permute-done | bytes 524320 | tf_op jit(solution)/shard_map/ppermute | solution.py:126
  152.1 11.0 %collective-permute-done.39.refs_4_ = bf16[512,512]{1,0:T(8,128)(2,1)S(1)} collective-permute-done((bf16[512,512]{1,0:T(8,128)(2,1)S(1)}, bf16[512,512]{1,0:T(8,128)(2,1)S(1)}, u32[]{:S(2)}, u32[]{:S(2)}) %collective-permute-start.39) | collective-permute-done | bytes 524320 | tf_op jit(solution)/shard_map/ppermute | solution.py:126
  163.9 4.3 %collective-permute-start.31 = (bf16[528,384]{1,0:T(8,128)(2,1)S(1)}, bf16[528,384]{1,0:T(8,128)(2,1)S(1)}, u32[]{:S(2)}, u32[]{:S(2)}) collective-permute-start(bf16[528,384]{1,0:T(8,128)(2,1)S(1)} %get-tuple-element.67.refs_5_), channel_id=1, source_target_pairs={{0,4},{12,8},{1,5},{13,9},{2,6},{14,10},{3,7},{15,11},{16,20},{28,... | collective-permute-start | bytes 1216520 | tf_op jit(solution)/shard_map/ppermute | solution.py:619
  174.0 4.0 %collective-permute-done.31.refs_4_ = bf16[528,384]{1,0:T(8,128)(2,1)S(1)} collective-permute-done((bf16[528,384]{1,0:T(8,128)(2,1)S(1)}, bf16[528,384]{1,0:T(8,128)(2,1)S(1)}, u32[]{:S(2)}, u32[]{:S(2)}) %collective-permute-start.31) | collective-permute-done | bytes 405536 | tf_op jit(solution)/shard_map/ppermute | solution.py:619
  180.5 8.5 %collective-permute-start.42 = (bf16[528,384]{1,0:T(8,128)(2,1)S(1)}, bf16[528,384]{1,0:T(8,128)(2,1)S(1)}, u32[]{:S(2)}, u32[]{:S(2)}) collective-permute-start(bf16[528,384]{1,0:T(8,128)(2,1)S(1)} %shard_map.108), channel_id=1, source_target_pairs={{0,4},{12,8},{1,5},{13,9},{2,6},{14,10},{3,7},{15,11},{16,20},{28,... | collective-permute-start | bytes 1216520 | tf_op jit(solution)/shard_map/ppermute | solution.py:619
  191.5 6.2 %collective-permute-start.28 = (bf16[528,384]{1,0:T(8,128)(2,1)S(1)}, bf16[528,384]{1,0:T(8,128)(2,1)S(1)}, u32[]{:S(2)}, u32[]{:S(2)}) collective-permute-start(bf16[528,384]{1,0:T(8,128)(2,1)S(1)} %shard_map.98), channel_id=1, source_target_pairs={{0,4},{12,8},{1,5},{13,9},{2,6},{14,10},{3,7},{15,11},{16,20},{28,... | collective-permute-start | bytes 1216520 | tf_op jit(solution)/shard_map/ppermute | solution.py:619
  200.2 6.2 %collective-permute-start.41 = (bf16[528,384]{1,0:T(8,128)(2,1)S(1)}, bf16[528,384]{1,0:T(8,128)(2,1)S(1)}, u32[]{:S(2)}, u32[]{:S(2)}) collective-permute-start(bf16[528,384]{1,0:T(8,128)(2,1)S(1)} %shard_map.107), channel_id=1, source_target_pairs={{0,4},{12,8},{1,5},{13,9},{2,6},{14,10},{3,7},{15,11},{16,20},{28,... | collective-permute-start | bytes 1216520 | tf_op jit(solution)/shard_map/ppermute | solution.py:619
  216.8 4.2 %collective-permute-done.41.refs_4_ = bf16[528,384]{1,0:T(8,128)(2,1)S(1)} collective-permute-done((bf16[528,384]{1,0:T(8,128)(2,1)S(1)}, bf16[528,384]{1,0:T(8,128)(2,1)S(1)}, u32[]{:S(2)}, u32[]{:S(2)}) %collective-permute-start.41) | collective-permute-done | bytes 405536 | tf_op jit(solution)/shard_map/ppermute | solution.py:619
  221.0 6.4 %collective-permute-done.46.refs_6_ = bf16[528,384]{1,0:T(8,128)(2,1)S(1)} collective-permute-done((bf16[528,384]{1,0:T(8,128)(2,1)S(1)}, bf16[528,384]{1,0:T(8,128)(2,1)S(1)}, u32[]{:S(2)}, u32[]{:S(2)}) %collective-permute-start.46) | collective-permute-done | bytes 405536 | tf_op jit(solution)/shard_map/ppermute | solution.py:619
  227.4 3.7 %shard_map.114 = (bf16[512,128]{1,0:T(8,128)(2,1)S(1)}, bf16[1024,384]{1,0:T(8,128)(2,1)S(1)}) custom-call(s32[3]{0:T(128)S(1)} %pad_add_fusion.refs_0_, bf16[528,384]{1,0:T(8,128)(2,1)S(1)} %collective-permute-done.28.refs_1_, bf16[528,384]{1,0:T(8,128)(2,1)S(1)} %collective-permute-done.30.refs_2_, bf16[528,384]{1,0:T(8,128)(2,1)S(1)} %collective-permute-done.33.refs_3_, ...), custom_call_target="tpu_custom_call" | custom-call | flops 134217728 | bytes 5464064 | tf_op jit(solution)/shard_map/pallas_call | solution.py:141
  231.2 4.0 %collective-permute-start.47 = (bf16[512,128]{1,0:T(8,128)(2,1)S(1)}, bf16[512,128]{1,0:T(8,128)(2,1)S(1)}, u32[]{:S(2)}, u32[]{:S(2)}) collective-permute-start(bf16[512,128]{1,0:T(8,128)(2,1)S(1)} %get-tuple-element.73.refs_1_), channel_id=1, source_target_pairs={{0,4},{4,8},{8,12},{1,5},{5,9},{9,13},{2,6},{6,10},{10,14},{3,7},{... | collective-permute-start | bytes 393224 | tf_op jit(solution)/shard_map/ppermute | solution.py:454
  238.9 3.4 %shard_map.115.refs_7_.refs_1_ = bf16[512,128]{1,0:T(8,128)(2,1)S(1)} custom-call(s32[3]{0:T(128)S(1)} %pad_add_fusion.refs_0_, bf16[1024,384]{1,0:T(8,128)(2,1)S(1)} %get-tuple-element.74.refs_1_, f32[2,64,1024]{2,1,0:T(8,128)S(1)} %shard_map.74.refs_5_.refs_11_.refs_2_), custom_call_target="tpu_custom_call" | custom-call | flops 134217728 | bytes 1441792 | tf_op jit(solution)/shard_map/pallas_call | solution.py:141
  248.2 3.5 %collective-permute-start.59 = (bf16[512,128]{1,0:T(8,128)(2,1)S(1)}, bf16[512,128]{1,0:T(8,128)(2,1)S(1)}, u32[]{:S(2)}, u32[]{:S(2)}) collective-permute-start(bf16[512,128]{1,0:T(8,128)(2,1)S(1)} %shard_map.115.refs_7_.refs_1_), channel_id=1, source_target_pairs={{0,4},{4,8},{8,12},{1,5},{5,9},{9,13},{2,6},{6,10},{10,14},{3,7},{... | collective-permute-start | bytes 393224 | tf_op jit(solution)/shard_map/ppermute | solution.py:454
  258.9 4.2 %collective-permute-done.62.refs_5_ = bf16[512,128]{1,0:T(8,128)(2,1)S(1)} collective-permute-done((bf16[512,128]{1,0:T(8,128)(2,1)S(1)}, bf16[512,128]{1,0:T(8,128)(2,1)S(1)}, u32[]{:S(2)}, u32[]{:S(2)}) %collective-permute-start.62) | collective-permute-done | bytes 131104 | tf_op jit(solution)/shard_map/ppermute | solution.py:456
  268.7 5.1 %collective-permute-done.52.refs_3_ = bf16[512,256]{1,0:T(8,128)(2,1)S(1)} collective-permute-done((bf16[512,256]{1,0:T(8,128)(2,1)S(1)}, bf16[512,256]{1,0:T(8,128)(2,1)S(1)}, u32[]{:S(2)}, u32[]{:S(2)}) %collective-permute-start.52) | collective-permute-done | bytes 262176 | tf_op jit(solution)/shard_map/ppermute | solution.py:126
  274.5 3.5 %collective-permute-start.54 = (bf16[128,256]{1,0:T(8,128)(2,1)S(1)}, bf16[128,256]{1,0:T(8,128)(2,1)S(1)}, u32[]{:S(2)}, u32[]{:S(2)}) collective-permute-start(bf16[128,256]{1,0:T(8,128)(2,1)S(1)} %get-tuple-element.81), channel_id=1, source_target_pairs={{0,8},{4,12},{8,0},{12,4},{1,9},{5,13},{9,1},{13,5},{2,10},{6,14},... | collective-permute-start | bytes 196616 | tf_op jit(solution)/shard_map/ppermute | solution.py:244
  293.1 3.8 %collective-permute-done.68.refs_6_ = bf16[512,256]{1,0:T(8,128)(2,1)S(1)} collective-permute-done((bf16[512,256]{1,0:T(8,128)(2,1)S(1)}, bf16[512,256]{1,0:T(8,128)(2,1)S(1)}, u32[]{:S(2)}, u32[]{:S(2)}) %collective-permute-start.68) | collective-permute-done | bytes 262176 | tf_op jit(solution)/shard_map/ppermute | solution.py:126
  (170 shorter events, 138.9 us)
Async XLA Ops:
  4.9 11.2 %collective-permute-start.1 = (bf16[256,256]{1,0:T(8,128)(2,1)S(1)}, bf16[256,256]{1,0:T(8,128)(2,1)S(1)}, u32[]{:S(2)}, u32[]{:S(2)}) collective-permute-start(bf16[256,256]{1,0:T(8,128)(2,1)S(1)} %get-tuple-element.50), channel_id=1, source_target_pairs={{0,8},{4,12},{8,0},{12,4},{1,9},{5,13},{9,1},{13,5},{2,10},{6,14},... | collective-permute-start | bytes 393224 | tf_op jit(solution)/shard_map/ppermute | solution.py:244
  26.4 12.5 %collective-permute-start.13 = (bf16[512,256]{1,0:T(8,128)(2,1)S(1)}, bf16[512,256]{1,0:T(8,128)(2,1)S(1)}, u32[]{:S(2)}, u32[]{:S(2)}) collective-permute-start(bf16[512,256]{1,0:T(8,128)(2,1)S(1)} %get-tuple-element.56.refs_1_), channel_id=1, source_target_pairs={{0,1},{1,0},{2,3},{3,2},{4,5},{5,4},{6,7},{7,6},{8,9},{9,8},{10,11... | collective-permute-start | bytes 786440 | tf_op jit(solution)/shard_map/ppermute | solution.py:126
  33.6 15.0 %collective-permute-start.9 = (bf16[528,384]{1,0:T(8,128)(2,1)S(1)}, bf16[528,384]{1,0:T(8,128)(2,1)S(1)}, u32[]{:S(2)}, u32[]{:S(2)}) collective-permute-start(bf16[528,384]{1,0:T(8,128)(2,1)S(1)} %get-tuple-element.55), channel_id=1, source_target_pairs={{0,4},{12,8},{1,5},{13,9},{2,6},{14,10},{3,7},{15,11},{16,20},{28,... | collective-permute-start | bytes 1216520 | tf_op jit(solution)/shard_map/ppermute | solution.py:619
  40.8 16.6 %collective-permute-start.18 = (bf16[528,384]{1,0:T(8,128)(2,1)S(1)}, bf16[528,384]{1,0:T(8,128)(2,1)S(1)}, u32[]{:S(2)}, u32[]{:S(2)}) collective-permute-start(bf16[528,384]{1,0:T(8,128)(2,1)S(1)} %get-tuple-element.60), channel_id=1, source_target_pairs={{0,4},{12,8},{1,5},{13,9},{2,6},{14,10},{3,7},{15,11},{16,20},{28,... | collective-permute-start | bytes 1216520 | tf_op jit(solution)/shard_map/ppermute | solution.py:619
  43.3 23.4 %collective-permute-start.7 = (bf16[528,384]{1,0:T(8,128)(2,1)S(1)}, bf16[528,384]{1,0:T(8,128)(2,1)S(1)}, u32[]{:S(2)}, u32[]{:S(2)}) collective-permute-start(bf16[528,384]{1,0:T(8,128)(2,1)S(1)} %shard_map.79), channel_id=1, source_target_pairs={{0,4},{12,8},{1,5},{13,9},{2,6},{14,10},{3,7},{15,11},{16,20},{28,... | collective-permute-start | bytes 1216520 | tf_op jit(solution)/shard_map/ppermute | solution.py:619
  45.9 28.8 %collective-permute-start.16 = (bf16[528,384]{1,0:T(8,128)(2,1)S(1)}, bf16[528,384]{1,0:T(8,128)(2,1)S(1)}, u32[]{:S(2)}, u32[]{:S(2)}) collective-permute-start(bf16[528,384]{1,0:T(8,128)(2,1)S(1)} %shard_map.85), channel_id=1, source_target_pairs={{0,4},{12,8},{1,5},{13,9},{2,6},{14,10},{3,7},{15,11},{16,20},{28,... | collective-permute-start | bytes 1216520 | tf_op jit(solution)/shard_map/ppermute | solution.py:619
  49.2 26.8 %collective-permute-start.10 = (bf16[528,384]{1,0:T(8,128)(2,1)S(1)}, bf16[528,384]{1,0:T(8,128)(2,1)S(1)}, u32[]{:S(2)}, u32[]{:S(2)}) collective-permute-start(bf16[528,384]{1,0:T(8,128)(2,1)S(1)} %shard_map.81), channel_id=1, source_target_pairs={{4,8},{8,4},{5,9},{9,5},{6,10},{10,6},{7,11},{11,7},{20,24},{24,20... | collective-permute-start | bytes 1216520 | tf_op jit(solution)/shard_map/ppermute | solution.py:619
  57.9 19.3 %collective-permute-start.19 = (bf16[528,384]{1,0:T(8,128)(2,1)S(1)}, bf16[528,384]{1,0:T(8,128)(2,1)S(1)}, u32[]{:S(2)}, u32[]{:S(2)}) collective-permute-start(bf16[528,384]{1,0:T(8,128)(2,1)S(1)} %shard_map.87), channel_id=1, source_target_pairs={{4,8},{8,4},{5,9},{9,5},{6,10},{10,6},{7,11},{11,7},{20,24},{24,20... | collective-permute-start | bytes 1216520 | tf_op jit(solution)/shard_map/ppermute | solution.py:619
  59.9 23.5 %collective-permute-start.6 = (bf16[528,384]{1,0:T(8,128)(2,1)S(1)}, bf16[528,384]{1,0:T(8,128)(2,1)S(1)}, u32[]{:S(2)}, u32[]{:S(2)}) collective-permute-start(bf16[528,384]{1,0:T(8,128)(2,1)S(1)} %shard_map.78), channel_id=1, source_target_pairs={{0,4},{12,8},{1,5},{13,9},{2,6},{14,10},{3,7},{15,11},{16,20},{28,... | collective-permute-start | bytes 1216520 | tf_op jit(solution)/shard_map/ppermute | solution.py:619
  66.8 24.8 %collective-permute-start.15 = (bf16[528,384]{1,0:T(8,128)(2,1)S(1)}, bf16[528,384]{1,0:T(8,128)(2,1)S(1)}, u32[]{:S(2)}, u32[]{:S(2)}) collective-permute-start(bf16[528,384]{1,0:T(8,128)(2,1)S(1)} %shard_map.84), channel_id=1, source_target_pairs={{0,4},{12,8},{1,5},{13,9},{2,6},{14,10},{3,7},{15,11},{16,20},{28,... | collective-permute-start | bytes 1216520 | tf_op jit(solution)/shard_map/ppermute | solution.py:619
  74.7 16.9 %collective-permute-start.8 = (bf16[528,384]{1,0:T(8,128)(2,1)S(1)}, bf16[528,384]{1,0:T(8,128)(2,1)S(1)}, u32[]{:S(2)}, u32[]{:S(2)}) collective-permute-start(bf16[528,384]{1,0:T(8,128)(2,1)S(1)} %shard_map.80), channel_id=1, source_target_pairs={{4,8},{8,4},{5,9},{9,5},{6,10},{10,6},{7,11},{11,7},{20,24},{24,20... | collective-permute-start | bytes 1216520 | tf_op jit(solution)/shard_map/ppermute | solution.py:619
  76.0 15.7 %collective-permute-start.17 = (bf16[528,384]{1,0:T(8,128)(2,1)S(1)}, bf16[528,384]{1,0:T(8,128)(2,1)S(1)}, u32[]{:S(2)}, u32[]{:S(2)}) collective-permute-start(bf16[528,384]{1,0:T(8,128)(2,1)S(1)} %shard_map.86), channel_id=1, source_target_pairs={{4,8},{8,4},{5,9},{9,5},{6,10},{10,6},{7,11},{11,7},{20,24},{24,20... | collective-permute-start | bytes 1216520 | tf_op jit(solution)/shard_map/ppermute | solution.py:619
  77.2 19.9 %collective-permute-start.11 = (bf16[528,384]{1,0:T(8,128)(2,1)S(1)}, bf16[528,384]{1,0:T(8,128)(2,1)S(1)}, u32[]{:S(2)}, u32[]{:S(2)}) collective-permute-start(bf16[528,384]{1,0:T(8,128)(2,1)S(1)} %shard_map.82), channel_id=1, source_target_pairs={{8,12},{4,0},{9,13},{5,1},{10,14},{6,2},{11,15},{7,3},{24,28},{20,... | collective-permute-start | bytes 1216520 | tf_op jit(solution)/shard_map/ppermute | solution.py:619
  83.4 20.3 %collective-permute-start.20 = (bf16[528,384]{1,0:T(8,128)(2,1)S(1)}, bf16[528,384]{1,0:T(8,128)(2,1)S(1)}, u32[]{:S(2)}, u32[]{:S(2)}) collective-permute-start(bf16[528,384]{1,0:T(8,128)(2,1)S(1)} %shard_map.88), channel_id=1, source_target_pairs={{8,12},{4,0},{9,13},{5,1},{10,14},{6,2},{11,15},{7,3},{24,28},{20,... | collective-permute-start | bytes 1216520 | tf_op jit(solution)/shard_map/ppermute | solution.py:619
  107.6 11.1 %collective-permute-start.21 = (bf16[512,128]{1,0:T(8,128)(2,1)S(1)}, bf16[512,128]{1,0:T(8,128)(2,1)S(1)}, u32[]{:S(2)}, u32[]{:S(2)}) collective-permute-start(bf16[512,128]{1,0:T(8,128)(2,1)S(1)} %get-tuple-element.61.refs_1_), channel_id=1, source_target_pairs={{0,4},{4,8},{8,12},{1,5},{5,9},{9,13},{2,6},{6,10},{10,14},{3,7},{... | collective-permute-start | bytes 393224 | tf_op jit(solution)/shard_map/ppermute | solution.py:454
  133.7 13.5 %collective-permute-start.26 = (bf16[512,512]{1,0:T(8,128)(2,1)S(1)}, bf16[512,512]{1,0:T(8,128)(2,1)S(1)}, u32[]{:S(2)}, u32[]{:S(2)}) collective-permute-start(bf16[512,512]{1,0:T(8,128)(2,1)S(1)} %shard_map.95.refs_3_.refs_7_), channel_id=1, source_target_pairs={{0,2},{1,3},{2,0},{3,1},{4,6},{5,7},{6,4},{7,5},{8,10},{9,11},{10,... | collective-permute-start | bytes 1572872 | tf_op jit(solution)/shard_map/ppermute | solution.py:126
  148.7 14.4 %collective-permute-start.39 = (bf16[512,512]{1,0:T(8,128)(2,1)S(1)}, bf16[512,512]{1,0:T(8,128)(2,1)S(1)}, u32[]{:S(2)}, u32[]{:S(2)}) collective-permute-start(bf16[512,512]{1,0:T(8,128)(2,1)S(1)} %shard_map.104.refs_3_), channel_id=1, source_target_pairs={{0,2},{1,3},{2,0},{3,1},{4,6},{5,7},{6,4},{7,5},{8,10},{9,11},{10,... | collective-permute-start | bytes 1572872 | tf_op jit(solution)/shard_map/ppermute | solution.py:126
  163.9 14.0 %collective-permute-start.31 = (bf16[528,384]{1,0:T(8,128)(2,1)S(1)}, bf16[528,384]{1,0:T(8,128)(2,1)S(1)}, u32[]{:S(2)}, u32[]{:S(2)}) collective-permute-start(bf16[528,384]{1,0:T(8,128)(2,1)S(1)} %get-tuple-element.67.refs_5_), channel_id=1, source_target_pairs={{0,4},{12,8},{1,5},{13,9},{2,6},{14,10},{3,7},{15,11},{16,20},{28,... | collective-permute-start | bytes 1216520 | tf_op jit(solution)/shard_map/ppermute | solution.py:619
  170.0 18.9 %collective-permute-start.44 = (bf16[528,384]{1,0:T(8,128)(2,1)S(1)}, bf16[528,384]{1,0:T(8,128)(2,1)S(1)}, u32[]{:S(2)}, u32[]{:S(2)}) collective-permute-start(bf16[528,384]{1,0:T(8,128)(2,1)S(1)} %get-tuple-element.72), channel_id=1, source_target_pairs={{0,4},{12,8},{1,5},{13,9},{2,6},{14,10},{3,7},{15,11},{16,20},{28,... | collective-permute-start | bytes 1216520 | tf_op jit(solution)/shard_map/ppermute | solution.py:619
  172.6 25.0 %collective-permute-start.29 = (bf16[528,384]{1,0:T(8,128)(2,1)S(1)}, bf16[528,384]{1,0:T(8,128)(2,1)S(1)}, u32[]{:S(2)}, u32[]{:S(2)}) collective-permute-start(bf16[528,384]{1,0:T(8,128)(2,1)S(1)} %shard_map.99), channel_id=1, source_target_pairs={{0,4},{12,8},{1,5},{13,9},{2,6},{14,10},{3,7},{15,11},{16,20},{28,... | collective-permute-start | bytes 1216520 | tf_op jit(solution)/shard_map/ppermute | solution.py:619
  178.5 21.7 %collective-permute-start.32 = (bf16[528,384]{1,0:T(8,128)(2,1)S(1)}, bf16[528,384]{1,0:T(8,128)(2,1)S(1)}, u32[]{:S(2)}, u32[]{:S(2)}) collective-permute-start(bf16[528,384]{1,0:T(8,128)(2,1)S(1)} %shard_map.101), channel_id=1, source_target_pairs={{4,8},{8,4},{5,9},{9,5},{6,10},{10,6},{7,11},{11,7},{20,24},{24,20... | collective-permute-start | bytes 1216520 | tf_op jit(solution)/shard_map/ppermute | solution.py:619
  180.5 26.5 %collective-permute-start.42 = (bf16[528,384]{1,0:T(8,128)(2,1)S(1)}, bf16[528,384]{1,0:T(8,128)(2,1)S(1)}, u32[]{:S(2)}, u32[]{:S(2)}) collective-permute-start(bf16[528,384]{1,0:T(8,128)(2,1)S(1)} %shard_map.108), channel_id=1, source_target_pairs={{0,4},{12,8},{1,5},{13,9},{2,6},{14,10},{3,7},{15,11},{16,20},{28,... | collective-permute-start | bytes 1216520 | tf_op jit(solution)/shard_map/ppermute | solution.py:619
  189.6 19.3 %collective-permute-start.45 = (bf16[528,384]{1,0:T(8,128)(2,1)S(1)}, bf16[528,384]{1,0:T(8,128)(2,1)S(1)}, u32[]{:S(2)}, u32[]{:S(2)}) collective-permute-start(bf16[528,384]{1,0:T(8,128)(2,1)S(1)} %shard_map.110), channel_id=1, source_target_pairs={{4,8},{8,4},{5,9},{9,5},{6,10},{10,6},{7,11},{11,7},{20,24},{24,20... | collective-permute-start | bytes 1216520 | tf_op jit(solution)/shard_map/ppermute | solution.py:619
  191.5 21.2 %collective-permute-start.28 = (bf16[528,384]{1,0:T(8,128)(2,1)S(1)}, bf16[528,384]{1,0:T(8,128)(2,1)S(1)}, u32[]{:S(2)}, u32[]{:S(2)}) collective-permute-start(bf16[528,384]{1,0:T(8,128)(2,1)S(1)} %shard_map.98), channel_id=1, source_target_pairs={{0,4},{12,8},{1,5},{13,9},{2,6},{14,10},{3,7},{15,11},{16,20},{28,... | collective-permute-start | bytes 1216520 | tf_op jit(solution)/shard_map/ppermute | solution.py:619
  198.2 18.5 %collective-permute-start.30 = (bf16[528,384]{1,0:T(8,128)(2,1)S(1)}, bf16[528,384]{1,0:T(8,128)(2,1)S(1)}, u32[]{:S(2)}, u32[]{:S(2)}) collective-permute-start(bf16[528,384]{1,0:T(8,128)(2,1)S(1)} %shard_map.100), channel_id=1, source_target_pairs={{4,8},{8,4},{5,9},{9,5},{6,10},{10,6},{7,11},{11,7},{20,24},{24,20... | collective-permute-start | bytes 1216520 | tf_op jit(solution)/shard_map/ppermute | solution.py:619
  200.2 20.7 %collective-permute-start.41 = (bf16[528,384]{1,0:T(8,128)(2,1)S(1)}, bf16[528,384]{1,0:T(8,128)(2,1)S(1)}, u32[]{:S(2)}, u32[]{:S(2)}) collective-permute-start(bf16[528,384]{1,0:T(8,128)(2,1)S(1)} %shard_map.107), channel_id=1, source_target_pairs={{0,4},{12,8},{1,5},{13,9},{2,6},{14,10},{3,7},{15,11},{16,20},{28,... | collective-permute-start | bytes 1216520 | tf_op jit(solution)/shard_map/ppermute | solution.py:619
  206.9 14.0 %collective-permute-start.33 = (bf16[528,384]{1,0:T(8,128)(2,1)S(1)}, bf16[528,384]{1,0:T(8,128)(2,1)S(1)}, u32[]{:S(2)}, u32[]{:S(2)}) collective-permute-start(bf16[528,384]{1,0:T(8,128)(2,1)S(1)} %shard_map.102), channel_id=1, source_target_pairs={{8,12},{4,0},{9,13},{5,1},{10,14},{6,2},{11,15},{7,3},{24,28},{20,... | collective-permute-start | bytes 1216520 | tf_op jit(solution)/shard_map/ppermute | solution.py:619
  208.8 12.2 %collective-permute-start.43 = (bf16[528,384]{1,0:T(8,128)(2,1)S(1)}, bf16[528,384]{1,0:T(8,128)(2,1)S(1)}, u32[]{:S(2)}, u32[]{:S(2)}) collective-permute-start(bf16[528,384]{1,0:T(8,128)(2,1)S(1)} %shard_map.109), channel_id=1, source_target_pairs={{4,8},{8,4},{5,9},{9,5},{6,10},{10,6},{7,11},{11,7},{20,24},{24,20... | collective-permute-start | bytes 1216520 | tf_op jit(solution)/shard_map/ppermute | solution.py:619
  212.7 14.7 %collective-permute-start.46 = (bf16[528,384]{1,0:T(8,128)(2,1)S(1)}, bf16[528,384]{1,0:T(8,128)(2,1)S(1)}, u32[]{:S(2)}, u32[]{:S(2)}) collective-permute-start(bf16[528,384]{1,0:T(8,128)(2,1)S(1)} %shard_map.111), channel_id=1, source_target_pairs={{8,12},{4,0},{9,13},{5,1},{10,14},{6,2},{11,15},{7,3},{24,28},{20,... | collective-permute-start | bytes 1216520 | tf_op jit(solution)/shard_map/ppermute | solution.py:619
  231.2 11.0 %collective-permute-start.47 = (bf16[512,128]{1,0:T(8,128)(2,1)S(1)}, bf16[512,128]{1,0:T(8,128)(2,1)S(1)}, u32[]{:S(2)}, u32[]{:S(2)}) collective-permute-start(bf16[512,128]{1,0:T(8,128)(2,1)S(1)} %get-tuple-element.73.refs_1_), channel_id=1, source_target_pairs={{0,4},{4,8},{8,12},{1,5},{5,9},{9,13},{2,6},{6,10},{10,14},{3,7},{... | collective-permute-start | bytes 393224 | tf_op jit(solution)/shard_map/ppermute | solution.py:454
  246.2 11.2 %collective-permute-start.51 = (bf16[512,512]{1,0:T(8,128)(2,1)S(1)}, bf16[512,512]{1,0:T(8,128)(2,1)S(1)}, u32[]{:S(2)}, u32[]{:S(2)}) collective-permute-start(bf16[512,512]{1,0:T(8,128)(2,1)S(1)} %get-tuple-element.76), channel_id=1, source_target_pairs={{0,1},{1,0},{2,3},{3,2},{4,5},{5,4},{6,7},{7,6},{8,9},{9,8},{10,11... | collective-permute-start | bytes 1572872 | tf_op jit(solution)/shard_map/ppermute | solution.py:126
  267.1 11.8 %collective-permute-start.64 = (bf16[512,256]{1,0:T(8,128)(2,1)S(1)}, bf16[512,256]{1,0:T(8,128)(2,1)S(1)}, u32[]{:S(2)}, u32[]{:S(2)}) collective-permute-start(bf16[512,256]{1,0:T(8,128)(2,1)S(1)} %get-tuple-element.86), channel_id=1, source_target_pairs={{0,2},{1,3},{2,0},{3,1},{4,6},{5,7},{6,4},{7,5},{8,10},{9,11},{10,... | collective-permute-start | bytes 786440 | tf_op jit(solution)/shard_map/ppermute | solution.py:126
  (42 other events, 311.7 us)

commit v6 on v5

--- a/solution.py
+++ b/solution.py
@@ -301,7 +301,7 @@
     return terms[0] + (terms[1] + terms[2])
 
 
-def share(source, staged, layer, place, link, message, arrived=None):
+def share(source, staged, layer, place, chunk_shift, arrived=None):
     fresh = len(source) == 3
     sp_count, feats, total_width = staged.shape
     arrays = (*source[0], source[2]) if fresh else source
@@ -334,22 +334,15 @@
                 squares_ref[pl.ds(run, 1), :] = jnp.sum(total.T, axis=0, keepdims=True)
         else:
             scaled_ref, squares_ref = array_refs
-        forward = place_ref[0] == link
-        backward = place_ref[0] == sp_count - 1 - link
-
-        @pl.when(forward | backward)
-        def _():
-            chunk = jnp.where(forward, sp_count - 1 - message, message)
-            total = jnp.dot(
-                scaled_ref[...], staged_ref[chunk], preferred_element_type=jnp.float32
-            )
-            squares = squares_ref[...]
-            if arrived is not None:
-                arrived_ref = refs[count + 1]
-                total += arrived_ref[pl.ds(0, tok), :].astype(jnp.float32)
-                squares += get_squares(arrived_ref, tok)
-            out_ref[pl.ds(0, tok), :] = total.astype(jnp.bfloat16)
-            put_squares(out_ref, squares, tok)
+        chunk = lax.rem(place_ref[0] + chunk_shift, sp_count)
+        total = jnp.dot(scaled_ref[...], staged_ref[chunk], preferred_element_type=jnp.float32)
+        squares = squares_ref[...]
+        if arrived is not None:
+            arrived_ref = refs[count + 1]
+            total += arrived_ref[pl.ds(0, tok), :].astype(jnp.float32)
+            squares += get_squares(arrived_ref, tok)
+        out_ref[pl.ds(0, tok), :] = total.astype(jnp.bfloat16)
+        put_squares(out_ref, squares, tok)
 
     outs = [shaped(tok + EXTRA, total_width)]
     if fresh:
@@ -447,44 +440,17 @@
     return out0, out1[0]
 
 
-def gathered_on_line(block):
-    count = lax.axis_size("sp")
-    up = [(i, i + 1) for i in range(count - 1)]
-    across = lax.ppermute(block, "sp", ring(count, 2))
-    below = lax.ppermute(block, "sp", up)
-    above = lax.ppermute(block, "sp", [(target, source) for source, target in up])
-    relayed = lax.ppermute(across, "sp", [(count - 2, count - 1), (1, 0)])
-    return block, below, above, across, relayed
-
-
 def spread(attended, w_out, layer, place, after):
     sp_count = lax.axis_size("sp")
     rows, width = attended[0].shape
     inner, feats = w_out.shape[1:]
     half = feats // 2
 
-    def body(place_ref, own_ref, below_ref, above_ref, across_ref, relayed_ref, w_ref, *rest):
-        sent_ref, kept_ref, gathered = rest
-        here = place_ref[0]
-
-        def put(ref, index):
-            gathered[:, aligned(lax.rem(index + sp_count, sp_count), width)] = ref[...]
-
-        put(own_ref, here)
-        put(across_ref, here + 2)
-
-        @pl.when(here > 0)
-        def _():
-            put(below_ref, here - 1)
-
-        @pl.when(here < sp_count - 1)
-        def _():
-            put(above_ref, here + 1)
-
-        @pl.when((here == 0) | (here == sp_count - 1))
-        def _():
-            put(relayed_ref, sp_count - 1 - here)
-
+    def body(place_ref, *refs):
+        piece_refs, (w_ref, sent_ref, kept_ref, gathered) = refs[:sp_count], refs[sp_count:]
+        for shift in range(sp_count):
+            source = lax.rem(place_ref[0] + sp_count - shift, sp_count)
+            gathered[:, aligned(source, width)] = piece_refs[shift][...]
         core = place_ref[1]
         for index, out_ref in ((1 - core, sent_ref), (core, kept_ref)):
             out_ref[...] = jnp.dot(
@@ -612,18 +578,18 @@
     weights = (w_query, w_key, w_value)
     halves = [None, None]
     sources = [None, None]
-    links = sp_count - 1
-
-    def line(block, link):
-        pairs = [(link, link + 1), (sp_count - 1 - link, sp_count - 2 - link)]
-        return lax.ppermute(block, "sp", pairs)
-
-    def made(layer, link, message, part, arrived=None):
-        return share(sources[part], staged[layer], layer, place, link, message, arrived)
+    shifts = (1, -1)
+
+    def sent_on(block, part):
+        return lax.ppermute(block, "sp", ring(sp_count, shifts[part]))
+
+    def made(layer, part, step, arrived=None):
+        chunk = (-shifts[part] * (step + 1)) % sp_count
+        return share(sources[part], staged[layer], layer, place, chunk, arrived)
 
     def first_made(layer, part):
         sources[part] = (halves[part], SLOTS if layer == 0 else HALF_SLOTS, norm_gain)
-        block, scaled, squares = made(layer, 0, 0, part)
+        block, scaled, squares = made(layer, part, 0)
         sources[part] = (scaled, squares)
         return block
 
@@ -643,23 +609,17 @@
     first[1] = first_made(0, 1)
 
     for layer in range(LAYERS):
-        came = [{}, {}]
-        for link in range(links):
-            for message in range(links - link):
-                for part in range(2):
-                    if link == 0 and message == 0:
-                        block = first[part]
-                    else:
-                        arrived = came[part].get((link - 1, message))
-                        block = made(layer, link, message, part, arrived)[0]
-                    came[part][link, message] = line(block, link)
-        arrived = [[came[part][link, links - 1 - link] for link in range(links)] for part in range(2)]
+        travelling = [sent_on(first[part], part) for part in range(2)]
+        for step in range(1, sp_count - 1):
+            for part in range(2):
+                block = made(layer, part, step, travelling[part])[0]
+                travelling[part] = sent_on(block, part)
         own = []
         for part in range(2):
             own.append(own_share(sources[part][0], staged[layer], place))
         squares = [source[1] for source in sources]
         attended = attend(
-            arrived,
+            [travelling[:1], travelling[1:]],
             own,
             squares,
             bias,
@@ -674,7 +634,7 @@
         residuals = [pieces[:2] if layer == 0 else pieces[:1] for pieces in halves]
         pairs, after = [], (attended[1],)
         for part in range(2):
-            gathered = gathered_on_line(attended[part])
+            gathered = over_sp([attended[part]] * sp_count, sp_count)
             sent, kept = spread(gathered, w_out, layer, place, after)
             other = swapped(sent, "tp", 1)
             pair = (pair_up if layer < LAYERS - 1 else pair_apart)(kept, other, place)
@@ -699,7 +659,7 @@
     heads_here, sp_count = offset_bias.shape[1], lax.axis_size("sp")
     part_rows = tokens.shape[0] // 2
     arrays = (tokens, norm_gain, w_query, w_key, w_value, w_out, offset_bias)
-    if heads_here == sp_count == 4 and lax.axis_size("tp") == 4 and part_rows % HD == 0:
+    if heads_here % sp_count == 0 and lax.axis_size("tp") == 4 and part_rows % HD == 0:
         return stationary_plan(*arrays)
     return gathered_plan(*arrays)
 

time: 302 us -> 273 us (0.904)
  starting transfers between devices: 115 us -> 66.9 us
  waiting for transfers between devices: 118 us -> 148 us
  Pallas kernels: 65.6 us -> 57.8 us
    ppermute x40 -> x12, starting transfers between devices: 86.5 us -> 17.5 us  [sent_on(): return lax.ppermute(block, 'sp', ring(sp_count, shifts[part]))]
    ppermute x9 -> x21, waiting for transfers between devices: 5.63 us -> 30.5 us  [over_sp(): lax.ppermute(blocks[shift], 'sp', ring(count, shift))]
    ppermute x9 -> x21, starting transfers between devices: 15.5 us -> 35.8 us  [over_sp(): lax.ppermute(blocks[shift], 'sp', ring(count, shift))]
    pallas_call x52 -> x40, Pallas kernels: 65.6 us -> 57.8 us  [local_kernel(): pl.pallas_call(ordered, out_shape=list(outs), in_specs=[smem] + [vmem] *...]
    ppermute x40 -> x12, waiting for transfers between devices: 69.1 us -> 73.9 us  [sent_on(): return lax.ppermute(block, 'sp', ring(sp_count, shifts[part]))]
  transfers between devices with their start and end apart: 71 -> 55, of which waited for: 35 -> 32; matrix products, arithmetic and copies ran while one was open for 0% -> 0% of each run, Pallas kernels for 16% -> 15%
where the time goes in v6:
time: 273 us
  waiting for transfers between devices  148 us (54%)
  starting transfers between devices  66.9 us (25%)
  Pallas kernels  57.8 us (21%)
    ppermute x12, waiting for transfers between devices, sent_on(): return lax.ppermute(block, 'sp', ring(sp_count, shifts[part]))  73.9 us
    pallas_call x40, Pallas kernels, local_kernel(): pl.pallas_call(ordered, out_shape=list(outs), in_specs=[smem] + [vmem] *...  57.8 us
    ppermute x22, waiting for transfers between devices, swapped(): return lax.ppermute(array, axis, [(i, i ^ distance) for i in range(count)])  43.8 us
    ppermute x21, starting transfers between devices, over_sp(): lax.ppermute(blocks[shift], 'sp', ring(count, shift))  35.8 us
    ppermute x21, waiting for transfers between devices, over_sp(): lax.ppermute(blocks[shift], 'sp', ring(count, shift))  30.5 us
    ppermute x12, starting transfers between devices, sent_on(): return lax.ppermute(block, 'sp', ring(sp_count, shifts[part]))  17.5 us
    ppermute x22, starting transfers between devices, swapped(): return lax.ppermute(array, axis, [(i, i ^ distance) for i in range(count)])  13.5 us
  transfers between devices with their start and end apart: 55, of which 32 were waited for; matrix products, arithmetic and copies ran while one was open for 0% of the time, Pallas kernels for 15%

profile of v6, /device:TPU:0, one launch (start us, length us, event | category | flops | bytes accessed | tf_op | source)
XLA Modules:
  0.0 273.3 jit_solution(3037029236194131071)
XLA Ops:
  1.8 3.1 %collective-permute-start = (bf16[256,256]{1,0:T(8,128)(2,1)S(1)}, bf16[256,256]{1,0:T(8,128)(2,1)S(1)}, u32[]{:S(2)}, u32[]{:S(2)}) collective-permute-start(bf16[256,256]{1,0:T(8,128)(2,1)S(1)} %get-tuple-element.49), channel_id=1, source_target_pairs={{0,4},{4,8},{8,12},{12,0},{1,5},{5,9},{9,13},{13,1},{2,6},{6,10},{... | collective-permute-start | bytes 393224 | tf_op jit(solution)/shard_map/ppermute | solution.py:244
  12.3 3.8 %collective-permute-done.1.refs_3_ = bf16[256,256]{1,0:T(8,128)(2,1)S(1)} collective-permute-done((bf16[256,256]{1,0:T(8,128)(2,1)S(1)}, bf16[256,256]{1,0:T(8,128)(2,1)S(1)}, u32[]{:S(2)}, u32[]{:S(2)}) %collective-permute-start.1) | collective-permute-done | bytes 131104 | tf_op jit(solution)/shard_map/ppermute | solution.py:244
  18.3 6.6 %collective-permute-done.3.refs_2_ = bf16[512,256]{1,0:T(8,128)(2,1)S(1)} collective-permute-done((bf16[512,256]{1,0:T(8,128)(2,1)S(1)}, bf16[512,256]{1,0:T(8,128)(2,1)S(1)}, u32[]{:S(2)}, u32[]{:S(2)}) %collective-permute-start.3) | collective-permute-done | bytes 262176 | tf_op jit(solution)/shard_map/ppermute | solution.py:126
  28.3 5.3 %collective-permute-done.9.refs_2_ = bf16[512,256]{1,0:T(8,128)(2,1)S(1)} collective-permute-done((bf16[512,256]{1,0:T(8,128)(2,1)S(1)}, bf16[512,256]{1,0:T(8,128)(2,1)S(1)}, u32[]{:S(2)}, u32[]{:S(2)}) %collective-permute-start.9) | collective-permute-done | bytes 262176 | tf_op jit(solution)/shard_map/ppermute | solution.py:126
  33.6 3.4 %collective-permute-start.6 = (bf16[528,384]{1,0:T(8,128)(2,1)S(1)}, bf16[528,384]{1,0:T(8,128)(2,1)S(1)}, u32[]{:S(2)}, u32[]{:S(2)}) collective-permute-start(bf16[528,384]{1,0:T(8,128)(2,1)S(1)} %get-tuple-element.55), channel_id=1, source_target_pairs={{0,4},{4,8},{8,12},{12,0},{1,5},{5,9},{9,13},{13,1},{2,6},{6,10},{... | collective-permute-start | bytes 1216520 | tf_op jit(solution)/shard_map/ppermute | solution.py:584
  40.3 7.5 %collective-permute-done.6.refs_4_ = bf16[528,384]{1,0:T(8,128)(2,1)S(1)} collective-permute-done((bf16[528,384]{1,0:T(8,128)(2,1)S(1)}, bf16[528,384]{1,0:T(8,128)(2,1)S(1)}, u32[]{:S(2)}, u32[]{:S(2)}) %collective-permute-start.6) | collective-permute-done | bytes 405536 | tf_op jit(solution)/shard_map/ppermute | solution.py:584
  50.6 5.8 %collective-permute-done.12.refs_4_ = bf16[528,384]{1,0:T(8,128)(2,1)S(1)} collective-permute-done((bf16[528,384]{1,0:T(8,128)(2,1)S(1)}, bf16[528,384]{1,0:T(8,128)(2,1)S(1)}, u32[]{:S(2)}, u32[]{:S(2)}) %collective-permute-start.12) | collective-permute-done | bytes 405536 | tf_op jit(solution)/shard_map/ppermute | solution.py:584
  57.6 3.5 %collective-permute-start.13 = (bf16[528,384]{1,0:T(8,128)(2,1)S(1)}, bf16[528,384]{1,0:T(8,128)(2,1)S(1)}, u32[]{:S(2)}, u32[]{:S(2)}) collective-permute-start(bf16[528,384]{1,0:T(8,128)(2,1)S(1)} %shard_map.81), channel_id=1, source_target_pairs={{0,12},{4,0},{8,4},{12,8},{1,13},{5,1},{9,5},{13,9},{2,14},{6,2},{... | collective-permute-start | bytes 1216520 | tf_op jit(solution)/shard_map/ppermute | solution.py:584
  61.1 4.0 %collective-permute-done.7.refs_4_ = bf16[528,384]{1,0:T(8,128)(2,1)S(1)} collective-permute-done((bf16[528,384]{1,0:T(8,128)(2,1)S(1)}, bf16[528,384]{1,0:T(8,128)(2,1)S(1)}, u32[]{:S(2)}, u32[]{:S(2)}) %collective-permute-start.7) | collective-permute-done | bytes 405536 | tf_op jit(solution)/shard_map/ppermute | solution.py:584
  68.0 5.8 %collective-permute-done.13.refs_4_ = bf16[528,384]{1,0:T(8,128)(2,1)S(1)} collective-permute-done((bf16[528,384]{1,0:T(8,128)(2,1)S(1)}, bf16[528,384]{1,0:T(8,128)(2,1)S(1)}, u32[]{:S(2)}, u32[]{:S(2)}) %collective-permute-start.13) | collective-permute-done | bytes 405536 | tf_op jit(solution)/shard_map/ppermute | solution.py:584
  75.0 3.5 %collective-permute-start.14 = (bf16[528,384]{1,0:T(8,128)(2,1)S(1)}, bf16[528,384]{1,0:T(8,128)(2,1)S(1)}, u32[]{:S(2)}, u32[]{:S(2)}) collective-permute-start(bf16[528,384]{1,0:T(8,128)(2,1)S(1)} %shard_map.82), channel_id=1, source_target_pairs={{0,12},{4,0},{8,4},{12,8},{1,13},{5,1},{9,5},{13,9},{2,14},{6,2},{... | collective-permute-start | bytes 1216520 | tf_op jit(solution)/shard_map/ppermute | solution.py:584
  83.6 7.1 %collective-permute-done.14.refs_2_ = bf16[528,384]{1,0:T(8,128)(2,1)S(1)} collective-permute-done((bf16[528,384]{1,0:T(8,128)(2,1)S(1)}, bf16[528,384]{1,0:T(8,128)(2,1)S(1)}, u32[]{:S(2)}, u32[]{:S(2)}) %collective-permute-start.14) | collective-permute-done | bytes 405536 | tf_op jit(solution)/shard_map/ppermute | solution.py:584
  90.8 3.6 %shard_map.86 = (bf16[512,128]{1,0:T(8,128)(2,1)S(1)}, bf16[1024,384]{1,0:T(8,128)(2,1)S(1)}) custom-call(s32[3]{0:T(128)S(1)} %pad_add_fusion.refs_0_, bf16[528,384]{1,0:T(8,128)(2,1)S(1)} %collective-permute-done.8.refs_1_, bf16[528,384]{1,0:T(8,128)(2,1)S(1)} %collective-permute-done.14.refs_2_, f32[512,384]{1,0:T(8,128)S(1)} %shard_map.83.refs_3_, ...), custom_call_target="tpu_custom_call" | custom-call | flops 134217728 | bytes 3842048 | tf_op jit(solution)/shard_map/pallas_call | solution.py:141
  95.0 3.4 %collective-permute-start.16 = (bf16[512,128]{1,0:T(8,128)(2,1)S(1)}, bf16[512,128]{1,0:T(8,128)(2,1)S(1)}, u32[]{:S(2)}, u32[]{:S(2)}) collective-permute-start(bf16[512,128]{1,0:T(8,128)(2,1)S(1)} %get-tuple-element.61.refs_1_), channel_id=1, source_target_pairs={{0,8},{4,12},{8,0},{12,4},{1,9},{5,13},{9,1},{13,5},{2,10},{6,14},... | collective-permute-start | bytes 393224 | tf_op jit(solution)/shard_map/ppermute | solution.py:244
  98.4 3.3 %shard_map.87.refs_6_.refs_1_ = bf16[512,128]{1,0:T(8,128)(2,1)S(1)} custom-call(s32[3]{0:T(128)S(1)} %pad_add_fusion.refs_0_, bf16[1024,384]{1,0:T(8,128)(2,1)S(1)} %get-tuple-element.62.refs_1_, f32[2,64,1024]{2,1,0:T(8,128)S(1)} %shard_map.74.refs_5_.refs_7_.refs_2_), custom_call_target="tpu_custom_call" | custom-call | flops 134217728 | bytes 1441792 | tf_op jit(solution)/shard_map/pallas_call | solution.py:141
  102.7 4.7 %collective-permute-done.16.refs_3_ = bf16[512,128]{1,0:T(8,128)(2,1)S(1)} collective-permute-done((bf16[512,128]{1,0:T(8,128)(2,1)S(1)}, bf16[512,128]{1,0:T(8,128)(2,1)S(1)}, u32[]{:S(2)}, u32[]{:S(2)}) %collective-permute-start.16) | collective-permute-done | bytes 131104 | tf_op jit(solution)/shard_map/ppermute | solution.py:244
  117.1 5.1 %collective-permute-done.25.refs_3_ = bf16[512,128]{1,0:T(8,128)(2,1)S(1)} collective-permute-done((bf16[512,128]{1,0:T(8,128)(2,1)S(1)}, bf16[512,128]{1,0:T(8,128)(2,1)S(1)}, u32[]{:S(2)}, u32[]{:S(2)}) %collective-permute-start.25) | collective-permute-done | bytes 131104 | tf_op jit(solution)/shard_map/ppermute | solution.py:244
  123.5 5.1 %collective-permute-done.19.refs_4_ = bf16[512,512]{1,0:T(8,128)(2,1)S(1)} collective-permute-done((bf16[512,512]{1,0:T(8,128)(2,1)S(1)}, bf16[512,512]{1,0:T(8,128)(2,1)S(1)}, u32[]{:S(2)}, u32[]{:S(2)}) %collective-permute-start.19) | collective-permute-done | bytes 524320 | tf_op jit(solution)/shard_map/ppermute | solution.py:126
  133.4 11.2 %collective-permute-done.28.refs_4_ = bf16[512,512]{1,0:T(8,128)(2,1)S(1)} collective-permute-done((bf16[512,512]{1,0:T(8,128)(2,1)S(1)}, bf16[512,512]{1,0:T(8,128)(2,1)S(1)}, u32[]{:S(2)}, u32[]{:S(2)}) %collective-permute-start.28) | collective-permute-done | bytes 524320 | tf_op jit(solution)/shard_map/ppermute | solution.py:126
  150.9 8.6 %collective-permute-done.21.refs_4_ = bf16[528,384]{1,0:T(8,128)(2,1)S(1)} collective-permute-done((bf16[528,384]{1,0:T(8,128)(2,1)S(1)}, bf16[528,384]{1,0:T(8,128)(2,1)S(1)}, u32[]{:S(2)}, u32[]{:S(2)}) %collective-permute-start.21) | collective-permute-done | bytes 405536 | tf_op jit(solution)/shard_map/ppermute | solution.py:584
  160.9 7.4 %collective-permute-done.30.refs_4_ = bf16[528,384]{1,0:T(8,128)(2,1)S(1)} collective-permute-done((bf16[528,384]{1,0:T(8,128)(2,1)S(1)}, bf16[528,384]{1,0:T(8,128)(2,1)S(1)}, u32[]{:S(2)}, u32[]{:S(2)}) %collective-permute-start.30) | collective-permute-done | bytes 405536 | tf_op jit(solution)/shard_map/ppermute | solution.py:584
  169.6 7.4 %collective-permute-done.22.refs_4_ = bf16[528,384]{1,0:T(8,128)(2,1)S(1)} collective-permute-done((bf16[528,384]{1,0:T(8,128)(2,1)S(1)}, bf16[528,384]{1,0:T(8,128)(2,1)S(1)}, u32[]{:S(2)}, u32[]{:S(2)}) %collective-permute-start.22) | collective-permute-done | bytes 405536 | tf_op jit(solution)/shard_map/ppermute | solution.py:584
  178.3 7.3 %collective-permute-done.31.refs_4_ = bf16[528,384]{1,0:T(8,128)(2,1)S(1)} collective-permute-done((bf16[528,384]{1,0:T(8,128)(2,1)S(1)}, bf16[528,384]{1,0:T(8,128)(2,1)S(1)}, u32[]{:S(2)}, u32[]{:S(2)}) %collective-permute-start.31) | collective-permute-done | bytes 405536 | tf_op jit(solution)/shard_map/ppermute | solution.py:584
  189.5 4.9 %collective-permute-done.23.refs_1_ = bf16[528,384]{1,0:T(8,128)(2,1)S(1)} collective-permute-done((bf16[528,384]{1,0:T(8,128)(2,1)S(1)}, bf16[528,384]{1,0:T(8,128)(2,1)S(1)}, u32[]{:S(2)}, u32[]{:S(2)}) %collective-permute-start.23) | collective-permute-done | bytes 405536 | tf_op jit(solution)/shard_map/ppermute | solution.py:584
  194.4 8.1 %collective-permute-done.32.refs_2_ = bf16[528,384]{1,0:T(8,128)(2,1)S(1)} collective-permute-done((bf16[528,384]{1,0:T(8,128)(2,1)S(1)}, bf16[528,384]{1,0:T(8,128)(2,1)S(1)}, u32[]{:S(2)}, u32[]{:S(2)}) %collective-permute-start.32) | collective-permute-done | bytes 405536 | tf_op jit(solution)/shard_map/ppermute | solution.py:584
  202.5 3.6 %shard_map.102 = (bf16[512,128]{1,0:T(8,128)(2,1)S(1)}, bf16[1024,384]{1,0:T(8,128)(2,1)S(1)}) custom-call(s32[3]{0:T(128)S(1)} %pad_add_fusion.refs_0_, bf16[528,384]{1,0:T(8,128)(2,1)S(1)} %collective-permute-done.23.refs_1_, bf16[528,384]{1,0:T(8,128)(2,1)S(1)} %collective-permute-done.32.refs_2_, f32[512,384]{1,0:T(8,128)S(1)} %shard_map.100.refs_3_, ...), custom_call_target="tpu_custom_call" | custom-call | flops 134217728 | bytes 3842048 | tf_op jit(solution)/shard_map/pallas_call | solution.py:141
  210.0 3.3 %shard_map.103.refs_6_.refs_1_ = bf16[512,128]{1,0:T(8,128)(2,1)S(1)} custom-call(s32[3]{0:T(128)S(1)} %pad_add_fusion.refs_0_, bf16[1024,384]{1,0:T(8,128)(2,1)S(1)} %get-tuple-element.74.refs_1_, f32[2,64,1024]{2,1,0:T(8,128)S(1)} %shard_map.74.refs_5_.refs_7_.refs_2_), custom_call_target="tpu_custom_call" | custom-call | flops 134217728 | bytes 1441792 | tf_op jit(solution)/shard_map/pallas_call | solution.py:141
  214.5 4.7 %collective-permute-done.34.refs_3_ = bf16[512,128]{1,0:T(8,128)(2,1)S(1)} collective-permute-done((bf16[512,128]{1,0:T(8,128)(2,1)S(1)}, bf16[512,128]{1,0:T(8,128)(2,1)S(1)}, u32[]{:S(2)}, u32[]{:S(2)}) %collective-permute-start.34) | collective-permute-done | bytes 131104 | tf_op jit(solution)/shard_map/ppermute | solution.py:244
  228.9 5.1 %collective-permute-done.45.refs_3_ = bf16[512,128]{1,0:T(8,128)(2,1)S(1)} collective-permute-done((bf16[512,128]{1,0:T(8,128)(2,1)S(1)}, bf16[512,128]{1,0:T(8,128)(2,1)S(1)}, u32[]{:S(2)}, u32[]{:S(2)}) %collective-permute-start.45) | collective-permute-done | bytes 131104 | tf_op jit(solution)/shard_map/ppermute | solution.py:244
  239.5 5.1 %collective-permute-done.37.refs_3_ = bf16[512,256]{1,0:T(8,128)(2,1)S(1)} collective-permute-done((bf16[512,256]{1,0:T(8,128)(2,1)S(1)}, bf16[512,256]{1,0:T(8,128)(2,1)S(1)}, u32[]{:S(2)}, u32[]{:S(2)}) %collective-permute-start.37) | collective-permute-done | bytes 262176 | tf_op jit(solution)/shard_map/ppermute | solution.py:126
  245.3 3.3 %collective-permute-start.38 = (bf16[128,256]{1,0:T(8,128)(2,1)S(1)}, bf16[128,256]{1,0:T(8,128)(2,1)S(1)}, u32[]{:S(2)}, u32[]{:S(2)}) collective-permute-start(bf16[128,256]{1,0:T(8,128)(2,1)S(1)} %get-tuple-element.80), channel_id=1, source_target_pairs={{0,4},{4,8},{8,12},{12,0},{1,5},{5,9},{9,13},{13,1},{2,6},{6,10},{... | collective-permute-start | bytes 196616 | tf_op jit(solution)/shard_map/ppermute | solution.py:244
  265.7 3.9 %collective-permute-done.52.refs_6_ = bf16[512,256]{1,0:T(8,128)(2,1)S(1)} collective-permute-done((bf16[512,256]{1,0:T(8,128)(2,1)S(1)}, bf16[512,256]{1,0:T(8,128)(2,1)S(1)}, u32[]{:S(2)}, u32[]{:S(2)}) %collective-permute-start.52) | collective-permute-done | bytes 262176 | tf_op jit(solution)/shard_map/ppermute | solution.py:126
  (126 shorter events, 104.3 us)
Async XLA Ops:
  1.8 10.5 %collective-permute-start = (bf16[256,256]{1,0:T(8,128)(2,1)S(1)}, bf16[256,256]{1,0:T(8,128)(2,1)S(1)}, u32[]{:S(2)}, u32[]{:S(2)}) collective-permute-start(bf16[256,256]{1,0:T(8,128)(2,1)S(1)} %get-tuple-element.49), channel_id=1, source_target_pairs={{0,4},{4,8},{8,12},{12,0},{1,5},{5,9},{9,13},{13,1},{2,6},{6,10},{... | collective-permute-start | bytes 393224 | tf_op jit(solution)/shard_map/ppermute | solution.py:244
  4.9 11.2 %collective-permute-start.1 = (bf16[256,256]{1,0:T(8,128)(2,1)S(1)}, bf16[256,256]{1,0:T(8,128)(2,1)S(1)}, u32[]{:S(2)}, u32[]{:S(2)}) collective-permute-start(bf16[256,256]{1,0:T(8,128)(2,1)S(1)} %get-tuple-element.50), channel_id=1, source_target_pairs={{0,8},{4,12},{8,0},{12,4},{1,9},{5,13},{9,1},{13,5},{2,10},{6,14},... | collective-permute-start | bytes 393224 | tf_op jit(solution)/shard_map/ppermute | solution.py:244
  7.5 8.6 %collective-permute-start.2 = (bf16[256,256]{1,0:T(8,128)(2,1)S(1)}, bf16[256,256]{1,0:T(8,128)(2,1)S(1)}, u32[]{:S(2)}, u32[]{:S(2)}) collective-permute-start(bf16[256,256]{1,0:T(8,128)(2,1)S(1)} %get-tuple-element.51), channel_id=1, source_target_pairs={{0,12},{4,0},{8,4},{12,8},{1,13},{5,1},{9,5},{13,9},{2,14},{6,2},{... | collective-permute-start | bytes 393224 | tf_op jit(solution)/shard_map/ppermute | solution.py:244
  24.9 8.7 %collective-permute-start.9 = (bf16[512,256]{1,0:T(8,128)(2,1)S(1)}, bf16[512,256]{1,0:T(8,128)(2,1)S(1)}, u32[]{:S(2)}, u32[]{:S(2)}) collective-permute-start(bf16[512,256]{1,0:T(8,128)(2,1)S(1)} %get-tuple-element.56.refs_1_), channel_id=1, source_target_pairs={{0,2},{1,3},{2,0},{3,1},{4,6},{5,7},{6,4},{7,5},{8,10},{9,11},{10,... | collective-permute-start | bytes 786440 | tf_op jit(solution)/shard_map/ppermute | solution.py:126
  26.4 10.6 %collective-permute-start.10 = (bf16[512,256]{1,0:T(8,128)(2,1)S(1)}, bf16[512,256]{1,0:T(8,128)(2,1)S(1)}, u32[]{:S(2)}, u32[]{:S(2)}) collective-permute-start(bf16[512,256]{1,0:T(8,128)(2,1)S(1)} %get-tuple-element.56.refs_1_), channel_id=1, source_target_pairs={{0,1},{1,0},{2,3},{3,2},{4,5},{5,4},{6,7},{7,6},{8,9},{9,8},{10,11... | collective-permute-start | bytes 786440 | tf_op jit(solution)/shard_map/ppermute | solution.py:126
  33.6 14.1 %collective-permute-start.6 = (bf16[528,384]{1,0:T(8,128)(2,1)S(1)}, bf16[528,384]{1,0:T(8,128)(2,1)S(1)}, u32[]{:S(2)}, u32[]{:S(2)}) collective-permute-start(bf16[528,384]{1,0:T(8,128)(2,1)S(1)} %get-tuple-element.55), channel_id=1, source_target_pairs={{0,4},{4,8},{8,12},{12,0},{1,5},{5,9},{9,13},{13,1},{2,6},{6,10},{... | collective-permute-start | bytes 1216520 | tf_op jit(solution)/shard_map/ppermute | solution.py:584
  38.7 17.7 %collective-permute-start.12 = (bf16[528,384]{1,0:T(8,128)(2,1)S(1)}, bf16[528,384]{1,0:T(8,128)(2,1)S(1)}, u32[]{:S(2)}, u32[]{:S(2)}) collective-permute-start(bf16[528,384]{1,0:T(8,128)(2,1)S(1)} %get-tuple-element.60), channel_id=1, source_target_pairs={{0,12},{4,0},{8,4},{12,8},{1,13},{5,1},{9,5},{13,9},{2,14},{6,2},{... | collective-permute-start | bytes 1216520 | tf_op jit(solution)/shard_map/ppermute | solution.py:584
  49.0 16.2 %collective-permute-start.7 = (bf16[528,384]{1,0:T(8,128)(2,1)S(1)}, bf16[528,384]{1,0:T(8,128)(2,1)S(1)}, u32[]{:S(2)}, u32[]{:S(2)}) collective-permute-start(bf16[528,384]{1,0:T(8,128)(2,1)S(1)} %shard_map.78), channel_id=1, source_target_pairs={{0,4},{4,8},{8,12},{12,0},{1,5},{5,9},{9,13},{13,1},{2,6},{6,10},{... | collective-permute-start | bytes 1216520 | tf_op jit(solution)/shard_map/ppermute | solution.py:584
  57.6 16.2 %collective-permute-start.13 = (bf16[528,384]{1,0:T(8,128)(2,1)S(1)}, bf16[528,384]{1,0:T(8,128)(2,1)S(1)}, u32[]{:S(2)}, u32[]{:S(2)}) collective-permute-start(bf16[528,384]{1,0:T(8,128)(2,1)S(1)} %shard_map.81), channel_id=1, source_target_pairs={{0,12},{4,0},{8,4},{12,8},{1,13},{5,1},{9,5},{13,9},{2,14},{6,2},{... | collective-permute-start | bytes 1216520 | tf_op jit(solution)/shard_map/ppermute | solution.py:584
  66.4 17.2 %collective-permute-start.8 = (bf16[528,384]{1,0:T(8,128)(2,1)S(1)}, bf16[528,384]{1,0:T(8,128)(2,1)S(1)}, u32[]{:S(2)}, u32[]{:S(2)}) collective-permute-start(bf16[528,384]{1,0:T(8,128)(2,1)S(1)} %shard_map.79), channel_id=1, source_target_pairs={{0,4},{4,8},{8,12},{12,0},{1,5},{5,9},{9,13},{13,1},{2,6},{6,10},{... | collective-permute-start | bytes 1216520 | tf_op jit(solution)/shard_map/ppermute | solution.py:584
  75.0 15.7 %collective-permute-start.14 = (bf16[528,384]{1,0:T(8,128)(2,1)S(1)}, bf16[528,384]{1,0:T(8,128)(2,1)S(1)}, u32[]{:S(2)}, u32[]{:S(2)}) collective-permute-start(bf16[528,384]{1,0:T(8,128)(2,1)S(1)} %shard_map.82), channel_id=1, source_target_pairs={{0,12},{4,0},{8,4},{12,8},{1,13},{5,1},{9,5},{13,9},{2,14},{6,2},{... | collective-permute-start | bytes 1216520 | tf_op jit(solution)/shard_map/ppermute | solution.py:584
  95.0 12.4 %collective-permute-start.16 = (bf16[512,128]{1,0:T(8,128)(2,1)S(1)}, bf16[512,128]{1,0:T(8,128)(2,1)S(1)}, u32[]{:S(2)}, u32[]{:S(2)}) collective-permute-start(bf16[512,128]{1,0:T(8,128)(2,1)S(1)} %get-tuple-element.61.refs_1_), channel_id=1, source_target_pairs={{0,8},{4,12},{8,0},{12,4},{1,9},{5,13},{9,1},{13,5},{2,10},{6,14},... | collective-permute-start | bytes 393224 | tf_op jit(solution)/shard_map/ppermute | solution.py:244
  98.4 9.0 %collective-permute-start.17 = (bf16[512,128]{1,0:T(8,128)(2,1)S(1)}, bf16[512,128]{1,0:T(8,128)(2,1)S(1)}, u32[]{:S(2)}, u32[]{:S(2)}) collective-permute-start(bf16[512,128]{1,0:T(8,128)(2,1)S(1)} %get-tuple-element.61.refs_1_), channel_id=1, source_target_pairs={{0,12},{4,0},{8,4},{12,8},{1,13},{5,1},{9,5},{13,9},{2,14},{6,2},{... | collective-permute-start | bytes 393224 | tf_op jit(solution)/shard_map/ppermute | solution.py:244
  111.8 10.3 %collective-permute-start.25 = (bf16[512,128]{1,0:T(8,128)(2,1)S(1)}, bf16[512,128]{1,0:T(8,128)(2,1)S(1)}, u32[]{:S(2)}, u32[]{:S(2)}) collective-permute-start(bf16[512,128]{1,0:T(8,128)(2,1)S(1)} %shard_map.87.refs_6_.refs_1_), channel_id=1, source_target_pairs={{0,8},{4,12},{8,0},{12,4},{1,9},{5,13},{9,1},{13,5},{2,10},{6,14},... | collective-permute-start | bytes 393224 | tf_op jit(solution)/shard_map/ppermute | solution.py:244
  111.9 10.2 %collective-permute-start.26 = (bf16[512,128]{1,0:T(8,128)(2,1)S(1)}, bf16[512,128]{1,0:T(8,128)(2,1)S(1)}, u32[]{:S(2)}, u32[]{:S(2)}) collective-permute-start(bf16[512,128]{1,0:T(8,128)(2,1)S(1)} %shard_map.87.refs_6_.refs_1_), channel_id=1, source_target_pairs={{0,12},{4,0},{8,4},{12,8},{1,13},{5,1},{9,5},{13,9},{2,14},{6,2},{... | collective-permute-start | bytes 393224 | tf_op jit(solution)/shard_map/ppermute | solution.py:244
  114.9 13.7 %collective-permute-start.19 = (bf16[512,512]{1,0:T(8,128)(2,1)S(1)}, bf16[512,512]{1,0:T(8,128)(2,1)S(1)}, u32[]{:S(2)}, u32[]{:S(2)}) collective-permute-start(bf16[512,512]{1,0:T(8,128)(2,1)S(1)} %shard_map.89.refs_3_.refs_6_), channel_id=1, source_target_pairs={{0,2},{1,3},{2,0},{3,1},{4,6},{5,7},{6,4},{7,5},{8,10},{9,11},{10,... | collective-permute-start | bytes 1572872 | tf_op jit(solution)/shard_map/ppermute | solution.py:126
  130.2 14.4 %collective-permute-start.28 = (bf16[512,512]{1,0:T(8,128)(2,1)S(1)}, bf16[512,512]{1,0:T(8,128)(2,1)S(1)}, u32[]{:S(2)}, u32[]{:S(2)}) collective-permute-start(bf16[512,512]{1,0:T(8,128)(2,1)S(1)} %shard_map.95.refs_3_), channel_id=1, source_target_pairs={{0,2},{1,3},{2,0},{3,1},{4,6},{5,7},{6,4},{7,5},{8,10},{9,11},{10,... | collective-permute-start | bytes 1572872 | tf_op jit(solution)/shard_map/ppermute | solution.py:126
  145.4 14.2 %collective-permute-start.21 = (bf16[528,384]{1,0:T(8,128)(2,1)S(1)}, bf16[528,384]{1,0:T(8,128)(2,1)S(1)}, u32[]{:S(2)}, u32[]{:S(2)}) collective-permute-start(bf16[528,384]{1,0:T(8,128)(2,1)S(1)} %get-tuple-element.67.refs_5_), channel_id=1, source_target_pairs={{0,4},{4,8},{8,12},{12,0},{1,5},{5,9},{9,13},{13,1},{2,6},{6,10},{... | collective-permute-start | bytes 1216520 | tf_op jit(solution)/shard_map/ppermute | solution.py:584
  148.9 19.4 %collective-permute-start.30 = (bf16[528,384]{1,0:T(8,128)(2,1)S(1)}, bf16[528,384]{1,0:T(8,128)(2,1)S(1)}, u32[]{:S(2)}, u32[]{:S(2)}) collective-permute-start(bf16[528,384]{1,0:T(8,128)(2,1)S(1)} %get-tuple-element.72), channel_id=1, source_target_pairs={{0,12},{4,0},{8,4},{12,8},{1,13},{5,1},{9,5},{13,9},{2,14},{6,2},{... | collective-permute-start | bytes 1216520 | tf_op jit(solution)/shard_map/ppermute | solution.py:584
  160.8 16.2 %collective-permute-start.22 = (bf16[528,384]{1,0:T(8,128)(2,1)S(1)}, bf16[528,384]{1,0:T(8,128)(2,1)S(1)}, u32[]{:S(2)}, u32[]{:S(2)}) collective-permute-start(bf16[528,384]{1,0:T(8,128)(2,1)S(1)} %shard_map.92), channel_id=1, source_target_pairs={{0,4},{4,8},{8,12},{12,0},{1,5},{5,9},{9,13},{13,1},{2,6},{6,10},{... | collective-permute-start | bytes 1216520 | tf_op jit(solution)/shard_map/ppermute | solution.py:584
  169.5 16.1 %collective-permute-start.31 = (bf16[528,384]{1,0:T(8,128)(2,1)S(1)}, bf16[528,384]{1,0:T(8,128)(2,1)S(1)}, u32[]{:S(2)}, u32[]{:S(2)}) collective-permute-start(bf16[528,384]{1,0:T(8,128)(2,1)S(1)} %shard_map.98), channel_id=1, source_target_pairs={{0,12},{4,0},{8,4},{12,8},{1,13},{5,1},{9,5},{13,9},{2,14},{6,2},{... | collective-permute-start | bytes 1216520 | tf_op jit(solution)/shard_map/ppermute | solution.py:584
  178.2 16.2 %collective-permute-start.23 = (bf16[528,384]{1,0:T(8,128)(2,1)S(1)}, bf16[528,384]{1,0:T(8,128)(2,1)S(1)}, u32[]{:S(2)}, u32[]{:S(2)}) collective-permute-start(bf16[528,384]{1,0:T(8,128)(2,1)S(1)} %shard_map.93), channel_id=1, source_target_pairs={{0,4},{4,8},{8,12},{12,0},{1,5},{5,9},{9,13},{13,1},{2,6},{6,10},{... | collective-permute-start | bytes 1216520 | tf_op jit(solution)/shard_map/ppermute | solution.py:584
  186.9 15.7 %collective-permute-start.32 = (bf16[528,384]{1,0:T(8,128)(2,1)S(1)}, bf16[528,384]{1,0:T(8,128)(2,1)S(1)}, u32[]{:S(2)}, u32[]{:S(2)}) collective-permute-start(bf16[528,384]{1,0:T(8,128)(2,1)S(1)} %shard_map.99), channel_id=1, source_target_pairs={{0,12},{4,0},{8,4},{12,8},{1,13},{5,1},{9,5},{13,9},{2,14},{6,2},{... | collective-permute-start | bytes 1216520 | tf_op jit(solution)/shard_map/ppermute | solution.py:584
  206.8 12.4 %collective-permute-start.34 = (bf16[512,128]{1,0:T(8,128)(2,1)S(1)}, bf16[512,128]{1,0:T(8,128)(2,1)S(1)}, u32[]{:S(2)}, u32[]{:S(2)}) collective-permute-start(bf16[512,128]{1,0:T(8,128)(2,1)S(1)} %get-tuple-element.73.refs_1_), channel_id=1, source_target_pairs={{0,8},{4,12},{8,0},{12,4},{1,9},{5,13},{9,1},{13,5},{2,10},{6,14},... | collective-permute-start | bytes 393224 | tf_op jit(solution)/shard_map/ppermute | solution.py:244
  207.0 12.1 %collective-permute-start.35 = (bf16[512,128]{1,0:T(8,128)(2,1)S(1)}, bf16[512,128]{1,0:T(8,128)(2,1)S(1)}, u32[]{:S(2)}, u32[]{:S(2)}) collective-permute-start(bf16[512,128]{1,0:T(8,128)(2,1)S(1)} %get-tuple-element.73.refs_1_), channel_id=1, source_target_pairs={{0,12},{4,0},{8,4},{12,8},{1,13},{5,1},{9,5},{13,9},{2,14},{6,2},{... | collective-permute-start | bytes 393224 | tf_op jit(solution)/shard_map/ppermute | solution.py:244
  223.3 10.7 %collective-permute-start.45 = (bf16[512,128]{1,0:T(8,128)(2,1)S(1)}, bf16[512,128]{1,0:T(8,128)(2,1)S(1)}, u32[]{:S(2)}, u32[]{:S(2)}) collective-permute-start(bf16[512,128]{1,0:T(8,128)(2,1)S(1)} %shard_map.103.refs_6_.refs_1_), channel_id=1, source_target_pairs={{0,8},{4,12},{8,0},{12,4},{1,9},{5,13},{9,1},{13,5},{2,10},{6,14},... | collective-permute-start | bytes 393224 | tf_op jit(solution)/shard_map/ppermute | solution.py:244
  223.6 10.4 %collective-permute-start.46 = (bf16[512,128]{1,0:T(8,128)(2,1)S(1)}, bf16[512,128]{1,0:T(8,128)(2,1)S(1)}, u32[]{:S(2)}, u32[]{:S(2)}) collective-permute-start(bf16[512,128]{1,0:T(8,128)(2,1)S(1)} %shard_map.103.refs_6_.refs_1_), channel_id=1, source_target_pairs={{0,12},{4,0},{8,4},{12,8},{1,13},{5,1},{9,5},{13,9},{2,14},{6,2},{... | collective-permute-start | bytes 393224 | tf_op jit(solution)/shard_map/ppermute | solution.py:244
  235.4 9.2 %collective-permute-start.37 = (bf16[512,256]{1,0:T(8,128)(2,1)S(1)}, bf16[512,256]{1,0:T(8,128)(2,1)S(1)}, u32[]{:S(2)}, u32[]{:S(2)}) collective-permute-start(bf16[512,256]{1,0:T(8,128)(2,1)S(1)} %get-tuple-element.78.refs_6_), channel_id=1, source_target_pairs={{0,2},{1,3},{2,0},{3,1},{4,6},{5,7},{6,4},{7,5},{8,10},{9,11},{10,... | collective-permute-start | bytes 786440 | tf_op jit(solution)/shard_map/ppermute | solution.py:126
  237.9 13.1 %collective-permute-start.48 = (bf16[512,256]{1,0:T(8,128)(2,1)S(1)}, bf16[512,256]{1,0:T(8,128)(2,1)S(1)}, u32[]{:S(2)}, u32[]{:S(2)}) collective-permute-start(bf16[512,256]{1,0:T(8,128)(2,1)S(1)} %get-tuple-element.86), channel_id=1, source_target_pairs={{0,2},{1,3},{2,0},{3,1},{4,6},{5,7},{6,4},{7,5},{8,10},{9,11},{10,... | collective-permute-start | bytes 786440 | tf_op jit(solution)/shard_map/ppermute | solution.py:126
  245.3 9.9 %collective-permute-start.38 = (bf16[128,256]{1,0:T(8,128)(2,1)S(1)}, bf16[128,256]{1,0:T(8,128)(2,1)S(1)}, u32[]{:S(2)}, u32[]{:S(2)}) collective-permute-start(bf16[128,256]{1,0:T(8,128)(2,1)S(1)} %get-tuple-element.80), channel_id=1, source_target_pairs={{0,4},{4,8},{8,12},{12,0},{1,5},{5,9},{9,13},{13,1},{2,6},{6,10},{... | collective-permute-start | bytes 196616 | tf_op jit(solution)/shard_map/ppermute | solution.py:244
  256.7 8.5 %collective-permute-start.41 = (bf16[512,256]{1,0:T(8,128)(2,1)S(1)}, bf16[512,256]{1,0:T(8,128)(2,1)S(1)}, u32[]{:S(2)}, u32[]{:S(2)}) collective-permute-start(bf16[512,256]{1,0:T(8,128)(2,1)S(1)} %shard_map.107.refs_1_), channel_id=1, source_target_pairs={{0,2},{1,3},{2,0},{3,1},{4,6},{5,7},{6,4},{7,5},{8,10},{9,11},{10,... | collective-permute-start | bytes 786440 | tf_op jit(solution)/shard_map/ppermute | solution.py:126
  260.8 8.8 %collective-permute-start.52 = (bf16[512,256]{1,0:T(8,128)(2,1)S(1)}, bf16[512,256]{1,0:T(8,128)(2,1)S(1)}, u32[]{:S(2)}, u32[]{:S(2)}) collective-permute-start(bf16[512,256]{1,0:T(8,128)(2,1)S(1)} %shard_map.111.refs_5_), channel_id=1, source_target_pairs={{0,2},{1,3},{2,0},{3,1},{4,6},{5,7},{6,4},{7,5},{8,10},{9,11},{10,... | collective-permute-start | bytes 786440 | tf_op jit(solution)/shard_map/ppermute | solution.py:126
  (26 other events, 163.5 us)

commit v7 on v6

--- a/solution.py
+++ b/solution.py
@@ -372,28 +372,37 @@
     grid_rows = qkv_ref.shape[0] // GRID_W
     width = heads * HD
     part_grid = grid_rows // sp_count // 2
+    done = []
     for head in range(heads):
         lanes = head * HD
-        for index in range(sp_count * part_grid):
-            plane, inner = divmod(index, part_grid)
-            row = (2 * plane + part) * part_grid + inner
-            first = min(max(row - KR // 2, 0), grid_rows - KR)
-            offset = first - row + KR - 1
-            queries = qkv_ref[pl.ds(row * GRID_W, GRID_W), pl.ds(lanes, HD)]
-            span = pl.ds(first * GRID_W, KR * GRID_W)
+        for plane in range(sp_count):
+            rows = [(2 * plane + part) * part_grid + inner for inner in range(part_grid)]
+            firsts = [min(max(row - KR // 2, 0), grid_rows - KR) for row in rows]
+            low, reach = firsts[0], firsts[-1] - firsts[0] + KR
+            queries = qkv_ref[pl.ds(rows[0] * GRID_W, part_grid * GRID_W), pl.ds(lanes, HD)]
+            span = pl.ds(low * GRID_W, reach * GRID_W)
             keys = qkv_ref[span, pl.ds(width + lanes, HD)]
             values = qkv_ref[span, pl.ds(2 * width + lanes, HD)]
             scores = lax.dot_general(
                 queries, keys, (((1,), (1,)), ((), ())), preferred_element_type=jnp.float32
             )
-            bias_here = bias_ref[layer * heads + head, :, pl.ds(offset * GRID_W, KR * GRID_W)]
-            scores = scores * HD ** (-0.5) + bias_here
+            biases = []
+            for row, first in zip(rows, firsts):
+                offset = low - row + KR - 1
+                here = bias_ref[layer * heads + head, :, pl.ds(offset * GRID_W, reach * GRID_W)]
+                if reach > KR:
+                    key_row = lax.broadcasted_iota(jnp.int32, here.shape, 1) // GRID_W + low
+                    here = jnp.where((key_row >= first) & (key_row < first + KR), here, -jnp.inf)
+                biases.append(here)
+            scores = scores * HD ** (-0.5) + jnp.concatenate(biases, axis=0)
             powers = jnp.exp(scores - jnp.max(scores, axis=-1, keepdims=True))
             weights = powers * (1.0 / jnp.sum(powers, axis=-1, keepdims=True))
             mixed = jnp.dot(
                 weights.astype(jnp.bfloat16), values, preferred_element_type=jnp.float32
             )
-            out_ref[pl.ds(index * GRID_W, GRID_W), pl.ds(lanes, HD)] = mixed.astype(jnp.bfloat16)
+            done.append((plane * part_grid * GRID_W, lanes, mixed.astype(jnp.bfloat16)))
+    for at, lanes, block in done:
+        out_ref[pl.ds(at, part_grid * GRID_W), pl.ds(lanes, HD)] = block
 
 
 def attend(arrived, own, squares, bias, place, sp_count, heads, layer, every_feat, after):

time: 273 us -> 271 us (level)
  Pallas kernels: 57.8 us -> 53.1 us
    pallas_call x40, Pallas kernels: 57.8 us -> 53.1 us  [local_kernel(): pl.pallas_call(ordered, out_shape=list(outs), in_specs=[smem] + [vmem] *...]
  transfers between devices with their start and end apart: 55 -> 55, of which waited for: 32 -> 32; matrix products, arithmetic and copies ran while one was open for 0% -> 0% of each run, Pallas kernels for 15% -> 14%
where the time goes in v7:
time: 271 us
  waiting for transfers between devices  150 us (55%)
  starting transfers between devices  66.8 us (25%)
  Pallas kernels  53.1 us (20%)
    ppermute x12, waiting for transfers between devices, sent_on(): return lax.ppermute(block, 'sp', ring(sp_count, shifts[part]))  73.9 us
    pallas_call x40, Pallas kernels, local_kernel(): pl.pallas_call(ordered, out_shape=list(outs), in_specs=[smem] + [vmem] *...  53.1 us
    ppermute x22, waiting for transfers between devices, swapped(): return lax.ppermute(array, axis, [(i, i ^ distance) for i in range(count)])  43.9 us
    ppermute x21, starting transfers between devices, over_sp(): lax.ppermute(blocks[shift], 'sp', ring(count, shift))  35.8 us
    ppermute x21, waiting for transfers between devices, over_sp(): lax.ppermute(blocks[shift], 'sp', ring(count, shift))  32.8 us
    ppermute x12, starting transfers between devices, sent_on(): return lax.ppermute(block, 'sp', ring(sp_count, shifts[part]))  17.5 us
    ppermute x22, starting transfers between devices, swapped(): return lax.ppermute(array, axis, [(i, i ^ distance) for i in range(count)])  13.5 us
  transfers between devices with their start and end apart: 55, of which 32 were waited for; matrix products, arithmetic and copies ran while one was open for 0% of the time, Pallas kernels for 14%

profile of v7, /device:TPU:0, one launch (start us, length us, event | category | flops | bytes accessed | tf_op | source)
XLA Modules:
  0.0 270.9 jit_solution(16137782636958964255)
XLA Ops:
  1.8 3.1 %collective-permute-start = (bf16[256,256]{1,0:T(8,128)(2,1)S(1)}, bf16[256,256]{1,0:T(8,128)(2,1)S(1)}, u32[]{:S(2)}, u32[]{:S(2)}) collective-permute-start(bf16[256,256]{1,0:T(8,128)(2,1)S(1)} %get-tuple-element.49), channel_id=1, source_target_pairs={{0,4},{4,8},{8,12},{12,0},{1,5},{5,9},{9,13},{13,1},{2,6},{6,10},{... | collective-permute-start | bytes 393224 | tf_op jit(solution)/shard_map/ppermute | solution.py:244
  12.3 3.8 %collective-permute-done.1.refs_3_ = bf16[256,256]{1,0:T(8,128)(2,1)S(1)} collective-permute-done((bf16[256,256]{1,0:T(8,128)(2,1)S(1)}, bf16[256,256]{1,0:T(8,128)(2,1)S(1)}, u32[]{:S(2)}, u32[]{:S(2)}) %collective-permute-start.1) | collective-permute-done | bytes 131104 | tf_op jit(solution)/shard_map/ppermute | solution.py:244
  18.3 6.6 %collective-permute-done.3.refs_2_ = bf16[512,256]{1,0:T(8,128)(2,1)S(1)} collective-permute-done((bf16[512,256]{1,0:T(8,128)(2,1)S(1)}, bf16[512,256]{1,0:T(8,128)(2,1)S(1)}, u32[]{:S(2)}, u32[]{:S(2)}) %collective-permute-start.3) | collective-permute-done | bytes 262176 | tf_op jit(solution)/shard_map/ppermute | solution.py:126
  28.3 5.3 %collective-permute-done.9.refs_2_ = bf16[512,256]{1,0:T(8,128)(2,1)S(1)} collective-permute-done((bf16[512,256]{1,0:T(8,128)(2,1)S(1)}, bf16[512,256]{1,0:T(8,128)(2,1)S(1)}, u32[]{:S(2)}, u32[]{:S(2)}) %collective-permute-start.9) | collective-permute-done | bytes 262176 | tf_op jit(solution)/shard_map/ppermute | solution.py:126
  33.6 3.4 %collective-permute-start.6 = (bf16[528,384]{1,0:T(8,128)(2,1)S(1)}, bf16[528,384]{1,0:T(8,128)(2,1)S(1)}, u32[]{:S(2)}, u32[]{:S(2)}) collective-permute-start(bf16[528,384]{1,0:T(8,128)(2,1)S(1)} %get-tuple-element.55), channel_id=1, source_target_pairs={{0,4},{4,8},{8,12},{12,0},{1,5},{5,9},{9,13},{13,1},{2,6},{6,10},{... | collective-permute-start | bytes 1216520 | tf_op jit(solution)/shard_map/ppermute | solution.py:593
  40.3 7.5 %collective-permute-done.6.refs_4_ = bf16[528,384]{1,0:T(8,128)(2,1)S(1)} collective-permute-done((bf16[528,384]{1,0:T(8,128)(2,1)S(1)}, bf16[528,384]{1,0:T(8,128)(2,1)S(1)}, u32[]{:S(2)}, u32[]{:S(2)}) %collective-permute-start.6) | collective-permute-done | bytes 405536 | tf_op jit(solution)/shard_map/ppermute | solution.py:593
  50.6 5.8 %collective-permute-done.12.refs_4_ = bf16[528,384]{1,0:T(8,128)(2,1)S(1)} collective-permute-done((bf16[528,384]{1,0:T(8,128)(2,1)S(1)}, bf16[528,384]{1,0:T(8,128)(2,1)S(1)}, u32[]{:S(2)}, u32[]{:S(2)}) %collective-permute-start.12) | collective-permute-done | bytes 405536 | tf_op jit(solution)/shard_map/ppermute | solution.py:593
  57.6 3.5 %collective-permute-start.13 = (bf16[528,384]{1,0:T(8,128)(2,1)S(1)}, bf16[528,384]{1,0:T(8,128)(2,1)S(1)}, u32[]{:S(2)}, u32[]{:S(2)}) collective-permute-start(bf16[528,384]{1,0:T(8,128)(2,1)S(1)} %shard_map.81), channel_id=1, source_target_pairs={{0,12},{4,0},{8,4},{12,8},{1,13},{5,1},{9,5},{13,9},{2,14},{6,2},{... | collective-permute-start | bytes 1216520 | tf_op jit(solution)/shard_map/ppermute | solution.py:593
  61.1 4.0 %collective-permute-done.7.refs_4_ = bf16[528,384]{1,0:T(8,128)(2,1)S(1)} collective-permute-done((bf16[528,384]{1,0:T(8,128)(2,1)S(1)}, bf16[528,384]{1,0:T(8,128)(2,1)S(1)}, u32[]{:S(2)}, u32[]{:S(2)}) %collective-permute-start.7) | collective-permute-done | bytes 405536 | tf_op jit(solution)/shard_map/ppermute | solution.py:593
  68.0 5.8 %collective-permute-done.13.refs_4_ = bf16[528,384]{1,0:T(8,128)(2,1)S(1)} collective-permute-done((bf16[528,384]{1,0:T(8,128)(2,1)S(1)}, bf16[528,384]{1,0:T(8,128)(2,1)S(1)}, u32[]{:S(2)}, u32[]{:S(2)}) %collective-permute-start.13) | collective-permute-done | bytes 405536 | tf_op jit(solution)/shard_map/ppermute | solution.py:593
  75.0 3.5 %collective-permute-start.14 = (bf16[528,384]{1,0:T(8,128)(2,1)S(1)}, bf16[528,384]{1,0:T(8,128)(2,1)S(1)}, u32[]{:S(2)}, u32[]{:S(2)}) collective-permute-start(bf16[528,384]{1,0:T(8,128)(2,1)S(1)} %shard_map.82), channel_id=1, source_target_pairs={{0,12},{4,0},{8,4},{12,8},{1,13},{5,1},{9,5},{13,9},{2,14},{6,2},{... | collective-permute-start | bytes 1216520 | tf_op jit(solution)/shard_map/ppermute | solution.py:593
  83.6 7.1 %collective-permute-done.14.refs_2_ = bf16[528,384]{1,0:T(8,128)(2,1)S(1)} collective-permute-done((bf16[528,384]{1,0:T(8,128)(2,1)S(1)}, bf16[528,384]{1,0:T(8,128)(2,1)S(1)}, u32[]{:S(2)}, u32[]{:S(2)}) %collective-permute-start.14) | collective-permute-done | bytes 405536 | tf_op jit(solution)/shard_map/ppermute | solution.py:593
  93.8 3.4 %collective-permute-start.16 = (bf16[512,128]{1,0:T(8,128)(2,1)S(1)}, bf16[512,128]{1,0:T(8,128)(2,1)S(1)}, u32[]{:S(2)}, u32[]{:S(2)}) collective-permute-start(bf16[512,128]{1,0:T(8,128)(2,1)S(1)} %get-tuple-element.61.refs_1_), channel_id=1, source_target_pairs={{0,8},{4,12},{8,0},{12,4},{1,9},{5,13},{9,1},{13,5},{2,10},{6,14},... | collective-permute-start | bytes 393224 | tf_op jit(solution)/shard_map/ppermute | solution.py:244
  101.5 4.7 %collective-permute-done.16.refs_3_ = bf16[512,128]{1,0:T(8,128)(2,1)S(1)} collective-permute-done((bf16[512,128]{1,0:T(8,128)(2,1)S(1)}, bf16[512,128]{1,0:T(8,128)(2,1)S(1)}, u32[]{:S(2)}, u32[]{:S(2)}) %collective-permute-start.16) | collective-permute-done | bytes 131104 | tf_op jit(solution)/shard_map/ppermute | solution.py:244
  107.6 3.1 %collective-permute-start.24 = (bf16[512,128]{1,0:T(8,128)(2,1)S(1)}, bf16[512,128]{1,0:T(8,128)(2,1)S(1)}, u32[]{:S(2)}, u32[]{:S(2)}) collective-permute-start(bf16[512,128]{1,0:T(8,128)(2,1)S(1)} %shard_map.87.refs_6_.refs_1_), channel_id=1, source_target_pairs={{0,4},{4,8},{8,12},{12,0},{1,5},{5,9},{9,13},{13,1},{2,6},{6,10},{... | collective-permute-start | bytes 393224 | tf_op jit(solution)/shard_map/ppermute | solution.py:244
  115.9 5.1 %collective-permute-done.25.refs_3_ = bf16[512,128]{1,0:T(8,128)(2,1)S(1)} collective-permute-done((bf16[512,128]{1,0:T(8,128)(2,1)S(1)}, bf16[512,128]{1,0:T(8,128)(2,1)S(1)}, u32[]{:S(2)}, u32[]{:S(2)}) %collective-permute-start.25) | collective-permute-done | bytes 131104 | tf_op jit(solution)/shard_map/ppermute | solution.py:244
  122.4 5.1 %collective-permute-done.19.refs_4_ = bf16[512,512]{1,0:T(8,128)(2,1)S(1)} collective-permute-done((bf16[512,512]{1,0:T(8,128)(2,1)S(1)}, bf16[512,512]{1,0:T(8,128)(2,1)S(1)}, u32[]{:S(2)}, u32[]{:S(2)}) %collective-permute-start.19) | collective-permute-done | bytes 524320 | tf_op jit(solution)/shard_map/ppermute | solution.py:126
  132.2 11.2 %collective-permute-done.28.refs_4_ = bf16[512,512]{1,0:T(8,128)(2,1)S(1)} collective-permute-done((bf16[512,512]{1,0:T(8,128)(2,1)S(1)}, bf16[512,512]{1,0:T(8,128)(2,1)S(1)}, u32[]{:S(2)}, u32[]{:S(2)}) %collective-permute-start.28) | collective-permute-done | bytes 524320 | tf_op jit(solution)/shard_map/ppermute | solution.py:126
  149.8 8.6 %collective-permute-done.21.refs_4_ = bf16[528,384]{1,0:T(8,128)(2,1)S(1)} collective-permute-done((bf16[528,384]{1,0:T(8,128)(2,1)S(1)}, bf16[528,384]{1,0:T(8,128)(2,1)S(1)}, u32[]{:S(2)}, u32[]{:S(2)}) %collective-permute-start.21) | collective-permute-done | bytes 405536 | tf_op jit(solution)/shard_map/ppermute | solution.py:593
  159.7 7.4 %collective-permute-done.30.refs_4_ = bf16[528,384]{1,0:T(8,128)(2,1)S(1)} collective-permute-done((bf16[528,384]{1,0:T(8,128)(2,1)S(1)}, bf16[528,384]{1,0:T(8,128)(2,1)S(1)}, u32[]{:S(2)}, u32[]{:S(2)}) %collective-permute-start.30) | collective-permute-done | bytes 405536 | tf_op jit(solution)/shard_map/ppermute | solution.py:593
  168.4 7.4 %collective-permute-done.22.refs_4_ = bf16[528,384]{1,0:T(8,128)(2,1)S(1)} collective-permute-done((bf16[528,384]{1,0:T(8,128)(2,1)S(1)}, bf16[528,384]{1,0:T(8,128)(2,1)S(1)}, u32[]{:S(2)}, u32[]{:S(2)}) %collective-permute-start.22) | collective-permute-done | bytes 405536 | tf_op jit(solution)/shard_map/ppermute | solution.py:593
  177.1 7.3 %collective-permute-done.31.refs_4_ = bf16[528,384]{1,0:T(8,128)(2,1)S(1)} collective-permute-done((bf16[528,384]{1,0:T(8,128)(2,1)S(1)}, bf16[528,384]{1,0:T(8,128)(2,1)S(1)}, u32[]{:S(2)}, u32[]{:S(2)}) %collective-permute-start.31) | collective-permute-done | bytes 405536 | tf_op jit(solution)/shard_map/ppermute | solution.py:593
  188.3 4.9 %collective-permute-done.23.refs_1_ = bf16[528,384]{1,0:T(8,128)(2,1)S(1)} collective-permute-done((bf16[528,384]{1,0:T(8,128)(2,1)S(1)}, bf16[528,384]{1,0:T(8,128)(2,1)S(1)}, u32[]{:S(2)}, u32[]{:S(2)}) %collective-permute-start.23) | collective-permute-done | bytes 405536 | tf_op jit(solution)/shard_map/ppermute | solution.py:593
  193.2 8.1 %collective-permute-done.32.refs_2_ = bf16[528,384]{1,0:T(8,128)(2,1)S(1)} collective-permute-done((bf16[528,384]{1,0:T(8,128)(2,1)S(1)}, bf16[528,384]{1,0:T(8,128)(2,1)S(1)}, u32[]{:S(2)}, u32[]{:S(2)}) %collective-permute-start.32) | collective-permute-done | bytes 405536 | tf_op jit(solution)/shard_map/ppermute | solution.py:593
  204.7 3.0 %collective-permute-start.35 = (bf16[512,128]{1,0:T(8,128)(2,1)S(1)}, bf16[512,128]{1,0:T(8,128)(2,1)S(1)}, u32[]{:S(2)}, u32[]{:S(2)}) collective-permute-start(bf16[512,128]{1,0:T(8,128)(2,1)S(1)} %get-tuple-element.73.refs_1_), channel_id=1, source_target_pairs={{0,12},{4,0},{8,4},{12,8},{1,13},{5,1},{9,5},{13,9},{2,14},{6,2},{... | collective-permute-start | bytes 393224 | tf_op jit(solution)/shard_map/ppermute | solution.py:244
  212.1 4.7 %collective-permute-done.34.refs_3_ = bf16[512,128]{1,0:T(8,128)(2,1)S(1)} collective-permute-done((bf16[512,128]{1,0:T(8,128)(2,1)S(1)}, bf16[512,128]{1,0:T(8,128)(2,1)S(1)}, u32[]{:S(2)}, u32[]{:S(2)}) %collective-permute-start.34) | collective-permute-done | bytes 131104 | tf_op jit(solution)/shard_map/ppermute | solution.py:244
  218.2 2.7 collective-permute-start.44
  226.5 5.1 %collective-permute-done.45.refs_3_ = bf16[512,128]{1,0:T(8,128)(2,1)S(1)} collective-permute-done((bf16[512,128]{1,0:T(8,128)(2,1)S(1)}, bf16[512,128]{1,0:T(8,128)(2,1)S(1)}, u32[]{:S(2)}, u32[]{:S(2)}) %collective-permute-start.45) | collective-permute-done | bytes 131104 | tf_op jit(solution)/shard_map/ppermute | solution.py:244
  237.1 5.1 %collective-permute-done.37.refs_3_ = bf16[512,256]{1,0:T(8,128)(2,1)S(1)} collective-permute-done((bf16[512,256]{1,0:T(8,128)(2,1)S(1)}, bf16[512,256]{1,0:T(8,128)(2,1)S(1)}, u32[]{:S(2)}, u32[]{:S(2)}) %collective-permute-start.37) | collective-permute-done | bytes 262176 | tf_op jit(solution)/shard_map/ppermute | solution.py:126
  242.9 3.3 %collective-permute-start.38 = (bf16[128,256]{1,0:T(8,128)(2,1)S(1)}, bf16[128,256]{1,0:T(8,128)(2,1)S(1)}, u32[]{:S(2)}, u32[]{:S(2)}) collective-permute-start(bf16[128,256]{1,0:T(8,128)(2,1)S(1)} %get-tuple-element.80), channel_id=1, source_target_pairs={{0,4},{4,8},{8,12},{12,0},{1,5},{5,9},{9,13},{13,1},{2,6},{6,10},{... | collective-permute-start | bytes 196616 | tf_op jit(solution)/shard_map/ppermute | solution.py:244
  260.0 2.8 %collective-permute-done.41.refs_2_ = bf16[512,256]{1,0:T(8,128)(2,1)S(1)} collective-permute-done((bf16[512,256]{1,0:T(8,128)(2,1)S(1)}, bf16[512,256]{1,0:T(8,128)(2,1)S(1)}, u32[]{:S(2)}, u32[]{:S(2)}) %collective-permute-start.41) | collective-permute-done | bytes 262176 | tf_op jit(solution)/shard_map/ppermute | solution.py:126
  263.3 3.9 %collective-permute-done.52.refs_6_ = bf16[512,256]{1,0:T(8,128)(2,1)S(1)} collective-permute-done((bf16[512,256]{1,0:T(8,128)(2,1)S(1)}, bf16[512,256]{1,0:T(8,128)(2,1)S(1)}, u32[]{:S(2)}, u32[]{:S(2)}) %collective-permute-start.52) | collective-permute-done | bytes 262176 | tf_op jit(solution)/shard_map/ppermute | solution.py:126
  (126 shorter events, 104.3 us)
Async XLA Ops:
  1.8 10.5 %collective-permute-start = (bf16[256,256]{1,0:T(8,128)(2,1)S(1)}, bf16[256,256]{1,0:T(8,128)(2,1)S(1)}, u32[]{:S(2)}, u32[]{:S(2)}) collective-permute-start(bf16[256,256]{1,0:T(8,128)(2,1)S(1)} %get-tuple-element.49), channel_id=1, source_target_pairs={{0,4},{4,8},{8,12},{12,0},{1,5},{5,9},{9,13},{13,1},{2,6},{6,10},{... | collective-permute-start | bytes 393224 | tf_op jit(solution)/shard_map/ppermute | solution.py:244
  4.9 11.2 %collective-permute-start.1 = (bf16[256,256]{1,0:T(8,128)(2,1)S(1)}, bf16[256,256]{1,0:T(8,128)(2,1)S(1)}, u32[]{:S(2)}, u32[]{:S(2)}) collective-permute-start(bf16[256,256]{1,0:T(8,128)(2,1)S(1)} %get-tuple-element.50), channel_id=1, source_target_pairs={{0,8},{4,12},{8,0},{12,4},{1,9},{5,13},{9,1},{13,5},{2,10},{6,14},... | collective-permute-start | bytes 393224 | tf_op jit(solution)/shard_map/ppermute | solution.py:244
  7.5 8.6 %collective-permute-start.2 = (bf16[256,256]{1,0:T(8,128)(2,1)S(1)}, bf16[256,256]{1,0:T(8,128)(2,1)S(1)}, u32[]{:S(2)}, u32[]{:S(2)}) collective-permute-start(bf16[256,256]{1,0:T(8,128)(2,1)S(1)} %get-tuple-element.51), channel_id=1, source_target_pairs={{0,12},{4,0},{8,4},{12,8},{1,13},{5,1},{9,5},{13,9},{2,14},{6,2},{... | collective-permute-start | bytes 393224 | tf_op jit(solution)/shard_map/ppermute | solution.py:244
  24.9 8.7 %collective-permute-start.9 = (bf16[512,256]{1,0:T(8,128)(2,1)S(1)}, bf16[512,256]{1,0:T(8,128)(2,1)S(1)}, u32[]{:S(2)}, u32[]{:S(2)}) collective-permute-start(bf16[512,256]{1,0:T(8,128)(2,1)S(1)} %get-tuple-element.56.refs_1_), channel_id=1, source_target_pairs={{0,2},{1,3},{2,0},{3,1},{4,6},{5,7},{6,4},{7,5},{8,10},{9,11},{10,... | collective-permute-start | bytes 786440 | tf_op jit(solution)/shard_map/ppermute | solution.py:126
  26.4 10.6 %collective-permute-start.10 = (bf16[512,256]{1,0:T(8,128)(2,1)S(1)}, bf16[512,256]{1,0:T(8,128)(2,1)S(1)}, u32[]{:S(2)}, u32[]{:S(2)}) collective-permute-start(bf16[512,256]{1,0:T(8,128)(2,1)S(1)} %get-tuple-element.56.refs_1_), channel_id=1, source_target_pairs={{0,1},{1,0},{2,3},{3,2},{4,5},{5,4},{6,7},{7,6},{8,9},{9,8},{10,11... | collective-permute-start | bytes 786440 | tf_op jit(solution)/shard_map/ppermute | solution.py:126
  33.6 14.1 %collective-permute-start.6 = (bf16[528,384]{1,0:T(8,128)(2,1)S(1)}, bf16[528,384]{1,0:T(8,128)(2,1)S(1)}, u32[]{:S(2)}, u32[]{:S(2)}) collective-permute-start(bf16[528,384]{1,0:T(8,128)(2,1)S(1)} %get-tuple-element.55), channel_id=1, source_target_pairs={{0,4},{4,8},{8,12},{12,0},{1,5},{5,9},{9,13},{13,1},{2,6},{6,10},{... | collective-permute-start | bytes 1216520 | tf_op jit(solution)/shard_map/ppermute | solution.py:593
  38.7 17.7 %collective-permute-start.12 = (bf16[528,384]{1,0:T(8,128)(2,1)S(1)}, bf16[528,384]{1,0:T(8,128)(2,1)S(1)}, u32[]{:S(2)}, u32[]{:S(2)}) collective-permute-start(bf16[528,384]{1,0:T(8,128)(2,1)S(1)} %get-tuple-element.60), channel_id=1, source_target_pairs={{0,12},{4,0},{8,4},{12,8},{1,13},{5,1},{9,5},{13,9},{2,14},{6,2},{... | collective-permute-start | bytes 1216520 | tf_op jit(solution)/shard_map/ppermute | solution.py:593
  49.0 16.2 %collective-permute-start.7 = (bf16[528,384]{1,0:T(8,128)(2,1)S(1)}, bf16[528,384]{1,0:T(8,128)(2,1)S(1)}, u32[]{:S(2)}, u32[]{:S(2)}) collective-permute-start(bf16[528,384]{1,0:T(8,128)(2,1)S(1)} %shard_map.78), channel_id=1, source_target_pairs={{0,4},{4,8},{8,12},{12,0},{1,5},{5,9},{9,13},{13,1},{2,6},{6,10},{... | collective-permute-start | bytes 1216520 | tf_op jit(solution)/shard_map/ppermute | solution.py:593
  57.6 16.2 %collective-permute-start.13 = (bf16[528,384]{1,0:T(8,128)(2,1)S(1)}, bf16[528,384]{1,0:T(8,128)(2,1)S(1)}, u32[]{:S(2)}, u32[]{:S(2)}) collective-permute-start(bf16[528,384]{1,0:T(8,128)(2,1)S(1)} %shard_map.81), channel_id=1, source_target_pairs={{0,12},{4,0},{8,4},{12,8},{1,13},{5,1},{9,5},{13,9},{2,14},{6,2},{... | collective-permute-start | bytes 1216520 | tf_op jit(solution)/shard_map/ppermute | solution.py:593
  66.4 17.2 %collective-permute-start.8 = (bf16[528,384]{1,0:T(8,128)(2,1)S(1)}, bf16[528,384]{1,0:T(8,128)(2,1)S(1)}, u32[]{:S(2)}, u32[]{:S(2)}) collective-permute-start(bf16[528,384]{1,0:T(8,128)(2,1)S(1)} %shard_map.79), channel_id=1, source_target_pairs={{0,4},{4,8},{8,12},{12,0},{1,5},{5,9},{9,13},{13,1},{2,6},{6,10},{... | collective-permute-start | bytes 1216520 | tf_op jit(solution)/shard_map/ppermute | solution.py:593
  75.0 15.7 %collective-permute-start.14 = (bf16[528,384]{1,0:T(8,128)(2,1)S(1)}, bf16[528,384]{1,0:T(8,128)(2,1)S(1)}, u32[]{:S(2)}, u32[]{:S(2)}) collective-permute-start(bf16[528,384]{1,0:T(8,128)(2,1)S(1)} %shard_map.82), channel_id=1, source_target_pairs={{0,12},{4,0},{8,4},{12,8},{1,13},{5,1},{9,5},{13,9},{2,14},{6,2},{... | collective-permute-start | bytes 1216520 | tf_op jit(solution)/shard_map/ppermute | solution.py:593
  93.8 12.4 %collective-permute-start.16 = (bf16[512,128]{1,0:T(8,128)(2,1)S(1)}, bf16[512,128]{1,0:T(8,128)(2,1)S(1)}, u32[]{:S(2)}, u32[]{:S(2)}) collective-permute-start(bf16[512,128]{1,0:T(8,128)(2,1)S(1)} %get-tuple-element.61.refs_1_), channel_id=1, source_target_pairs={{0,8},{4,12},{8,0},{12,4},{1,9},{5,13},{9,1},{13,5},{2,10},{6,14},... | collective-permute-start | bytes 393224 | tf_op jit(solution)/shard_map/ppermute | solution.py:244
  97.2 9.0 %collective-permute-start.17 = (bf16[512,128]{1,0:T(8,128)(2,1)S(1)}, bf16[512,128]{1,0:T(8,128)(2,1)S(1)}, u32[]{:S(2)}, u32[]{:S(2)}) collective-permute-start(bf16[512,128]{1,0:T(8,128)(2,1)S(1)} %get-tuple-element.61.refs_1_), channel_id=1, source_target_pairs={{0,12},{4,0},{8,4},{12,8},{1,13},{5,1},{9,5},{13,9},{2,14},{6,2},{... | collective-permute-start | bytes 393224 | tf_op jit(solution)/shard_map/ppermute | solution.py:244
  110.7 10.3 %collective-permute-start.25 = (bf16[512,128]{1,0:T(8,128)(2,1)S(1)}, bf16[512,128]{1,0:T(8,128)(2,1)S(1)}, u32[]{:S(2)}, u32[]{:S(2)}) collective-permute-start(bf16[512,128]{1,0:T(8,128)(2,1)S(1)} %shard_map.87.refs_6_.refs_1_), channel_id=1, source_target_pairs={{0,8},{4,12},{8,0},{12,4},{1,9},{5,13},{9,1},{13,5},{2,10},{6,14},... | collective-permute-start | bytes 393224 | tf_op jit(solution)/shard_map/ppermute | solution.py:244
  110.8 10.2 %collective-permute-start.26 = (bf16[512,128]{1,0:T(8,128)(2,1)S(1)}, bf16[512,128]{1,0:T(8,128)(2,1)S(1)}, u32[]{:S(2)}, u32[]{:S(2)}) collective-permute-start(bf16[512,128]{1,0:T(8,128)(2,1)S(1)} %shard_map.87.refs_6_.refs_1_), channel_id=1, source_target_pairs={{0,12},{4,0},{8,4},{12,8},{1,13},{5,1},{9,5},{13,9},{2,14},{6,2},{... | collective-permute-start | bytes 393224 | tf_op jit(solution)/shard_map/ppermute | solution.py:244
  113.8 13.7 %collective-permute-start.19 = (bf16[512,512]{1,0:T(8,128)(2,1)S(1)}, bf16[512,512]{1,0:T(8,128)(2,1)S(1)}, u32[]{:S(2)}, u32[]{:S(2)}) collective-permute-start(bf16[512,512]{1,0:T(8,128)(2,1)S(1)} %shard_map.89.refs_3_.refs_6_), channel_id=1, source_target_pairs={{0,2},{1,3},{2,0},{3,1},{4,6},{5,7},{6,4},{7,5},{8,10},{9,11},{10,... | collective-permute-start | bytes 1572872 | tf_op jit(solution)/shard_map/ppermute | solution.py:126
  129.0 14.4 %collective-permute-start.28 = (bf16[512,512]{1,0:T(8,128)(2,1)S(1)}, bf16[512,512]{1,0:T(8,128)(2,1)S(1)}, u32[]{:S(2)}, u32[]{:S(2)}) collective-permute-start(bf16[512,512]{1,0:T(8,128)(2,1)S(1)} %shard_map.95.refs_3_), channel_id=1, source_target_pairs={{0,2},{1,3},{2,0},{3,1},{4,6},{5,7},{6,4},{7,5},{8,10},{9,11},{10,... | collective-permute-start | bytes 1572872 | tf_op jit(solution)/shard_map/ppermute | solution.py:126
  144.2 14.2 %collective-permute-start.21 = (bf16[528,384]{1,0:T(8,128)(2,1)S(1)}, bf16[528,384]{1,0:T(8,128)(2,1)S(1)}, u32[]{:S(2)}, u32[]{:S(2)}) collective-permute-start(bf16[528,384]{1,0:T(8,128)(2,1)S(1)} %get-tuple-element.67.refs_5_), channel_id=1, source_target_pairs={{0,4},{4,8},{8,12},{12,0},{1,5},{5,9},{9,13},{13,1},{2,6},{6,10},{... | collective-permute-start | bytes 1216520 | tf_op jit(solution)/shard_map/ppermute | solution.py:593
  147.7 19.4 %collective-permute-start.30 = (bf16[528,384]{1,0:T(8,128)(2,1)S(1)}, bf16[528,384]{1,0:T(8,128)(2,1)S(1)}, u32[]{:S(2)}, u32[]{:S(2)}) collective-permute-start(bf16[528,384]{1,0:T(8,128)(2,1)S(1)} %get-tuple-element.72), channel_id=1, source_target_pairs={{0,12},{4,0},{8,4},{12,8},{1,13},{5,1},{9,5},{13,9},{2,14},{6,2},{... | collective-permute-start | bytes 1216520 | tf_op jit(solution)/shard_map/ppermute | solution.py:593
  159.6 16.2 %collective-permute-start.22 = (bf16[528,384]{1,0:T(8,128)(2,1)S(1)}, bf16[528,384]{1,0:T(8,128)(2,1)S(1)}, u32[]{:S(2)}, u32[]{:S(2)}) collective-permute-start(bf16[528,384]{1,0:T(8,128)(2,1)S(1)} %shard_map.92), channel_id=1, source_target_pairs={{0,4},{4,8},{8,12},{12,0},{1,5},{5,9},{9,13},{13,1},{2,6},{6,10},{... | collective-permute-start | bytes 1216520 | tf_op jit(solution)/shard_map/ppermute | solution.py:593
  168.3 16.1 %collective-permute-start.31 = (bf16[528,384]{1,0:T(8,128)(2,1)S(1)}, bf16[528,384]{1,0:T(8,128)(2,1)S(1)}, u32[]{:S(2)}, u32[]{:S(2)}) collective-permute-start(bf16[528,384]{1,0:T(8,128)(2,1)S(1)} %shard_map.98), channel_id=1, source_target_pairs={{0,12},{4,0},{8,4},{12,8},{1,13},{5,1},{9,5},{13,9},{2,14},{6,2},{... | collective-permute-start | bytes 1216520 | tf_op jit(solution)/shard_map/ppermute | solution.py:593
  177.1 16.2 %collective-permute-start.23 = (bf16[528,384]{1,0:T(8,128)(2,1)S(1)}, bf16[528,384]{1,0:T(8,128)(2,1)S(1)}, u32[]{:S(2)}, u32[]{:S(2)}) collective-permute-start(bf16[528,384]{1,0:T(8,128)(2,1)S(1)} %shard_map.93), channel_id=1, source_target_pairs={{0,4},{4,8},{8,12},{12,0},{1,5},{5,9},{9,13},{13,1},{2,6},{6,10},{... | collective-permute-start | bytes 1216520 | tf_op jit(solution)/shard_map/ppermute | solution.py:593
  185.7 15.7 %collective-permute-start.32 = (bf16[528,384]{1,0:T(8,128)(2,1)S(1)}, bf16[528,384]{1,0:T(8,128)(2,1)S(1)}, u32[]{:S(2)}, u32[]{:S(2)}) collective-permute-start(bf16[528,384]{1,0:T(8,128)(2,1)S(1)} %shard_map.99), channel_id=1, source_target_pairs={{0,12},{4,0},{8,4},{12,8},{1,13},{5,1},{9,5},{13,9},{2,14},{6,2},{... | collective-permute-start | bytes 1216520 | tf_op jit(solution)/shard_map/ppermute | solution.py:593
  204.4 12.4 %collective-permute-start.34 = (bf16[512,128]{1,0:T(8,128)(2,1)S(1)}, bf16[512,128]{1,0:T(8,128)(2,1)S(1)}, u32[]{:S(2)}, u32[]{:S(2)}) collective-permute-start(bf16[512,128]{1,0:T(8,128)(2,1)S(1)} %get-tuple-element.73.refs_1_), channel_id=1, source_target_pairs={{0,8},{4,12},{8,0},{12,4},{1,9},{5,13},{9,1},{13,5},{2,10},{6,14},... | collective-permute-start | bytes 393224 | tf_op jit(solution)/shard_map/ppermute | solution.py:244
  204.7 12.1 %collective-permute-start.35 = (bf16[512,128]{1,0:T(8,128)(2,1)S(1)}, bf16[512,128]{1,0:T(8,128)(2,1)S(1)}, u32[]{:S(2)}, u32[]{:S(2)}) collective-permute-start(bf16[512,128]{1,0:T(8,128)(2,1)S(1)} %get-tuple-element.73.refs_1_), channel_id=1, source_target_pairs={{0,12},{4,0},{8,4},{12,8},{1,13},{5,1},{9,5},{13,9},{2,14},{6,2},{... | collective-permute-start | bytes 393224 | tf_op jit(solution)/shard_map/ppermute | solution.py:244
  220.9 10.7 %collective-permute-start.45 = (bf16[512,128]{1,0:T(8,128)(2,1)S(1)}, bf16[512,128]{1,0:T(8,128)(2,1)S(1)}, u32[]{:S(2)}, u32[]{:S(2)}) collective-permute-start(bf16[512,128]{1,0:T(8,128)(2,1)S(1)} %shard_map.103.refs_6_.refs_1_), channel_id=1, source_target_pairs={{0,8},{4,12},{8,0},{12,4},{1,9},{5,13},{9,1},{13,5},{2,10},{6,14},... | collective-permute-start | bytes 393224 | tf_op jit(solution)/shard_map/ppermute | solution.py:244
  221.2 10.4 %collective-permute-start.46 = (bf16[512,128]{1,0:T(8,128)(2,1)S(1)}, bf16[512,128]{1,0:T(8,128)(2,1)S(1)}, u32[]{:S(2)}, u32[]{:S(2)}) collective-permute-start(bf16[512,128]{1,0:T(8,128)(2,1)S(1)} %shard_map.103.refs_6_.refs_1_), channel_id=1, source_target_pairs={{0,12},{4,0},{8,4},{12,8},{1,13},{5,1},{9,5},{13,9},{2,14},{6,2},{... | collective-permute-start | bytes 393224 | tf_op jit(solution)/shard_map/ppermute | solution.py:244
  233.0 9.2 %collective-permute-start.37 = (bf16[512,256]{1,0:T(8,128)(2,1)S(1)}, bf16[512,256]{1,0:T(8,128)(2,1)S(1)}, u32[]{:S(2)}, u32[]{:S(2)}) collective-permute-start(bf16[512,256]{1,0:T(8,128)(2,1)S(1)} %get-tuple-element.78.refs_6_), channel_id=1, source_target_pairs={{0,2},{1,3},{2,0},{3,1},{4,6},{5,7},{6,4},{7,5},{8,10},{9,11},{10,... | collective-permute-start | bytes 786440 | tf_op jit(solution)/shard_map/ppermute | solution.py:126
  235.6 13.1 %collective-permute-start.48 = (bf16[512,256]{1,0:T(8,128)(2,1)S(1)}, bf16[512,256]{1,0:T(8,128)(2,1)S(1)}, u32[]{:S(2)}, u32[]{:S(2)}) collective-permute-start(bf16[512,256]{1,0:T(8,128)(2,1)S(1)} %get-tuple-element.86), channel_id=1, source_target_pairs={{0,2},{1,3},{2,0},{3,1},{4,6},{5,7},{6,4},{7,5},{8,10},{9,11},{10,... | collective-permute-start | bytes 786440 | tf_op jit(solution)/shard_map/ppermute | solution.py:126
  242.9 9.9 %collective-permute-start.38 = (bf16[128,256]{1,0:T(8,128)(2,1)S(1)}, bf16[128,256]{1,0:T(8,128)(2,1)S(1)}, u32[]{:S(2)}, u32[]{:S(2)}) collective-permute-start(bf16[128,256]{1,0:T(8,128)(2,1)S(1)} %get-tuple-element.80), channel_id=1, source_target_pairs={{0,4},{4,8},{8,12},{12,0},{1,5},{5,9},{9,13},{13,1},{2,6},{6,10},{... | collective-permute-start | bytes 196616 | tf_op jit(solution)/shard_map/ppermute | solution.py:244
  254.4 8.5 %collective-permute-start.41 = (bf16[512,256]{1,0:T(8,128)(2,1)S(1)}, bf16[512,256]{1,0:T(8,128)(2,1)S(1)}, u32[]{:S(2)}, u32[]{:S(2)}) collective-permute-start(bf16[512,256]{1,0:T(8,128)(2,1)S(1)} %shard_map.107.refs_1_), channel_id=1, source_target_pairs={{0,2},{1,3},{2,0},{3,1},{4,6},{5,7},{6,4},{7,5},{8,10},{9,11},{10,... | collective-permute-start | bytes 786440 | tf_op jit(solution)/shard_map/ppermute | solution.py:126
  258.5 8.8 %collective-permute-start.52 = (bf16[512,256]{1,0:T(8,128)(2,1)S(1)}, bf16[512,256]{1,0:T(8,128)(2,1)S(1)}, u32[]{:S(2)}, u32[]{:S(2)}) collective-permute-start(bf16[512,256]{1,0:T(8,128)(2,1)S(1)} %shard_map.111.refs_5_), channel_id=1, source_target_pairs={{0,2},{1,3},{2,0},{3,1},{4,6},{5,7},{6,4},{7,5},{8,10},{9,11},{10,... | collective-permute-start | bytes 786440 | tf_op jit(solution)/shard_map/ppermute | solution.py:126
  (26 other events, 162.4 us)

commit v8 on v7

--- a/solution.py
+++ b/solution.py
@@ -301,13 +301,15 @@
     return terms[0] + (terms[1] + terms[2])
 
 
-def share(source, staged, layer, place, chunk_shift, arrived=None):
+def share(source, staged, layer, place, chunk_shift, arrived=None, others=None, extra=0):
     fresh = len(source) == 3
     sp_count, feats, total_width = staged.shape
     arrays = (*source[0], source[2]) if fresh else source
     tok = arrays[0].shape[0]
     count = len(arrays)
-    inputs = (*arrays, staged) + (() if arrived is None else (arrived,))
+    inputs = (*arrays, staged)
+    inputs += () if arrived is None else (arrived,)
+    inputs += () if others is None else (others,)
 
     def body(place_ref, *refs):
         array_refs, staged_ref = refs[:count], refs[count]
@@ -324,27 +326,29 @@
                 array_refs[len(pieces)],
                 scaled_ref,
             )
-            squares_ref[...] = jnp.zeros_like(squares_ref)
+            squares_ref[...] = jnp.zeros_like(squares_ref) if others is None else refs[count + 1][...]
+            start = 0 if others is None else tok // HD
             for run in range(tok // HD):
                 total = jnp.zeros((HD, HD), jnp.float32)
                 for ref in array_refs[: len(pieces)]:
                     for lane in range(ref.shape[1] // HD):
                         part = ref[pl.ds(run * HD, HD), pl.ds(lane * HD, HD)].astype(jnp.float32)
                         total += part * part
-                squares_ref[pl.ds(run, 1), :] = jnp.sum(total.T, axis=0, keepdims=True)
+                squares_ref[pl.ds(start + run, 1), :] = jnp.sum(total.T, axis=0, keepdims=True)
         else:
             scaled_ref, squares_ref = array_refs
         chunk = lax.rem(place_ref[0] + chunk_shift, sp_count)
         total = jnp.dot(scaled_ref[...], staged_ref[chunk], preferred_element_type=jnp.float32)
-        squares = squares_ref[...]
         if arrived is not None:
-            arrived_ref = refs[count + 1]
-            total += arrived_ref[pl.ds(0, tok), :].astype(jnp.float32)
-            squares += get_squares(arrived_ref, tok)
+            total += refs[count + 1][pl.ds(0, tok), :].astype(jnp.float32)
         out_ref[pl.ds(0, tok), :] = total.astype(jnp.bfloat16)
-        put_squares(out_ref, squares, tok)
-
-    outs = [shaped(tok + EXTRA, total_width)]
+        if extra:
+            squares = squares_ref[...]
+            if arrived is not None:
+                squares += get_squares(refs[count + 1], tok)
+            put_squares(out_ref, squares, tok)
+
+    outs = [shaped(tok + extra, total_width)]
     if fresh:
         outs += [shaped(tok, feats), shaped(EXTRA, HD, dtype=jnp.float32)]
     return local_kernel(body, place, inputs, outs, flops=2 * tok * feats * total_width)
@@ -415,14 +419,15 @@
 
     def low(place_ref, *refs):
         arrived_refs, refs = (refs[:count], refs[count : 2 * count]), refs[2 * count :]
-        own_refs, square_refs, (bias_ref, out_ref, qkv_ref) = refs[:2], refs[2:4], refs[4:]
+        own_refs, (squares_ref, bias_ref, out_ref, qkv_ref) = refs[:2], refs[2:]
+        squares = squares_ref[...]
+        for ref in arrived_refs[1]:
+            squares += get_squares(ref, rows)
+        norm = lax.rsqrt(squares / every_feat + norm_eps)
         for part in range(2):
-            total_squares = square_refs[part][...]
-            for ref in arrived_refs[part]:
-                total_squares += get_squares(ref, rows)
-            norm = lax.rsqrt(total_squares / every_feat + norm_eps)
             for run in range(runs):
-                factor = jnp.broadcast_to(norm[run : run + 1, :], (HD, HD)).T
+                at = part * runs + run
+                factor = jnp.broadcast_to(norm[at : at + 1, :], (HD, HD)).T
                 plane, inner = divmod(run * HD, part_rows)
                 to = pl.ds((2 * plane + part) * part_rows + inner, HD)
                 span = pl.ds(run * HD, HD)
@@ -440,7 +445,7 @@
     out0, qkv = local_kernel(
         low,
         place,
-        (*arrived[0], *arrived[1], *own, *squares, bias),
+        (*arrived[0], *arrived[1], *own, squares, bias),
         [shaped(rows, width), shaped(2 * rows, total_width)],
         flops=flops,
         after=after,
@@ -552,28 +557,43 @@
 HALF_SLOTS = (lambda core, far: core, lambda core, far: 1 - core)
 
 
-def assemble(parts, place, sp_count):
-    rows, piece = parts[0][0].shape
+def assemble(pieces, place, sp_count, index, so_far):
+    rows, piece = pieces[0].shape
     part = rows // sp_count
-    count = len(parts[0])
+    count = len(pieces)
+    width = piece * count * sp_count
+    earlier = () if so_far is None else (so_far,)
 
     def body(place_ref, *refs):
-        out_ref = refs[-1]
-        for index in range(len(parts)):
-            for which in range(count):
-                slot = SLOTS[which](place_ref[1], place_ref[2])
-                for plane in range(sp_count):
-                    out_ref[pl.ds(index * part, part), aligned(plane * count + slot, piece)] = refs[
-                        index * count + which
-                    ][pl.ds(plane * part, part), :]
-
-    flat = [array for pieces in parts for array in pieces]
-    return local_kernel(body, place, flat, [shaped(part * len(parts), piece * count * sp_count)])[0]
+        out_ref, laid, sem = refs[-3:]
+        for which in range(count):
+            slot = SLOTS[which](place_ref[1], place_ref[2])
+            for plane in range(sp_count):
+                laid[:, aligned(plane * count + slot, piece)] = refs[which][
+                    pl.ds(plane * part, part), :
+                ]
+        copy = pltpu.make_async_copy(laid, out_ref.at[pl.ds(index * part, part), :], sem)
+        copy.start()
+        copy.wait()
+
+    vmem, hbm = pl.BlockSpec(memory_space=pltpu.VMEM), pl.BlockSpec(memory_space=pltpu.HBM)
+    return pl.pallas_call(
+        body,
+        out_shape=shaped(2 * part, width),
+        in_specs=[pl.BlockSpec(memory_space=pltpu.SMEM)] + [vmem] * count + [hbm] * len(earlier),
+        out_specs=hbm,
+        scratch_shapes=[pltpu.VMEM((part, width), jnp.bfloat16), pltpu.SemaphoreType.DMA],
+        input_output_aliases={1 + count: 0} if earlier else {},
+        compiler_params=pltpu.CompilerParams(vmem_limit_bytes=VMEM_BYTES),
+        cost_estimate=pl.CostEstimate(flops=0, bytes_accessed=4 * part * width, transcendentals=0),
+        name="assemble",
+    )(place, *pieces, *earlier)
 
 
 def exchanged(held):
     far = swapped(held, "tp", 2)
-    return [held, far, swapped(held, "tp", 1), swapped(far, "tp", 1)]
+    near = swapped(held, "tp", 1)
+    return [held, far, near, swapped(far, "tp", 1)]
 
 
 def stationary_plan(tokens, norm_gain, w_query, w_key, w_value, w_out, offset_bias):
@@ -594,7 +614,9 @@
 
     def made(layer, part, step, arrived=None):
         chunk = (-shifts[part] * (step + 1)) % sp_count
-        return share(sources[part], staged[layer], layer, place, chunk, arrived)
+        others = sources[0][1] if part and not step else None
+        extra = EXTRA if part else 0
+        return share(sources[part], staged[layer], layer, place, chunk, arrived, others, extra)
 
     def first_made(layer, part):
         sources[part] = (halves[part], SLOTS if layer == 0 else HALF_SLOTS, norm_gain)
@@ -626,7 +648,7 @@
         own = []
         for part in range(2):
             own.append(own_share(sources[part][0], staged[layer], place))
-        squares = [source[1] for source in sources]
+        squares = sources[1][1]
         attended = attend(
             [travelling[:1], travelling[1:]],
             own,
@@ -656,12 +678,14 @@
                 mine = renew(residuals[part], pair[0], other, place, after)
                 halves[part] = [mine, swapped(mine, "tp", 1)]
                 first[part] = first_made(layer + 1, part)
-                after = (first[part],)
             else:
                 blocks = finish(residuals[part][0], pair[1], other, place, sp_count)
                 stacked = stack_blocks(over_sp(blocks, sp_count), place)[0]
                 halves[part] = exchanged(stacked)
-    return assemble(halves, place, sp_count)
+    mixed = None
+    for part in range(2):
+        mixed = assemble(halves[part], place, sp_count, part, mixed)
+    return mixed
 
 
 def on_device(tokens, norm_gain, w_query, w_key, w_value, w_out, offset_bias):

time: 271 us -> 286 us (1.055)
  waiting for transfers between devices: 150 us -> 159 us
  starting transfers between devices: 66.8 us -> 72.1 us
    ppermute x12, waiting for transfers between devices: 73.9 us -> 80.4 us  [sent_on(): return lax.ppermute(block, 'sp', ring(sp_count, shifts[part]))]
    ppermute x12, starting transfers between devices: 17.5 us -> 23.5 us  [sent_on(): return lax.ppermute(block, 'sp', ring(sp_count, shifts[part]))]
    ppermute x22, waiting for transfers between devices: 43.9 us -> 47.3 us  [swapped(): return lax.ppermute(array, axis, [(i, i ^ distance) for i in range(count)])]
    pallas_call x0 -> x2, Pallas kernels: none -> 3.33 us  [assemble(): pl.pallas_call(body, out_shape=shaped(2 * part, width), in_specs=[pl.Bloc...]
    pallas_call x40 -> x39, Pallas kernels: 53.1 us -> 50.9 us  [local_kernel(): pl.pallas_call(ordered, out_shape=list(outs), in_specs=[smem] + [vmem] *...]
  transfers between devices with their start and end apart: 55 -> 55, of which waited for: 32 -> 29; matrix products, arithmetic and copies ran while one was open for 0% -> 0% of each run, Pallas kernels for 14% -> 13%
where the time goes in v8:
time: 286 us
  waiting for transfers between devices  159 us (56%)
  starting transfers between devices  72.1 us (25%)
  Pallas kernels  54.3 us (19%)
    ppermute x12, waiting for transfers between devices, sent_on(): return lax.ppermute(block, 'sp', ring(sp_count, shifts[part]))  80.4 us
    pallas_call x39, Pallas kernels, local_kernel(): pl.pallas_call(ordered, out_shape=list(outs), in_specs=[smem] + [vmem] *...  50.9 us
    ppermute x22, waiting for transfers between devices, swapped(): return lax.ppermute(array, axis, [(i, i ^ distance) for i in range(count)])  47.3 us
    ppermute x21, starting transfers between devices, over_sp(): lax.ppermute(blocks[shift], 'sp', ring(count, shift))  35.3 us
    ppermute x21, waiting for transfers between devices, over_sp(): lax.ppermute(blocks[shift], 'sp', ring(count, shift))  31.6 us
    ppermute x12, starting transfers between devices, sent_on(): return lax.ppermute(block, 'sp', ring(sp_count, shifts[part]))  23.5 us
    ppermute x22, starting transfers between devices, swapped(): return lax.ppermute(array, axis, [(i, i ^ distance) for i in range(count)])  13.3 us
  transfers between devices with their start and end apart: 55, of which 29 were waited for; matrix products, arithmetic and copies ran while one was open for 0% of the time, Pallas kernels for 13%

profile of v8, /device:TPU:0, one launch (start us, length us, event | category | flops | bytes accessed | tf_op | source)
XLA Modules:
  0.0 286.2 jit_solution(15884718422069701044)
XLA Ops:
  1.8 3.1 %collective-permute-start = (bf16[256,256]{1,0:T(8,128)(2,1)S(1)}, bf16[256,256]{1,0:T(8,128)(2,1)S(1)}, u32[]{:S(2)}, u32[]{:S(2)}) collective-permute-start(bf16[256,256]{1,0:T(8,128)(2,1)S(1)} %get-tuple-element.49), channel_id=1, source_target_pairs={{0,4},{4,8},{8,12},{12,0},{1,5},{5,9},{9,13},{13,1},{2,6},{6,10},{... | collective-permute-start | bytes 393224 | tf_op jit(solution)/shard_map/ppermute | solution.py:244
  4.9 2.6 collective-permute-start.1
  9.7 2.6 shard_map.75.refs_6_.refs_3_.refs_2_
  12.3 3.8 %collective-permute-done.1.refs_3_ = bf16[256,256]{1,0:T(8,128)(2,1)S(1)} collective-permute-done((bf16[256,256]{1,0:T(8,128)(2,1)S(1)}, bf16[256,256]{1,0:T(8,128)(2,1)S(1)}, u32[]{:S(2)}, u32[]{:S(2)}) %collective-permute-start.1) | collective-permute-done | bytes 131104 | tf_op jit(solution)/shard_map/ppermute | solution.py:244
  18.3 6.6 %collective-permute-done.4.refs_2_ = bf16[512,256]{1,0:T(8,128)(2,1)S(1)} collective-permute-done((bf16[512,256]{1,0:T(8,128)(2,1)S(1)}, bf16[512,256]{1,0:T(8,128)(2,1)S(1)}, u32[]{:S(2)}, u32[]{:S(2)}) %collective-permute-start.4) | collective-permute-done | bytes 262176 | tf_op jit(solution)/shard_map/ppermute | solution.py:126
  28.3 5.4 %collective-permute-done.3.refs_2_ = bf16[512,256]{1,0:T(8,128)(2,1)S(1)} collective-permute-done((bf16[512,256]{1,0:T(8,128)(2,1)S(1)}, bf16[512,256]{1,0:T(8,128)(2,1)S(1)}, u32[]{:S(2)}, u32[]{:S(2)}) %collective-permute-start.3) | collective-permute-done | bytes 262176 | tf_op jit(solution)/shard_map/ppermute | solution.py:126
  36.8 3.5 %collective-permute-start.12 = (bf16[528,384]{1,0:T(8,128)(2,1)S(1)}, bf16[528,384]{1,0:T(8,128)(2,1)S(1)}, u32[]{:S(2)}, u32[]{:S(2)}) collective-permute-start(bf16[528,384]{1,0:T(8,128)(2,1)S(1)} %get-tuple-element.60), channel_id=1, source_target_pairs={{0,12},{4,0},{8,4},{12,8},{1,13},{5,1},{9,5},{13,9},{2,14},{6,2},{... | collective-permute-start | bytes 1216520 | tf_op jit(solution)/shard_map/ppermute | solution.py:613
  40.3 10.3 %collective-permute-done.12.refs_4_ = bf16[528,384]{1,0:T(8,128)(2,1)S(1)} collective-permute-done((bf16[528,384]{1,0:T(8,128)(2,1)S(1)}, bf16[528,384]{1,0:T(8,128)(2,1)S(1)}, u32[]{:S(2)}, u32[]{:S(2)}) %collective-permute-start.12) | collective-permute-done | bytes 405536 | tf_op jit(solution)/shard_map/ppermute | solution.py:613
  51.9 3.8 %collective-permute-start.13 = (bf16[528,384]{1,0:T(8,128)(2,1)S(1)}, bf16[528,384]{1,0:T(8,128)(2,1)S(1)}, u32[]{:S(2)}, u32[]{:S(2)}) collective-permute-start(bf16[528,384]{1,0:T(8,128)(2,1)S(1)} %shard_map.81), channel_id=1, source_target_pairs={{0,12},{4,0},{8,4},{12,8},{1,13},{5,1},{9,5},{13,9},{2,14},{6,2},{... | collective-permute-start | bytes 1216520 | tf_op jit(solution)/shard_map/ppermute | solution.py:613
  55.7 3.7 %collective-permute-done.7.refs_4_ = bf16[512,384]{1,0:T(8,128)(2,1)S(1)} collective-permute-done((bf16[512,384]{1,0:T(8,128)(2,1)S(1)}, bf16[512,384]{1,0:T(8,128)(2,1)S(1)}, u32[]{:S(2)}, u32[]{:S(2)}) %collective-permute-start.7) | collective-permute-done | bytes 393248 | tf_op jit(solution)/shard_map/ppermute | solution.py:613
  62.8 15.2 %collective-permute-done.13.refs_4_ = bf16[528,384]{1,0:T(8,128)(2,1)S(1)} collective-permute-done((bf16[528,384]{1,0:T(8,128)(2,1)S(1)}, bf16[528,384]{1,0:T(8,128)(2,1)S(1)}, u32[]{:S(2)}, u32[]{:S(2)}) %collective-permute-start.13) | collective-permute-done | bytes 405536 | tf_op jit(solution)/shard_map/ppermute | solution.py:613
  82.6 2.6 shard_map.85.refs_7_.refs_4_.refs_3_.refs_2_
  87.7 9.7 %collective-permute-done.9.refs_1_ = bf16[512,384]{1,0:T(8,128)(2,1)S(1)} collective-permute-done((bf16[512,384]{1,0:T(8,128)(2,1)S(1)}, bf16[512,384]{1,0:T(8,128)(2,1)S(1)}, u32[]{:S(2)}, u32[]{:S(2)}) %collective-permute-start.9) | collective-permute-done | bytes 393248 | tf_op jit(solution)/shard_map/ppermute | solution.py:613
  107.3 3.2 %collective-permute-done.19.refs_3_ = bf16[512,128]{1,0:T(8,128)(2,1)S(1)} collective-permute-done((bf16[512,128]{1,0:T(8,128)(2,1)S(1)}, bf16[512,128]{1,0:T(8,128)(2,1)S(1)}, u32[]{:S(2)}, u32[]{:S(2)}) %collective-permute-start.19) | collective-permute-done | bytes 131104 | tf_op jit(solution)/shard_map/ppermute | solution.py:244
  117.1 3.2 %collective-permute-done.15.refs_2_ = bf16[512,128]{1,0:T(8,128)(2,1)S(1)} collective-permute-done((bf16[512,128]{1,0:T(8,128)(2,1)S(1)}, bf16[512,128]{1,0:T(8,128)(2,1)S(1)}, u32[]{:S(2)}, u32[]{:S(2)}) %collective-permute-start.15) | collective-permute-done | bytes 131104 | tf_op jit(solution)/shard_map/ppermute | solution.py:244
  120.3 5.1 %collective-permute-done.16.refs_3_ = bf16[512,128]{1,0:T(8,128)(2,1)S(1)} collective-permute-done((bf16[512,128]{1,0:T(8,128)(2,1)S(1)}, bf16[512,128]{1,0:T(8,128)(2,1)S(1)}, u32[]{:S(2)}, u32[]{:S(2)}) %collective-permute-start.16) | collective-permute-done | bytes 131104 | tf_op jit(solution)/shard_map/ppermute | solution.py:244
  130.9 10.8 %collective-permute-done.24.refs_4_ = bf16[512,512]{1,0:T(8,128)(2,1)S(1)} collective-permute-done((bf16[512,512]{1,0:T(8,128)(2,1)S(1)}, bf16[512,512]{1,0:T(8,128)(2,1)S(1)}, u32[]{:S(2)}, u32[]{:S(2)}) %collective-permute-start.24) | collective-permute-done | bytes 524320 | tf_op jit(solution)/shard_map/ppermute | solution.py:126
  142.5 9.9 %collective-permute-done.23.refs_4_ = bf16[512,512]{1,0:T(8,128)(2,1)S(1)} collective-permute-done((bf16[512,512]{1,0:T(8,128)(2,1)S(1)}, bf16[512,512]{1,0:T(8,128)(2,1)S(1)}, u32[]{:S(2)}, u32[]{:S(2)}) %collective-permute-start.23) | collective-permute-done | bytes 524320 | tf_op jit(solution)/shard_map/ppermute | solution.py:126
  156.7 3.6 %collective-permute-start.30 = (bf16[528,384]{1,0:T(8,128)(2,1)S(1)}, bf16[528,384]{1,0:T(8,128)(2,1)S(1)}, u32[]{:S(2)}, u32[]{:S(2)}) collective-permute-start(bf16[528,384]{1,0:T(8,128)(2,1)S(1)} %get-tuple-element.72), channel_id=1, source_target_pairs={{0,12},{4,0},{8,4},{12,8},{1,13},{5,1},{9,5},{13,9},{2,14},{6,2},{... | collective-permute-start | bytes 1216520 | tf_op jit(solution)/shard_map/ppermute | solution.py:613
  160.3 10.1 %collective-permute-done.30.refs_4_ = bf16[528,384]{1,0:T(8,128)(2,1)S(1)} collective-permute-done((bf16[528,384]{1,0:T(8,128)(2,1)S(1)}, bf16[528,384]{1,0:T(8,128)(2,1)S(1)}, u32[]{:S(2)}, u32[]{:S(2)}) %collective-permute-start.30) | collective-permute-done | bytes 405536 | tf_op jit(solution)/shard_map/ppermute | solution.py:613
  171.6 4.1 %collective-permute-start.31 = (bf16[528,384]{1,0:T(8,128)(2,1)S(1)}, bf16[528,384]{1,0:T(8,128)(2,1)S(1)}, u32[]{:S(2)}, u32[]{:S(2)}) collective-permute-start(bf16[528,384]{1,0:T(8,128)(2,1)S(1)} %shard_map.98), channel_id=1, source_target_pairs={{0,12},{4,0},{8,4},{12,8},{1,13},{5,1},{9,5},{13,9},{2,14},{6,2},{... | collective-permute-start | bytes 1216520 | tf_op jit(solution)/shard_map/ppermute | solution.py:613
  175.7 3.5 %collective-permute-done.26.refs_4_ = bf16[512,384]{1,0:T(8,128)(2,1)S(1)} collective-permute-done((bf16[512,384]{1,0:T(8,128)(2,1)S(1)}, bf16[512,384]{1,0:T(8,128)(2,1)S(1)}, u32[]{:S(2)}, u32[]{:S(2)}) %collective-permute-start.26) | collective-permute-done | bytes 393248 | tf_op jit(solution)/shard_map/ppermute | solution.py:613
  182.7 15.4 %collective-permute-done.31.refs_4_ = bf16[528,384]{1,0:T(8,128)(2,1)S(1)} collective-permute-done((bf16[528,384]{1,0:T(8,128)(2,1)S(1)}, bf16[528,384]{1,0:T(8,128)(2,1)S(1)}, u32[]{:S(2)}, u32[]{:S(2)}) %collective-permute-start.31) | collective-permute-done | bytes 405536 | tf_op jit(solution)/shard_map/ppermute | solution.py:613
  205.3 12.4 %collective-permute-done.28.refs_1_ = bf16[512,384]{1,0:T(8,128)(2,1)S(1)} collective-permute-done((bf16[512,384]{1,0:T(8,128)(2,1)S(1)}, bf16[512,384]{1,0:T(8,128)(2,1)S(1)}, u32[]{:S(2)}, u32[]{:S(2)}) %collective-permute-start.28) | collective-permute-done | bytes 393248 | tf_op jit(solution)/shard_map/ppermute | solution.py:613
  217.7 2.4 shard_map.102
  228.4 3.1 %collective-permute-done.37.refs_3_ = bf16[512,128]{1,0:T(8,128)(2,1)S(1)} collective-permute-done((bf16[512,128]{1,0:T(8,128)(2,1)S(1)}, bf16[512,128]{1,0:T(8,128)(2,1)S(1)}, u32[]{:S(2)}, u32[]{:S(2)}) %collective-permute-start.37) | collective-permute-done | bytes 131104 | tf_op jit(solution)/shard_map/ppermute | solution.py:244
  232.9 3.2 %collective-permute-start.33 = (bf16[512,128]{1,0:T(8,128)(2,1)S(1)}, bf16[512,128]{1,0:T(8,128)(2,1)S(1)}, u32[]{:S(2)}, u32[]{:S(2)}) collective-permute-start(bf16[512,128]{1,0:T(8,128)(2,1)S(1)} %shard_map.103.refs_6_.refs_1_), channel_id=1, source_target_pairs={{0,4},{4,8},{8,12},{12,0},{1,5},{5,9},{9,13},{13,1},{2,6},{6,10},{... | collective-permute-start | bytes 393224 | tf_op jit(solution)/shard_map/ppermute | solution.py:244
  241.7 5.3 %collective-permute-done.34.refs_3_ = bf16[512,128]{1,0:T(8,128)(2,1)S(1)} collective-permute-done((bf16[512,128]{1,0:T(8,128)(2,1)S(1)}, bf16[512,128]{1,0:T(8,128)(2,1)S(1)}, u32[]{:S(2)}, u32[]{:S(2)}) %collective-permute-start.34) | collective-permute-done | bytes 131104 | tf_op jit(solution)/shard_map/ppermute | solution.py:244
  252.5 5.2 %collective-permute-done.48.refs_3_ = bf16[512,256]{1,0:T(8,128)(2,1)S(1)} collective-permute-done((bf16[512,256]{1,0:T(8,128)(2,1)S(1)}, bf16[512,256]{1,0:T(8,128)(2,1)S(1)}, u32[]{:S(2)}, u32[]{:S(2)}) %collective-permute-start.48) | collective-permute-done | bytes 262176 | tf_op jit(solution)/shard_map/ppermute | solution.py:126
  258.3 3.3 %collective-permute-start.49 = (bf16[128,256]{1,0:T(8,128)(2,1)S(1)}, bf16[128,256]{1,0:T(8,128)(2,1)S(1)}, u32[]{:S(2)}, u32[]{:S(2)}) collective-permute-start(bf16[128,256]{1,0:T(8,128)(2,1)S(1)} %get-tuple-element.88), channel_id=1, source_target_pairs={{0,4},{4,8},{8,12},{12,0},{1,5},{5,9},{9,13},{13,1},{2,6},{6,10},{... | collective-permute-start | bytes 196616 | tf_op jit(solution)/shard_map/ppermute | solution.py:244
  275.3 2.9 %collective-permute-done.52.refs_1_ = bf16[512,256]{1,0:T(8,128)(2,1)S(1)} collective-permute-done((bf16[512,256]{1,0:T(8,128)(2,1)S(1)}, bf16[512,256]{1,0:T(8,128)(2,1)S(1)}, u32[]{:S(2)}, u32[]{:S(2)}) %collective-permute-start.52) | collective-permute-done | bytes 262176 | tf_op jit(solution)/shard_map/ppermute | solution.py:126
  278.8 3.9 %collective-permute-done.45.refs_1_ = bf16[512,256]{1,0:T(8,128)(2,1)S(1)} collective-permute-done((bf16[512,256]{1,0:T(8,128)(2,1)S(1)}, bf16[512,256]{1,0:T(8,128)(2,1)S(1)}, u32[]{:S(2)}, u32[]{:S(2)}) %collective-permute-start.45) | collective-permute-done | bytes 262176 | tf_op jit(solution)/shard_map/ppermute | solution.py:126
  (127 shorter events, 102.1 us)
Async XLA Ops:
  1.8 10.5 %collective-permute-start = (bf16[256,256]{1,0:T(8,128)(2,1)S(1)}, bf16[256,256]{1,0:T(8,128)(2,1)S(1)}, u32[]{:S(2)}, u32[]{:S(2)}) collective-permute-start(bf16[256,256]{1,0:T(8,128)(2,1)S(1)} %get-tuple-element.49), channel_id=1, source_target_pairs={{0,4},{4,8},{8,12},{12,0},{1,5},{5,9},{9,13},{13,1},{2,6},{6,10},{... | collective-permute-start | bytes 393224 | tf_op jit(solution)/shard_map/ppermute | solution.py:244
  4.9 11.2 %collective-permute-start.1 = (bf16[256,256]{1,0:T(8,128)(2,1)S(1)}, bf16[256,256]{1,0:T(8,128)(2,1)S(1)}, u32[]{:S(2)}, u32[]{:S(2)}) collective-permute-start(bf16[256,256]{1,0:T(8,128)(2,1)S(1)} %get-tuple-element.50), channel_id=1, source_target_pairs={{0,8},{4,12},{8,0},{12,4},{1,9},{5,13},{9,1},{13,5},{2,10},{6,14},... | collective-permute-start | bytes 393224 | tf_op jit(solution)/shard_map/ppermute | solution.py:244
  7.5 8.6 %collective-permute-start.2 = (bf16[256,256]{1,0:T(8,128)(2,1)S(1)}, bf16[256,256]{1,0:T(8,128)(2,1)S(1)}, u32[]{:S(2)}, u32[]{:S(2)}) collective-permute-start(bf16[256,256]{1,0:T(8,128)(2,1)S(1)} %get-tuple-element.51), channel_id=1, source_target_pairs={{0,12},{4,0},{8,4},{12,8},{1,13},{5,1},{9,5},{13,9},{2,14},{6,2},{... | collective-permute-start | bytes 393224 | tf_op jit(solution)/shard_map/ppermute | solution.py:244
  24.9 8.7 %collective-permute-start.3 = (bf16[512,256]{1,0:T(8,128)(2,1)S(1)}, bf16[512,256]{1,0:T(8,128)(2,1)S(1)}, u32[]{:S(2)}, u32[]{:S(2)}) collective-permute-start(bf16[512,256]{1,0:T(8,128)(2,1)S(1)} %get-tuple-element.52.refs_1_), channel_id=1, source_target_pairs={{0,2},{1,3},{2,0},{3,1},{4,6},{5,7},{6,4},{7,5},{8,10},{9,11},{10,... | collective-permute-start | bytes 786440 | tf_op jit(solution)/shard_map/ppermute | solution.py:126
  36.8 13.8 %collective-permute-start.12 = (bf16[528,384]{1,0:T(8,128)(2,1)S(1)}, bf16[528,384]{1,0:T(8,128)(2,1)S(1)}, u32[]{:S(2)}, u32[]{:S(2)}) collective-permute-start(bf16[528,384]{1,0:T(8,128)(2,1)S(1)} %get-tuple-element.60), channel_id=1, source_target_pairs={{0,12},{4,0},{8,4},{12,8},{1,13},{5,1},{9,5},{13,9},{2,14},{6,2},{... | collective-permute-start | bytes 1216520 | tf_op jit(solution)/shard_map/ppermute | solution.py:613
  40.3 19.1 %collective-permute-start.7 = (bf16[512,384]{1,0:T(8,128)(2,1)S(1)}, bf16[512,384]{1,0:T(8,128)(2,1)S(1)}, u32[]{:S(2)}, u32[]{:S(2)}) collective-permute-start(bf16[512,384]{1,0:T(8,128)(2,1)S(1)} %get-tuple-element.54), channel_id=1, source_target_pairs={{0,4},{4,8},{8,12},{12,0},{1,5},{5,9},{9,13},{13,1},{2,6},{6,10},{... | collective-permute-start | bytes 1179656 | tf_op jit(solution)/shard_map/ppermute | solution.py:613
  51.9 26.1 %collective-permute-start.13 = (bf16[528,384]{1,0:T(8,128)(2,1)S(1)}, bf16[528,384]{1,0:T(8,128)(2,1)S(1)}, u32[]{:S(2)}, u32[]{:S(2)}) collective-permute-start(bf16[528,384]{1,0:T(8,128)(2,1)S(1)} %shard_map.81), channel_id=1, source_target_pairs={{0,12},{4,0},{8,4},{12,8},{1,13},{5,1},{9,5},{13,9},{2,14},{6,2},{... | collective-permute-start | bytes 1216520 | tf_op jit(solution)/shard_map/ppermute | solution.py:613
  60.6 18.6 %collective-permute-start.8 = (bf16[512,384]{1,0:T(8,128)(2,1)S(1)}, bf16[512,384]{1,0:T(8,128)(2,1)S(1)}, u32[]{:S(2)}, u32[]{:S(2)}) collective-permute-start(bf16[512,384]{1,0:T(8,128)(2,1)S(1)} %shard_map.78), channel_id=1, source_target_pairs={{0,4},{4,8},{8,12},{12,0},{1,5},{5,9},{9,13},{13,1},{2,6},{6,10},{... | collective-permute-start | bytes 1179656 | tf_op jit(solution)/shard_map/ppermute | solution.py:613
  79.2 18.2 %collective-permute-start.14 = (bf16[528,384]{1,0:T(8,128)(2,1)S(1)}, bf16[528,384]{1,0:T(8,128)(2,1)S(1)}, u32[]{:S(2)}, u32[]{:S(2)}) collective-permute-start(bf16[528,384]{1,0:T(8,128)(2,1)S(1)} %shard_map.82), channel_id=1, source_target_pairs={{0,12},{4,0},{8,4},{12,8},{1,13},{5,1},{9,5},{13,9},{2,14},{6,2},{... | collective-permute-start | bytes 1216520 | tf_op jit(solution)/shard_map/ppermute | solution.py:613
  80.6 16.9 %collective-permute-start.9 = (bf16[512,384]{1,0:T(8,128)(2,1)S(1)}, bf16[512,384]{1,0:T(8,128)(2,1)S(1)}, u32[]{:S(2)}, u32[]{:S(2)}) collective-permute-start(bf16[512,384]{1,0:T(8,128)(2,1)S(1)} %shard_map.79), channel_id=1, source_target_pairs={{0,4},{4,8},{8,12},{12,0},{1,5},{5,9},{9,13},{13,1},{2,6},{6,10},{... | collective-permute-start | bytes 1179656 | tf_op jit(solution)/shard_map/ppermute | solution.py:613
  101.4 9.2 %collective-permute-start.19 = (bf16[512,128]{1,0:T(8,128)(2,1)S(1)}, bf16[512,128]{1,0:T(8,128)(2,1)S(1)}, u32[]{:S(2)}, u32[]{:S(2)}) collective-permute-start(bf16[512,128]{1,0:T(8,128)(2,1)S(1)} %get-tuple-element.62.refs_1_), channel_id=1, source_target_pairs={{0,8},{4,12},{8,0},{12,4},{1,9},{5,13},{9,1},{13,5},{2,10},{6,14},... | collective-permute-start | bytes 393224 | tf_op jit(solution)/shard_map/ppermute | solution.py:244
  101.4 9.2 %collective-permute-start.20 = (bf16[512,128]{1,0:T(8,128)(2,1)S(1)}, bf16[512,128]{1,0:T(8,128)(2,1)S(1)}, u32[]{:S(2)}, u32[]{:S(2)}) collective-permute-start(bf16[512,128]{1,0:T(8,128)(2,1)S(1)} %get-tuple-element.62.refs_1_), channel_id=1, source_target_pairs={{0,12},{4,0},{8,4},{12,8},{1,13},{5,1},{9,5},{13,9},{2,14},{6,2},{... | collective-permute-start | bytes 393224 | tf_op jit(solution)/shard_map/ppermute | solution.py:244
  114.0 11.4 %collective-permute-start.16 = (bf16[512,128]{1,0:T(8,128)(2,1)S(1)}, bf16[512,128]{1,0:T(8,128)(2,1)S(1)}, u32[]{:S(2)}, u32[]{:S(2)}) collective-permute-start(bf16[512,128]{1,0:T(8,128)(2,1)S(1)} %shard_map.87.refs_6_.refs_1_), channel_id=1, source_target_pairs={{0,8},{4,12},{8,0},{12,4},{1,9},{5,13},{9,1},{13,5},{2,10},{6,14},... | collective-permute-start | bytes 393224 | tf_op jit(solution)/shard_map/ppermute | solution.py:244
  115.2 10.2 %collective-permute-start.17 = (bf16[512,128]{1,0:T(8,128)(2,1)S(1)}, bf16[512,128]{1,0:T(8,128)(2,1)S(1)}, u32[]{:S(2)}, u32[]{:S(2)}) collective-permute-start(bf16[512,128]{1,0:T(8,128)(2,1)S(1)} %shard_map.87.refs_6_.refs_1_), channel_id=1, source_target_pairs={{0,12},{4,0},{8,4},{12,8},{1,13},{5,1},{9,5},{13,9},{2,14},{6,2},{... | collective-permute-start | bytes 393224 | tf_op jit(solution)/shard_map/ppermute | solution.py:244
  126.8 14.9 %collective-permute-start.24 = (bf16[512,512]{1,0:T(8,128)(2,1)S(1)}, bf16[512,512]{1,0:T(8,128)(2,1)S(1)}, u32[]{:S(2)}, u32[]{:S(2)}) collective-permute-start(bf16[512,512]{1,0:T(8,128)(2,1)S(1)} %shard_map.89.refs_6_.refs_3_), channel_id=1, source_target_pairs={{0,2},{1,3},{2,0},{3,1},{4,6},{5,7},{6,4},{7,5},{8,10},{9,11},{10,... | collective-permute-start | bytes 1572872 | tf_op jit(solution)/shard_map/ppermute | solution.py:126
  129.4 23.0 %collective-permute-start.23 = (bf16[512,512]{1,0:T(8,128)(2,1)S(1)}, bf16[512,512]{1,0:T(8,128)(2,1)S(1)}, u32[]{:S(2)}, u32[]{:S(2)}) collective-permute-start(bf16[512,512]{1,0:T(8,128)(2,1)S(1)} %shard_map.91.refs_3_), channel_id=1, source_target_pairs={{0,2},{1,3},{2,0},{3,1},{4,6},{5,7},{6,4},{7,5},{8,10},{9,11},{10,... | collective-permute-start | bytes 1572872 | tf_op jit(solution)/shard_map/ppermute | solution.py:126
  142.4 10.8 %collective-permute-start.25 = (bf16[512,512]{1,0:T(8,128)(2,1)S(1)}, bf16[512,512]{1,0:T(8,128)(2,1)S(1)}, u32[]{:S(2)}, u32[]{:S(2)}) collective-permute-start(bf16[512,512]{1,0:T(8,128)(2,1)S(1)} %shard_map.93.refs_1_), channel_id=1, source_target_pairs={{0,1},{1,0},{2,3},{3,2},{4,5},{5,4},{6,7},{7,6},{8,9},{9,8},{10,11... | collective-permute-start | bytes 1572872 | tf_op jit(solution)/shard_map/ppermute | solution.py:126
  156.7 13.6 %collective-permute-start.30 = (bf16[528,384]{1,0:T(8,128)(2,1)S(1)}, bf16[528,384]{1,0:T(8,128)(2,1)S(1)}, u32[]{:S(2)}, u32[]{:S(2)}) collective-permute-start(bf16[528,384]{1,0:T(8,128)(2,1)S(1)} %get-tuple-element.72), channel_id=1, source_target_pairs={{0,12},{4,0},{8,4},{12,8},{1,13},{5,1},{9,5},{13,9},{2,14},{6,2},{... | collective-permute-start | bytes 1216520 | tf_op jit(solution)/shard_map/ppermute | solution.py:613
  160.3 19.0 %collective-permute-start.26 = (bf16[512,384]{1,0:T(8,128)(2,1)S(1)}, bf16[512,384]{1,0:T(8,128)(2,1)S(1)}, u32[]{:S(2)}, u32[]{:S(2)}) collective-permute-start(bf16[512,384]{1,0:T(8,128)(2,1)S(1)} %get-tuple-element.69), channel_id=1, source_target_pairs={{0,4},{4,8},{8,12},{12,0},{1,5},{5,9},{9,13},{13,1},{2,6},{6,10},{... | collective-permute-start | bytes 1179656 | tf_op jit(solution)/shard_map/ppermute | solution.py:613
  171.6 26.5 %collective-permute-start.31 = (bf16[528,384]{1,0:T(8,128)(2,1)S(1)}, bf16[528,384]{1,0:T(8,128)(2,1)S(1)}, u32[]{:S(2)}, u32[]{:S(2)}) collective-permute-start(bf16[528,384]{1,0:T(8,128)(2,1)S(1)} %shard_map.98), channel_id=1, source_target_pairs={{0,12},{4,0},{8,4},{12,8},{1,13},{5,1},{9,5},{13,9},{2,14},{6,2},{... | collective-permute-start | bytes 1216520 | tf_op jit(solution)/shard_map/ppermute | solution.py:613
  180.5 18.9 %collective-permute-start.27 = (bf16[512,384]{1,0:T(8,128)(2,1)S(1)}, bf16[512,384]{1,0:T(8,128)(2,1)S(1)}, u32[]{:S(2)}, u32[]{:S(2)}) collective-permute-start(bf16[512,384]{1,0:T(8,128)(2,1)S(1)} %shard_map.95), channel_id=1, source_target_pairs={{0,4},{4,8},{8,12},{12,0},{1,5},{5,9},{9,13},{13,1},{2,6},{6,10},{... | collective-permute-start | bytes 1179656 | tf_op jit(solution)/shard_map/ppermute | solution.py:613
  199.4 18.3 %collective-permute-start.32 = (bf16[528,384]{1,0:T(8,128)(2,1)S(1)}, bf16[528,384]{1,0:T(8,128)(2,1)S(1)}, u32[]{:S(2)}, u32[]{:S(2)}) collective-permute-start(bf16[528,384]{1,0:T(8,128)(2,1)S(1)} %shard_map.99), channel_id=1, source_target_pairs={{0,12},{4,0},{8,4},{12,8},{1,13},{5,1},{9,5},{13,9},{2,14},{6,2},{... | collective-permute-start | bytes 1216520 | tf_op jit(solution)/shard_map/ppermute | solution.py:613
  200.7 17.0 %collective-permute-start.28 = (bf16[512,384]{1,0:T(8,128)(2,1)S(1)}, bf16[512,384]{1,0:T(8,128)(2,1)S(1)}, u32[]{:S(2)}, u32[]{:S(2)}) collective-permute-start(bf16[512,384]{1,0:T(8,128)(2,1)S(1)} %shard_map.96), channel_id=1, source_target_pairs={{0,4},{4,8},{8,12},{12,0},{1,5},{5,9},{9,13},{13,1},{2,6},{6,10},{... | collective-permute-start | bytes 1179656 | tf_op jit(solution)/shard_map/ppermute | solution.py:613
  221.7 9.9 %collective-permute-start.37 = (bf16[512,128]{1,0:T(8,128)(2,1)S(1)}, bf16[512,128]{1,0:T(8,128)(2,1)S(1)}, u32[]{:S(2)}, u32[]{:S(2)}) collective-permute-start(bf16[512,128]{1,0:T(8,128)(2,1)S(1)} %get-tuple-element.74.refs_1_), channel_id=1, source_target_pairs={{0,8},{4,12},{8,0},{12,4},{1,9},{5,13},{9,1},{13,5},{2,10},{6,14},... | collective-permute-start | bytes 393224 | tf_op jit(solution)/shard_map/ppermute | solution.py:244
  222.5 9.0 %collective-permute-start.38 = (bf16[512,128]{1,0:T(8,128)(2,1)S(1)}, bf16[512,128]{1,0:T(8,128)(2,1)S(1)}, u32[]{:S(2)}, u32[]{:S(2)}) collective-permute-start(bf16[512,128]{1,0:T(8,128)(2,1)S(1)} %get-tuple-element.74.refs_1_), channel_id=1, source_target_pairs={{0,12},{4,0},{8,4},{12,8},{1,13},{5,1},{9,5},{13,9},{2,14},{6,2},{... | collective-permute-start | bytes 393224 | tf_op jit(solution)/shard_map/ppermute | solution.py:244
  232.9 8.7 %collective-permute-start.33 = (bf16[512,128]{1,0:T(8,128)(2,1)S(1)}, bf16[512,128]{1,0:T(8,128)(2,1)S(1)}, u32[]{:S(2)}, u32[]{:S(2)}) collective-permute-start(bf16[512,128]{1,0:T(8,128)(2,1)S(1)} %shard_map.103.refs_6_.refs_1_), channel_id=1, source_target_pairs={{0,4},{4,8},{8,12},{12,0},{1,5},{5,9},{9,13},{13,1},{2,6},{6,10},{... | collective-permute-start | bytes 393224 | tf_op jit(solution)/shard_map/ppermute | solution.py:244
  236.2 10.9 %collective-permute-start.34 = (bf16[512,128]{1,0:T(8,128)(2,1)S(1)}, bf16[512,128]{1,0:T(8,128)(2,1)S(1)}, u32[]{:S(2)}, u32[]{:S(2)}) collective-permute-start(bf16[512,128]{1,0:T(8,128)(2,1)S(1)} %shard_map.103.refs_6_.refs_1_), channel_id=1, source_target_pairs={{0,8},{4,12},{8,0},{12,4},{1,9},{5,13},{9,1},{13,5},{2,10},{6,14},... | collective-permute-start | bytes 393224 | tf_op jit(solution)/shard_map/ppermute | solution.py:244
  237.8 9.2 %collective-permute-start.35 = (bf16[512,128]{1,0:T(8,128)(2,1)S(1)}, bf16[512,128]{1,0:T(8,128)(2,1)S(1)}, u32[]{:S(2)}, u32[]{:S(2)}) collective-permute-start(bf16[512,128]{1,0:T(8,128)(2,1)S(1)} %shard_map.103.refs_6_.refs_1_), channel_id=1, source_target_pairs={{0,12},{4,0},{8,4},{12,8},{1,13},{5,1},{9,5},{13,9},{2,14},{6,2},{... | collective-permute-start | bytes 393224 | tf_op jit(solution)/shard_map/ppermute | solution.py:244
  248.4 9.2 %collective-permute-start.48 = (bf16[512,256]{1,0:T(8,128)(2,1)S(1)}, bf16[512,256]{1,0:T(8,128)(2,1)S(1)}, u32[]{:S(2)}, u32[]{:S(2)}) collective-permute-start(bf16[512,256]{1,0:T(8,128)(2,1)S(1)} %get-tuple-element.77.refs_6_), channel_id=1, source_target_pairs={{0,2},{1,3},{2,0},{3,1},{4,6},{5,7},{6,4},{7,5},{8,10},{9,11},{10,... | collective-permute-start | bytes 786440 | tf_op jit(solution)/shard_map/ppermute | solution.py:126
  251.0 13.1 %collective-permute-start.41 = (bf16[512,256]{1,0:T(8,128)(2,1)S(1)}, bf16[512,256]{1,0:T(8,128)(2,1)S(1)}, u32[]{:S(2)}, u32[]{:S(2)}) collective-permute-start(bf16[512,256]{1,0:T(8,128)(2,1)S(1)} %get-tuple-element.81), channel_id=1, source_target_pairs={{0,2},{1,3},{2,0},{3,1},{4,6},{5,7},{6,4},{7,5},{8,10},{9,11},{10,... | collective-permute-start | bytes 786440 | tf_op jit(solution)/shard_map/ppermute | solution.py:126
  258.3 9.7 %collective-permute-start.49 = (bf16[128,256]{1,0:T(8,128)(2,1)S(1)}, bf16[128,256]{1,0:T(8,128)(2,1)S(1)}, u32[]{:S(2)}, u32[]{:S(2)}) collective-permute-start(bf16[128,256]{1,0:T(8,128)(2,1)S(1)} %get-tuple-element.88), channel_id=1, source_target_pairs={{0,4},{4,8},{8,12},{12,0},{1,5},{5,9},{9,13},{13,1},{2,6},{6,10},{... | collective-permute-start | bytes 196616 | tf_op jit(solution)/shard_map/ppermute | solution.py:244
  273.8 8.9 %collective-permute-start.45 = (bf16[512,256]{1,0:T(8,128)(2,1)S(1)}, bf16[512,256]{1,0:T(8,128)(2,1)S(1)}, u32[]{:S(2)}, u32[]{:S(2)}) collective-permute-start(bf16[512,256]{1,0:T(8,128)(2,1)S(1)} %shard_map.109.refs_0_), channel_id=1, source_target_pairs={{0,2},{1,3},{2,0},{3,1},{4,6},{5,7},{6,4},{7,5},{8,10},{9,11},{10,... | collective-permute-start | bytes 786440 | tf_op jit(solution)/shard_map/ppermute | solution.py:126
  (26 other events, 159.9 us)

commit v9 on v8

--- a/solution.py
+++ b/solution.py
@@ -121,6 +121,15 @@
     return [(i, (i + shift) % count) for i in range(count)]
 
 
+def fold(count):
+    return [2 * i if 2 * i < count else 2 * (count - 1 - i) + 1 for i in range(count)]
+
+
+def folded_ring(count, shift):
+    order = fold(count)
+    return [(order[i], order[(i + shift) % count]) for i in range(count)]
+
+
 def swapped(array, axis, distance):
     count = lax.axis_size(axis)
     return lax.ppermute(array, axis, [(i, i ^ distance) for i in range(count)])
@@ -196,31 +205,34 @@
 
 
 def scatter_tokens(tokens, place, sp_count, feats, piece):
-    tok_here = tokens.shape[0]
+    rows = tokens.shape[0] // 2
 
     def body(place_ref, tokens_ref, *rest):
         out_refs, sem = rest[:-1], rest[-1]
         slot = place_ref[1] * 2 + place_ref[2]
         copies = []
-        for shift in range(sp_count):
+        for part, shift in [(part, shift) for part in range(2) for shift in range(sp_count)]:
             target = lax.rem(place_ref[0] + shift, sp_count)
             column = pl.multiple_of(target * feats + slot * piece, piece)
             copy = pltpu.make_async_copy(
-                tokens_ref.at[:, pl.ds(column, piece)], out_refs[shift], sem.at[shift]
+                tokens_ref.at[pl.ds(part * rows, rows), pl.ds(column, piece)],
+                out_refs[part * sp_count + shift],
+                sem.at[part, shift],
             )
             copy.start()
             copies.append(copy)
         for copy in copies:
             copy.wait()
 
-    return local_kernel(
+    blocks = local_kernel(
         body,
         place,
         (),
-        [shaped(tok_here, piece)] * sp_count,
-        scratch=[pltpu.SemaphoreType.DMA((sp_count,))],
+        [shaped(rows, piece)] * (2 * sp_count),
+        scratch=[pltpu.SemaphoreType.DMA((2, sp_count))],
         hbm=(tokens,),
     )
+    return blocks[:sp_count], blocks[sp_count:]
 
 
 def stack_blocks(blocks, place, parts=1, after=()):
@@ -337,7 +349,8 @@
                 squares_ref[pl.ds(start + run, 1), :] = jnp.sum(total.T, axis=0, keepdims=True)
         else:
             scaled_ref, squares_ref = array_refs
-        chunk = lax.rem(place_ref[0] + chunk_shift, sp_count)
+        at = lax.rem(place_ref[3] + chunk_shift, sp_count)
+        chunk = jnp.where(2 * at < sp_count, 2 * at, 2 * (sp_count - 1 - at) + 1)
         total = jnp.dot(scaled_ref[...], staged_ref[chunk], preferred_element_type=jnp.float32)
         if arrived is not None:
             total += refs[count + 1][pl.ds(0, tok), :].astype(jnp.float32)
@@ -599,7 +612,8 @@
 def stationary_plan(tokens, norm_gain, w_query, w_key, w_value, w_out, offset_bias):
     sp_count = lax.axis_size("sp")
     sp_index, tp_index = lax.axis_index("sp"), lax.axis_index("tp")
-    place = jnp.stack([sp_index, tp_index % 2, tp_index // 2]).astype(jnp.int32)
+    folded = jnp.where(sp_index % 2 == 0, sp_index // 2, sp_count - 1 - sp_index // 2)
+    place = jnp.stack([sp_index, tp_index % 2, tp_index // 2, folded]).astype(jnp.int32)
     feats = w_query.shape[1]
     heads = offset_bias.shape[1] // sp_count
     piece = feats // 4
@@ -607,10 +621,10 @@
     weights = (w_query, w_key, w_value)
     halves = [None, None]
     sources = [None, None]
-    shifts = (1, -1)
+    shifts = (-1, -1)
 
     def sent_on(block, part):
-        return lax.ppermute(block, "sp", ring(sp_count, shifts[part]))
+        return lax.ppermute(block, "sp", folded_ring(sp_count, shifts[part]))
 
     def made(layer, part, step, arrived=None):
         chunk = (-shifts[part] * (step + 1)) % sp_count
@@ -628,11 +642,14 @@
     staged = []
     for layer in range(LAYERS):
         staged.append(stage_weights(weights, layer, place, sp_count))
-    blocks = over_sp(scatter_tokens(tokens, place, sp_count, feats, piece), sp_count)
-    held = stack_blocks(blocks, place, 2, (bias, staged[0]))
-    far = [swapped(h, "tp", 2) for h in held]
+    held, far = [], []
+    for part, blocks in enumerate(scatter_tokens(tokens, place, sp_count, feats, piece)):
+        blocks = over_sp(blocks, sp_count)
+        held += stack_blocks(blocks, place)
+        far.append(swapped(held[part], "tp", 2))
     near = [swapped(h, "tp", 1) for h in held]
-    halves[0] = [held[0], far[0], near[0], swapped(far[0], "tp", 1)]
+    near_far = swapped(far[0], "tp", 1)
+    halves[0] = [held[0], far[0], near[0], near_far]
     first = [first_made(0, 0), None]
     far[1] = lax.optimization_barrier((far[1], first[0]))[0]
     near_far = swapped(far[1], "tp", 1)

time: 286 us -> 274 us (0.958)
  waiting for transfers between devices: 159 us -> 145 us
    ppermute x12, waiting for transfers between devices: 80.4 us -> 69.5 us  [sent_on(): return lax.ppermute(block, 'sp', folded_ring(sp_count, shifts[part]))]
    ppermute x21 -> x24, starting transfers between devices: 35.3 us -> 42.2 us  [over_sp(): lax.ppermute(blocks[shift], 'sp', ring(count, shift))]
    ppermute x22, waiting for transfers between devices: 47.3 us -> 41.2 us  [swapped(): return lax.ppermute(array, axis, [(i, i ^ distance) for i in range(count)])]
    ppermute x22, starting transfers between devices: 13.3 us -> 9.72 us  [swapped(): return lax.ppermute(array, axis, [(i, i ^ distance) for i in range(count)])]
    ppermute x21 -> x24, waiting for transfers between devices: 31.6 us -> 34 us  [over_sp(): lax.ppermute(blocks[shift], 'sp', ring(count, shift))]
    pallas_call x39 -> x40, Pallas kernels: 50.9 us -> 51.6 us  [local_kernel(): pl.pallas_call(ordered, out_shape=list(outs), in_specs=[smem] + [vmem] *...]
  transfers between devices with their start and end apart: 55 -> 58, of which waited for: 29 -> 38; matrix products, arithmetic and copies ran while one was open for 0% -> 0% of each run, Pallas kernels for 13% -> 14%
where the time goes in v9:
time: 274 us
  waiting for transfers between devices  145 us (53%)
  starting transfers between devices  73.9 us (27%)
  Pallas kernels  54.9 us (20%)
    ppermute x12, waiting for transfers between devices, sent_on(): return lax.ppermute(block, 'sp', folded_ring(sp_count, shifts[part]))  69.5 us
    pallas_call x40, Pallas kernels, local_kernel(): pl.pallas_call(ordered, out_shape=list(outs), in_specs=[smem] + [vmem] *...  51.6 us
    ppermute x24, starting transfers between devices, over_sp(): lax.ppermute(blocks[shift], 'sp', ring(count, shift))  42.2 us
    ppermute x22, waiting for transfers between devices, swapped(): return lax.ppermute(array, axis, [(i, i ^ distance) for i in range(count)])  41.2 us
    ppermute x24, waiting for transfers between devices, over_sp(): lax.ppermute(blocks[shift], 'sp', ring(count, shift))  34 us
    ppermute x12, starting transfers between devices, sent_on(): return lax.ppermute(block, 'sp', folded_ring(sp_count, shifts[part]))  22 us
    ppermute x22, starting transfers between devices, swapped(): return lax.ppermute(array, axis, [(i, i ^ distance) for i in range(count)])  9.72 us
  transfers between devices with their start and end apart: 58, of which 38 were waited for; matrix products, arithmetic and copies ran while one was open for 0% of the time, Pallas kernels for 14%

profile of v9, /device:TPU:0, one launch (start us, length us, event | category | flops | bytes accessed | tf_op | source)
XLA Modules:
  0.0 274.2 jit_solution(18373055587984032069)
XLA Ops:
  1.8 3.1 %collective-permute-start.4 = (bf16[128,256]{1,0:T(8,128)(2,1)S(1)}, bf16[128,256]{1,0:T(8,128)(2,1)S(1)}, u32[]{:S(2)}, u32[]{:S(2)}) collective-permute-start(bf16[128,256]{1,0:T(8,128)(2,1)S(1)} %get-tuple-element.55), channel_id=1, source_target_pairs={{0,4},{4,8},{8,12},{12,0},{1,5},{5,9},{9,13},{13,1},{2,6},{6,10},{... | collective-permute-start | bytes 196616 | tf_op jit(solution)/shard_map/ppermute | solution.py:256
  4.9 2.6 collective-permute-start.5
  9.4 2.6 collective-permute-done.5.refs_3_
  23.9 2.6 shard_map.76.refs_6_.refs_3_.refs_2_
  35.6 10.8 %collective-permute-done.15.refs_4_ = bf16[528,384]{1,0:T(8,128)(2,1)S(1)} collective-permute-done((bf16[528,384]{1,0:T(8,128)(2,1)S(1)}, bf16[528,384]{1,0:T(8,128)(2,1)S(1)}, u32[]{:S(2)}, u32[]{:S(2)}) %collective-permute-start.15) | collective-permute-done | bytes 405536 | tf_op jit(solution)/shard_map/ppermute | solution.py:627
  48.8 6.0 %collective-permute-done.10.refs_4_ = bf16[512,384]{1,0:T(8,128)(2,1)S(1)} collective-permute-done((bf16[512,384]{1,0:T(8,128)(2,1)S(1)}, bf16[512,384]{1,0:T(8,128)(2,1)S(1)}, u32[]{:S(2)}, u32[]{:S(2)}) %collective-permute-start.10) | collective-permute-done | bytes 393248 | tf_op jit(solution)/shard_map/ppermute | solution.py:627
  57.2 6.3 %collective-permute-done.16.refs_4_ = bf16[528,384]{1,0:T(8,128)(2,1)S(1)} collective-permute-done((bf16[528,384]{1,0:T(8,128)(2,1)S(1)}, bf16[528,384]{1,0:T(8,128)(2,1)S(1)}, u32[]{:S(2)}, u32[]{:S(2)}) %collective-permute-start.16) | collective-permute-done | bytes 405536 | tf_op jit(solution)/shard_map/ppermute | solution.py:627
  65.9 6.0 %collective-permute-done.11.refs_4_ = bf16[512,384]{1,0:T(8,128)(2,1)S(1)} collective-permute-done((bf16[512,384]{1,0:T(8,128)(2,1)S(1)}, bf16[512,384]{1,0:T(8,128)(2,1)S(1)}, u32[]{:S(2)}, u32[]{:S(2)}) %collective-permute-start.11) | collective-permute-done | bytes 393248 | tf_op jit(solution)/shard_map/ppermute | solution.py:627
  74.3 2.6 shard_map.86.refs_7_.refs_4_.refs_3_.refs_2_
  80.3 7.9 %collective-permute-done.12.refs_1_ = bf16[512,384]{1,0:T(8,128)(2,1)S(1)} collective-permute-done((bf16[512,384]{1,0:T(8,128)(2,1)S(1)}, bf16[512,384]{1,0:T(8,128)(2,1)S(1)}, u32[]{:S(2)}, u32[]{:S(2)}) %collective-permute-start.12) | collective-permute-done | bytes 393248 | tf_op jit(solution)/shard_map/ppermute | solution.py:627
  98.9 4.0 %collective-permute-done.22.refs_3_ = bf16[512,128]{1,0:T(8,128)(2,1)S(1)} collective-permute-done((bf16[512,128]{1,0:T(8,128)(2,1)S(1)}, bf16[512,128]{1,0:T(8,128)(2,1)S(1)}, u32[]{:S(2)}, u32[]{:S(2)}) %collective-permute-start.22) | collective-permute-done | bytes 131104 | tf_op jit(solution)/shard_map/ppermute | solution.py:256
  104.3 3.2 %collective-permute-start.18 = (bf16[512,128]{1,0:T(8,128)(2,1)S(1)}, bf16[512,128]{1,0:T(8,128)(2,1)S(1)}, u32[]{:S(2)}, u32[]{:S(2)}) collective-permute-start(bf16[512,128]{1,0:T(8,128)(2,1)S(1)} %shard_map.88.refs_6_.refs_1_), channel_id=1, source_target_pairs={{0,4},{4,8},{8,12},{12,0},{1,5},{5,9},{9,13},{13,1},{2,6},{6,10},{... | collective-permute-start | bytes 393224 | tf_op jit(solution)/shard_map/ppermute | solution.py:256
  112.6 5.1 %collective-permute-done.19.refs_3_ = bf16[512,128]{1,0:T(8,128)(2,1)S(1)} collective-permute-done((bf16[512,128]{1,0:T(8,128)(2,1)S(1)}, bf16[512,128]{1,0:T(8,128)(2,1)S(1)}, u32[]{:S(2)}, u32[]{:S(2)}) %collective-permute-start.19) | collective-permute-done | bytes 131104 | tf_op jit(solution)/shard_map/ppermute | solution.py:256
  122.7 11.3 %collective-permute-done.27.refs_4_ = bf16[512,512]{1,0:T(8,128)(2,1)S(1)} collective-permute-done((bf16[512,512]{1,0:T(8,128)(2,1)S(1)}, bf16[512,512]{1,0:T(8,128)(2,1)S(1)}, u32[]{:S(2)}, u32[]{:S(2)}) %collective-permute-start.27) | collective-permute-done | bytes 524320 | tf_op jit(solution)/shard_map/ppermute | solution.py:135
  134.8 9.9 %collective-permute-done.26.refs_4_ = bf16[512,512]{1,0:T(8,128)(2,1)S(1)} collective-permute-done((bf16[512,512]{1,0:T(8,128)(2,1)S(1)}, bf16[512,512]{1,0:T(8,128)(2,1)S(1)}, u32[]{:S(2)}, u32[]{:S(2)}) %collective-permute-start.26) | collective-permute-done | bytes 524320 | tf_op jit(solution)/shard_map/ppermute | solution.py:135
  149.0 3.3 %collective-permute-start.33 = (bf16[528,384]{1,0:T(8,128)(2,1)S(1)}, bf16[528,384]{1,0:T(8,128)(2,1)S(1)}, u32[]{:S(2)}, u32[]{:S(2)}) collective-permute-start(bf16[528,384]{1,0:T(8,128)(2,1)S(1)} %get-tuple-element.76), channel_id=1, source_target_pairs={{0,4},{8,0},{12,8},{4,12},{1,5},{9,1},{13,9},{5,13},{2,6},{10,2},{... | collective-permute-start | bytes 1216520 | tf_op jit(solution)/shard_map/ppermute | solution.py:627
  154.4 7.9 %collective-permute-done.33.refs_4_ = bf16[528,384]{1,0:T(8,128)(2,1)S(1)} collective-permute-done((bf16[528,384]{1,0:T(8,128)(2,1)S(1)}, bf16[528,384]{1,0:T(8,128)(2,1)S(1)}, u32[]{:S(2)}, u32[]{:S(2)}) %collective-permute-start.33) | collective-permute-done | bytes 405536 | tf_op jit(solution)/shard_map/ppermute | solution.py:627
  163.5 2.4 collective-permute-start.34
  166.0 4.7 %collective-permute-done.29.refs_4_ = bf16[512,384]{1,0:T(8,128)(2,1)S(1)} collective-permute-done((bf16[512,384]{1,0:T(8,128)(2,1)S(1)}, bf16[512,384]{1,0:T(8,128)(2,1)S(1)}, u32[]{:S(2)}, u32[]{:S(2)}) %collective-permute-start.29) | collective-permute-done | bytes 393248 | tf_op jit(solution)/shard_map/ppermute | solution.py:627
  174.4 5.0 %collective-permute-done.34.refs_4_ = bf16[528,384]{1,0:T(8,128)(2,1)S(1)} collective-permute-done((bf16[528,384]{1,0:T(8,128)(2,1)S(1)}, bf16[528,384]{1,0:T(8,128)(2,1)S(1)}, u32[]{:S(2)}, u32[]{:S(2)}) %collective-permute-start.34) | collective-permute-done | bytes 405536 | tf_op jit(solution)/shard_map/ppermute | solution.py:627
  180.6 2.4 collective-permute-start.35
  183.1 4.7 %collective-permute-done.30.refs_4_ = bf16[512,384]{1,0:T(8,128)(2,1)S(1)} collective-permute-done((bf16[512,384]{1,0:T(8,128)(2,1)S(1)}, bf16[512,384]{1,0:T(8,128)(2,1)S(1)}, u32[]{:S(2)}, u32[]{:S(2)}) %collective-permute-start.30) | collective-permute-done | bytes 393248 | tf_op jit(solution)/shard_map/ppermute | solution.py:627
  189.0 2.4 collective-permute-start.31
  194.0 10.2 %collective-permute-done.31.refs_1_ = bf16[512,384]{1,0:T(8,128)(2,1)S(1)} collective-permute-done((bf16[512,384]{1,0:T(8,128)(2,1)S(1)}, bf16[512,384]{1,0:T(8,128)(2,1)S(1)}, u32[]{:S(2)}, u32[]{:S(2)}) %collective-permute-start.31) | collective-permute-done | bytes 393248 | tf_op jit(solution)/shard_map/ppermute | solution.py:627
  209.1 2.9 %collective-permute-start.40 = (bf16[512,128]{1,0:T(8,128)(2,1)S(1)}, bf16[512,128]{1,0:T(8,128)(2,1)S(1)}, u32[]{:S(2)}, u32[]{:S(2)}) collective-permute-start(bf16[512,128]{1,0:T(8,128)(2,1)S(1)} %get-tuple-element.78.refs_1_), channel_id=1, source_target_pairs={{0,8},{4,12},{8,0},{12,4},{1,9},{5,13},{9,1},{13,5},{2,10},{6,14},... | collective-permute-start | bytes 393224 | tf_op jit(solution)/shard_map/ppermute | solution.py:256
  215.9 4.3 %collective-permute-done.40.refs_3_ = bf16[512,128]{1,0:T(8,128)(2,1)S(1)} collective-permute-done((bf16[512,128]{1,0:T(8,128)(2,1)S(1)}, bf16[512,128]{1,0:T(8,128)(2,1)S(1)}, u32[]{:S(2)}, u32[]{:S(2)}) %collective-permute-start.40) | collective-permute-done | bytes 131104 | tf_op jit(solution)/shard_map/ppermute | solution.py:256
  221.6 3.3 %collective-permute-start.36 = (bf16[512,128]{1,0:T(8,128)(2,1)S(1)}, bf16[512,128]{1,0:T(8,128)(2,1)S(1)}, u32[]{:S(2)}, u32[]{:S(2)}) collective-permute-start(bf16[512,128]{1,0:T(8,128)(2,1)S(1)} %shard_map.104.refs_6_.refs_1_), channel_id=1, source_target_pairs={{0,4},{4,8},{8,12},{12,0},{1,5},{5,9},{9,13},{13,1},{2,6},{6,10},{... | collective-permute-start | bytes 393224 | tf_op jit(solution)/shard_map/ppermute | solution.py:256
  229.9 5.1 %collective-permute-done.37.refs_3_ = bf16[512,128]{1,0:T(8,128)(2,1)S(1)} collective-permute-done((bf16[512,128]{1,0:T(8,128)(2,1)S(1)}, bf16[512,128]{1,0:T(8,128)(2,1)S(1)}, u32[]{:S(2)}, u32[]{:S(2)}) %collective-permute-start.37) | collective-permute-done | bytes 131104 | tf_op jit(solution)/shard_map/ppermute | solution.py:256
  240.1 5.5 %collective-permute-done.51.refs_3_ = bf16[512,256]{1,0:T(8,128)(2,1)S(1)} collective-permute-done((bf16[512,256]{1,0:T(8,128)(2,1)S(1)}, bf16[512,256]{1,0:T(8,128)(2,1)S(1)}, u32[]{:S(2)}, u32[]{:S(2)}) %collective-permute-start.51) | collective-permute-done | bytes 262176 | tf_op jit(solution)/shard_map/ppermute | solution.py:135
  246.3 3.4 %collective-permute-start.52 = (bf16[128,256]{1,0:T(8,128)(2,1)S(1)}, bf16[128,256]{1,0:T(8,128)(2,1)S(1)}, u32[]{:S(2)}, u32[]{:S(2)}) collective-permute-start(bf16[128,256]{1,0:T(8,128)(2,1)S(1)} %get-tuple-element.92), channel_id=1, source_target_pairs={{0,4},{4,8},{8,12},{12,0},{1,5},{5,9},{9,13},{13,1},{2,6},{6,10},{... | collective-permute-start | bytes 196616 | tf_op jit(solution)/shard_map/ppermute | solution.py:256
  263.3 2.8 %collective-permute-done.55.refs_1_ = bf16[512,256]{1,0:T(8,128)(2,1)S(1)} collective-permute-done((bf16[512,256]{1,0:T(8,128)(2,1)S(1)}, bf16[512,256]{1,0:T(8,128)(2,1)S(1)}, u32[]{:S(2)}, u32[]{:S(2)}) %collective-permute-start.55) | collective-permute-done | bytes 262176 | tf_op jit(solution)/shard_map/ppermute | solution.py:135
  266.6 4.0 %collective-permute-done.48.refs_1_ = bf16[512,256]{1,0:T(8,128)(2,1)S(1)} collective-permute-done((bf16[512,256]{1,0:T(8,128)(2,1)S(1)}, bf16[512,256]{1,0:T(8,128)(2,1)S(1)}, u32[]{:S(2)}, u32[]{:S(2)}) %collective-permute-start.48) | collective-permute-done | bytes 262176 | tf_op jit(solution)/shard_map/ppermute | solution.py:135
  (134 shorter events, 115.2 us)
Async XLA Ops:
  18.3 8.2 %collective-permute-start.8 = (bf16[512,256]{1,0:T(8,128)(2,1)S(1)}, bf16[512,256]{1,0:T(8,128)(2,1)S(1)}, u32[]{:S(2)}, u32[]{:S(2)}) collective-permute-start(bf16[512,256]{1,0:T(8,128)(2,1)S(1)} %shard_map.75.refs_1_), channel_id=1, source_target_pairs={{0,1},{1,0},{2,3},{3,2},{4,5},{5,4},{6,7},{7,6},{8,9},{9,8},{10,11... | collective-permute-start | bytes 786440 | tf_op jit(solution)/shard_map/ppermute | solution.py:135
  33.2 13.2 %collective-permute-start.15 = (bf16[528,384]{1,0:T(8,128)(2,1)S(1)}, bf16[528,384]{1,0:T(8,128)(2,1)S(1)}, u32[]{:S(2)}, u32[]{:S(2)}) collective-permute-start(bf16[528,384]{1,0:T(8,128)(2,1)S(1)} %get-tuple-element.64), channel_id=1, source_target_pairs={{0,4},{8,0},{12,8},{4,12},{1,5},{9,1},{13,9},{5,13},{2,6},{10,2},{... | collective-permute-start | bytes 1216520 | tf_op jit(solution)/shard_map/ppermute | solution.py:627
  35.2 19.6 %collective-permute-start.10 = (bf16[512,384]{1,0:T(8,128)(2,1)S(1)}, bf16[512,384]{1,0:T(8,128)(2,1)S(1)}, u32[]{:S(2)}, u32[]{:S(2)}) collective-permute-start(bf16[512,384]{1,0:T(8,128)(2,1)S(1)} %get-tuple-element.58), channel_id=1, source_target_pairs={{0,4},{8,0},{12,8},{4,12},{1,5},{9,1},{13,9},{5,13},{2,6},{10,2},{... | collective-permute-start | bytes 1179656 | tf_op jit(solution)/shard_map/ppermute | solution.py:627
  47.7 15.8 %collective-permute-start.16 = (bf16[528,384]{1,0:T(8,128)(2,1)S(1)}, bf16[528,384]{1,0:T(8,128)(2,1)S(1)}, u32[]{:S(2)}, u32[]{:S(2)}) collective-permute-start(bf16[528,384]{1,0:T(8,128)(2,1)S(1)} %shard_map.81), channel_id=1, source_target_pairs={{0,4},{8,0},{12,8},{4,12},{1,5},{9,1},{13,9},{5,13},{2,6},{10,2},{... | collective-permute-start | bytes 1216520 | tf_op jit(solution)/shard_map/ppermute | solution.py:627
  56.1 15.9 %collective-permute-start.11 = (bf16[512,384]{1,0:T(8,128)(2,1)S(1)}, bf16[512,384]{1,0:T(8,128)(2,1)S(1)}, u32[]{:S(2)}, u32[]{:S(2)}) collective-permute-start(bf16[512,384]{1,0:T(8,128)(2,1)S(1)} %shard_map.78), channel_id=1, source_target_pairs={{0,4},{8,0},{12,8},{4,12},{1,5},{9,1},{13,9},{5,13},{2,6},{10,2},{... | collective-permute-start | bytes 1179656 | tf_op jit(solution)/shard_map/ppermute | solution.py:627
  64.8 23.4 %collective-permute-start.17 = (bf16[528,384]{1,0:T(8,128)(2,1)S(1)}, bf16[528,384]{1,0:T(8,128)(2,1)S(1)}, u32[]{:S(2)}, u32[]{:S(2)}) collective-permute-start(bf16[528,384]{1,0:T(8,128)(2,1)S(1)} %shard_map.82), channel_id=1, source_target_pairs={{0,4},{8,0},{12,8},{4,12},{1,5},{9,1},{13,9},{5,13},{2,6},{10,2},{... | collective-permute-start | bytes 1216520 | tf_op jit(solution)/shard_map/ppermute | solution.py:627
  73.2 15.0 %collective-permute-start.12 = (bf16[512,384]{1,0:T(8,128)(2,1)S(1)}, bf16[512,384]{1,0:T(8,128)(2,1)S(1)}, u32[]{:S(2)}, u32[]{:S(2)}) collective-permute-start(bf16[512,384]{1,0:T(8,128)(2,1)S(1)} %shard_map.79), channel_id=1, source_target_pairs={{0,4},{8,0},{12,8},{4,12},{1,5},{9,1},{13,9},{5,13},{2,6},{10,2},{... | collective-permute-start | bytes 1179656 | tf_op jit(solution)/shard_map/ppermute | solution.py:627
  90.7 8.2 %collective-permute-start.21 = (bf16[512,128]{1,0:T(8,128)(2,1)S(1)}, bf16[512,128]{1,0:T(8,128)(2,1)S(1)}, u32[]{:S(2)}, u32[]{:S(2)}) collective-permute-start(bf16[512,128]{1,0:T(8,128)(2,1)S(1)} %get-tuple-element.66.refs_1_), channel_id=1, source_target_pairs={{0,4},{4,8},{8,12},{12,0},{1,5},{5,9},{9,13},{13,1},{2,6},{6,10},{... | collective-permute-start | bytes 393224 | tf_op jit(solution)/shard_map/ppermute | solution.py:256
  91.8 11.1 %collective-permute-start.22 = (bf16[512,128]{1,0:T(8,128)(2,1)S(1)}, bf16[512,128]{1,0:T(8,128)(2,1)S(1)}, u32[]{:S(2)}, u32[]{:S(2)}) collective-permute-start(bf16[512,128]{1,0:T(8,128)(2,1)S(1)} %get-tuple-element.66.refs_1_), channel_id=1, source_target_pairs={{0,8},{4,12},{8,0},{12,4},{1,9},{5,13},{9,1},{13,5},{2,10},{6,14},... | collective-permute-start | bytes 393224 | tf_op jit(solution)/shard_map/ppermute | solution.py:256
  93.1 9.8 %collective-permute-start.23 = (bf16[512,128]{1,0:T(8,128)(2,1)S(1)}, bf16[512,128]{1,0:T(8,128)(2,1)S(1)}, u32[]{:S(2)}, u32[]{:S(2)}) collective-permute-start(bf16[512,128]{1,0:T(8,128)(2,1)S(1)} %get-tuple-element.66.refs_1_), channel_id=1, source_target_pairs={{0,12},{4,0},{8,4},{12,8},{1,13},{5,1},{9,5},{13,9},{2,14},{6,2},{... | collective-permute-start | bytes 393224 | tf_op jit(solution)/shard_map/ppermute | solution.py:256
  104.3 8.3 %collective-permute-start.18 = (bf16[512,128]{1,0:T(8,128)(2,1)S(1)}, bf16[512,128]{1,0:T(8,128)(2,1)S(1)}, u32[]{:S(2)}, u32[]{:S(2)}) collective-permute-start(bf16[512,128]{1,0:T(8,128)(2,1)S(1)} %shard_map.88.refs_6_.refs_1_), channel_id=1, source_target_pairs={{0,4},{4,8},{8,12},{12,0},{1,5},{5,9},{9,13},{13,1},{2,6},{6,10},{... | collective-permute-start | bytes 393224 | tf_op jit(solution)/shard_map/ppermute | solution.py:256
  107.5 10.2 %collective-permute-start.19 = (bf16[512,128]{1,0:T(8,128)(2,1)S(1)}, bf16[512,128]{1,0:T(8,128)(2,1)S(1)}, u32[]{:S(2)}, u32[]{:S(2)}) collective-permute-start(bf16[512,128]{1,0:T(8,128)(2,1)S(1)} %shard_map.88.refs_6_.refs_1_), channel_id=1, source_target_pairs={{0,8},{4,12},{8,0},{12,4},{1,9},{5,13},{9,1},{13,5},{2,10},{6,14},... | collective-permute-start | bytes 393224 | tf_op jit(solution)/shard_map/ppermute | solution.py:256
  107.6 10.1 %collective-permute-start.20 = (bf16[512,128]{1,0:T(8,128)(2,1)S(1)}, bf16[512,128]{1,0:T(8,128)(2,1)S(1)}, u32[]{:S(2)}, u32[]{:S(2)}) collective-permute-start(bf16[512,128]{1,0:T(8,128)(2,1)S(1)} %shard_map.88.refs_6_.refs_1_), channel_id=1, source_target_pairs={{0,12},{4,0},{8,4},{12,8},{1,13},{5,1},{9,5},{13,9},{2,14},{6,2},{... | collective-permute-start | bytes 393224 | tf_op jit(solution)/shard_map/ppermute | solution.py:256
  119.1 14.9 %collective-permute-start.27 = (bf16[512,512]{1,0:T(8,128)(2,1)S(1)}, bf16[512,512]{1,0:T(8,128)(2,1)S(1)}, u32[]{:S(2)}, u32[]{:S(2)}) collective-permute-start(bf16[512,512]{1,0:T(8,128)(2,1)S(1)} %shard_map.90.refs_6_.refs_3_), channel_id=1, source_target_pairs={{0,2},{1,3},{2,0},{3,1},{4,6},{5,7},{6,4},{7,5},{8,10},{9,11},{10,... | collective-permute-start | bytes 1572872 | tf_op jit(solution)/shard_map/ppermute | solution.py:135
  121.7 23.0 %collective-permute-start.26 = (bf16[512,512]{1,0:T(8,128)(2,1)S(1)}, bf16[512,512]{1,0:T(8,128)(2,1)S(1)}, u32[]{:S(2)}, u32[]{:S(2)}) collective-permute-start(bf16[512,512]{1,0:T(8,128)(2,1)S(1)} %shard_map.92.refs_3_), channel_id=1, source_target_pairs={{0,2},{1,3},{2,0},{3,1},{4,6},{5,7},{6,4},{7,5},{8,10},{9,11},{10,... | collective-permute-start | bytes 1572872 | tf_op jit(solution)/shard_map/ppermute | solution.py:135
  134.7 10.8 %collective-permute-start.28 = (bf16[512,512]{1,0:T(8,128)(2,1)S(1)}, bf16[512,512]{1,0:T(8,128)(2,1)S(1)}, u32[]{:S(2)}, u32[]{:S(2)}) collective-permute-start(bf16[512,512]{1,0:T(8,128)(2,1)S(1)} %shard_map.94.refs_1_), channel_id=1, source_target_pairs={{0,1},{1,0},{2,3},{3,2},{4,5},{5,4},{6,7},{7,6},{8,9},{9,8},{10,11... | collective-permute-start | bytes 1572872 | tf_op jit(solution)/shard_map/ppermute | solution.py:135
  149.0 13.2 %collective-permute-start.33 = (bf16[528,384]{1,0:T(8,128)(2,1)S(1)}, bf16[528,384]{1,0:T(8,128)(2,1)S(1)}, u32[]{:S(2)}, u32[]{:S(2)}) collective-permute-start(bf16[528,384]{1,0:T(8,128)(2,1)S(1)} %get-tuple-element.76), channel_id=1, source_target_pairs={{0,4},{8,0},{12,8},{4,12},{1,5},{9,1},{13,9},{5,13},{2,6},{10,2},{... | collective-permute-start | bytes 1216520 | tf_op jit(solution)/shard_map/ppermute | solution.py:627
  152.4 18.3 %collective-permute-start.29 = (bf16[512,384]{1,0:T(8,128)(2,1)S(1)}, bf16[512,384]{1,0:T(8,128)(2,1)S(1)}, u32[]{:S(2)}, u32[]{:S(2)}) collective-permute-start(bf16[512,384]{1,0:T(8,128)(2,1)S(1)} %get-tuple-element.73), channel_id=1, source_target_pairs={{0,4},{8,0},{12,8},{4,12},{1,5},{9,1},{13,9},{5,13},{2,6},{10,2},{... | collective-permute-start | bytes 1179656 | tf_op jit(solution)/shard_map/ppermute | solution.py:627
  163.5 15.9 %collective-permute-start.34 = (bf16[528,384]{1,0:T(8,128)(2,1)S(1)}, bf16[528,384]{1,0:T(8,128)(2,1)S(1)}, u32[]{:S(2)}, u32[]{:S(2)}) collective-permute-start(bf16[528,384]{1,0:T(8,128)(2,1)S(1)} %shard_map.99), channel_id=1, source_target_pairs={{0,4},{8,0},{12,8},{4,12},{1,5},{9,1},{13,9},{5,13},{2,6},{10,2},{... | collective-permute-start | bytes 1216520 | tf_op jit(solution)/shard_map/ppermute | solution.py:627
  171.9 15.9 %collective-permute-start.30 = (bf16[512,384]{1,0:T(8,128)(2,1)S(1)}, bf16[512,384]{1,0:T(8,128)(2,1)S(1)}, u32[]{:S(2)}, u32[]{:S(2)}) collective-permute-start(bf16[512,384]{1,0:T(8,128)(2,1)S(1)} %shard_map.96), channel_id=1, source_target_pairs={{0,4},{8,0},{12,8},{4,12},{1,5},{9,1},{13,9},{5,13},{2,6},{10,2},{... | collective-permute-start | bytes 1179656 | tf_op jit(solution)/shard_map/ppermute | solution.py:627
  180.6 23.5 %collective-permute-start.35 = (bf16[528,384]{1,0:T(8,128)(2,1)S(1)}, bf16[528,384]{1,0:T(8,128)(2,1)S(1)}, u32[]{:S(2)}, u32[]{:S(2)}) collective-permute-start(bf16[528,384]{1,0:T(8,128)(2,1)S(1)} %shard_map.100), channel_id=1, source_target_pairs={{0,4},{8,0},{12,8},{4,12},{1,5},{9,1},{13,9},{5,13},{2,6},{10,2},{... | collective-permute-start | bytes 1216520 | tf_op jit(solution)/shard_map/ppermute | solution.py:627
  189.0 15.1 %collective-permute-start.31 = (bf16[512,384]{1,0:T(8,128)(2,1)S(1)}, bf16[512,384]{1,0:T(8,128)(2,1)S(1)}, u32[]{:S(2)}, u32[]{:S(2)}) collective-permute-start(bf16[512,384]{1,0:T(8,128)(2,1)S(1)} %shard_map.97), channel_id=1, source_target_pairs={{0,4},{8,0},{12,8},{4,12},{1,5},{9,1},{13,9},{5,13},{2,6},{10,2},{... | collective-permute-start | bytes 1179656 | tf_op jit(solution)/shard_map/ppermute | solution.py:627
  206.6 9.2 %collective-permute-start.39 = (bf16[512,128]{1,0:T(8,128)(2,1)S(1)}, bf16[512,128]{1,0:T(8,128)(2,1)S(1)}, u32[]{:S(2)}, u32[]{:S(2)}) collective-permute-start(bf16[512,128]{1,0:T(8,128)(2,1)S(1)} %get-tuple-element.78.refs_1_), channel_id=1, source_target_pairs={{0,4},{4,8},{8,12},{12,0},{1,5},{5,9},{9,13},{13,1},{2,6},{6,10},{... | collective-permute-start | bytes 393224 | tf_op jit(solution)/shard_map/ppermute | solution.py:256
  209.1 11.1 %collective-permute-start.40 = (bf16[512,128]{1,0:T(8,128)(2,1)S(1)}, bf16[512,128]{1,0:T(8,128)(2,1)S(1)}, u32[]{:S(2)}, u32[]{:S(2)}) collective-permute-start(bf16[512,128]{1,0:T(8,128)(2,1)S(1)} %get-tuple-element.78.refs_1_), channel_id=1, source_target_pairs={{0,8},{4,12},{8,0},{12,4},{1,9},{5,13},{9,1},{13,5},{2,10},{6,14},... | collective-permute-start | bytes 393224 | tf_op jit(solution)/shard_map/ppermute | solution.py:256
  221.6 8.3 %collective-permute-start.36 = (bf16[512,128]{1,0:T(8,128)(2,1)S(1)}, bf16[512,128]{1,0:T(8,128)(2,1)S(1)}, u32[]{:S(2)}, u32[]{:S(2)}) collective-permute-start(bf16[512,128]{1,0:T(8,128)(2,1)S(1)} %shard_map.104.refs_6_.refs_1_), channel_id=1, source_target_pairs={{0,4},{4,8},{8,12},{12,0},{1,5},{5,9},{9,13},{13,1},{2,6},{6,10},{... | collective-permute-start | bytes 393224 | tf_op jit(solution)/shard_map/ppermute | solution.py:256
  224.9 10.1 %collective-permute-start.37 = (bf16[512,128]{1,0:T(8,128)(2,1)S(1)}, bf16[512,128]{1,0:T(8,128)(2,1)S(1)}, u32[]{:S(2)}, u32[]{:S(2)}) collective-permute-start(bf16[512,128]{1,0:T(8,128)(2,1)S(1)} %shard_map.104.refs_6_.refs_1_), channel_id=1, source_target_pairs={{0,8},{4,12},{8,0},{12,4},{1,9},{5,13},{9,1},{13,5},{2,10},{6,14},... | collective-permute-start | bytes 393224 | tf_op jit(solution)/shard_map/ppermute | solution.py:256
  225.7 9.2 %collective-permute-start.38 = (bf16[512,128]{1,0:T(8,128)(2,1)S(1)}, bf16[512,128]{1,0:T(8,128)(2,1)S(1)}, u32[]{:S(2)}, u32[]{:S(2)}) collective-permute-start(bf16[512,128]{1,0:T(8,128)(2,1)S(1)} %shard_map.104.refs_6_.refs_1_), channel_id=1, source_target_pairs={{0,12},{4,0},{8,4},{12,8},{1,13},{5,1},{9,5},{13,9},{2,14},{6,2},{... | collective-permute-start | bytes 393224 | tf_op jit(solution)/shard_map/ppermute | solution.py:256
  236.4 9.2 %collective-permute-start.51 = (bf16[512,256]{1,0:T(8,128)(2,1)S(1)}, bf16[512,256]{1,0:T(8,128)(2,1)S(1)}, u32[]{:S(2)}, u32[]{:S(2)}) collective-permute-start(bf16[512,256]{1,0:T(8,128)(2,1)S(1)} %get-tuple-element.81.refs_6_), channel_id=1, source_target_pairs={{0,2},{1,3},{2,0},{3,1},{4,6},{5,7},{6,4},{7,5},{8,10},{9,11},{10,... | collective-permute-start | bytes 786440 | tf_op jit(solution)/shard_map/ppermute | solution.py:135
  238.9 13.1 %collective-permute-start.44 = (bf16[512,256]{1,0:T(8,128)(2,1)S(1)}, bf16[512,256]{1,0:T(8,128)(2,1)S(1)}, u32[]{:S(2)}, u32[]{:S(2)}) collective-permute-start(bf16[512,256]{1,0:T(8,128)(2,1)S(1)} %get-tuple-element.85), channel_id=1, source_target_pairs={{0,2},{1,3},{2,0},{3,1},{4,6},{5,7},{6,4},{7,5},{8,10},{9,11},{10,... | collective-permute-start | bytes 786440 | tf_op jit(solution)/shard_map/ppermute | solution.py:135
  246.3 10.5 %collective-permute-start.52 = (bf16[128,256]{1,0:T(8,128)(2,1)S(1)}, bf16[128,256]{1,0:T(8,128)(2,1)S(1)}, u32[]{:S(2)}, u32[]{:S(2)}) collective-permute-start(bf16[128,256]{1,0:T(8,128)(2,1)S(1)} %get-tuple-element.92), channel_id=1, source_target_pairs={{0,4},{4,8},{8,12},{12,0},{1,5},{5,9},{9,13},{13,1},{2,6},{6,10},{... | collective-permute-start | bytes 196616 | tf_op jit(solution)/shard_map/ppermute | solution.py:256
  257.7 8.4 %collective-permute-start.55 = (bf16[512,256]{1,0:T(8,128)(2,1)S(1)}, bf16[512,256]{1,0:T(8,128)(2,1)S(1)}, u32[]{:S(2)}, u32[]{:S(2)}) collective-permute-start(bf16[512,256]{1,0:T(8,128)(2,1)S(1)} %shard_map.112.refs_0_), channel_id=1, source_target_pairs={{0,2},{1,3},{2,0},{3,1},{4,6},{5,7},{6,4},{7,5},{8,10},{9,11},{10,... | collective-permute-start | bytes 786440 | tf_op jit(solution)/shard_map/ppermute | solution.py:135
  262.1 8.5 %collective-permute-start.48 = (bf16[512,256]{1,0:T(8,128)(2,1)S(1)}, bf16[512,256]{1,0:T(8,128)(2,1)S(1)}, u32[]{:S(2)}, u32[]{:S(2)}) collective-permute-start(bf16[512,256]{1,0:T(8,128)(2,1)S(1)} %shard_map.110.refs_0_), channel_id=1, source_target_pairs={{0,2},{1,3},{2,0},{3,1},{4,6},{5,7},{6,4},{7,5},{8,10},{9,11},{10,... | collective-permute-start | bytes 786440 | tf_op jit(solution)/shard_map/ppermute | solution.py:135
  (29 other events, 160.8 us)
